TPU v7x, 512 devices: a whole 4x4x16 slice. The times are simulated.
512 devices in a mesh: sp: 128 (over z, x, core), tp: 4 (over y).
Axes of the slice: x: 4, y: 4, z: 16, core: 2. Of those that a mesh axis runs over, the one named last changes fastest.
Arguments:
- tokens: bfloat16 [65536, 2048], P('sp', 'tp'), may hold values from -6 to 6
- norm_gain: float32 [2048], replicated, may hold values from 0.1 to 1.9
- proj_state: bfloat16 [2048, 1024], P('sp', 'tp'), may hold values from -0.125 to 0.125
- proj_value: bfloat16 [2048, 1024], P('sp', 'tp'), may hold values from -0.125 to 0.125
- proj_gate: bfloat16 [2048, 1024], P('sp', 'tp'), may hold values from -0.125 to 0.125
- eigen_real: float32 [64, 64], P('tp')
- eigen_imag: float32 [64, 64], P('tp')
- log_step: float32 [64], P('tp')
- decay_shift: float32 [64, 65536], P('tp', 'sp'), may hold values from -2.2 to 0
- state_input: float32 [2, 64, 16, 64], P(None, 'tp'), may hold values from -1 to 1
- state_readout_matrices: float32 [2, 64, 16, 64], P(None, 'tp'), may hold values from -0.5 to 0.5
- skip_gain: float32 [1024], P('tp'), may hold values from -5 to 5
- init_state: float32 [2, 64, 64], P(None, 'tp'), may hold values from -5 to 5
- conv_taps: float32 [31, 1024], P(None, 'tp')
- channel_gain: float32 [1024], P('tp'), may hold values from 0.1 to 1.9
- merge_state: bfloat16 [1024, 2048], P('tp', 'sp'), may hold values from -0.125 to 0.125
- merge_conv: bfloat16 [1024, 2048], P('tp', 'sp'), may hold values from -0.125 to 0.125
Outputs:
- mixed: bfloat16 [65536, 2048], P(('sp', 'tp'))
All inputs are finite; a program needn't handle non-finite values.
Results may differ from a plain program's by a relative error of at most 0.011.
Values may be sent and summed in bfloat16 or wider, within the bound.
No kernel may reach another device: no remote copies, remote signals or barrier semaphores. Data moves between devices by JAX's collectives and lax.ppermute only.
A program may use at most 128 MiB of HBM per device.

v0:
```python
import jax
import jax.numpy as jnp
from jax import lax
from jax.sharding import Mesh
from jax.sharding import PartitionSpec as P

CONV_W = 1024
SP = ("sp_0", "sp_1", "sp_2")
SP_TP = ("sp_0", "sp_1", "sp_2", "tp")


epsilon = 1e-06


def filled_with(value, identity):
    return jax.tree.map(
        lambda a, e: jnp.broadcast_to(jnp.asarray(e, a.dtype), a.shape), value, identity
    )


def collected_together(value, axis):
    leaves = jax.tree.leaves(value)
    sequence = sorted(range(len(leaves)), key=lambda k: -leaves[k].size)
    width = (1, *leaves[sequence[0]].shape)[-1]
    lines = [
        jnp.pad(leaves[k].reshape(-1), (0, -leaves[k].size % width)).reshape(-1, width)
        for k in sequence
    ]
    both, at, found = (lax.all_gather(jnp.concatenate(lines), axis), 0, {})
    for k, line in zip(sequence, lines):
        piece = both[:, at : at + len(line)].reshape(len(both), -1)
        found[k] = piece[:, : leaves[k].size].reshape(-1, *leaves[k].shape)
        at += len(line)
    numbers = iter(range(len(leaves)))
    return jax.tree.map(lambda _: found[next(numbers)], value)


def prefix_by_axis(value, axes, combine, identity):
    before = start = filled_with(value, identity)
    total = value
    for axis in reversed(axes):
        peers, place = (lax.axis_size(axis), lax.axis_index(axis))
        pieces = collected_together(total, axis)
        inside, total = (start, start)
        for k in range(peers):
            passed = k < place
            total = combine(total, jax.tree.map(lambda part: part[k], pieces))
            inside = jax.tree.map(lambda new, old: jnp.where(passed, new, old), total, inside)
        before = combine(inside, before)
    return before


def passed_along(block, axis, distance):
    devices = range(lax.axis_size(axis))
    route = [(i - distance, i) for i in devices if i - distance in devices]
    return lax.ppermute(block, axis, route)


def copy_for_each(value, axis):
    peers = lax.axis_size(axis)
    return lax.all_to_all(
        jnp.broadcast_to(value[None], (peers, *value.shape)), axis, 0, 0, tiled=True
    )


def taken_together(value, axis):
    everything = copy_for_each(value, axis)
    return jnp.sum(everything, axis=0)


def in_one(arrays, axis):
    line, at, done = (jnp.concatenate([a.reshape(-1) for a in arrays]), 0, [])
    total = taken_together(line, axis)
    for a in arrays:
        done.append(total[at : at + a.size].reshape(a.shape))
        at += a.size
    return tuple(done)


def joined_along(tiles, dim):
    lengths = list(tiles.shape[1:])
    lengths[dim] *= tiles.shape[0]
    return jnp.moveaxis(tiles, 0, dim).reshape(lengths)


def gathered_copies(value, axis, dim):
    return joined_along(copy_for_each(value, axis), dim)


def side_by_side(arrays, axis, dim, along):
    widths = [a.shape[along] for a in arrays]
    both = jnp.concatenate(arrays, axis=along)
    whole = lax.all_gather(both, axis, axis=dim, tiled=True)
    return tuple(jnp.split(whole, [sum(widths[:k]) for k in range(1, len(widths))], axis=along))


def turned_gather(arrays, axis, dims):
    turned = [jnp.moveaxis(a, dim, 0) for a, dim in zip(arrays, dims)]
    widths = [t[0].size for t in turned]
    both = jnp.concatenate([t.reshape(-1, w) for t, w in zip(turned, widths)], axis=1)
    whole = lax.all_gather(both, axis, axis=0, tiled=True)
    tiles = jnp.split(whole, [sum(widths[:k]) for k in range(1, len(widths))], axis=1)
    return tuple(
        (
            jnp.moveaxis(b.reshape(-1, *t.shape[1:]), 0, dim)
            for b, t, dim in zip(tiles, turned, dims)
        )
    )


def in_blocks(value, dim, peers):
    before, after = (value.shape[:dim], value.shape[dim + 1 :])
    return jnp.moveaxis(value.reshape(*before, peers, -1, *after), dim, 0)


def sent_and_summed(value, axis, dim):
    tiles = in_blocks(value, dim, lax.axis_size(axis))
    arrived = lax.all_to_all(tiles, axis, split_axis=0, concat_axis=0, tiled=True)
    return arrived.astype(jnp.float32).sum(axis=0)


def round_half(value):
    return lax.optimization_barrier(value.astype(jnp.bfloat16))


def input_matrix(eigen_real, eigen_imag, step, state_input):
    base = eigen_real * step[:, None]
    theta = eigen_imag * step[:, None]
    magnitude = jnp.exp(base)
    near_re = magnitude * jnp.cos(theta) - 1.0
    near_im = magnitude * jnp.sin(theta)
    modulus = eigen_real * eigen_real + eigen_imag * eigen_imag
    ratio_re = (near_re * eigen_real + near_im * eigen_imag) / modulus
    ratio_im = (near_im * eigen_real - near_re * eigen_imag) / modulus
    in_re = state_input[0]
    in_im = state_input[1]
    discrete_decay_real = ratio_re[:, None, :] * in_re - ratio_im[:, None, :] * in_im
    discrete_decay_imaginary = ratio_re[:, None, :] * in_im + ratio_im[:, None, :] * in_re
    return (discrete_decay_real, discrete_decay_imaginary)


def block_states(c_re, c_im, delta_real, delta_imaginary, shift, base, theta, counts, lower):
    level = jnp.cumsum(shift, axis=0)[:, :, None] + counts * base
    angle = counts * theta
    cosine = jnp.cos(angle)
    sine = jnp.sin(angle)
    grow = jnp.exp(level)
    shrink = jnp.exp(-level)
    w_re = shrink * (cosine * delta_real + sine * delta_imaginary)
    w_im = shrink * (cosine * delta_imaginary - sine * delta_real)
    length, groups, states = delta_real.shape
    stacked = jnp.concatenate([w_re, w_im], axis=1).reshape(length, 2 * groups * states)
    summed = jnp.dot(lower, stacked).reshape(length, 2 * groups, states)
    t_re = summed[:, :groups] + c_re
    t_im = summed[:, groups:] + c_im
    input_real = grow * (cosine * t_re - sine * t_im)
    input_imaginary = grow * (cosine * t_im + sine * t_re)
    return (input_real, input_imaginary)


def chain(earlier, later):
    a_re, a_im, b_re, b_im = earlier
    c_re, c_im, delta_real, delta_imaginary = later
    return (
        a_re * c_re - a_im * c_im,
        a_re * c_im + a_im * c_re,
        c_re * b_re - c_im * b_im + delta_real,
        c_re * b_im + c_im * b_re + delta_imaginary,
    )


def state_local(
    u_in, eigen_real, eigen_imag, log_step, decay_shift, state_input, state_readout_matrices
):
    count, width = u_in.shape
    groups, states = eigen_real.shape
    group = width // groups
    step = jnp.exp(log_step)
    base = eigen_real * step[:, None]
    theta = eigen_imag * step[:, None]
    discrete_decay_real, discrete_decay_imaginary = input_matrix(
        eigen_real, eigen_imag, step, state_input
    )
    float_values = u_in.astype(jnp.float32).reshape(count, groups, group)
    forcing_real = jnp.einsum("ovi,viu->ovu", float_values, discrete_decay_real)
    forcing_imaginary = jnp.einsum("ovi,viu->ovu", float_values, discrete_decay_imaginary)
    shift = decay_shift.T
    length = min(32, count)
    blocks = count // length
    counts = (jnp.arange(length) + 1).astype(jnp.float32)[:, None, None]
    lower = (jnp.arange(length)[:, None] >= jnp.arange(length)[None, :]).astype(jnp.float32)

    def advance(carry, inputs):
        delta_real, delta_imaginary, block_shift = inputs
        input_real, input_imaginary = block_states(
            carry[0], carry[1], delta_real, delta_imaginary, block_shift, base, theta, counts, lower
        )
        return ((input_real[-1], input_imaginary[-1]), (input_real, input_imaginary))

    zero = jnp.zeros((groups, states), jnp.float32)
    last, (input_real, input_imaginary) = lax.scan(
        advance,
        (zero, zero),
        (
            forcing_real.reshape(blocks, length, groups, states),
            forcing_imaginary.reshape(blocks, length, groups, states),
            shift.reshape(blocks, length, groups),
        ),
    )
    input_real = input_real.reshape(count, groups, states)
    input_imaginary = input_imaginary.reshape(count, groups, states)
    local_output = jnp.einsum("lan,arn->lar", input_real, state_readout_matrices[0]) - jnp.einsum(
        "lan,arn->lar", input_imaginary, state_readout_matrices[1]
    )
    whole_count = (jnp.arange(count) + 1).astype(jnp.float32)[:, None, None]
    level = jnp.cumsum(shift, axis=0)[:, :, None] + whole_count * base
    angle = whole_count * theta
    grow = jnp.exp(level)
    exponent_real = grow * jnp.cos(angle)
    exponent_imaginary = grow * jnp.sin(angle)
    summary = (exponent_real[-1], exponent_imaginary[-1], last[0], last[1])
    return (local_output, exponent_real, exponent_imaginary, summary)


def carry_in(summary, init_state):
    groups, states = summary[0].shape
    ones = jnp.ones((groups, states), jnp.float32)
    zeros = jnp.zeros((groups, states), jnp.float32)
    identity = (ones, zeros, zeros, zeros)
    before = prefix_by_axis(summary, SP, chain, identity)
    a_re, a_im, b_re, b_im = before
    s_re = init_state[0]
    s_im = init_state[1]
    return (a_re * s_re - a_im * s_im + b_re, a_re * s_im + a_im * s_re + b_im)


def state_finish(
    local_output,
    exponent_real,
    exponent_imaginary,
    carried,
    state_readout_matrices,
    skip_gain,
    u_in,
):
    h_re, h_im = carried
    output_real = state_readout_matrices[0]
    output_imaginary = state_readout_matrices[1]
    blend_real = output_real * h_re[:, None, :] - output_imaginary * h_im[:, None, :]
    blend_imaginary = output_real * h_im[:, None, :] + output_imaginary * h_re[:, None, :]
    total = (
        local_output
        + jnp.einsum("lan,arn->lar", exponent_real, blend_real)
        - jnp.einsum("lan,arn->lar", exponent_imaginary, blend_imaginary)
    )
    count, width = u_in.shape
    groups = local_output.shape[1]
    float_values = u_in.astype(jnp.float32).reshape(count, groups, width // groups)
    total = total + skip_gain.reshape(groups, width // groups) * float_values
    return jax.nn.gelu(total).reshape(count, width).astype(jnp.bfloat16)


def conv_branch(value, gate, conv_taps, channel_gain):
    glu = round_half(value.astype(jnp.float32) * jax.nn.sigmoid(gate.astype(jnp.float32)))
    reach = conv_taps.shape[0] - 1
    count = glu.shape[0]
    before = passed_along(glu[count - reach :], SP, 1)
    extended = jnp.concatenate([before, glu], axis=0).astype(jnp.float32)
    raw = jnp.zeros(glu.shape, jnp.float32)
    for offset in range(reach + 1):
        raw = raw + conv_taps[offset] * extended[offset : offset + count]
    first, second = in_one(
        (jnp.sum(raw, axis=1, keepdims=True), jnp.sum(raw * raw, axis=1, keepdims=True)), "tp"
    )
    middle = first / CONV_W
    spread = second / CONV_W - middle * middle
    scaled = (raw - middle) * lax.rsqrt(spread + epsilon) * channel_gain
    return jax.nn.silu(scaled).astype(jnp.bfloat16)


def per_device(
    tokens,
    norm_gain,
    proj_state,
    proj_value,
    proj_gate,
    eigen_real,
    eigen_imag,
    log_step,
    decay_shift,
    state_input,
    state_readout_matrices,
    skip_gain,
    init_state,
    conv_taps,
    channel_gain,
    merge_state,
    merge_conv,
):
    whole = gathered_copies(tokens, "tp", 1)
    wide = whole.astype(jnp.float32)
    normed = (
        wide * lax.rsqrt(jnp.mean(wide * wide, axis=1, keepdims=True) + epsilon) * norm_gain
    ).astype(jnp.bfloat16)
    pieces = side_by_side((proj_state, proj_value, proj_gate), SP, 0, 1)
    state_sum, value_sum, gate_sum = tuple(
        (jnp.dot(normed, piece, preferred_element_type=jnp.float32) for piece in pieces)
    )
    u_in = round_half(state_sum)
    local_output, exponent_real, exponent_imaginary, summary = state_local(
        u_in, eigen_real, eigen_imag, log_step, decay_shift, state_input, state_readout_matrices
    )
    carried = carry_in(summary, init_state)
    conv_out = conv_branch(round_half(value_sum), round_half(gate_sum), conv_taps, channel_gain)
    ssm_out = state_finish(
        local_output,
        exponent_real,
        exponent_imaginary,
        carried,
        state_readout_matrices,
        skip_gain,
        u_in,
    )
    full_state, full_conv = turned_gather((merge_state, merge_conv), SP, (1, 1))
    mixed = sent_and_summed(
        (
            jnp.dot(ssm_out, full_state, preferred_element_type=jnp.float32)
            + jnp.dot(conv_out, full_conv, preferred_element_type=jnp.float32)
        ).astype(jnp.bfloat16),
        "tp",
        0,
    )
    return mixed.astype(jnp.bfloat16)


def solution(mesh):
    finer = Mesh(mesh.devices.reshape(16, 4, 2, mesh.shape["tp"]), ("sp_0", "sp_1", "sp_2", "tp"))
    return jax.shard_map(
        per_device,
        mesh=finer,
        in_specs=(
            P(SP, "tp"),
            P(),
            P(SP, "tp"),
            P(SP, "tp"),
            P(SP, "tp"),
            P("tp", None),
            P("tp", None),
            P("tp"),
            P("tp", SP),
            P(None, "tp", None, None),
            P(None, "tp", None, None),
            P("tp"),
            P(None, "tp", None),
            P(None, "tp"),
            P("tp"),
            P("tp", SP),
            P("tp", SP),
        ),
        out_specs=P(SP_TP, None),
        check_vma=False,
    )
```

profile of v0, /device:TPU:6, one launch (start us, length us, event | category | flops | bytes accessed | tf_op | source)
XLA Modules:
  0.0 354.7 jit_solution(10762016056615935425)
XLA Ops:
  6.5 1.3 pad_maximum_fusion.4
  7.9 1.3 copy.54
  9.2 1.6 broadcast_in_dim.10
  10.8 4.6 %all-to-all-start = ((bf16[4,512,512]{1,2,0:T(8,128)(2,1)}), bf16[4,512,512]{1,2,0:T(8,128)(2,1)S(1)}, u32[]{:S(2)}, u32[]{:S(2)}) async-start(bf16[4,512,512]{1,2,0:T(8,128)(2,1)} %broadcast_in_dim.10), calls=%async_computation | async-start | bytes 4194304 | tf_op jit(solution)/shard_map/all_to_all | solution.py:61
  16.4 1.2 reduce-window.6
  18.3 16.7 %fusion.23 = (f32[512,16,64]{2,1,0:T(8,128)S(1)}, f32[512,16,64]{2,1,0:T(8,128)S(1)}) fusion(f32[16,64]{1,0:T(8,128)S(1)} %get-tuple-element.329, f32[16,64]{1,0:T(8,128)S(1)} %get-tuple-element.328, f32[512]{0:T(512)S(1)} %add_convert_fusion.1, f32[512,16]{1,0:T(8,128)S(1)} %copy.62), kind=kLoop, calls=%fused_computation.38 | loop fusion | flops 2621440 | bytes 4237312 | tf_op jit(solution)/shard_map/mul | solution.py:220
  35.0 1.9 copy-done
  37.0 1.3 copy-done.2
  38.3 3.5 all-to-all-done
  42.3 1.9 fusion.25
  44.2 110.8 %all-gather.6.cloned.1.call-done = bf16[2048,768]{1,0:T(8,128)(2,1)} async-done(((bf16[16,768]{1,0:T(8,128)(2,1)}), bf16[2048,768]{1,0:T(8,128)(2,1)}) %all-gather.6.cloned.1.call-update) | async-done | bytes 3145744 | tf_op jit(solution)/shard_map/all_gather | solution.py:93
  155.0 2.6 convolution_convert_fusion.2
  157.7 1.8 convolution_bitcast_fusion.1
  160.1 2.0 convolution_convert_fusion.1
  162.1 2.0 convolution_convert_fusion
  164.2 2.1 collective-permute-start
  166.4 4.9 %copy.57 = f32[512,16,64]{2,1,0:T(8,128)} copy(f32[512,16,64]{0,2,1:T(8,128)} %convolution_bitcast_fusion.1) | data formatting | bytes 4194304 | tf_op jit(solution)/shard_map/ovi,viu->ovu/transpose | solution.py:186
  171.2 3.8 %copy.56 = f32[512,16,64]{2,1,0:T(8,128)} copy(f32[512,16,64]{0,2,1:T(8,128)S(1)} %convolution_bitcast_fusion.2) | data formatting | bytes 4194304 | tf_op jit(solution)/shard_map/ovi,viu->ovu/transpose | solution.py:185
  175.0 78.4 %while.18 = (s32[]{:T(128)}, f32[16,64]{1,0:T(8,128)S(1)}, f32[16,64]{1,0:T(8,128)S(1)}, bf16[16,32,16,64]{3,2,1,0:T(8,128)(2,1)}, bf16[16,32,16,64]{3,2,1,0:T(8...) while((s32[]{:T(128)}, f32[16,64]{1,0:T(8,128)S(1)}, ...), condition=%wide.region_3.4_spmd.clone.clone, body=%wide.region_1.3_spmd.clone.clone.sunk | while | flops 5359170 | bytes 2937857 | solution.py:201
  175.1 2.2 fusion.232
  178.0 1.9 bitcast_dynamic-update-slice_fusion.3
  180.0 2.2 fusion.232
  182.9 1.9 bitcast_dynamic-update-slice_fusion.3
  184.9 2.2 fusion.232
  187.8 1.9 bitcast_dynamic-update-slice_fusion.3
  189.8 2.2 fusion.232
  192.7 1.9 bitcast_dynamic-update-slice_fusion.3
  194.7 2.2 fusion.232
  197.6 1.9 bitcast_dynamic-update-slice_fusion.3
  199.6 2.2 fusion.232
  202.5 1.9 bitcast_dynamic-update-slice_fusion.3
  204.5 2.2 fusion.232
  207.4 1.9 bitcast_dynamic-update-slice_fusion.3
  209.4 2.2 fusion.232
  212.3 1.9 bitcast_dynamic-update-slice_fusion.3
  214.3 2.2 fusion.232
  217.2 1.9 bitcast_dynamic-update-slice_fusion.3
  219.2 2.2 fusion.232
  222.1 1.9 bitcast_dynamic-update-slice_fusion.3
  224.1 2.2 fusion.232
  227.0 1.9 bitcast_dynamic-update-slice_fusion.3
  229.0 2.2 fusion.232
  231.9 1.9 bitcast_dynamic-update-slice_fusion.3
  233.9 2.2 fusion.232
  236.8 1.9 bitcast_dynamic-update-slice_fusion.3
  238.8 2.2 fusion.232
  241.7 1.9 bitcast_dynamic-update-slice_fusion.3
  243.7 2.2 fusion.232
  246.6 1.9 bitcast_dynamic-update-slice_fusion.3
  248.5 2.2 fusion.232
  251.5 1.9 bitcast_dynamic-update-slice_fusion.3
  253.4 3.5 all-gather
  256.9 12.1 %all-gather.1 = f32[256,64]{1,0:T(8,128)S(1)} all-gather(f32[64,64]{1,0:T(8,128)S(1)} %pad_maximum_fusion.2), channel_id=3, replica_groups=mesh['sp_0'=16,'sp_1'=4,'sp_2'=2,'tp'=4] {'sp_1'}, dimensions={0}, use_global_device_ids=true | all-gather | bytes 81920 | tf_op jit(solution)/shard_map/all_gather | solution.py:29
  269.1 31.3 %all-gather.2 = f32[1024,64]{1,0:T(8,128)S(1)} all-gather(f32[64,64]{1,0:T(8,128)S(1)} %pad_maximum_fusion.3), channel_id=4, replica_groups=mesh['sp_0'=16,'sp_1'=4,'sp_2'=2,'tp'=4] {'sp_0'}, dimensions={0}, use_global_device_ids=true | all-gather | bytes 278528 | tf_op jit(solution)/shard_map/all_gather | solution.py:29
  300.6 2.6 fusion.30
  304.0 2.2 fusion.46
  306.2 2.2 fusion.70
  308.5 2.4 fusion.200
  311.5 4.3 %all-to-all-start.1 = ((f32[4,1,1024]{2,1,0:T(1,128)}), f32[4,1,1024]{2,1,0:T(1,128)S(1)}, u32[]{:S(2)}, u32[]{:S(2)}) async-start(f32[4,1,1024]{2,1,0:T(1,128)} %broadcast_in_dim.11), calls=%async_computation.1 | async-start | bytes 32768 | tf_op jit(solution)/shard_map/all_to_all | solution.py:61
  315.8 4.1 %fusion.58 = f32[512,2048]{1,0:T(8,128)} fusion(bf16[512,256]{0,1:T(8,128)(2,1)S(1)} %bitcast.1695, bf16[2048,512]{1,0:T(8,128)(2,1)} %all-gather.8.cloned.1.call-done), kind=kOutput, calls=%fused_computation.68 | convolution fusion | flops 536870912 | bytes 5505024 | tf_op jit(solution)/shard_map/dot_general | solution.py:327
  319.9 1.3 all-to-all-done.1
  321.2 3.0 add_convert_fusion
  324.2 22.4 %all_to_all.16 = bf16[4,128,2048]{2,1,0:T(8,128)(2,1)S(1)} all-to-all(bf16[4,128,2048]{2,1,0:T(8,128)(2,1)S(1)} %bitcast.1683), channel_id=1, replica_groups=mesh['sp_0'=16,'sp_1'=4,'sp_2'=2,'tp'=4] {'tp'}, dimensions={0} | all-to-all | bytes 4194304 | tf_op jit(solution)/shard_map/all_to_all | solution.py:118
  346.6 1.3 reduce_sum.52
  (214 shorter events, 17.1 us)
Async XLA Ops:
  6.5 148.4 %all-gather.6.cloned.1.call-start = ((), (), s32[]{:S(2)}) async-start(), calls=%async_computation.3 | async-start | bytes 3170304 | tf_op jit(solution)/shard_map/all_gather | solution.py:93
  10.8 4.7 %copy-start.15 = (bf16[256,16]{0,1:T(8,128)(2,1)S(1)}, bf16[256,16]{0,1:T(8,128)(2,1)}, u32[]{:S(2)}) copy-start(bf16[256,16]{0,1:T(8,128)(2,1)} %param.35) | copy-start | bytes 24580
  10.8 4.7 %copy-start.16 = (bf16[256,16]{0,1:T(8,128)(2,1)S(1)}, bf16[256,16]{0,1:T(8,128)(2,1)}, u32[]{:S(2)}) copy-start(bf16[256,16]{0,1:T(8,128)(2,1)} %param.34) | copy-start | bytes 24580
  10.8 5.4 %copy-start.19 = (f32[16]{0:T(128)S(1)}, f32[16]{0:T(128)}, u32[]{:S(2)}) copy-start(f32[16]{0:T(128)} %param.26) | copy-start | bytes 196
  10.8 5.5 %copy-start.9 = (f32[16,512]{1,0:T(8,128)S(1)}, f32[16,512]{1,0:T(8,128)}, u32[]{:S(2)}) copy-start(f32[16,512]{1,0:T(8,128)} %param.27) | copy-start | bytes 98308
  10.8 7.2 %copy-start.17 = (f32[256]{0:T(256)S(1)}, f32[256]{0:T(256)}, u32[]{:S(2)}) copy-start(f32[256]{0:T(256)} %param.30) | copy-start | bytes 3076
  10.8 7.3 %copy-start.11 = (f32[31,256]{1,0:T(8,128)S(1)}, f32[31,256]{1,0:T(8,128)}, u32[]{:S(2)}) copy-start(f32[31,256]{1,0:T(8,128)} %param.32) | copy-start | bytes 95236
  10.8 7.3 %copy-start.13 = (f32[16,64]{1,0:T(8,128)S(1)}, f32[16,64]{1,0:T(8,128)}, u32[]{:S(2)}) copy-start(f32[16,64]{1,0:T(8,128)} %param.25) | copy-start | bytes 12292
  10.8 7.3 %copy-start.14 = (f32[16,64]{1,0:T(8,128)S(1)}, f32[16,64]{1,0:T(8,128)}, u32[]{:S(2)}) copy-start(f32[16,64]{1,0:T(8,128)} %param.24) | copy-start | bytes 12292
  10.8 30.9 %all-to-all-start = ((bf16[4,512,512]{1,2,0:T(8,128)(2,1)}), bf16[4,512,512]{1,2,0:T(8,128)(2,1)S(1)}, u32[]{:S(2)}, u32[]{:S(2)}) async-start(bf16[4,512,512]{1,2,0:T(8,128)(2,1)} %broadcast_in_dim.10), calls=%async_computation | async-start | bytes 4194304 | tf_op jit(solution)/shard_map/all_to_all | solution.py:61
  15.4 300.3 %all-gather.8.cloned.1.call-start = ((), (), s32[]{:S(2)}) async-start(), calls=%async_computation.4 | async-start | bytes 2113536 | tf_op jit(solution)/shard_map/all_gather | solution.py:101
  35.0 1.9 copy-start
  35.0 3.2 copy-start.2
  35.0 7.3 %copy-start.12 = (f32[2048]{0:T(1024)S(1)}, f32[2048]{0:T(1024)}, u32[]{:S(2)}) copy-start(f32[2048]{0:T(1024)} %param.20) | copy-start | bytes 24580
  44.2 113.6 %copy-start.7 = (f32[2,16,16,64]{3,2,1,0:T(8,128)S(1)}, f32[2,16,16,64]{3,2,1,0:T(8,128)}, u32[]{:S(2)}) copy-start(f32[2,16,16,64]{3,2,1,0:T(8,128)} %param.28) | copy-start | bytes 393220
  157.7 2.3 copy-start.5
  164.2 144.2 %collective-permute-start = (bf16[30,256]{1,0:T(8,128)(2,1)S(1)}, bf16[30,256]{1,0:T(8,128)(2,1)S(1)}, u32[]{:S(2)}, u32[]{:S(2)}) collective-permute-start(bf16[30,256]{1,0:T(8,128)(2,1)S(1)} %slice.869), channel_id=1, source_target_pairs={{0,4},{4,8},{8,12},{12,16},{16,20},{20,24},{24,28},{28,32},{32,36}... | collective-permute-start | bytes 46088 | tf_op jit(solution)/shard_map/ppermute | solution.py:56
  175.0 125.4 %copy-start.10 = (f32[2,16,64]{2,1,0:T(8,128)S(1)}, f32[2,16,64]{2,1,0:T(8,128)}, u32[]{:S(2)}) copy-start(f32[2,16,64]{2,1,0:T(8,128)} %param.31) | copy-start | bytes 24580
  253.4 47.2 %copy-start.8 = (f32[2,16,16,64]{3,2,1,0:T(8,128)S(1)}, f32[2,16,16,64]{3,2,1,0:T(8,128)}, u32[]{:S(2)}) copy-start(f32[2,16,16,64]{3,2,1,0:T(8,128)} %param.29) | copy-start | bytes 393220
  269.1 34.1 %copy-start.4 = (bf16[16,32,16,64]{3,2,1,0:T(8,128)(2,1)S(1)}, bf16[16,32,16,64]{3,2,1,0:T(8,128)(2,1)}, u32[]{:S(2)}) copy-start(bf16[16,32,16,64]{3,2,1,0:T(8,128)(2,1)} %get-tuple-element.73) | copy-start | bytes 3145732
  300.6 3.4 copy-start.1
  303.2 3.0 copy-start.3
  311.5 9.6 %all-to-all-start.1 = ((f32[4,1,1024]{2,1,0:T(1,128)}), f32[4,1,1024]{2,1,0:T(1,128)S(1)}, u32[]{:S(2)}, u32[]{:S(2)}) async-start(f32[4,1,1024]{2,1,0:T(1,128)} %broadcast_in_dim.11), calls=%async_computation.1 | async-start | bytes 32768 | tf_op jit(solution)/shard_map/all_to_all | solution.py:61
  315.8 5.4 %copy-start.6 = (bf16[2048,512]{1,0:T(8,128)(2,1)S(1)}, bf16[2048,512]{1,0:T(8,128)(2,1)}, u32[]{:S(2)}) copy-start(bf16[2048,512]{1,0:T(8,128)(2,1)} %all-gather.8.cloned.1.call-done) | copy-start | bytes 6291460
  315.8 5.4 %copy-start.18 = (f32[256]{0:T(256)S(1)}, f32[256]{0:T(256)}, u32[]{:S(2)}) copy-start(f32[256]{0:T(256)} %param.33) | copy-start | bytes 3076
Sparse Core Ops, SparseCore 0:
  10.5 144.4 all-gather.5
  158.1 137.2 all-gather.7
where the time goes:
time: 356 us; the launch traced here: 355 us
  waiting for transfers between devices  116 us (33%)
  other arithmetic  94 us (26%)
  blocking collectives  69.3 us (19%)
  matrix products  26.4 us (7%)
  local copies, waits for them, and re-layouts  23.9 us (7%)
  between operations  13.9 us (4%)
  starting transfers between devices  11 us (3%)
    all_gather x1, waiting for transfers between devices, side_by_side(): whole = lax.all_gather(both, axis, axis=dim, tiled=True)  111 us
    all_gather x3, blocking collectives, collected_together(): both, at, found = (lax.all_gather(jnp.concatenate(lines), axis), 0, {})  46.9 us
    mul x16, other arithmetic, block_states(): w_re = shrink * (cosine * delta_real + sine * delta_imaginary)  35.1 us
    dynamic_update_slice x16, other arithmetic, state_local(): lax.scan(advance, (zero, zero), (forcing_real.reshape(blocks, length, gro...  30.4 us
    all_to_all x1, blocking collectives, sent_and_summed(): lax.all_to_all(tiles, axis, split_axis=0, concat_axis=0, tiled=True)  22.4 us
    mul x1, other arithmetic, state_local(): exponent_imaginary = grow * jnp.sin(angle)  16.7 us
    all_to_all x2, starting transfers between devices, copy_for_each(): lax.all_to_all(jnp.broadcast_to(value[None], (peers, *value.shape)), axis...  8.89 us
  transfers between devices with their start and end apart: 5, of which 3 were waited for; matrix products, arithmetic and copies ran while one was open for 38% of the time, Pallas kernels for 0%

commit v1 on v0

v1 whole, which is shorter than its diff:
```python
import jax
import jax.numpy as jnp
from jax import lax
from jax.experimental import pallas as pl
from jax.experimental.pallas import tpu as pltpu
from jax.sharding import Mesh
from jax.sharding import PartitionSpec as P

CONV_W = 1024
SP = ("z", "x", "c")
SP_TP = ("z", "x", "c", "tp")
CHUNK = 32
EPS = 1e-06
EXACT = lax.Precision.HIGHEST
F32 = jnp.float32
BF16 = jnp.bfloat16


def copies(value, axis):
    peers = lax.axis_size(axis)
    return lax.all_to_all(
        jnp.broadcast_to(value[None], (peers, *value.shape)), axis, 0, 0, tiled=True
    )


def next_along(block, axis):
    count = lax.axis_size(axis)
    return lax.ppermute(block, axis, [(i, i + 1) for i in range(count - 1)])


def partner(block):
    return lax.ppermute(block, "c", [(0, 1), (1, 0)])


def after(value, *others):
    return lax.optimization_barrier((value, *others))[0]


def along_z(piece):
    return copies(piece, "z")


def along_x(planes):
    return copies(planes, "x")


def whole_specs(arrays):
    return [pl.BlockSpec(memory_space=pltpu.VMEM) for _ in arrays]


def call(body, outs, arrays, scalars=(), scratch=(), **costs):
    return pl.pallas_call(
        body,
        out_shape=outs,
        in_specs=[pl.BlockSpec(memory_space=pltpu.SMEM) for _ in scalars] + whole_specs(arrays),
        out_specs=jax.tree.map(lambda _: pl.BlockSpec(memory_space=pltpu.VMEM), outs),
        scratch_shapes=list(scratch),
        cost_estimate=pl.CostEstimate(**costs) if costs else None,
    )(*scalars, *arrays)


def natural_order(core_ref, own_ref, other_ref, into_ref):
    peers_x, peers_z, rows, _ = own_ref.shape

    def place(first, second):
        for z in range(peers_z):
            for x in range(peers_x):
                for c, source in enumerate((first, second)):
                    at = ((z * peers_x + x) * 2 + c) * rows
                    into_ref[at : at + rows, :] = source[x, z]

    @pl.when(core_ref[0] == 0)
    def _():
        place(own_ref, other_ref)

    @pl.when(core_ref[0] == 1)
    def _():
        place(other_ref, own_ref)


def dot_rows(a, b):
    return lax.dot_general(a, b, (((1,), (1,)), ((), ())), preferred_element_type=F32)


def state_in_kernel(core_ref, normed_ref, own_ref, other_ref, out_ref, weight_ref):
    natural_order(core_ref, own_ref, other_ref, weight_ref)
    out_ref[...] = jnp.dot(
        normed_ref[...], weight_ref[...], preferred_element_type=F32
    ).astype(BF16)


def glu_kernel(core_ref, normed_ref, own_ref, other_ref, out_ref, weight_ref):
    natural_order(core_ref, own_ref, other_ref, weight_ref)
    width = out_ref.shape[1]
    both = jnp.dot(normed_ref[...], weight_ref[...], preferred_element_type=F32)
    value = both[:, :width].astype(BF16).astype(F32)
    gate = both[:, width:].astype(BF16).astype(F32)
    out_ref[...] = (value * jax.nn.sigmoid(gate)).astype(BF16)


def scan_kernel(
    u_ref,
    grow_ref,
    shrink_ref,
    in_ref,
    out_mat_ref,
    fwd_re_ref,
    fwd_im_ref,
    inv_re_ref,
    inv_im_ref,
    hop_re_ref,
    hop_im_ref,
    lower_ref,
    skip_ref,
    y_ref,
    last_ref,
    cum_re_ref,
    cum_im_ref,
    end_re_ref,
    end_im_ref,
):
    count, width = u_ref.shape
    states = fwd_re_ref.shape[1]
    chunks = count // CHUNK
    block = lower_ref.shape[0]
    slab = 256
    u = u_ref[...].astype(F32)
    scaled = (u * shrink_ref[...]).astype(BF16)

    def chunked(value):
        return value.reshape(chunks, CHUNK, slab)

    def summed(value):
        value = value.reshape(count, slab).astype(BF16)
        return jnp.concatenate(
            [
                jnp.dot(lower_ref[...], value[k : k + block], preferred_element_type=F32)
                for k in range(0, count, block)
            ]
        )

    def first_pass(j, _):
        at = pl.ds(pl.multiple_of(j * slab, slab), slab)
        at_im = pl.ds(pl.multiple_of(states + j * slab, slab), slab)
        d_re = chunked(jnp.dot(scaled, in_ref[:, at], preferred_element_type=F32))
        d_im = chunked(jnp.dot(scaled, in_ref[:, at_im], preferred_element_type=F32))
        i_re, i_im = inv_re_ref[:, at][None], inv_im_ref[:, at][None]
        cum_re = summed(i_re * d_re - i_im * d_im)
        cum_im = summed(i_re * d_im + i_im * d_re)
        cum_re_ref[:, at] = cum_re
        cum_im_ref[:, at] = cum_im
        end_re_ref[:, at] = chunked(cum_re)[:, CHUNK - 1]
        end_im_ref[:, at] = chunked(cum_im)[:, CHUNK - 1]
        return 0

    lax.fori_loop(0, states // slab, first_pass, 0)

    h_re, h_im = hop_re_ref[0], hop_im_ref[0]
    t_re, t_im = end_re_ref[...], end_im_ref[...]
    s_re = h_re * t_re - h_im * t_im
    s_im = h_re * t_im + h_im * t_re
    for level in range(1, hop_re_ref.shape[0]):
        h_re, h_im = hop_re_ref[level], hop_im_ref[level]
        p_re, p_im = pltpu.roll(s_re, 1 << (level - 1), 0), pltpu.roll(s_im, 1 << (level - 1), 0)
        s_re, s_im = s_re + h_re * p_re - h_im * p_im, s_im + h_re * p_im + h_im * p_re
    lanes = last_ref.shape[1]
    for k in range(states // lanes):
        last_ref[k : k + 1, :] = s_re[chunks - 1 :, k * lanes : (k + 1) * lanes]
        row = states // lanes + k
        last_ref[row : row + 1, :] = s_im[chunks - 1 :, k * lanes : (k + 1) * lanes]
    begins = lax.broadcasted_iota(jnp.int32, s_re.shape, 0) > 0
    end_re_ref[...] = jnp.where(begins, pltpu.roll(s_re, 1, 0), 0.0)
    end_im_ref[...] = jnp.where(begins, pltpu.roll(s_im, 1, 0), 0.0)
    y_ref[...] = jnp.zeros(y_ref.shape, F32)

    def second_pass(j, _):
        at = pl.ds(pl.multiple_of(j * slab, slab), slab)
        at_im = pl.ds(pl.multiple_of(states + j * slab, slab), slab)
        t_re = chunked(cum_re_ref[:, at]) + end_re_ref[:, at][:, None]
        t_im = chunked(cum_im_ref[:, at]) + end_im_ref[:, at][:, None]
        f_re, f_im = fwd_re_ref[:, at][None], fwd_im_ref[:, at][None]
        x_re = (f_re * t_re - f_im * t_im).reshape(count, slab).astype(BF16)
        x_im = (f_re * t_im + f_im * t_re).reshape(count, slab).astype(BF16)
        y_ref[...] += dot_rows(x_re, out_mat_ref[:, at]) + dot_rows(x_im, out_mat_ref[:, at_im])
        return 0

    lax.fori_loop(0, states // slab, second_pass, 0)
    y_ref[...] = y_ref[...] * grow_ref[...] + skip_ref[...] * u


def merge_kernel(
    core_ref,
    y_ref,
    power_ref,
    h_re_ref,
    h_im_ref,
    read_re_ref,
    read_im_ref,
    conv_ref,
    own_ref,
    other_ref,
    out_ref,
    weight_ref,
):
    natural_order(core_ref, own_ref, other_ref, weight_ref)
    width = y_ref.shape[1]
    h_re, h_im = h_re_ref[...], h_im_ref[...]
    c_re, c_im = read_re_ref[...], read_im_ref[...]
    blend = jnp.concatenate(
        [(c_re * h_re - c_im * h_im).astype(BF16), (-c_re * h_im - c_im * h_re).astype(BF16)], axis=1
    )
    total = y_ref[...] + dot_rows(power_ref[...], blend)
    ssm = jax.nn.gelu(total).astype(BF16)
    both = jnp.concatenate([ssm, conv_ref[...]], axis=1)
    out_ref[...] = dot_rows(both, weight_ref[...]).astype(BF16)


def input_matrix(eigen_real, eigen_imag, step, state_input):
    base = eigen_real * step[:, None]
    theta = eigen_imag * step[:, None]
    magnitude = jnp.exp(base)
    near_re = magnitude * jnp.cos(theta) - 1.0
    near_im = magnitude * jnp.sin(theta)
    modulus = eigen_real * eigen_real + eigen_imag * eigen_imag
    ratio_re = (near_re * eigen_real + near_im * eigen_imag) / modulus
    ratio_im = (near_im * eigen_real - near_re * eigen_imag) / modulus
    in_re, in_im = state_input[0], state_input[1]
    return (
        ratio_re[:, None, :] * in_re - ratio_im[:, None, :] * in_im,
        ratio_re[:, None, :] * in_im + ratio_im[:, None, :] * in_re,
    )


def on_diagonal(blocks):
    groups, rows, cols = blocks.shape
    tiled = jnp.tile(blocks.reshape(groups * rows, cols), (1, groups))
    row_group = lax.broadcasted_iota(jnp.int32, tiled.shape, 0) // rows
    col_group = lax.broadcasted_iota(jnp.int32, tiled.shape, 1) // cols
    return jnp.where(row_group == col_group, tiled, 0.0)


def spread_over(groups, each):
    row = lax.broadcasted_iota(jnp.int32, (groups, groups * each), 0)
    col = lax.broadcasted_iota(jnp.int32, (groups, groups * each), 1) // each
    return (row == col).astype(F32)


def squared(re, im):
    return re * re - im * im, 2.0 * re * im


def times(a, b):
    return a[0] * b[0] - a[1] * b[1], a[0] * b[1] + a[1] * b[0]


def tables(eigen_real, eigen_imag, log_step, decay_shift, state_input, readout):
    groups, states = eigen_real.shape
    lanes = groups * states
    count = decay_shift.shape[1]
    chunks = count // CHUNK
    step = jnp.exp(log_step)
    base = (eigen_real * step[:, None]).reshape(1, lanes)
    theta = (eigen_imag * step[:, None]).reshape(1, lanes)
    inside = jnp.arange(1, CHUNK + 1, dtype=F32)[:, None]
    level, angle = inside * base, inside * theta
    cosine, sine = jnp.cos(angle), jnp.sin(angle)
    grow, shrink = jnp.exp(level), jnp.exp(-level)
    forward = (grow * cosine, grow * sine)
    inverse = (shrink * cosine, -shrink * sine)
    shift = decay_shift.T
    lower = jnp.tril(jnp.ones((CHUNK, CHUNK), F32))
    partial = jnp.einsum(
        "ls,csg->clg", lower, shift.reshape(chunks, CHUNK, groups), precision=EXACT
    )
    sums = partial[:, -1]
    earlier = jnp.tril(jnp.ones((chunks, chunks), F32), -1)
    before = jnp.dot(earlier, sums, precision=EXACT)
    whole = (partial + before[:, None]).reshape(count, groups)
    partial = partial.reshape(count, groups)
    spread = spread_over(groups, states)
    wide = jnp.dot(whole, spread, precision=EXACT)
    narrow = jnp.dot(partial, spread_over(groups, 16), precision=EXACT)
    chunk_rot = (jnp.cos(CHUNK * theta), jnp.sin(CHUNK * theta))
    rots = [chunk_rot]
    while (1 << len(rots)) <= chunks:
        rots.append(squared(*rots[-1]))
    index = jnp.arange(chunks)
    hops = [(jnp.exp(CHUNK * base + jnp.dot(sums, spread, precision=EXACT)), rots[0])]
    distance, place = 1, 0
    while distance < chunks:
        window = (
            (index[:, None] >= index[None, :]) & (index[:, None] - index[None, :] < distance)
        ).astype(F32)
        near = jnp.dot(jnp.dot(window, sums, precision=EXACT), spread, precision=EXACT)
        size = jnp.where(index[:, None] >= distance, jnp.exp(distance * CHUNK * base + near), 0.0)
        hops.append((size, rots[place]))
        distance, place = distance * 2, place + 1
    hop_re = jnp.stack([size * rot[0] for size, rot in hops])
    hop_im = jnp.stack([size * rot[1] for size, rot in hops])
    starts = index.astype(F32)[:, None] * CHUNK * theta
    turn = times(
        (jnp.cos(starts)[:, None], jnp.sin(starts)[:, None]), (cosine[None], sine[None])
    )
    counts = jnp.arange(1, count + 1, dtype=F32)[:, None]
    size = jnp.exp(counts * base + wide)
    power = jnp.concatenate(
        [(size * t.reshape(count, lanes)).astype(BF16) for t in turn], axis=1
    )
    b_re, b_im = input_matrix(eigen_real, eigen_imag, step, state_input)
    into = jnp.concatenate([on_diagonal(b_re), on_diagonal(b_im)], axis=1).astype(BF16)
    c_re, c_im = on_diagonal(readout[0]), on_diagonal(readout[1])
    out = jnp.concatenate([c_re, -c_im], axis=1).astype(BF16)
    block = min(count, 256)
    at = jnp.arange(block)
    lower_block = (
        (at[:, None] >= at[None, :]) & (at[:, None] // CHUNK == at[None, :] // CHUNK)
    ).astype(BF16)
    device = dict(
        base=base.reshape(-1, 128),
        turn=tuple(r.reshape(-1, 128) for r in rots[-1]),
        shift=wide[-1].reshape(-1, 128),
    )
    scan = (jnp.exp(narrow), jnp.exp(-narrow), into, out, *forward, *inverse, hop_re, hop_im, lower_block)
    return scan, power, (c_re.astype(BF16), c_im.astype(BF16)), device, count


def pulled(packed, rows):
    return packed[:rows], packed[rows : 2 * rows], packed[2 * rows :]


def carry_in(last, device, count, init_state):
    rows = device["base"].shape[0]
    base, turn = device["base"], device["turn"]
    plane = ("x", "c")
    packed = jnp.concatenate([last, device["shift"]])
    near = copies(packed, plane)
    peers, place = lax.axis_size(plane), lax.axis_index(plane)
    zero = jnp.zeros_like(base)
    run = (zero, zero)
    before, shift_before = run, zero
    shift_run = zero
    for k in range(peers):
        re, im, shift = pulled(near[k], rows)
        size = jnp.exp(count * base + shift)
        moved = times((size * turn[0], size * turn[1]), run)
        run = (moved[0] + re, moved[1] + im)
        shift_run = shift_run + shift
        passed = k < place
        before = jax.tree.map(lambda new, old: jnp.where(passed, new, old), run, before)
        shift_before = jnp.where(passed, shift_run, shift_before)
    far = copies(jnp.concatenate([*run, shift_run]), "z")
    plane_turn, at = turn, 1
    while at < peers:
        plane_turn, at = squared(*plane_turn), at * 2
    h = tuple(s.reshape(-1, 128) for s in (init_state[0], init_state[1]))
    for k in range(lax.axis_size("z")):
        re, im, shift = pulled(far[k], rows)
        size = jnp.exp(peers * count * base + shift)
        moved = times((size * plane_turn[0], size * plane_turn[1]), h)
        passed = k < lax.axis_index("z")
        h = tuple(jnp.where(passed, m + s, o) for m, s, o in zip(moved, (re, im), h))
    turns = (jnp.ones_like(base), zero)
    for k in range(peers):
        passed = k < place
        turns = tuple(jnp.where(passed, new, old) for new, old in zip(times(turns, turn), turns))
    size = jnp.exp(place * count * base + shift_before)
    moved = times((size * turns[0], size * turns[1]), h)
    return moved[0] + before[0], moved[1] + before[1]


def summed_over(arrays, axis):
    line = jnp.concatenate([a.reshape(-1) for a in arrays]).reshape(-1, 128)
    total = jnp.sum(copies(line, axis), axis=0).reshape(-1)
    done, at = [], 0
    for a in arrays:
        done.append(total[at : at + a.size].reshape(a.shape))
        at += a.size
    return done


def conv_branch(glu, conv_taps, channel_gain):
    reach = conv_taps.shape[0] - 1
    count = glu.shape[0]
    before = next_along(glu[count - 32 :], SP)[32 - reach :]
    extended = jnp.concatenate([before, glu], axis=0).astype(F32)
    raw = jnp.zeros(glu.shape, F32)
    for offset in range(reach + 1):
        raw = raw + conv_taps[offset] * extended[offset : offset + count]
    first, second = summed_over(
        (jnp.sum(raw, axis=1, keepdims=True), jnp.sum(raw * raw, axis=1, keepdims=True)), "tp"
    )
    middle = first / CONV_W
    spread = second / CONV_W - middle * middle
    scaled = (raw - middle) * lax.rsqrt(spread + EPS) * channel_gain
    return jax.nn.silu(scaled).astype(BF16)


def per_device(
    tokens,
    norm_gain,
    proj_state,
    proj_value,
    proj_gate,
    eigen_real,
    eigen_imag,
    log_step,
    decay_shift,
    state_input,
    readout,
    skip_gain,
    init_state,
    conv_taps,
    channel_gain,
    merge_state,
    merge_conv,
):
    core = lax.axis_index("c").reshape(1).astype(jnp.int32)
    parts = lax.axis_size("tp")
    blocks = copies(tokens, "tp")
    count = tokens.shape[0]
    width = proj_state.shape[1]
    in_z = along_z(proj_state)
    vg_z = along_z(jnp.concatenate([proj_value, proj_gate], axis=1))
    merge_z = along_z(jnp.concatenate([merge_state.T, merge_conv.T], axis=1))
    in_x = along_x(in_z)
    vg_x = along_x(vg_z)
    merge_x = along_x(merge_z)

    scan_tables, power, reads, device, _ = tables(
        eigen_real, eigen_imag, log_step, decay_shift, state_input, readout
    )

    whole = jnp.moveaxis(blocks, 0, 1).reshape(count, -1)
    wide = whole.astype(F32)
    normed = (
        wide * lax.rsqrt(jnp.mean(wide * wide, axis=1, keepdims=True) + EPS) * norm_gain
    ).astype(BF16)

    depth = normed.shape[1]
    u_in = call(
        state_in_kernel,
        jax.ShapeDtypeStruct((count, width), BF16),
        (normed, in_x, partner(in_x)),
        scalars=(core,),
        scratch=(pltpu.VMEM((depth, width), BF16),),
        flops=2 * count * depth * width,
        bytes_accessed=4 * depth * count,
        transcendentals=0,
    )
    lanes = eigen_real.size
    chunks = count // CHUNK
    y_local, last = call(
        scan_kernel,
        (
            jax.ShapeDtypeStruct((count, width), F32),
            jax.ShapeDtypeStruct((2 * lanes // 128, 128), F32),
        ),
        (u_in, *scan_tables, skip_gain.reshape(1, -1)),
        scratch=(
            pltpu.VMEM((count, lanes), F32),
            pltpu.VMEM((count, lanes), F32),
            pltpu.VMEM((chunks, lanes), F32),
            pltpu.VMEM((chunks, lanes), F32),
        ),
        flops=12 * count * width * lanes,
        bytes_accessed=8 * count * lanes,
        transcendentals=0,
    )
    h_re, h_im = carry_in(last, device, count, init_state)

    glu = call(
        glu_kernel,
        jax.ShapeDtypeStruct((count, width), BF16),
        (normed, vg_x, partner(vg_x)),
        scalars=(core,),
        scratch=(pltpu.VMEM((depth, 2 * width), BF16),),
        flops=4 * count * depth * width,
        bytes_accessed=4 * depth * count,
        transcendentals=0,
    )
    conv_out = conv_branch(glu, conv_taps, channel_gain)

    product = call(
        merge_kernel,
        jax.ShapeDtypeStruct((count, depth), BF16),
        (
            y_local,
            power,
            h_re.reshape(1, -1),
            h_im.reshape(1, -1),
            *reads,
            conv_out,
            merge_x,
            partner(merge_x),
        ),
        scalars=(core,),
        scratch=(pltpu.VMEM((depth, 2 * width), BF16),),
        flops=4 * count * depth * width,
        bytes_accessed=4 * depth * count,
        transcendentals=0,
    )
    arrived = lax.all_to_all(
        product.reshape(parts, count // parts, depth), "tp", split_axis=0, concat_axis=0, tiled=True
    )
    return arrived.astype(F32).sum(axis=0).astype(BF16)


def finer_mesh(mesh):
    cores = 2
    return Mesh(mesh.devices.reshape(16, 4, cores, mesh.shape["tp"]), SP_TP)


def solution(mesh):
    return jax.shard_map(
        per_device,
        mesh=finer_mesh(mesh),
        in_specs=(
            P(SP, "tp"),
            P(),
            P(SP, "tp"),
            P(SP, "tp"),
            P(SP, "tp"),
            P("tp", None),
            P("tp", None),
            P("tp"),
            P("tp", SP),
            P(None, "tp", None, None),
            P(None, "tp", None, None),
            P("tp"),
            P(None, "tp", None),
            P(None, "tp"),
            P("tp"),
            P("tp", SP),
            P("tp", SP),
        ),
        out_specs=P(SP_TP, None),
        check_vma=False,
    )
```

time: 356 us -> 270 us (0.76)
  starting transfers between devices: 11 us -> 74.9 us
  other arithmetic: 94 us -> 32.4 us
  waiting for transfers between devices: 116 us -> 55 us
  blocking collectives: 69.3 us -> 38.6 us
  Pallas kernels: 0 us -> 22.2 us
  matrix products: 26.4 us -> 11 us
  between operations: 13.9 us -> 1.36 us
  local copies, waits for them, and re-layouts: 23.9 us -> 32.4 us
    all_gather x2 -> x0, waiting for transfers between devices: 111 us -> none  [the longest x1 111 us: side_by_side(): whole = lax.all_gather(both, axis, axis=dim, tiled=True)]
    all_to_all x2 -> x9, starting transfers between devices: 8.89 us -> 66.8 us  [copies(): lax.all_to_all(jnp.broadcast_to(value[None], (peers, *value.shape)), axis...]
    mul x33 -> x3, other arithmetic: 51.9 us -> 2.12 us  [the longest x1 1.45 us: carry_in(): size = jnp.exp(peers * count * base + shift)]
    all_to_all x2 -> x9, waiting for transfers between devices: 4.78 us -> 53.5 us  [copies(): lax.all_to_all(jnp.broadcast_to(value[None], (peers, *value.shape)), axis...]
    all_gather x3 -> x0, blocking collectives: 46.9 us -> none  [collected_together(): both, at, found = (lax.all_gather(jnp.concatenate(lines), axis), 0, {})]
    dynamic_update_slice x16 -> x0, other arithmetic: 30.4 us -> none  [state_local(): lax.scan(advance, (zero, zero), (forcing_real.reshape(blocks, length, gro...]
    pallas_call x0 -> x4, Pallas kernels: none -> 22.2 us  [call(): pl.pallas_call(body, out_shape=outs, in_specs=[pl.BlockSpec(memory_space=...]
    all_to_all x1 -> x2, blocking collectives: 22.4 us -> 38.6 us  [the longest x1 30.5 us: per_device(): lax.all_to_all(product.reshape(parts, count // parts, depth), 'tp', split...]
  transfers between devices with their start and end apart: 5 -> 13, of which waited for: 3 -> 9; matrix products, arithmetic and copies ran while one was open for 38% -> 24% of each run, Pallas kernels for 0% -> 6%
where the time goes in v1:
time: 270 us; the launch traced here: 268 us
  starting transfers between devices  74.9 us (28%)
  waiting for transfers between devices  55 us (20%)
  blocking collectives  38.6 us (14%)
  local copies, waits for them, and re-layouts  32.4 us (12%)
  other arithmetic  32.4 us (12%)
  Pallas kernels  22.2 us (8%)
  matrix products  11 us (4%)
    all_to_all x9, starting transfers between devices, copies(): lax.all_to_all(jnp.broadcast_to(value[None], (peers, *value.shape)), axis...  66.8 us
    all_to_all x9, waiting for transfers between devices, copies(): lax.all_to_all(jnp.broadcast_to(value[None], (peers, *value.shape)), axis...  53.5 us
    all_to_all x1, blocking collectives, per_device(): lax.all_to_all(product.reshape(parts, count // parts, depth), 'tp', split...  30.5 us
    pallas_call x4, Pallas kernels, call(): pl.pallas_call(body, out_shape=outs, in_specs=[pl.BlockSpec(memory_space=...  22.2 us
    broadcast_in_dim x10, local copies, waits for them, and re-layouts, copies(): jnp.broadcast_to(value[None], (peers, *value.shape))  10 us
    all_to_all x1, blocking collectives, copies(): lax.all_to_all(jnp.broadcast_to(value[None], (peers, *value.shape)), axis...  8.17 us
    another operation x10, local copies, waits for them, and re-layouts, on_diagonal(): tiled = jnp.tile(blocks.reshape(groups * rows, cols), (1, groups))  7.84 us
    ppermute x3, starting transfers between devices, partner(): return lax.ppermute(block, 'c', [(0, 1), (1, 0)])  6.21 us
  transfers between devices with their start and end apart: 13, of which 9 were waited for; matrix products, arithmetic and copies ran while one was open for 24% of the time, Pallas kernels for 6%

profile of v1, /device:TPU:6, one launch (start us, length us, event | category | flops | bytes accessed | tf_op | source)
XLA Modules:
  0.0 267.9 jit_solution(10960439293517859361)
XLA Ops:
  0.0 1.4 broadcast_in_dim.75
  1.4 15.3 %all-to-all-start.1 = ((bf16[16,16,256]{2,1,0:T(8,128)(2,1)}), bf16[16,16,256]{2,1,0:T(8,128)(2,1)S(1)}, u32[]{:S(2)}, u32[]{:S(2)}) async-start(bf16[16,16,256]{2,1,0:T(8,128)(2,1)} %broadcast_in_dim.75), calls=%async_computation.1 | async-start | bytes 262144 | tf_op jit(solution)/shard_map/all_to_all | solution.py:21
  16.8 0.8 reshape.2923
  21.7 1.5 broadcast_multiply_fusion.1
  23.3 1.0 fusion.145
  25.0 1.3 multiply_cosine_fusion
  29.9 1.9 multiply_subtract_fusion
  31.8 0.8 broadcast_in_dim.76
  32.7 4.8 %all-to-all-start.2 = ((bf16[4,16,16,256]{3,2,1,0:T(8,128)(2,1)}), bf16[4,16,16,256]{3,2,1,0:T(8,128)(2,1)S(1)}, u32[]{:S(2)}, u32[]{:S(2)}) async-start(bf16[4,16,16,256]{3,2,1,0:T(8,128)(2,1)} %broadcast_in_dim.76), calls=%async_computation.2 | async-start | bytes 1048576 | tf_op jit(solution)/shard_map/all_to_all | solution.py:21
  37.4 5.2 %fusion.2 = (bf16[512,1024]{1,0:T(8,128)(2,1)}, bf16[512,1024]{1,0:T(8,128)(2,1)}, f32[512,1024]{1,0:T(8,128)}) fusion(f32[16,32,1024]{2,1,0:T(8,128)S(1)} %get-tuple-element.22, f32[1024]{0:T(1024)S(1)} %mul.4072, f32[512]{0:T(512)S(1)} %iota_add_fusion, f32[16,32,1024]{2,1,0:T(8,128)} %get-tuple-element.23, f32[512,16]{0,1:T(8,128)S(1)} %reshape.2926, ...), kind=kOutput, calls=%fused_computation.8 | convolution fusion | flops 103841792 | bytes 8436736 | tf_op jit(solution)/shard_map/dot_general | solution.py:281
  42.7 1.9 all-to-all-done.2.own_ref
  44.6 2.7 %broadcast_in_dim.74 = bf16[4,512,512]{2,1,0:T(8,128)(2,1)} broadcast(bf16[512,512]{1,0:T(8,128)(2,1)} %param.17), dimensions={1,2} | broadcast | bytes 2621440 | tf_op jit(solution)/shard_map/broadcast_in_dim | solution.py:22
  47.3 4.6 %all-to-all-start = ((bf16[4,512,512]{2,1,0:T(8,128)(2,1)}), bf16[4,512,512]{2,1,0:T(8,128)(2,1)S(1)}, u32[]{:S(2)}, u32[]{:S(2)}) async-start(bf16[4,512,512]{2,1,0:T(8,128)(2,1)} %broadcast_in_dim.74), calls=%async_computation | async-start | bytes 4194304 | tf_op jit(solution)/shard_map/all_to_all | solution.py:21
  53.2 0.8 fusion.50
  54.1 1.0 copy.61
  55.2 1.0 copy.63
  56.3 1.1 tile.44
  57.6 1.6 copy.67
  59.3 0.8 tile.41
  60.1 2.1 copy.65
  62.3 0.8 slice.1043
  63.1 0.8 bitcast_dynamic-update-slice_fusion.1
  64.0 0.8 bitcast_dynamic-update-slice_fusion
  64.8 2.6 select_convert_fusion.3
  67.4 1.2 pad_maximum_fusion.1.in_ref
  68.8 1.0 pad_maximum_fusion.2.out_mat_ref
  69.9 6.6 %all-to-all-done = bf16[4,512,512]{2,1,0:T(8,128)(2,1)S(1)} async-done(((bf16[4,512,512]{2,1,0:T(8,128)(2,1)}), bf16[4,512,512]{2,1,0:T(8,128)(2,1)S(1)}, u32[]{:S(2)}, u32[]{:S(2)}) %all-to-all-start) | async-done | bytes 2097184 | tf_op jit(solution)/shard_map/all_to_all | solution.py:21
  77.2 11.5 %all-to-all-start.5 = ((bf16[16,16,512]{2,1,0:T(8,128)(2,1)}), bf16[16,16,512]{2,1,0:T(8,128)(2,1)S(1)}, u32[]{:S(2)}, u32[]{:S(2)}) async-start(bf16[16,16,512]{2,1,0:T(8,128)(2,1)} %broadcast_in_dim.93), calls=%async_computation.5 | async-start | bytes 524288 | tf_op jit(solution)/shard_map/all_to_all | solution.py:21
  88.7 1.4 negate_exponential_fusion
  90.1 1.9 collective-permute-start
  92.5 2.6 convert_bitcast_fusion
  95.1 9.4 %all-to-all-done.5 = bf16[16,16,512]{2,1,0:T(8,128)(2,1)S(1)} async-done(((bf16[16,16,512]{2,1,0:T(8,128)(2,1)}), bf16[16,16,512]{2,1,0:T(8,128)(2,1)S(1)}, u32[]{:S(2)}, u32[]{:S(2)}) %all-to-all-start.5) | async-done | bytes 262176 | tf_op jit(solution)/shard_map/all_to_all | solution.py:21
  105.2 5.2 %all-to-all-start.8 = ((bf16[16,16,512]{2,1,0:T(8,128)(2,1)}), bf16[16,16,512]{2,1,0:T(8,128)(2,1)S(1)}, u32[]{:S(2)}, u32[]{:S(2)}) async-start(bf16[16,16,512]{2,1,0:T(8,128)(2,1)} %broadcast_in_dim.96), calls=%async_computation.8 | async-start | bytes 524288 | tf_op jit(solution)/shard_map/all_to_all | solution.py:21
  110.5 2.8 %copy.69 = f32[4,64,8,512]{3,2,0,1:T(8,128)S(1)} copy(f32[4,64,8,512]{3,2,1,0:T(8,128)} %convert_bitcast_fusion) | data formatting | bytes 8388608 | tf_op jit(solution)/shard_map/convert_element_type | solution.py:434
  113.3 1.8 multiply_convert_fusion.normed_ref
  115.1 3.5 %shard_map.163.u_ref = bf16[512,256]{1,0:T(8,128)(2,1)} custom-call(s32[1]{0:T(128)} %bitcast.core_ref, bf16[512,2048]{1,0:T(8,128)(2,1)} %multiply_convert_fusion.normed_ref, bf16[4,16,16,256]{3,2,1,0:T(8,128)(2,1)} %copy-done.4, bf16[4,16,16,256]{3,2,1,0:T(8,128)(2,1)} %collective-permute-done.other_ref), custom_call_target="tpu_custom_call" | custom-call | flops 536870912 | bytes 4194304 | tf_op jit(solution)/shard_map/pallas_call | solution.py:52
  118.6 7.2 %shard_map.164 = (f32[512,256]{1,0:T(8,128)}, f32[16,128]{1,0:T(8,128)}) custom-call(bf16[512,256]{1,0:T(8,128)(2,1)} %shard_map.163.u_ref, f32[512,256]{1,0:T(8,128)} %get-tuple-element.21.grow_ref, f32[512,256]{1,0:T(8,128)} %get-tuple-element.20.shrink_ref, bf16[256,2048]{1,0:T(8,128)(2,1)} %pad_maximum_fusion.1.in_ref, ...), custom_call_target="tpu_custom_call" | custom-call | flops 1610612736 | bytes 4194304 | tf_op jit(solution)/shard_map/pallas_call | solution.py:52
  126.5 0.9 all-to-all-done.8
  127.4 8.2 %all_to_all.55 = f32[8,24,128]{2,1,0:T(8,128)S(1)} all-to-all(f32[8,24,128]{2,1,0:T(8,128)S(1)} %broadcast_in_dim.88), channel_id=1, replica_groups=mesh['z'=16,'x'=4,'c'=2,'tp'=4] {'x','c'}, dimensions={0} | all-to-all | bytes 196608 | tf_op jit(solution)/shard_map/all_to_all | solution.py:21
  135.6 1.1 broadcast_in_dim.94
  136.8 5.6 %all-to-all-start.6 = ((bf16[4,16,16,512]{3,2,1,0:T(8,128)(2,1)}), bf16[4,16,16,512]{3,2,1,0:T(8,128)(2,1)S(1)}, u32[]{:S(2)}, u32[]{:S(2)}) async-start(bf16[4,16,16,512]{3,2,1,0:T(8,128)(2,1)} %broadcast_in_dim.94), calls=%async_computation.6 | async-start | bytes 2097152 | tf_op jit(solution)/shard_map/all_to_all | solution.py:21
  143.2 12.2 %all-to-all-done.6.own_ref = bf16[4,16,16,512]{3,2,1,0:T(8,128)(2,1)S(1)} async-done(((bf16[4,16,16,512]{3,2,1,0:T(8,128)(2,1)}), bf16[4,16,16,512]{3,2,1,0:T(8,128)(2,1)S(1)}, u32[]{:S(2)}, u32[]{:S(2)}) %all-to-all-start.6) | async-done | bytes 1048608 | tf_op jit(solution)/shard_map/all_to_all | solution.py:21
  155.5 1.2 broadcast_in_dim.97
  156.7 5.6 %all-to-all-start.9 = ((bf16[4,16,16,512]{3,2,1,0:T(8,128)(2,1)}), bf16[4,16,16,512]{3,2,1,0:T(8,128)(2,1)S(1)}, u32[]{:S(2)}, u32[]{:S(2)}) async-start(bf16[4,16,16,512]{3,2,1,0:T(8,128)(2,1)} %broadcast_in_dim.97), calls=%async_computation.9 | async-start | bytes 2097152 | tf_op jit(solution)/shard_map/all_to_all | solution.py:21
  162.3 12.2 %all-to-all-done.9.own_ref = bf16[4,16,16,512]{3,2,1,0:T(8,128)(2,1)S(1)} async-done(((bf16[4,16,16,512]{3,2,1,0:T(8,128)(2,1)}), bf16[4,16,16,512]{3,2,1,0:T(8,128)(2,1)S(1)}, u32[]{:S(2)}, u32[]{:S(2)}) %all-to-all-start.9) | async-done | bytes 1048608 | tf_op jit(solution)/shard_map/all_to_all | solution.py:21
  175.3 11.1 %all-to-all-start.4 = ((f32[16,24,128]{2,1,0:T(8,128)}), f32[16,24,128]{2,1,0:T(8,128)S(1)}, u32[]{:S(2)}, u32[]{:S(2)}) async-start(f32[16,24,128]{2,1,0:T(8,128)} %broadcast_in_dim.92), calls=%async_computation.4 | async-start | bytes 393216 | tf_op jit(solution)/shard_map/all_to_all | solution.py:21
  188.2 2.7 %pad_maximum_fusion.power_ref = bf16[512,2048]{1,0:T(8,128)(2,1)} fusion(bf16[512,1024]{1,0:T(8,128)(2,1)} %get-tuple-element.19, bf16[512,1024]{1,0:T(8,128)(2,1)S(1)} %copy-done.3), kind=kLoop, calls=%fused_computation.4 | loop fusion | flops 4194304 | bytes 4194304 | tf_op jit(solution)/shard_map/concatenate | solution.py:306
  190.9 1.9 collective-permute-start.1
  193.5 2.4 collective-permute-start.3
  195.9 5.7 %all-to-all-done.4 = f32[16,24,128]{2,1,0:T(8,128)S(1)} async-done(((f32[16,24,128]{2,1,0:T(8,128)}), f32[16,24,128]{2,1,0:T(8,128)S(1)}, u32[]{:S(2)}, u32[]{:S(2)}) %all-to-all-start.4) | async-done | bytes 196640 | tf_op jit(solution)/shard_map/all_to_all | solution.py:21
  203.3 4.3 %shard_map.165 = bf16[512,256]{1,0:T(8,128)(2,1)} custom-call(s32[1]{0:T(128)} %bitcast.core_ref, bf16[512,2048]{1,0:T(8,128)(2,1)} %multiply_convert_fusion.normed_ref, bf16[4,16,16,512]{3,2,1,0:T(8,128)(2,1)} %copy-done.2, bf16[4,16,16,512]{3,2,1,0:T(8,128)(2,1)} %collective-permute-done.1.other_ref), custom_call_target="tpu_custom_call" | custom-call | flops 1073741824 | bytes 4194304 | tf_op jit(solution)/shard_map/pallas_call | solution.py:52
  208.3 1.9 collective-permute-start.2
  210.5 1.3 fusion.107
  211.8 1.6 collective-permute-done.2
  213.4 1.0 maximum_convert_fusion
  214.5 3.2 %fusion.143 = (f32[512]{0:T(512)S(1)}, f32[512]{0:T(512)S(1)}, f32[512,256]{1,0:T(8,128)S(1)}) fusion(f32[542,256]{1,0:T(8,128)S(1)} %maximum_convert_fusion, f32[256]{0:T(256)} %bitcast.580, f32[256]{0:T(256)} %bitcast.581, f32[256]{0:T(256)S(1)} %bitcast.552, f32[256]{0:T(256)S(1)} %bitcast.553, f32[256]{0:T(256)S(1)} %bitcast.554, f32[256]{0:T(256)S(1)} %bitcast.555, ...), kind=kLoop, calls=%fused_computation.425 | loop fusion | flops 8387584 | bytes 16813056 | tf_op jit(solution)/shard_map/reduce_sum | solution.py:390
  218.4 3.2 %all-to-all-start.7 = ((f32[4,8,128]{2,1,0:T(8,128)}), f32[4,8,128]{2,1,0:T(8,128)S(1)}, u32[]{:S(2)}, u32[]{:S(2)}) async-start(f32[4,8,128]{2,1,0:T(8,128)} %broadcast_in_dim.95), calls=%async_computation.7 | async-start | bytes 32768 | tf_op jit(solution)/shard_map/all_to_all | solution.py:21
  221.6 0.8 fusion.106.h_re_ref
  222.5 4.5 %all-to-all-done.7 = f32[4,8,128]{2,1,0:T(8,128)S(1)} async-done(((f32[4,8,128]{2,1,0:T(8,128)}), f32[4,8,128]{2,1,0:T(8,128)S(1)}, u32[]{:S(2)}, u32[]{:S(2)}) %all-to-all-start.7) | async-done | bytes 16416 | tf_op jit(solution)/shard_map/all_to_all | solution.py:21
  227.0 1.0 multiply_convert_fusion.1.conv_ref
  228.0 1.0 copy-done.6
  229.0 7.2 %shard_map.166 = bf16[512,2048]{1,0:T(8,128)(2,1)} custom-call(s32[1]{0:T(128)} %bitcast.core_ref, f32[512,256]{1,0:T(8,128)} %get-tuple-element.7.y_ref, bf16[512,2048]{1,0:T(8,128)(2,1)} %pad_maximum_fusion.power_ref, f32[1,1024]{1,0:T(1,128)} %fusion.106.h_re_ref, f32[1,1024]{1,0:T(1,128)} %get-tuple-element.12.h_im_ref, bf16[256,1024]{1,0:T(8,128)(2,1)} %copy-done, ...), custom_call_target="tpu_custom_call" | custom-call | flops 1073741824 | bytes 4194304 | tf_op jit(solution)/shard_map/pallas_call | solution.py:52
  236.1 30.5 %all_to_all.56 = bf16[4,128,2048]{2,1,0:T(8,128)(2,1)S(1)} all-to-all(bf16[4,128,2048]{2,1,0:T(8,128)(2,1)} %bitcast.441), channel_id=1, replica_groups=mesh['z'=16,'x'=4,'c'=2,'tp'=4] {'tp'}, dimensions={0} | all-to-all | bytes 4194304 | tf_op jit(solution)/shard_map/all_to_all | solution.py:502
  266.6 1.3 reduce_sum.52
  (249 shorter events, 20.1 us)
Async XLA Ops:
  1.4 27.9 %copy-start.57 = (bf16[16,256]{1,0:T(8,128)(2,1)S(1)}, bf16[16,256]{1,0:T(8,128)(2,1)}, u32[]{:S(2)}) copy-start(bf16[16,256]{1,0:T(8,128)(2,1)} %param.21) | copy-start | bytes 24580
  1.4 27.9 %copy-start.58 = (bf16[16,256]{1,0:T(8,128)(2,1)S(1)}, bf16[16,256]{1,0:T(8,128)(2,1)}, u32[]{:S(2)}) copy-start(bf16[16,256]{1,0:T(8,128)(2,1)} %param.20) | copy-start | bytes 24580
  1.4 30.5 %all-to-all-start.1 = ((bf16[16,16,256]{2,1,0:T(8,128)(2,1)}), bf16[16,16,256]{2,1,0:T(8,128)(2,1)S(1)}, u32[]{:S(2)}, u32[]{:S(2)}) async-start(bf16[16,16,256]{2,1,0:T(8,128)(2,1)} %broadcast_in_dim.75), calls=%async_computation.1 | async-start | bytes 262144 | tf_op jit(solution)/shard_map/all_to_all | solution.py:21
  16.7 20.7 %copy-start.10 = (s32[1024]{0:T(1024)}, s32[1024]{0:T(1024)S(1)}, u32[]{:S(2)}) copy-start(s32[1024]{0:T(1024)S(1)} %get-tuple-element.188) | copy-start | bytes 12292
  16.7 20.7 %copy-start.12 = (s32[1024]{0:T(1024)}, s32[1024]{0:T(1024)S(1)}, u32[]{:S(2)}) copy-start(s32[1024]{0:T(1024)S(1)} %get-tuple-element.189) | copy-start | bytes 12292
  16.7 20.7 %copy-start.52 = (pred[1024]{0:T(1024)(128)(4,1)}, pred[1024]{0:T(1024)(128)(4,1)S(1)}, u32[]{:S(2)}) copy-start(pred[1024]{0:T(1024)(128)(4,1)S(1)} %fusion.131) | copy-start | bytes 3076
  32.7 11.9 %all-to-all-start.2 = ((bf16[4,16,16,256]{3,2,1,0:T(8,128)(2,1)}), bf16[4,16,16,256]{3,2,1,0:T(8,128)(2,1)S(1)}, u32[]{:S(2)}, u32[]{:S(2)}) async-start(bf16[4,16,16,256]{3,2,1,0:T(8,128)(2,1)} %broadcast_in_dim.76), calls=%async_computation.2 | async-start | bytes 1048576 | tf_op jit(solution)/shard_map/all_to_all | solution.py:21
  47.3 29.2 %all-to-all-start = ((bf16[4,512,512]{2,1,0:T(8,128)(2,1)}), bf16[4,512,512]{2,1,0:T(8,128)(2,1)S(1)}, u32[]{:S(2)}, u32[]{:S(2)}) async-start(bf16[4,512,512]{2,1,0:T(8,128)(2,1)} %broadcast_in_dim.74), calls=%async_computation | async-start | bytes 4194304 | tf_op jit(solution)/shard_map/all_to_all | solution.py:21
  68.6 7.9 %copy-start.14 = (bf16[16,512]{1,0:T(8,128)(2,1)S(1)}, bf16[16,512]{1,0:T(8,128)(2,1)}, u32[]{:S(2)}) copy-start(bf16[16,512]{1,0:T(8,128)(2,1)} %pad_maximum_fusion.3) | copy-start | bytes 49156
  68.6 20.1 %copy-start.59 = (bf16[256,16]{0,1:T(8,128)(2,1)S(1)}, bf16[256,16]{0,1:T(8,128)(2,1)}, u32[]{:S(2)}) copy-start(bf16[256,16]{0,1:T(8,128)(2,1)} %param.33) | copy-start | bytes 24580
  68.6 20.1 %copy-start.60 = (bf16[256,16]{0,1:T(8,128)(2,1)S(1)}, bf16[256,16]{0,1:T(8,128)(2,1)}, u32[]{:S(2)}) copy-start(bf16[256,16]{0,1:T(8,128)(2,1)} %param.32) | copy-start | bytes 24580
  68.8 21.3 %copy-start.5 = (bf16[4,16,16,256]{3,2,1,0:T(8,128)(2,1)S(1)}, bf16[4,16,16,256]{3,2,1,0:T(8,128)(2,1)}, u32[]{:S(2)}) copy-start(bf16[4,16,16,256]{3,2,1,0:T(8,128)(2,1)} %copy-done.4) | copy-start | bytes 1572868
  77.2 27.3 %all-to-all-start.5 = ((bf16[16,16,512]{2,1,0:T(8,128)(2,1)}), bf16[16,16,512]{2,1,0:T(8,128)(2,1)S(1)}, u32[]{:S(2)}, u32[]{:S(2)}) async-start(bf16[16,16,512]{2,1,0:T(8,128)(2,1)} %broadcast_in_dim.93), calls=%async_computation.5 | async-start | bytes 524288 | tf_op jit(solution)/shard_map/all_to_all | solution.py:21
  90.1 25.0 %collective-permute-start = (bf16[4,16,16,256]{3,2,1,0:T(8,128)(2,1)S(1)}, bf16[4,16,16,256]{3,2,1,0:T(8,128)(2,1)}, u32[]{:S(2)}, u32[]{:S(2)}) collective-permute-start(bf16[4,16,16,256]{3,2,1,0:T(8,128)(2,1)S(1)} %copy-done.5), channel_id=1, source_target_pairs={{0,4},{4,0},{1,5},{5,1},{2,6},{6,2},{3,7},{7,3},{8,12},{12,8},{9,1... | collective-permute-start | bytes 1572872 | tf_op jit(solution)/shard_map/ppermute | solution.py:32
  105.2 22.2 %all-to-all-start.8 = ((bf16[16,16,512]{2,1,0:T(8,128)(2,1)}), bf16[16,16,512]{2,1,0:T(8,128)(2,1)S(1)}, u32[]{:S(2)}, u32[]{:S(2)}) async-start(bf16[16,16,512]{2,1,0:T(8,128)(2,1)} %broadcast_in_dim.96), calls=%async_computation.8 | async-start | bytes 524288 | tf_op jit(solution)/shard_map/all_to_all | solution.py:21
  125.8 16.5 %copy-start.9 = (f32[16,64]{1,0:T(8,128)S(1)}, f32[16,64]{1,0:T(8,128)}, u32[]{:S(2)}) copy-start(f32[16,64]{1,0:T(8,128)} %get-tuple-element.153) | copy-start | bytes 12292
  125.8 16.8 %copy-start.17 = (f32[31,256]{1,0:T(8,128)S(1)}, f32[31,256]{1,0:T(8,128)}, u32[]{:S(2)}) copy-start(f32[31,256]{1,0:T(8,128)} %param.30) | copy-start | bytes 95236
  136.8 18.7 %all-to-all-start.6 = ((bf16[4,16,16,512]{3,2,1,0:T(8,128)(2,1)}), bf16[4,16,16,512]{3,2,1,0:T(8,128)(2,1)S(1)}, u32[]{:S(2)}, u32[]{:S(2)}) async-start(bf16[4,16,16,512]{3,2,1,0:T(8,128)(2,1)} %broadcast_in_dim.94), calls=%async_computation.6 | async-start | bytes 2097152 | tf_op jit(solution)/shard_map/all_to_all | solution.py:21
  142.3 20.0 %copy-start.49 = (f32[2,16,64]{2,1,0:T(8,128)S(1)}, f32[2,16,64]{2,1,0:T(8,128)}, u32[]{:S(2)}) copy-start(f32[2,16,64]{2,1,0:T(8,128)} %param.29) | copy-start | bytes 24580
  143.2 44.1 %copy-start.16 = (f32[16,64]{1,0:T(8,128)S(1)}, f32[16,64]{1,0:T(8,128)}, u32[]{:S(2)}) copy-start(f32[16,64]{1,0:T(8,128)} %get-tuple-element.152) | copy-start | bytes 12292
  143.2 44.1 %copy-start.15 = (f32[16,64]{1,0:T(8,128)S(1)}, f32[16,64]{1,0:T(8,128)}, u32[]{:S(2)}) copy-start(f32[16,64]{1,0:T(8,128)} %get-tuple-element.151) | copy-start | bytes 12292
  143.2 45.0 %copy-start.3 = (bf16[512,1024]{1,0:T(8,128)(2,1)S(1)}, bf16[512,1024]{1,0:T(8,128)(2,1)}, u32[]{:S(2)}) copy-start(bf16[512,1024]{1,0:T(8,128)(2,1)} %get-tuple-element.18) | copy-start | bytes 3145732
  155.5 35.4 %copy-start.2 = (bf16[4,16,16,512]{3,2,1,0:T(8,128)(2,1)}, bf16[4,16,16,512]{3,2,1,0:T(8,128)(2,1)S(1)}, u32[]{:S(2)}) copy-start(bf16[4,16,16,512]{3,2,1,0:T(8,128)(2,1)S(1)} %all-to-all-done.6.own_ref) | copy-start | bytes 3145732
  156.7 17.9 %all-to-all-start.9 = ((bf16[4,16,16,512]{3,2,1,0:T(8,128)(2,1)}), bf16[4,16,16,512]{3,2,1,0:T(8,128)(2,1)S(1)}, u32[]{:S(2)}, u32[]{:S(2)}) async-start(bf16[4,16,16,512]{3,2,1,0:T(8,128)(2,1)} %broadcast_in_dim.97), calls=%async_computation.9 | async-start | bytes 2097152 | tf_op jit(solution)/shard_map/all_to_all | solution.py:21
  174.6 18.9 %copy-start.1 = (bf16[4,16,16,512]{3,2,1,0:T(8,128)(2,1)}, bf16[4,16,16,512]{3,2,1,0:T(8,128)(2,1)S(1)}, u32[]{:S(2)}) copy-start(bf16[4,16,16,512]{3,2,1,0:T(8,128)(2,1)S(1)} %all-to-all-done.9.own_ref) | copy-start | bytes 3145732
  175.3 26.3 %all-to-all-start.4 = ((f32[16,24,128]{2,1,0:T(8,128)}), f32[16,24,128]{2,1,0:T(8,128)S(1)}, u32[]{:S(2)}, u32[]{:S(2)}) async-start(f32[16,24,128]{2,1,0:T(8,128)} %broadcast_in_dim.92), calls=%async_computation.4 | async-start | bytes 393216 | tf_op jit(solution)/shard_map/all_to_all | solution.py:21
  190.9 12.3 %collective-permute-start.1 = (bf16[4,16,16,512]{3,2,1,0:T(8,128)(2,1)S(1)}, bf16[4,16,16,512]{3,2,1,0:T(8,128)(2,1)}, u32[]{:S(2)}, u32[]{:S(2)}) collective-permute-start(bf16[4,16,16,512]{3,2,1,0:T(8,128)(2,1)S(1)} %all-to-all-done.6.own_ref), channel_id=1, source_target_pairs={{0,4},{4,0},{1,5},{5,1},{2,6},{6,2},{3,7},{7,3},{8,12},{12,8},{9,1... | collective-permute-start | bytes 3145736 | tf_op jit(solution)/shard_map/ppermute | solution.py:32
  193.5 34.5 %collective-permute-start.3 = (bf16[4,16,16,512]{3,2,1,0:T(8,128)(2,1)S(1)}, bf16[4,16,16,512]{3,2,1,0:T(8,128)(2,1)S(1)}, u32[]{:S(2)}, u32[]{:S(2)}) collective-permute-start(bf16[4,16,16,512]{3,2,1,0:T(8,128)(2,1)S(1)} %all-to-all-done.9.own_ref), channel_id=1, source_target_pairs={{0,4},{4,0},{1,5},{5,1},{2,6},{6,2},{3,7},{7,3},{8,12},{12,8},{9,1... | collective-permute-start | bytes 3145736 | tf_op jit(solution)/shard_map/ppermute | solution.py:32
  202.9 7.4 %copy-start.20 = (f32[1,8,128]{2,1,0:T(8,128)S(1)}, f32[1,8,128]{2,1,0:T(8,128)}, u32[]{:S(2)}) copy-start(f32[1,8,128]{2,1,0:T(8,128)} %get-tuple-element.38) | copy-start | bytes 12292
  202.9 7.4 %copy-start.21 = (f32[1,8,128]{2,1,0:T(8,128)S(1)}, f32[1,8,128]{2,1,0:T(8,128)}, u32[]{:S(2)}) copy-start(f32[1,8,128]{2,1,0:T(8,128)} %get-tuple-element.39) | copy-start | bytes 12292
  202.9 7.4 %copy-start.22 = (f32[1,8,128]{2,1,0:T(8,128)S(1)}, f32[1,8,128]{2,1,0:T(8,128)}, u32[]{:S(2)}) copy-start(f32[1,8,128]{2,1,0:T(8,128)} %get-tuple-element.40) | copy-start | bytes 12292
  202.9 7.4 %copy-start.23 = (f32[1,8,128]{2,1,0:T(8,128)S(1)}, f32[1,8,128]{2,1,0:T(8,128)}, u32[]{:S(2)}) copy-start(f32[1,8,128]{2,1,0:T(8,128)} %get-tuple-element.41) | copy-start | bytes 12292
  202.9 7.4 %copy-start.24 = (f32[1,8,128]{2,1,0:T(8,128)S(1)}, f32[1,8,128]{2,1,0:T(8,128)}, u32[]{:S(2)}) copy-start(f32[1,8,128]{2,1,0:T(8,128)} %get-tuple-element.42) | copy-start | bytes 12292
  202.9 7.4 %copy-start.25 = (f32[1,8,128]{2,1,0:T(8,128)S(1)}, f32[1,8,128]{2,1,0:T(8,128)}, u32[]{:S(2)}) copy-start(f32[1,8,128]{2,1,0:T(8,128)} %get-tuple-element.43) | copy-start | bytes 12292
  203.0 7.4 %copy-start.26 = (f32[1,8,128]{2,1,0:T(8,128)S(1)}, f32[1,8,128]{2,1,0:T(8,128)}, u32[]{:S(2)}) copy-start(f32[1,8,128]{2,1,0:T(8,128)} %get-tuple-element.44) | copy-start | bytes 12292
  203.0 7.4 %copy-start.27 = (f32[1,8,128]{2,1,0:T(8,128)S(1)}, f32[1,8,128]{2,1,0:T(8,128)}, u32[]{:S(2)}) copy-start(f32[1,8,128]{2,1,0:T(8,128)} %get-tuple-element.45) | copy-start | bytes 12292
  203.0 7.4 %copy-start.28 = (f32[1,8,128]{2,1,0:T(8,128)S(1)}, f32[1,8,128]{2,1,0:T(8,128)}, u32[]{:S(2)}) copy-start(f32[1,8,128]{2,1,0:T(8,128)} %get-tuple-element.46) | copy-start | bytes 12292
  203.0 7.4 %copy-start.29 = (f32[1,8,128]{2,1,0:T(8,128)S(1)}, f32[1,8,128]{2,1,0:T(8,128)}, u32[]{:S(2)}) copy-start(f32[1,8,128]{2,1,0:T(8,128)} %get-tuple-element.47) | copy-start | bytes 12292
  203.0 7.4 %copy-start.30 = (f32[1,8,128]{2,1,0:T(8,128)S(1)}, f32[1,8,128]{2,1,0:T(8,128)}, u32[]{:S(2)}) copy-start(f32[1,8,128]{2,1,0:T(8,128)} %get-tuple-element.48) | copy-start | bytes 12292
  203.0 7.4 %copy-start.31 = (f32[1,8,128]{2,1,0:T(8,128)S(1)}, f32[1,8,128]{2,1,0:T(8,128)}, u32[]{:S(2)}) copy-start(f32[1,8,128]{2,1,0:T(8,128)} %get-tuple-element.49) | copy-start | bytes 12292
  203.0 7.4 %copy-start.32 = (f32[1,8,128]{2,1,0:T(8,128)S(1)}, f32[1,8,128]{2,1,0:T(8,128)}, u32[]{:S(2)}) copy-start(f32[1,8,128]{2,1,0:T(8,128)} %get-tuple-element.50) | copy-start | bytes 12292
  203.0 7.4 %copy-start.33 = (f32[1,8,128]{2,1,0:T(8,128)S(1)}, f32[1,8,128]{2,1,0:T(8,128)}, u32[]{:S(2)}) copy-start(f32[1,8,128]{2,1,0:T(8,128)} %get-tuple-element.51) | copy-start | bytes 12292
  203.0 7.4 %copy-start.34 = (f32[1,8,128]{2,1,0:T(8,128)S(1)}, f32[1,8,128]{2,1,0:T(8,128)}, u32[]{:S(2)}) copy-start(f32[1,8,128]{2,1,0:T(8,128)} %get-tuple-element.52) | copy-start | bytes 12292
  203.0 7.4 %copy-start.35 = (f32[1,8,128]{2,1,0:T(8,128)S(1)}, f32[1,8,128]{2,1,0:T(8,128)}, u32[]{:S(2)}) copy-start(f32[1,8,128]{2,1,0:T(8,128)} %get-tuple-element.53) | copy-start | bytes 12292
  203.1 7.4 %copy-start.36 = (f32[1,8,128]{2,1,0:T(8,128)S(1)}, f32[1,8,128]{2,1,0:T(8,128)}, u32[]{:S(2)}) copy-start(f32[1,8,128]{2,1,0:T(8,128)} %get-tuple-element.54) | copy-start | bytes 12292
  203.1 7.4 %copy-start.37 = (f32[1,8,128]{2,1,0:T(8,128)S(1)}, f32[1,8,128]{2,1,0:T(8,128)}, u32[]{:S(2)}) copy-start(f32[1,8,128]{2,1,0:T(8,128)} %get-tuple-element.55) | copy-start | bytes 12292
  203.1 7.4 %copy-start.38 = (f32[1,8,128]{2,1,0:T(8,128)S(1)}, f32[1,8,128]{2,1,0:T(8,128)}, u32[]{:S(2)}) copy-start(f32[1,8,128]{2,1,0:T(8,128)} %get-tuple-element.56) | copy-start | bytes 12292
  203.1 7.4 %copy-start.39 = (f32[1,8,128]{2,1,0:T(8,128)S(1)}, f32[1,8,128]{2,1,0:T(8,128)}, u32[]{:S(2)}) copy-start(f32[1,8,128]{2,1,0:T(8,128)} %get-tuple-element.57) | copy-start | bytes 12292
  203.1 7.4 %copy-start.40 = (f32[1,8,128]{2,1,0:T(8,128)S(1)}, f32[1,8,128]{2,1,0:T(8,128)}, u32[]{:S(2)}) copy-start(f32[1,8,128]{2,1,0:T(8,128)} %get-tuple-element.58) | copy-start | bytes 12292
  203.1 7.4 %copy-start.41 = (f32[1,8,128]{2,1,0:T(8,128)S(1)}, f32[1,8,128]{2,1,0:T(8,128)}, u32[]{:S(2)}) copy-start(f32[1,8,128]{2,1,0:T(8,128)} %get-tuple-element.59) | copy-start | bytes 12292
  203.1 7.4 %copy-start.42 = (f32[1,8,128]{2,1,0:T(8,128)S(1)}, f32[1,8,128]{2,1,0:T(8,128)}, u32[]{:S(2)}) copy-start(f32[1,8,128]{2,1,0:T(8,128)} %get-tuple-element.60) | copy-start | bytes 12292
  203.1 7.4 %copy-start.43 = (f32[1,8,128]{2,1,0:T(8,128)S(1)}, f32[1,8,128]{2,1,0:T(8,128)}, u32[]{:S(2)}) copy-start(f32[1,8,128]{2,1,0:T(8,128)} %get-tuple-element.61) | copy-start | bytes 12292
  203.2 11.2 %copy-start.62 = (f32[1,256]{1,0:T(1,128)S(1)}, f32[1,256]{1,0:T(1,128)}, u32[]{:S(2)}) copy-start(f32[1,256]{1,0:T(1,128)} %get-tuple-element.112) | copy-start | bytes 3076
  203.2 11.2 %copy-start.63 = (f32[1,256]{1,0:T(1,128)S(1)}, f32[1,256]{1,0:T(1,128)}, u32[]{:S(2)}) copy-start(f32[1,256]{1,0:T(1,128)} %get-tuple-element.113) | copy-start | bytes 3076
  203.2 11.2 %copy-start.64 = (f32[1,256]{1,0:T(1,128)S(1)}, f32[1,256]{1,0:T(1,128)}, u32[]{:S(2)}) copy-start(f32[1,256]{1,0:T(1,128)} %get-tuple-element.114) | copy-start | bytes 3076
  203.2 11.2 %copy-start.65 = (f32[1,256]{1,0:T(1,128)S(1)}, f32[1,256]{1,0:T(1,128)}, u32[]{:S(2)}) copy-start(f32[1,256]{1,0:T(1,128)} %get-tuple-element.115) | copy-start | bytes 3076
  203.2 11.2 %copy-start.66 = (f32[1,256]{1,0:T(1,128)S(1)}, f32[1,256]{1,0:T(1,128)}, u32[]{:S(2)}) copy-start(f32[1,256]{1,0:T(1,128)} %get-tuple-element.116) | copy-start | bytes 3076
  203.2 11.2 %copy-start.67 = (f32[1,256]{1,0:T(1,128)S(1)}, f32[1,256]{1,0:T(1,128)}, u32[]{:S(2)}) copy-start(f32[1,256]{1,0:T(1,128)} %get-tuple-element.117) | copy-start | bytes 3076
  203.2 11.2 %copy-start.68 = (f32[1,256]{1,0:T(1,128)S(1)}, f32[1,256]{1,0:T(1,128)}, u32[]{:S(2)}) copy-start(f32[1,256]{1,0:T(1,128)} %get-tuple-element.118) | copy-start | bytes 3076
  203.2 11.2 %copy-start.69 = (f32[1,256]{1,0:T(1,128)S(1)}, f32[1,256]{1,0:T(1,128)}, u32[]{:S(2)}) copy-start(f32[1,256]{1,0:T(1,128)} %get-tuple-element.119) | copy-start | bytes 3076
  203.3 11.2 %copy-start.70 = (f32[1,256]{1,0:T(1,128)S(1)}, f32[1,256]{1,0:T(1,128)}, u32[]{:S(2)}) copy-start(f32[1,256]{1,0:T(1,128)} %get-tuple-element.120) | copy-start | bytes 3076
  208.3 5.0 %collective-permute-start.2 = (bf16[32,256]{1,0:T(8,128)(2,1)S(1)}, bf16[32,256]{1,0:T(8,128)(2,1)S(1)}, u32[]{:S(2)}, u32[]{:S(2)}) collective-permute-start(bf16[32,256]{1,0:T(8,128)(2,1)S(1)} %slice.1116), channel_id=1, source_target_pairs={{0,4},{4,8},{8,12},{12,16},{16,20},{20,24},{24,28},{28,32},{32,36}... | collective-permute-start | bytes 49160 | tf_op jit(solution)/shard_map/ppermute | solution.py:28
  214.5 12.5 %copy-start.77 = (f32[256]{0:T(256)S(1)}, f32[256]{0:T(256)}, u32[]{:S(2)}) copy-start(f32[256]{0:T(256)} %param.31) | copy-start | bytes 3076
  218.4 8.6 %all-to-all-start.7 = ((f32[4,8,128]{2,1,0:T(8,128)}), f32[4,8,128]{2,1,0:T(8,128)S(1)}, u32[]{:S(2)}, u32[]{:S(2)}) async-start(f32[4,8,128]{2,1,0:T(8,128)} %broadcast_in_dim.95), calls=%async_computation.7 | async-start | bytes 32768 | tf_op jit(solution)/shard_map/all_to_all | solution.py:21
  (32 other events, 172.3 us)

commit v2 on v1

--- a/solution.py
+++ b/solution.py
@@ -36,21 +36,28 @@
     return lax.optimization_barrier((value, *others))[0]
 
 
+def from_ahead(block, axis, distance):
+    count = lax.axis_size(axis)
+    return lax.ppermute(block, axis, [(i, (i - distance) % count) for i in range(count)])
+
+
 def along_z(piece):
     return copies(piece, "z")
 
 
 def along_x(planes):
-    return copies(planes, "x")
+    peers = lax.axis_size("x")
+    return jnp.stack([planes] + [from_ahead(planes, "x", d) for d in range(1, peers)])
 
 
 def whole_specs(arrays):
     return [pl.BlockSpec(memory_space=pltpu.VMEM) for _ in arrays]
 
 
-def call(body, outs, arrays, scalars=(), scratch=(), **costs):
+def call(body, outs, arrays, scalars=(), scratch=(), mib=16, **costs):
     return pl.pallas_call(
         body,
+        compiler_params=pltpu.CompilerParams(vmem_limit_bytes=mib * 2**20),
         out_shape=outs,
         in_specs=[pl.BlockSpec(memory_space=pltpu.SMEM) for _ in scalars] + whole_specs(arrays),
         out_specs=jax.tree.map(lambda _: pl.BlockSpec(memory_space=pltpu.VMEM), outs),
@@ -59,43 +66,183 @@
     )(*scalars, *arrays)
 
 
-def natural_order(core_ref, own_ref, other_ref, into_ref):
-    peers_x, peers_z, rows, _ = own_ref.shape
-
-    def place(first, second):
-        for z in range(peers_z):
-            for x in range(peers_x):
-                for c, source in enumerate((first, second)):
-                    at = ((z * peers_x + x) * 2 + c) * rows
-                    into_ref[at : at + rows, :] = source[x, z]
-
-    @pl.when(core_ref[0] == 0)
+def natural_order(place_ref, own_ref, other_ref, into_ref, turned):
+    peers_x, _, rows, _ = own_ref.shape
+    blocks = into_ref.shape[0] // rows
+    core, place_x, part = place_ref[0], place_ref[1], place_ref[2]
+    first = part * turned
+
+    def place(by_core):
+        for k in range(blocks):
+            at = lax.rem(first + k, blocks)
+            x = lax.rem(lax.div(at, 2) - place_x + 2 * peers_x, peers_x)
+            into_ref[k * rows : (k + 1) * rows, :] = by_core[k % 2][x, lax.div(at, 2 * peers_x)]
+
+    @pl.when(core == 0)
     def _():
-        place(own_ref, other_ref)
-
-    @pl.when(core_ref[0] == 1)
+        place((own_ref, other_ref))
+
+    @pl.when(core == 1)
     def _():
-        place(other_ref, own_ref)
+        place((other_ref, own_ref))
 
 
 def dot_rows(a, b):
     return lax.dot_general(a, b, (((1,), (1,)), ((), ())), preferred_element_type=F32)
 
 
-def state_in_kernel(core_ref, normed_ref, own_ref, other_ref, out_ref, weight_ref):
-    natural_order(core_ref, own_ref, other_ref, weight_ref)
-    out_ref[...] = jnp.dot(
-        normed_ref[...], weight_ref[...], preferred_element_type=F32
-    ).astype(BF16)
-
-
-def glu_kernel(core_ref, normed_ref, own_ref, other_ref, out_ref, weight_ref):
-    natural_order(core_ref, own_ref, other_ref, weight_ref)
+def norm_kernel(place_ref, own_ref, ahead_ref, top_ref, bottom_ref, behind_ref, gain_ref, out_ref):
+    parts, count, depth = out_ref.shape
+    half = count // 2
+    part = place_ref[2]
+
+    def rows_of(at, opposite_ref):
+        rows = pl.ds(at, half)
+        blocks = [
+            ref.astype(F32)
+            for ref in (own_ref[rows], ahead_ref[rows], opposite_ref[...], behind_ref[rows])
+        ]
+        power = sum(jnp.sum(block * block, axis=1, keepdims=True) for block in blocks)
+        scale = lax.rsqrt(power / (parts * depth) + EPS)
+        for p, block in enumerate(blocks):
+            gain = gain_ref[lax.rem(part + p, parts)]
+            out_ref[p, rows] = (block * scale * gain).astype(BF16)
+
+    rows_of(0, top_ref)
+    rows_of(half, bottom_ref)
+
+
+def projected(normed_ref, weight_ref):
+    parts, _, depth = normed_ref.shape
+    return sum(
+        jnp.dot(
+            normed_ref[p],
+            weight_ref[p * depth : (p + 1) * depth],
+            preferred_element_type=F32,
+        )
+        for p in range(parts)
+    )
+
+
+def state_in_kernel(place_ref, normed_ref, own_ref, other_ref, out_ref, weight_ref):
+    parts = normed_ref.shape[0]
+    turned = weight_ref.shape[0] // own_ref.shape[2] // parts
+    natural_order(place_ref, own_ref, other_ref, weight_ref, turned)
+    out_ref[...] = projected(normed_ref, weight_ref).astype(BF16)
+
+
+def glu_kernel(place_ref, normed_ref, own_ref, other_ref, out_ref, weight_ref):
+    parts = normed_ref.shape[0]
+    turned = weight_ref.shape[0] // own_ref.shape[2] // parts
+    natural_order(place_ref, own_ref, other_ref, weight_ref, turned)
     width = out_ref.shape[1]
-    both = jnp.dot(normed_ref[...], weight_ref[...], preferred_element_type=F32)
+    both = projected(normed_ref, weight_ref)
     value = both[:, :width].astype(BF16).astype(F32)
     gate = both[:, width:].astype(BF16).astype(F32)
     out_ref[...] = (value * jax.nn.sigmoid(gate)).astype(BF16)
+
+
+def squared(re, im):
+    return re * re - im * im, 2.0 * re * im
+
+
+def times(a, b):
+    return a[0] * b[0] - a[1] * b[1], a[0] * b[1] + a[1] * b[0]
+
+
+def exact_dot(a, b):
+    return jnp.dot(a, b, preferred_element_type=F32, precision=EXACT)
+
+
+def spread_over(groups, each):
+    row = lax.broadcasted_iota(jnp.int32, (groups, groups * each), 0)
+    col = lax.broadcasted_iota(jnp.int32, (groups, groups * each), 1) // each
+    return (row == col).astype(F32)
+
+
+def write_diagonal(out_ref, at, blocks, groups):
+    rows, cols = blocks.shape
+    pair = jnp.concatenate([blocks, blocks], axis=1)
+    row_group = lax.broadcasted_iota(jnp.int32, pair.shape, 0) // (rows // groups)
+    col_group = lax.broadcasted_iota(jnp.int32, pair.shape, 1) // cols
+    for k in range(groups // 2):
+        mine = row_group == col_group + 2 * k
+        out_ref[:, at + 2 * k * cols : at + 2 * (k + 1) * cols] = jnp.where(mine, pair, 0.0).astype(BF16)
+
+
+def table_kernel(
+    shift_ref,
+    base_ref,
+    cos_ref,
+    sin_ref,
+    start_cos_ref,
+    start_sin_ref,
+    b_re_ref,
+    b_im_ref,
+    c_re_ref,
+    c_im_ref,
+    grow_ref,
+    shrink_ref,
+    into_ref,
+    out_ref,
+    hop_re_ref,
+    hop_im_ref,
+    power_ref,
+    total_ref,
+):
+    groups, count = shift_ref.shape
+    lanes = base_ref.shape[1]
+    width = grow_ref.shape[1]
+    chunks = count // CHUNK
+    base = base_ref[...]
+    row = lax.broadcasted_iota(jnp.int32, (count, count), 0)
+    col = lax.broadcasted_iota(jnp.int32, (count, count), 1)
+    earlier = row >= col
+    inside = earlier & (row // CHUNK == col // CHUNK)
+
+    def run(which):
+        return lax.dot_general(
+            which.astype(F32),
+            shift_ref[...],
+            (((1,), (1,)), ((), ())),
+            precision=EXACT,
+            preferred_element_type=F32,
+        )
+
+    partial, whole = run(inside), run(earlier)
+    narrow = exact_dot(partial, spread_over(groups, width // groups))
+    grow_ref[...] = jnp.exp(narrow)
+    shrink_ref[...] = jnp.exp(-narrow)
+    spread = spread_over(groups, lanes // groups)
+    wide = exact_dot(whole, spread)
+    wide_last = wide[count - 1 :]
+    for k in range(lanes // 128):
+        total_ref[k : k + 1, :] = wide_last[:, k * 128 : (k + 1) * 128]
+    sums = jnp.concatenate([partial[(c + 1) * CHUNK - 1 : (c + 1) * CHUNK] for c in range(chunks)])
+    near = exact_dot(sums, spread)
+    index = lax.broadcasted_iota(jnp.int32, (chunks, lanes), 0)
+    size = jnp.exp(CHUNK * base + near)
+    turn = (start_cos_ref[1:2], start_sin_ref[1:2])
+    hop_re_ref[0], hop_im_ref[0] = size * turn[0], size * turn[1]
+    distance, level = 1, 1
+    while distance < chunks:
+        size = jnp.where(index >= distance, jnp.exp(distance * CHUNK * base + near), 0.0)
+        turn = (start_cos_ref[distance : distance + 1], start_sin_ref[distance : distance + 1])
+        hop_re_ref[level], hop_im_ref[level] = size * turn[0], size * turn[1]
+        near = near + jnp.where(index >= distance, pltpu.roll(near, distance, 0), 0.0)
+        distance, level = distance * 2, level + 1
+    counts = lax.broadcasted_iota(jnp.int32, (CHUNK, 1), 0).astype(F32)
+    inner = (cos_ref[...], sin_ref[...])
+    for c in range(chunks):
+        at = slice(c * CHUNK, (c + 1) * CHUNK)
+        size = jnp.exp((counts + (c * CHUNK + 1)) * base + wide[at])
+        turn = times((start_cos_ref[c : c + 1], start_sin_ref[c : c + 1]), inner)
+        power_ref[at, :lanes] = (size * turn[0]).astype(BF16)
+        power_ref[at, lanes:] = (size * turn[1]).astype(BF16)
+    write_diagonal(into_ref, 0, b_re_ref[...], groups)
+    write_diagonal(into_ref, lanes, b_im_ref[...], groups)
+    write_diagonal(out_ref, 0, c_re_ref[...], groups)
+    write_diagonal(out_ref, lanes, -c_im_ref[...], groups)
 
 
 def scan_kernel(
@@ -189,27 +336,27 @@
 
 
 def merge_kernel(
-    core_ref,
+    place_ref,
     y_ref,
     power_ref,
     h_re_ref,
     h_im_ref,
-    read_re_ref,
-    read_im_ref,
+    read_ref,
     conv_ref,
     own_ref,
     other_ref,
     out_ref,
     weight_ref,
 ):
-    natural_order(core_ref, own_ref, other_ref, weight_ref)
-    width = y_ref.shape[1]
+    natural_order(place_ref, own_ref, other_ref, weight_ref, 0)
+    lanes = h_re_ref.shape[1]
     h_re, h_im = h_re_ref[...], h_im_ref[...]
-    c_re, c_im = read_re_ref[...], read_im_ref[...]
-    blend = jnp.concatenate(
-        [(c_re * h_re - c_im * h_im).astype(BF16), (-c_re * h_im - c_im * h_re).astype(BF16)], axis=1
-    )
-    total = y_ref[...] + dot_rows(power_ref[...], blend)
+    c_re, c_im = read_ref[:, :lanes].astype(F32), read_ref[:, lanes:].astype(F32)
+    total = (
+        y_ref[...]
+        + dot_rows(power_ref[:, :lanes], (c_re * h_re + c_im * h_im).astype(BF16))
+        + dot_rows(power_ref[:, lanes:], (c_im * h_re - c_re * h_im).astype(BF16))
+    )
     ssm = jax.nn.gelu(total).astype(BF16)
     both = jnp.concatenate([ssm, conv_ref[...]], axis=1)
     out_ref[...] = dot_rows(both, weight_ref[...]).astype(BF16)
@@ -231,29 +378,7 @@
     )
 
 
-def on_diagonal(blocks):
-    groups, rows, cols = blocks.shape
-    tiled = jnp.tile(blocks.reshape(groups * rows, cols), (1, groups))
-    row_group = lax.broadcasted_iota(jnp.int32, tiled.shape, 0) // rows
-    col_group = lax.broadcasted_iota(jnp.int32, tiled.shape, 1) // cols
-    return jnp.where(row_group == col_group, tiled, 0.0)
-
-
-def spread_over(groups, each):
-    row = lax.broadcasted_iota(jnp.int32, (groups, groups * each), 0)
-    col = lax.broadcasted_iota(jnp.int32, (groups, groups * each), 1) // each
-    return (row == col).astype(F32)
-
-
-def squared(re, im):
-    return re * re - im * im, 2.0 * re * im
-
-
-def times(a, b):
-    return a[0] * b[0] - a[1] * b[1], a[0] * b[1] + a[1] * b[0]
-
-
-def tables(eigen_real, eigen_imag, log_step, decay_shift, state_input, readout):
+def tables(eigen_real, eigen_imag, log_step, decay_shift, state_input, readout, width):
     groups, states = eigen_real.shape
     lanes = groups * states
     count = decay_shift.shape[1]
@@ -267,61 +392,53 @@
     grow, shrink = jnp.exp(level), jnp.exp(-level)
     forward = (grow * cosine, grow * sine)
     inverse = (shrink * cosine, -shrink * sine)
-    shift = decay_shift.T
-    lower = jnp.tril(jnp.ones((CHUNK, CHUNK), F32))
-    partial = jnp.einsum(
-        "ls,csg->clg", lower, shift.reshape(chunks, CHUNK, groups), precision=EXACT
-    )
-    sums = partial[:, -1]
-    earlier = jnp.tril(jnp.ones((chunks, chunks), F32), -1)
-    before = jnp.dot(earlier, sums, precision=EXACT)
-    whole = (partial + before[:, None]).reshape(count, groups)
-    partial = partial.reshape(count, groups)
-    spread = spread_over(groups, states)
-    wide = jnp.dot(whole, spread, precision=EXACT)
-    narrow = jnp.dot(partial, spread_over(groups, 16), precision=EXACT)
-    chunk_rot = (jnp.cos(CHUNK * theta), jnp.sin(CHUNK * theta))
-    rots = [chunk_rot]
-    while (1 << len(rots)) <= chunks:
-        rots.append(squared(*rots[-1]))
-    index = jnp.arange(chunks)
-    hops = [(jnp.exp(CHUNK * base + jnp.dot(sums, spread, precision=EXACT)), rots[0])]
-    distance, place = 1, 0
-    while distance < chunks:
-        window = (
-            (index[:, None] >= index[None, :]) & (index[:, None] - index[None, :] < distance)
-        ).astype(F32)
-        near = jnp.dot(jnp.dot(window, sums, precision=EXACT), spread, precision=EXACT)
-        size = jnp.where(index[:, None] >= distance, jnp.exp(distance * CHUNK * base + near), 0.0)
-        hops.append((size, rots[place]))
-        distance, place = distance * 2, place + 1
-    hop_re = jnp.stack([size * rot[0] for size, rot in hops])
-    hop_im = jnp.stack([size * rot[1] for size, rot in hops])
-    starts = index.astype(F32)[:, None] * CHUNK * theta
-    turn = times(
-        (jnp.cos(starts)[:, None], jnp.sin(starts)[:, None]), (cosine[None], sine[None])
-    )
-    counts = jnp.arange(1, count + 1, dtype=F32)[:, None]
-    size = jnp.exp(counts * base + wide)
-    power = jnp.concatenate(
-        [(size * t.reshape(count, lanes)).astype(BF16) for t in turn], axis=1
-    )
+    starts = jnp.arange(chunks).astype(F32)[:, None] * CHUNK * theta
+    start_cos, start_sin = jnp.cos(starts), jnp.sin(starts)
+    whole_turn = (start_cos[chunks // 2], start_sin[chunks // 2])
     b_re, b_im = input_matrix(eigen_real, eigen_imag, step, state_input)
-    into = jnp.concatenate([on_diagonal(b_re), on_diagonal(b_im)], axis=1).astype(BF16)
-    c_re, c_im = on_diagonal(readout[0]), on_diagonal(readout[1])
-    out = jnp.concatenate([c_re, -c_im], axis=1).astype(BF16)
+    rows = (groups * state_input.shape[2], states)
+    levels = 1 + (chunks - 1).bit_length()
     block = min(count, 256)
     at = jnp.arange(block)
     lower_block = (
         (at[:, None] >= at[None, :]) & (at[:, None] // CHUNK == at[None, :] // CHUNK)
     ).astype(BF16)
+    grow, shrink, into, out, hop_re, hop_im, power, total = call(
+        table_kernel,
+        (
+            jax.ShapeDtypeStruct((count, width), F32),
+            jax.ShapeDtypeStruct((count, width), F32),
+            jax.ShapeDtypeStruct((width, 2 * lanes), BF16),
+            jax.ShapeDtypeStruct((width, 2 * lanes), BF16),
+            jax.ShapeDtypeStruct((levels, chunks, lanes), F32),
+            jax.ShapeDtypeStruct((levels, chunks, lanes), F32),
+            jax.ShapeDtypeStruct((count, 2 * lanes), BF16),
+            jax.ShapeDtypeStruct((lanes // 128, 128), F32),
+        ),
+        (
+            decay_shift,
+            base,
+            cosine,
+            sine,
+            start_cos,
+            start_sin,
+            b_re.reshape(rows),
+            b_im.reshape(rows),
+            readout[0].reshape(rows),
+            readout[1].reshape(rows),
+        ),
+        mib=24,
+        flops=20 * count * count * groups,
+        bytes_accessed=8 * count * lanes,
+        transcendentals=count * lanes,
+    )
     device = dict(
         base=base.reshape(-1, 128),
-        turn=tuple(r.reshape(-1, 128) for r in rots[-1]),
-        shift=wide[-1].reshape(-1, 128),
-    )
-    scan = (jnp.exp(narrow), jnp.exp(-narrow), into, out, *forward, *inverse, hop_re, hop_im, lower_block)
-    return scan, power, (c_re.astype(BF16), c_im.astype(BF16)), device, count
+        turn=squared(*(r.reshape(-1, 128) for r in whole_turn)),
+        shift=total,
+    )
+    scan = (grow, shrink, into, out, *forward, *inverse, hop_re, hop_im, lower_block)
+    return scan, power, out, device
 
 
 def pulled(packed, rows):
@@ -414,35 +531,44 @@
     merge_state,
     merge_conv,
 ):
-    core = lax.axis_index("c").reshape(1).astype(jnp.int32)
+    place = jnp.stack([lax.axis_index("c"), lax.axis_index("x"), lax.axis_index("tp")]).astype(jnp.int32)
     parts = lax.axis_size("tp")
-    blocks = copies(tokens, "tp")
-    count = tokens.shape[0]
+    count, depth_part = tokens.shape
+    depth = depth_part * parts
+    half = count // 2
     width = proj_state.shape[1]
+    ahead = from_ahead(tokens, "tp", 1)
+    behind = from_ahead(tokens, "tp", -1)
     in_z = along_z(proj_state)
     vg_z = along_z(jnp.concatenate([proj_value, proj_gate], axis=1))
     merge_z = along_z(jnp.concatenate([merge_state.T, merge_conv.T], axis=1))
+    top = from_ahead(ahead[:half], "tp", 1)
+    bottom = from_ahead(behind[half:], "tp", -1)
     in_x = along_x(in_z)
     vg_x = along_x(vg_z)
     merge_x = along_x(merge_z)
 
-    scan_tables, power, reads, device, _ = tables(
-        eigen_real, eigen_imag, log_step, decay_shift, state_input, readout
-    )
-
-    whole = jnp.moveaxis(blocks, 0, 1).reshape(count, -1)
-    wide = whole.astype(F32)
-    normed = (
-        wide * lax.rsqrt(jnp.mean(wide * wide, axis=1, keepdims=True) + EPS) * norm_gain
-    ).astype(BF16)
-
-    depth = normed.shape[1]
+    scan_tables, power, reads, device = tables(
+        eigen_real, eigen_imag, log_step, decay_shift, state_input, readout, width
+    )
+    normed = call(
+        norm_kernel,
+        jax.ShapeDtypeStruct((parts, count, depth_part), BF16),
+        (tokens, ahead, top, bottom, behind, norm_gain.reshape(parts, 1, depth_part)),
+        scalars=(place,),
+        mib=12,
+        flops=8 * count * depth,
+        bytes_accessed=4 * count * depth,
+        transcendentals=count,
+    )
+
     u_in = call(
         state_in_kernel,
         jax.ShapeDtypeStruct((count, width), BF16),
         (normed, in_x, partner(in_x)),
-        scalars=(core,),
+        scalars=(place,),
         scratch=(pltpu.VMEM((depth, width), BF16),),
+        mib=12,
         flops=2 * count * depth * width,
         bytes_accessed=4 * depth * count,
         transcendentals=0,
@@ -462,6 +588,7 @@
             pltpu.VMEM((chunks, lanes), F32),
             pltpu.VMEM((chunks, lanes), F32),
         ),
+        mib=24,
         flops=12 * count * width * lanes,
         bytes_accessed=8 * count * lanes,
         transcendentals=0,
@@ -472,7 +599,7 @@
         glu_kernel,
         jax.ShapeDtypeStruct((count, width), BF16),
         (normed, vg_x, partner(vg_x)),
-        scalars=(core,),
+        scalars=(place,),
         scratch=(pltpu.VMEM((depth, 2 * width), BF16),),
         flops=4 * count * depth * width,
         bytes_accessed=4 * depth * count,
@@ -488,12 +615,12 @@
             power,
             h_re.reshape(1, -1),
             h_im.reshape(1, -1),
-            *reads,
+            reads,
             conv_out,
             merge_x,
             partner(merge_x),
         ),
-        scalars=(core,),
+        scalars=(place,),
         scratch=(pltpu.VMEM((depth, 2 * width), BF16),),
         flops=4 * count * depth * width,
         bytes_accessed=4 * depth * count,

time: 270 us -> 225 us (0.83)
  other arithmetic: 32.4 us -> 13 us
  starting transfers between devices: 74.9 us -> 93.9 us
  local copies, waits for them, and re-layouts: 32.4 us -> 20.8 us
  blocking collectives: 38.6 us -> 27.5 us
  matrix products: 11 us -> 0 us
  waiting for transfers between devices: 55 us -> 44.8 us
    ppermute x0 -> x13, starting transfers between devices: none -> 40.8 us  [from_ahead(): lax.ppermute(block, axis, [(i, (i - distance) % count) for i in range(cou...]
    all_to_all x9 -> x6, waiting for transfers between devices: 53.5 us -> 25.9 us  [copies(): lax.all_to_all(jnp.broadcast_to(value[None], (peers, *value.shape)), axis...]
    all_to_all x9 -> x6, starting transfers between devices: 66.8 us -> 44.9 us  [copies(): lax.all_to_all(jnp.broadcast_to(value[None], (peers, *value.shape)), axis...]
    ppermute x0 -> x13, waiting for transfers between devices: none -> 16.9 us  [from_ahead(): lax.ppermute(block, axis, [(i, (i - distance) % count) for i in range(cou...]
    dot_general x12 -> x0, matrix products: 10.7 us -> none  [the longest x1 5.21 us: tables(): wide = jnp.dot(whole, spread, precision=EXACT)]
    all_to_all x1 -> x0, blocking collectives: 8.17 us -> none  [copies(): lax.all_to_all(jnp.broadcast_to(value[None], (peers, *value.shape)), axis...]
    another operation x10 -> x0, local copies, waits for them, and re-layouts: 7.84 us -> none  [on_diagonal(): tiled = jnp.tile(blocks.reshape(groups * rows, cols), (1, groups))]
    unnamed x164 -> x110, local copies, waits for them, and re-layouts: 1.62 us -> 7 us
  transfers between devices with their start and end apart: 13 -> 23, of which waited for: 9 -> 11; matrix products, arithmetic and copies ran while one was open for 24% -> 11% of each run, Pallas kernels for 6% -> 8%
where the time goes in v2:
time: 225 us; the launch traced here: 223 us
  starting transfers between devices  93.9 us (42%)
  waiting for transfers between devices  44.8 us (20%)
  blocking collectives  27.5 us (12%)
  Pallas kernels  21.3 us (9%)
  local copies, waits for them, and re-layouts  20.8 us (9%)
  other arithmetic  13 us (6%)
    all_to_all x6, starting transfers between devices, copies(): lax.all_to_all(jnp.broadcast_to(value[None], (peers, *value.shape)), axis...  44.9 us
    ppermute x13, starting transfers between devices, from_ahead(): lax.ppermute(block, axis, [(i, (i - distance) % count) for i in range(cou...  40.8 us
    all_to_all x1, blocking collectives, per_device(): lax.all_to_all(product.reshape(parts, count // parts, depth), 'tp', split...  27.5 us
    all_to_all x6, waiting for transfers between devices, copies(): lax.all_to_all(jnp.broadcast_to(value[None], (peers, *value.shape)), axis...  25.9 us
    pallas_call x6, Pallas kernels, call(): pl.pallas_call(body, compiler_params=pltpu.CompilerParams(vmem_limit_byte...  21.3 us
    ppermute x13, waiting for transfers between devices, from_ahead(): lax.ppermute(block, axis, [(i, (i - distance) % count) for i in range(cou...  16.9 us
    unnamed x110, local copies, waits for them, and re-layouts  7 us
    ppermute x3, starting transfers between devices, partner(): return lax.ppermute(block, 'c', [(0, 1), (1, 0)])  5.76 us
  transfers between devices with their start and end apart: 23, of which 11 were waited for; matrix products, arithmetic and copies ran while one was open for 11% of the time, Pallas kernels for 8%

profile of v2, /device:TPU:6, one launch (start us, length us, event | category | flops | bytes accessed | tf_op | source)
XLA Modules:
  0.0 222.6 jit_solution(11776206106259198200)
XLA Ops:
  0.0 4.9 %collective-permute-start = (bf16[512,512]{1,0:T(8,128)(2,1)}, bf16[512,512]{1,0:T(8,128)(2,1)S(1)}, u32[]{:S(2)}, u32[]{:S(2)}) collective-permute-start(bf16[512,512]{1,0:T(8,128)(2,1)} %own_ref.1), channel_id=1, source_target_pairs={{0,3},{1,0},{2,1},{3,2},{4,7},{5,4},{6,5},{7,6},{8,11},{9,8},{10,9... | collective-permute-start | bytes 1572872 | tf_op jit(solution)/shard_map/ppermute | solution.py:41
  4.9 1.9 collective-permute-start.2
  6.9 1.4 broadcast_in_dim.18
  8.2 15.3 %all-to-all-start = ((bf16[16,16,256]{2,1,0:T(8,128)(2,1)}), bf16[16,16,256]{2,1,0:T(8,128)(2,1)S(1)}, u32[]{:S(2)}, u32[]{:S(2)}) async-start(bf16[16,16,256]{2,1,0:T(8,128)(2,1)} %broadcast_in_dim.18), calls=%async_computation | async-start | bytes 262144 | tf_op jit(solution)/shard_map/all_to_all | solution.py:21
  24.2 1.0 fusion.66
  25.9 0.8 broadcast_multiply_fusion
  26.9 1.0 fusion.65
  27.9 1.3 fusion.37
  29.2 8.7 %all-to-all-done = bf16[16,16,256]{2,1,0:T(8,128)(2,1)S(1)} async-done(((bf16[16,16,256]{2,1,0:T(8,128)(2,1)}), bf16[16,16,256]{2,1,0:T(8,128)(2,1)S(1)}, u32[]{:S(2)}, u32[]{:S(2)}) %all-to-all-start) | async-done | bytes 131104 | tf_op jit(solution)/shard_map/all_to_all | solution.py:21
  37.9 0.7 broadcast_in_dim.24
  38.7 4.2 %all-to-all-start.3 = ((bf16[16,16,512]{2,1,0:T(8,128)(2,1)}), bf16[16,16,512]{2,1,0:T(8,128)(2,1)}, u32[]{:S(2)}, u32[]{:S(2)}) async-start(bf16[16,16,512]{2,1,0:T(8,128)(2,1)} %broadcast_in_dim.24), calls=%async_computation.3 | async-start | bytes 524288 | tf_op jit(solution)/shard_map/all_to_all | solution.py:21
  42.9 2.4 %collective-permute-start.6 = (bf16[16,16,256]{2,1,0:T(8,128)(2,1)S(1)}, bf16[16,16,256]{2,1,0:T(8,128)(2,1)S(1)}, u32[]{:S(2)}, u32[]{:S(2)}) collective-permute-start(bf16[16,16,256]{2,1,0:T(8,128)(2,1)S(1)} %all-to-all-done), channel_id=1, source_target_pairs={{0,8},{8,16},{16,24},{24,0},{1,9},{9,17},{17,25},{25,1},{2,10},{10... | collective-permute-start | bytes 393224 | tf_op jit(solution)/shard_map/ppermute | solution.py:41
  45.3 4.3 %collective-permute-start.5 = (bf16[16,16,256]{2,1,0:T(8,128)(2,1)S(1)}, bf16[16,16,256]{2,1,0:T(8,128)(2,1)S(1)}, u32[]{:S(2)}, u32[]{:S(2)}) collective-permute-start(bf16[16,16,256]{2,1,0:T(8,128)(2,1)S(1)} %all-to-all-done), channel_id=1, source_target_pairs={{0,16},{8,24},{16,0},{24,8},{1,17},{9,25},{17,1},{25,9},{2,18},{10... | collective-permute-start | bytes 393224 | tf_op jit(solution)/shard_map/ppermute | solution.py:41
  49.6 1.9 collective-permute-start.4
  51.9 2.3 %collective-permute-done.5 = bf16[16,16,256]{2,1,0:T(8,128)(2,1)S(1)} collective-permute-done((bf16[16,16,256]{2,1,0:T(8,128)(2,1)S(1)}, bf16[16,16,256]{2,1,0:T(8,128)(2,1)S(1)}, u32[]{:S(2)}, u32[]{:S(2)}) %collective-permute-start.5) | collective-permute-done | bytes 131104 | tf_op jit(solution)/shard_map/ppermute | solution.py:41
  54.2 3.5 %collective-permute-done.4 = bf16[16,16,256]{2,1,0:T(8,128)(2,1)S(1)} collective-permute-done((bf16[16,16,256]{2,1,0:T(8,128)(2,1)S(1)}, bf16[16,16,256]{2,1,0:T(8,128)(2,1)S(1)}, u32[]{:S(2)}, u32[]{:S(2)}) %collective-permute-start.4) | collective-permute-done | bytes 131104 | tf_op jit(solution)/shard_map/ppermute | solution.py:41
  57.8 1.9 collective-permute-start.7
  60.4 5.0 %collective-permute-start.1 = (bf16[256,512]{1,0:T(8,128)(2,1)S(1)}, bf16[256,512]{1,0:T(8,128)(2,1)S(1)}, u32[]{:S(2)}, u32[]{:S(2)}) collective-permute-start(bf16[256,512]{1,0:T(8,128)(2,1)S(1)} %slice.1050), channel_id=1, source_target_pairs={{0,3},{1,0},{2,1},{3,2},{4,7},{5,4},{6,5},{7,6},{8,11},{9,8},{10,9... | collective-permute-start | bytes 786440 | tf_op jit(solution)/shard_map/ppermute | solution.py:41
  65.4 0.8 slice.1051
  66.2 1.9 collective-permute-start.3
  69.0 4.8 %shard_map.165 = (f32[512,256]{1,0:T(8,128)S(1)}, f32[512,256]{1,0:T(8,128)S(1)}, bf16[256,2048]{1,0:T(8,128)(2,1)S(1)}, bf16[256,2048]{1,0:T(8,128)(2,1)S(1)}, ...) custom-call(f32[16,512]{1,0:T(8,128)S(1)} %copy-done.17, ...), custom_call_target="tpu_custom_call" | custom-call | flops 83886080 | bytes 4194304 | tf_op jit(solution)/shard_map/pallas_call | solution.py:58
  73.9 4.0 %collective-permute-done.3.bottom_ref = bf16[256,512]{1,0:T(8,128)(2,1)S(1)} collective-permute-done((bf16[256,512]{1,0:T(8,128)(2,1)}, bf16[256,512]{1,0:T(8,128)(2,1)S(1)}, u32[]{:S(2)}, u32[]{:S(2)}) %collective-permute-start.3) | collective-permute-done | bytes 262176 | tf_op jit(solution)/shard_map/ppermute | solution.py:41
  78.6 1.0 copy-done.3
  79.7 1.0 copy-done.6
  80.7 0.9 copy-done.10
  81.7 1.3 shard_map.163.normed_ref
  83.1 2.8 %shard_map.164.u_ref = bf16[512,256]{1,0:T(8,128)(2,1)S(1)} custom-call(s32[3]{0:T(128)S(1)} %pad_add_fusion.place_ref, bf16[4,512,512]{2,1,0:T(8,128)(2,1)S(1)} %shard_map.163.normed_ref, bf16[4,16,16,256]{3,2,1,0:T(8,128)(2,1)S(1)} %pad_maximum_fusion.2.own_ref, bf16[4,16,16,256]{3,2,1,0:T(8,128)(2,1)} %collective-permute-done.7.other_ref), custom_call_target="tpu_custom_call" | custom-call | flops 536870912 | bytes 4194304 | tf_op jit(solution)/shard_map/pallas_call | solution.py:58
  86.0 4.1 %shard_map.166 = (f32[512,256]{1,0:T(8,128)S(1)}, f32[16,128]{1,0:T(8,128)S(1)}) custom-call(bf16[512,256]{1,0:T(8,128)(2,1)S(1)} %shard_map.164.u_ref, f32[512,256]{1,0:T(8,128)S(1)} %get-tuple-element.15.grow_ref, f32[512,256]{1,0:T(8,128)S(1)} %get-tuple-element.16.shrink_ref, bf16[256,2048]{1,0:T(8,128)(2,1)S(1)} %get-tuple-element.17.in_ref, ...), custom_call_target="tpu_custom_call" | custom-call | flops 1610612736 | bytes 4194304 | tf_op jit(solution)/shard_map/pallas_call | solution.py:58
  90.2 0.8 copy-done.7
  91.6 4.7 %all-to-all-start.1 = ((f32[8,24,128]{2,1,0:T(8,128)}), f32[8,24,128]{2,1,0:T(8,128)S(1)}, u32[]{:S(2)}, u32[]{:S(2)}) async-start(f32[8,24,128]{2,1,0:T(8,128)} %broadcast_in_dim.19), calls=%async_computation.1 | async-start | bytes 196608 | tf_op jit(solution)/shard_map/all_to_all | solution.py:21
  96.3 3.7 %all-to-all-done.1 = f32[8,24,128]{2,1,0:T(8,128)S(1)} async-done(((f32[8,24,128]{2,1,0:T(8,128)}), f32[8,24,128]{2,1,0:T(8,128)S(1)}, u32[]{:S(2)}, u32[]{:S(2)}) %all-to-all-start.1) | async-done | bytes 98336 | tf_op jit(solution)/shard_map/all_to_all | solution.py:21
  100.0 0.7 broadcast_in_dim.26
  100.7 11.9 %all-to-all-start.5 = ((bf16[16,16,512]{2,1,0:T(8,128)(2,1)}), bf16[16,16,512]{2,1,0:T(8,128)(2,1)S(1)}, u32[]{:S(2)}, u32[]{:S(2)}) async-start(bf16[16,16,512]{2,1,0:T(8,128)(2,1)} %broadcast_in_dim.26), calls=%async_computation.5 | async-start | bytes 524288 | tf_op jit(solution)/shard_map/all_to_all | solution.py:21
  112.7 0.8 multiply_subtract_fusion.3
  113.4 4.0 %collective-permute-start.10 = (bf16[16,16,512]{2,1,0:T(8,128)(2,1)}, bf16[16,16,512]{2,1,0:T(8,128)(2,1)S(1)}, u32[]{:S(2)}, u32[]{:S(2)}) collective-permute-start(bf16[16,16,512]{2,1,0:T(8,128)(2,1)} %all-to-all-done.3), channel_id=1, source_target_pairs={{0,8},{8,16},{16,24},{24,0},{1,9},{9,17},{17,25},{25,1},{2,10},{10... | collective-permute-start | bytes 786440 | tf_op jit(solution)/shard_map/ppermute | solution.py:41
  117.4 2.2 collective-permute-start.9
  119.6 3.0 %collective-permute-start.8 = (bf16[16,16,512]{2,1,0:T(8,128)(2,1)}, bf16[16,16,512]{2,1,0:T(8,128)(2,1)S(1)}, u32[]{:S(2)}, u32[]{:S(2)}) collective-permute-start(bf16[16,16,512]{2,1,0:T(8,128)(2,1)} %all-to-all-done.3), channel_id=1, source_target_pairs={{0,24},{8,0},{16,8},{24,16},{1,25},{9,1},{17,9},{25,17},{2,26},{10... | collective-permute-start | bytes 786440 | tf_op jit(solution)/shard_map/ppermute | solution.py:41
  122.8 8.3 %all-to-all-done.5 = bf16[16,16,512]{2,1,0:T(8,128)(2,1)S(1)} async-done(((bf16[16,16,512]{2,1,0:T(8,128)(2,1)}), bf16[16,16,512]{2,1,0:T(8,128)(2,1)S(1)}, u32[]{:S(2)}, u32[]{:S(2)}) %all-to-all-start.5) | async-done | bytes 262176 | tf_op jit(solution)/shard_map/all_to_all | solution.py:21
  131.8 5.6 %all-to-all-start.2 = ((f32[16,24,128]{2,1,0:T(8,128)}), f32[16,24,128]{2,1,0:T(8,128)}, u32[]{:S(2)}, u32[]{:S(2)}) async-start(f32[16,24,128]{2,1,0:T(8,128)} %broadcast_in_dim.23), calls=%async_computation.2 | async-start | bytes 393216 | tf_op jit(solution)/shard_map/all_to_all | solution.py:21
  137.4 1.6 fusion.73
  139.2 4.0 %collective-permute-start.15 = (bf16[16,16,512]{2,1,0:T(8,128)(2,1)S(1)}, bf16[16,16,512]{2,1,0:T(8,128)(2,1)S(1)}, u32[]{:S(2)}, u32[]{:S(2)}) collective-permute-start(bf16[16,16,512]{2,1,0:T(8,128)(2,1)S(1)} %all-to-all-done.5), channel_id=1, source_target_pairs={{0,8},{8,16},{16,24},{24,0},{1,9},{9,17},{17,25},{25,1},{2,10},{10... | collective-permute-start | bytes 786440 | tf_op jit(solution)/shard_map/ppermute | solution.py:41
  143.2 2.3 %collective-permute-start.14 = (bf16[16,16,512]{2,1,0:T(8,128)(2,1)S(1)}, bf16[16,16,512]{2,1,0:T(8,128)(2,1)S(1)}, u32[]{:S(2)}, u32[]{:S(2)}) collective-permute-start(bf16[16,16,512]{2,1,0:T(8,128)(2,1)S(1)} %all-to-all-done.5), channel_id=1, source_target_pairs={{0,16},{8,24},{16,0},{24,8},{1,17},{9,25},{17,1},{25,9},{2,18},{10... | collective-permute-start | bytes 786440 | tf_op jit(solution)/shard_map/ppermute | solution.py:41
  145.5 2.9 %collective-permute-start.13 = (bf16[16,16,512]{2,1,0:T(8,128)(2,1)S(1)}, bf16[16,16,512]{2,1,0:T(8,128)(2,1)S(1)}, u32[]{:S(2)}, u32[]{:S(2)}) collective-permute-start(bf16[16,16,512]{2,1,0:T(8,128)(2,1)S(1)} %all-to-all-done.5), channel_id=1, source_target_pairs={{0,24},{8,0},{16,8},{24,16},{1,25},{9,1},{17,9},{25,17},{2,26},{10... | collective-permute-start | bytes 786440 | tf_op jit(solution)/shard_map/ppermute | solution.py:41
  148.5 2.1 pad_maximum_fusion.own_ref
  150.5 1.9 collective-permute-start.11
  152.5 1.5 collective-permute-done.15
  154.0 1.8 collective-permute-done.14
  155.8 3.8 %collective-permute-done.13 = bf16[16,16,512]{2,1,0:T(8,128)(2,1)S(1)} collective-permute-done((bf16[16,16,512]{2,1,0:T(8,128)(2,1)S(1)}, bf16[16,16,512]{2,1,0:T(8,128)(2,1)S(1)}, u32[]{:S(2)}, u32[]{:S(2)}) %collective-permute-start.13) | collective-permute-done | bytes 262176 | tf_op jit(solution)/shard_map/ppermute | solution.py:41
  159.7 1.9 collective-permute-start.16
  161.7 0.7 fusion.69
  162.4 0.8 fusion.67
  163.2 0.8 fusion.68
  164.3 3.8 %shard_map.167 = bf16[512,256]{1,0:T(8,128)(2,1)S(1)} custom-call(s32[3]{0:T(128)S(1)} %pad_add_fusion.place_ref, bf16[4,512,512]{2,1,0:T(8,128)(2,1)S(1)} %shard_map.163.normed_ref, bf16[4,16,16,512]{3,2,1,0:T(8,128)(2,1)} %pad_maximum_fusion.own_ref, bf16[4,16,16,512]{3,2,1,0:T(8,128)(2,1)} %collective-permute-done.11.other_ref), custom_call_target="tpu_custom_call" | custom-call | flops 1073741824 | bytes 4194304 | tf_op jit(solution)/shard_map/pallas_call | solution.py:58
  168.1 2.4 %collective-permute-start.12 = (bf16[32,256]{1,0:T(8,128)(2,1)S(1)}, bf16[32,256]{1,0:T(8,128)(2,1)S(1)}, u32[]{:S(2)}, u32[]{:S(2)}) collective-permute-start(bf16[32,256]{1,0:T(8,128)(2,1)S(1)} %slice.1126), channel_id=1, source_target_pairs={{0,4},{4,8},{8,12},{12,16},{16,20},{20,24},{24,28},{28,32},{32,36}... | collective-permute-start | bytes 49160 | tf_op jit(solution)/shard_map/ppermute | solution.py:28
  171.1 2.1 collective-permute-done.12
  173.6 3.0 %fusion.63 = (f32[512]{0:T(512)S(1)}, f32[512]{0:T(512)S(1)}, f32[512,256]{1,0:T(8,128)}) fusion(f32[542,256]{1,0:T(8,128)S(1)} %maximum_convert_fusion, f32[256]{0:T(256)S(1)} %bitcast.540, f32[256]{0:T(256)S(1)} %bitcast.541, f32[256]{0:T(256)S(1)} %bitcast.512, f32[256]{0:T(256)S(1)} %bitcast.513, f32[256]{0:T(256)S(1)} %bitcast.514, ...), kind=kLoop, calls=%fused_computation.281 | loop fusion | flops 8387584 | bytes 16813056 | tf_op jit(solution)/shard_map/reduce_sum | solution.py:507
  177.2 3.2 %all-to-all-start.4 = ((f32[4,8,128]{2,1,0:T(8,128)}), f32[4,8,128]{2,1,0:T(8,128)S(1)}, u32[]{:S(2)}, u32[]{:S(2)}) async-start(f32[4,8,128]{2,1,0:T(8,128)} %broadcast_in_dim.25), calls=%async_computation.4 | async-start | bytes 32768 | tf_op jit(solution)/shard_map/all_to_all | solution.py:21
  180.7 5.1 %all-to-all-done.4 = f32[4,8,128]{2,1,0:T(8,128)S(1)} async-done(((f32[4,8,128]{2,1,0:T(8,128)}), f32[4,8,128]{2,1,0:T(8,128)S(1)}, u32[]{:S(2)}, u32[]{:S(2)}) %all-to-all-start.4) | async-done | bytes 16416 | tf_op jit(solution)/shard_map/all_to_all | solution.py:21
  185.8 1.3 multiply_convert_fusion.conv_ref
  187.1 1.2 copy-done.5
  188.3 1.0 copy-done.8
  189.4 4.4 %shard_map.168 = bf16[512,2048]{1,0:T(8,128)(2,1)S(1)} custom-call(s32[3]{0:T(128)S(1)} %pad_add_fusion.place_ref, f32[512,256]{1,0:T(8,128)S(1)} %copy-done.8, bf16[512,2048]{1,0:T(8,128)(2,1)S(1)} %copy-done.1, f32[1,1024]{1,0:T(1,128)S(1)} %fusion.45.h_re_ref, f32[1,1024]{1,0:T(1,128)S(1)} %get-tuple-element.28.h_im_ref, bf16[256,2048]{1,0:T(8,128)(2,1)S(1)} %copy-done.5, ...), custom_call_target="tpu_custom_call" | custom-call | flops 1073741824 | bytes 4194304 | tf_op jit(solution)/shard_map/pallas_call | solution.py:58
  193.8 27.5 %all_to_all.35 = bf16[4,128,2048]{2,1,0:T(8,128)(2,1)S(1)} all-to-all(bf16[4,128,2048]{2,1,0:T(8,128)(2,1)S(1)} %bitcast.393), channel_id=1, replica_groups=mesh['z'=16,'x'=4,'c'=2,'tp'=4] {'tp'}, dimensions={0} | all-to-all | bytes 4194304 | tf_op jit(solution)/shard_map/all_to_all | solution.py:629
  221.3 1.3 reduce_sum.42
  (155 shorter events, 7.8 us)
Async XLA Ops:
  0.0 60.4 %collective-permute-start = (bf16[512,512]{1,0:T(8,128)(2,1)}, bf16[512,512]{1,0:T(8,128)(2,1)S(1)}, u32[]{:S(2)}, u32[]{:S(2)}) collective-permute-start(bf16[512,512]{1,0:T(8,128)(2,1)} %own_ref.1), channel_id=1, source_target_pairs={{0,3},{1,0},{2,1},{3,2},{4,7},{5,4},{6,5},{7,6},{8,11},{9,8},{10,9... | collective-permute-start | bytes 1572872 | tf_op jit(solution)/shard_map/ppermute | solution.py:41
  4.9 60.5 %collective-permute-start.2 = (bf16[512,512]{1,0:T(8,128)(2,1)}, bf16[512,512]{1,0:T(8,128)(2,1)S(1)}, u32[]{:S(2)}, u32[]{:S(2)}) collective-permute-start(bf16[512,512]{1,0:T(8,128)(2,1)} %own_ref.1), channel_id=1, source_target_pairs={{0,1},{1,2},{2,3},{3,0},{4,5},{5,6},{6,7},{7,4},{8,9},{9,10},{10,1... | collective-permute-start | bytes 1572872 | tf_op jit(solution)/shard_map/ppermute | solution.py:41
  8.2 51.5 %copy-start.20 = (f32[31,256]{1,0:T(8,128)S(1)}, f32[31,256]{1,0:T(8,128)}, u32[]{:S(2)}) copy-start(f32[31,256]{1,0:T(8,128)} %param.30) | copy-start | bytes 95236
  8.2 29.7 %all-to-all-start = ((bf16[16,16,256]{2,1,0:T(8,128)(2,1)}), bf16[16,16,256]{2,1,0:T(8,128)(2,1)S(1)}, u32[]{:S(2)}, u32[]{:S(2)}) async-start(bf16[16,16,256]{2,1,0:T(8,128)(2,1)} %broadcast_in_dim.18), calls=%async_computation | async-start | bytes 262144 | tf_op jit(solution)/shard_map/all_to_all | solution.py:21
  27.9 41.0 %copy-start.17 = (f32[16,512]{1,0:T(8,128)S(1)}, f32[16,512]{1,0:T(8,128)}, u32[]{:S(2)}) copy-start(f32[16,512]{1,0:T(8,128)} %shift_ref.1) | copy-start | bytes 98308
  38.7 52.3 %all-to-all-start.3 = ((bf16[16,16,512]{2,1,0:T(8,128)(2,1)}), bf16[16,16,512]{2,1,0:T(8,128)(2,1)}, u32[]{:S(2)}, u32[]{:S(2)}) async-start(bf16[16,16,512]{2,1,0:T(8,128)(2,1)} %broadcast_in_dim.24), calls=%async_computation.3 | async-start | bytes 524288 | tf_op jit(solution)/shard_map/all_to_all | solution.py:21
  42.9 35.8 %copy-start.16 = (f32[2048]{0:T(1024)S(1)}, f32[2048]{0:T(1024)}, u32[]{:S(2)}) copy-start(f32[2048]{0:T(1024)} %param.18) | copy-start | bytes 24580
  42.9 9.0 %collective-permute-start.6 = (bf16[16,16,256]{2,1,0:T(8,128)(2,1)S(1)}, bf16[16,16,256]{2,1,0:T(8,128)(2,1)S(1)}, u32[]{:S(2)}, u32[]{:S(2)}) collective-permute-start(bf16[16,16,256]{2,1,0:T(8,128)(2,1)S(1)} %all-to-all-done), channel_id=1, source_target_pairs={{0,8},{8,16},{16,24},{24,0},{1,9},{9,17},{17,25},{25,1},{2,10},{10... | collective-permute-start | bytes 393224 | tf_op jit(solution)/shard_map/ppermute | solution.py:41
  45.3 8.9 %collective-permute-start.5 = (bf16[16,16,256]{2,1,0:T(8,128)(2,1)S(1)}, bf16[16,16,256]{2,1,0:T(8,128)(2,1)S(1)}, u32[]{:S(2)}, u32[]{:S(2)}) collective-permute-start(bf16[16,16,256]{2,1,0:T(8,128)(2,1)S(1)} %all-to-all-done), channel_id=1, source_target_pairs={{0,16},{8,24},{16,0},{24,8},{1,17},{9,25},{17,1},{25,9},{2,18},{10... | collective-permute-start | bytes 393224 | tf_op jit(solution)/shard_map/ppermute | solution.py:41
  49.6 8.1 %collective-permute-start.4 = (bf16[16,16,256]{2,1,0:T(8,128)(2,1)S(1)}, bf16[16,16,256]{2,1,0:T(8,128)(2,1)S(1)}, u32[]{:S(2)}, u32[]{:S(2)}) collective-permute-start(bf16[16,16,256]{2,1,0:T(8,128)(2,1)S(1)} %all-to-all-done), channel_id=1, source_target_pairs={{0,24},{8,0},{16,8},{24,16},{1,25},{9,1},{17,9},{25,17},{2,26},{10... | collective-permute-start | bytes 393224 | tf_op jit(solution)/shard_map/ppermute | solution.py:41
  51.9 26.0 %copy-start.14 = (f32[16,1024]{1,0:T(8,128)}, f32[16,1024]{1,0:T(8,128)S(1)}, u32[]{:S(2)}) copy-start(f32[16,1024]{1,0:T(8,128)S(1)} %get-tuple-element.162.start_sin_ref) | copy-start | bytes 196612
  51.9 26.0 %copy-start.15 = (f32[16,1024]{1,0:T(8,128)}, f32[16,1024]{1,0:T(8,128)S(1)}, u32[]{:S(2)}) copy-start(f32[16,1024]{1,0:T(8,128)S(1)} %get-tuple-element.163.start_cos_ref) | copy-start | bytes 196612
  57.8 25.3 %collective-permute-start.7 = (bf16[4,16,16,256]{3,2,1,0:T(8,128)(2,1)S(1)}, bf16[4,16,16,256]{3,2,1,0:T(8,128)(2,1)}, u32[]{:S(2)}, u32[]{:S(2)}) collective-permute-start(bf16[4,16,16,256]{3,2,1,0:T(8,128)(2,1)S(1)} %pad_maximum_fusion.2.own_ref), channel_id=1, source_target_pairs={{0,4},{4,0},{1,5},{5,1},{2,6},{6,2},{3,7},{7,3},{8,12},{12,8},{9,1... | collective-permute-start | bytes 1572872 | tf_op jit(solution)/shard_map/ppermute | solution.py:32
  60.4 13.5 %collective-permute-start.1 = (bf16[256,512]{1,0:T(8,128)(2,1)S(1)}, bf16[256,512]{1,0:T(8,128)(2,1)S(1)}, u32[]{:S(2)}, u32[]{:S(2)}) collective-permute-start(bf16[256,512]{1,0:T(8,128)(2,1)S(1)} %slice.1050), channel_id=1, source_target_pairs={{0,3},{1,0},{2,1},{3,2},{4,7},{5,4},{6,5},{7,6},{8,11},{9,8},{10,9... | collective-permute-start | bytes 786440 | tf_op jit(solution)/shard_map/ppermute | solution.py:41
  65.4 12.5 %copy-start.2 = (bf16[512,512]{1,0:T(8,128)(2,1)}, bf16[512,512]{1,0:T(8,128)(2,1)S(1)}, u32[]{:S(2)}) copy-start(bf16[512,512]{1,0:T(8,128)(2,1)S(1)} %collective-permute-done.2.behind_ref) | copy-start | bytes 1572868
  66.2 11.7 %collective-permute-start.3 = (bf16[256,512]{1,0:T(8,128)(2,1)}, bf16[256,512]{1,0:T(8,128)(2,1)S(1)}, u32[]{:S(2)}, u32[]{:S(2)}) collective-permute-start(bf16[256,512]{1,0:T(8,128)(2,1)} %slice.1051), channel_id=1, source_target_pairs={{0,1},{1,2},{2,3},{3,0},{4,5},{5,6},{6,7},{7,4},{8,9},{9,10},{10,1... | collective-permute-start | bytes 786440 | tf_op jit(solution)/shard_map/ppermute | solution.py:41
  73.8 12.1 %copy-start.4 = (bf16[256,2048]{1,0:T(8,128)(2,1)}, bf16[256,2048]{1,0:T(8,128)(2,1)S(1)}, u32[]{:S(2)}) copy-start(bf16[256,2048]{1,0:T(8,128)(2,1)S(1)} %get-tuple-element.18.out_mat_ref.read_ref) | copy-start | bytes 3145732
  86.0 10.3 %copy-start.22 = (bf16[256,16]{0,1:T(8,128)(2,1)S(1)}, bf16[256,16]{0,1:T(8,128)(2,1)}, u32[]{:S(2)}) copy-start(bf16[256,16]{0,1:T(8,128)(2,1)} %param.33) | copy-start | bytes 24580
  86.0 10.3 %copy-start.23 = (bf16[256,16]{0,1:T(8,128)(2,1)S(1)}, bf16[256,16]{0,1:T(8,128)(2,1)}, u32[]{:S(2)}) copy-start(bf16[256,16]{0,1:T(8,128)(2,1)} %param.32) | copy-start | bytes 24580
  86.0 26.7 %copy-start.21 = (f32[2,16,64]{2,1,0:T(8,128)S(1)}, f32[2,16,64]{2,1,0:T(8,128)}, u32[]{:S(2)}) copy-start(f32[2,16,64]{2,1,0:T(8,128)} %param.29) | copy-start | bytes 24580
  86.0 36.7 %copy-start.19 = (f32[8,128]{1,0:T(8,128)S(1)}, f32[8,128]{1,0:T(8,128)}, u32[]{:S(2)}) copy-start(f32[8,128]{1,0:T(8,128)} %mul.1744) | copy-start | bytes 12292
  91.6 8.4 %all-to-all-start.1 = ((f32[8,24,128]{2,1,0:T(8,128)}), f32[8,24,128]{2,1,0:T(8,128)S(1)}, u32[]{:S(2)}, u32[]{:S(2)}) async-start(f32[8,24,128]{2,1,0:T(8,128)} %broadcast_in_dim.19), calls=%async_computation.1 | async-start | bytes 196608 | tf_op jit(solution)/shard_map/all_to_all | solution.py:21
  100.7 30.3 %all-to-all-start.5 = ((bf16[16,16,512]{2,1,0:T(8,128)(2,1)}), bf16[16,16,512]{2,1,0:T(8,128)(2,1)S(1)}, u32[]{:S(2)}, u32[]{:S(2)}) async-start(bf16[16,16,512]{2,1,0:T(8,128)(2,1)} %broadcast_in_dim.26), calls=%async_computation.5 | async-start | bytes 524288 | tf_op jit(solution)/shard_map/all_to_all | solution.py:21
  113.4 32.1 %collective-permute-start.10 = (bf16[16,16,512]{2,1,0:T(8,128)(2,1)}, bf16[16,16,512]{2,1,0:T(8,128)(2,1)S(1)}, u32[]{:S(2)}, u32[]{:S(2)}) collective-permute-start(bf16[16,16,512]{2,1,0:T(8,128)(2,1)} %all-to-all-done.3), channel_id=1, source_target_pairs={{0,8},{8,16},{16,24},{24,0},{1,9},{9,17},{17,25},{25,1},{2,10},{10... | collective-permute-start | bytes 786440 | tf_op jit(solution)/shard_map/ppermute | solution.py:41
  117.4 31.0 %collective-permute-start.9 = (bf16[16,16,512]{2,1,0:T(8,128)(2,1)}, bf16[16,16,512]{2,1,0:T(8,128)(2,1)S(1)}, u32[]{:S(2)}, u32[]{:S(2)}) collective-permute-start(bf16[16,16,512]{2,1,0:T(8,128)(2,1)} %all-to-all-done.3), channel_id=1, source_target_pairs={{0,16},{8,24},{16,0},{24,8},{1,17},{9,25},{17,1},{25,9},{2,18},{10... | collective-permute-start | bytes 786440 | tf_op jit(solution)/shard_map/ppermute | solution.py:41
  119.6 28.8 %collective-permute-start.8 = (bf16[16,16,512]{2,1,0:T(8,128)(2,1)}, bf16[16,16,512]{2,1,0:T(8,128)(2,1)S(1)}, u32[]{:S(2)}, u32[]{:S(2)}) collective-permute-start(bf16[16,16,512]{2,1,0:T(8,128)(2,1)} %all-to-all-done.3), channel_id=1, source_target_pairs={{0,24},{8,0},{16,8},{24,16},{1,25},{9,1},{17,9},{25,17},{2,26},{10... | collective-permute-start | bytes 786440 | tf_op jit(solution)/shard_map/ppermute | solution.py:41
  131.8 29.9 %all-to-all-start.2 = ((f32[16,24,128]{2,1,0:T(8,128)}), f32[16,24,128]{2,1,0:T(8,128)}, u32[]{:S(2)}, u32[]{:S(2)}) async-start(f32[16,24,128]{2,1,0:T(8,128)} %broadcast_in_dim.23), calls=%async_computation.2 | async-start | bytes 393216 | tf_op jit(solution)/shard_map/all_to_all | solution.py:21
  139.2 14.8 %collective-permute-start.15 = (bf16[16,16,512]{2,1,0:T(8,128)(2,1)S(1)}, bf16[16,16,512]{2,1,0:T(8,128)(2,1)S(1)}, u32[]{:S(2)}, u32[]{:S(2)}) collective-permute-start(bf16[16,16,512]{2,1,0:T(8,128)(2,1)S(1)} %all-to-all-done.5), channel_id=1, source_target_pairs={{0,8},{8,16},{16,24},{24,0},{1,9},{9,17},{17,25},{25,1},{2,10},{10... | collective-permute-start | bytes 786440 | tf_op jit(solution)/shard_map/ppermute | solution.py:41
  143.2 12.6 %collective-permute-start.14 = (bf16[16,16,512]{2,1,0:T(8,128)(2,1)S(1)}, bf16[16,16,512]{2,1,0:T(8,128)(2,1)S(1)}, u32[]{:S(2)}, u32[]{:S(2)}) collective-permute-start(bf16[16,16,512]{2,1,0:T(8,128)(2,1)S(1)} %all-to-all-done.5), channel_id=1, source_target_pairs={{0,16},{8,24},{16,0},{24,8},{1,17},{9,25},{17,1},{25,9},{2,18},{10... | collective-permute-start | bytes 786440 | tf_op jit(solution)/shard_map/ppermute | solution.py:41
  145.5 14.1 %collective-permute-start.13 = (bf16[16,16,512]{2,1,0:T(8,128)(2,1)S(1)}, bf16[16,16,512]{2,1,0:T(8,128)(2,1)S(1)}, u32[]{:S(2)}, u32[]{:S(2)}) collective-permute-start(bf16[16,16,512]{2,1,0:T(8,128)(2,1)S(1)} %all-to-all-done.5), channel_id=1, source_target_pairs={{0,24},{8,0},{16,8},{24,16},{1,25},{9,1},{17,9},{25,17},{2,26},{10... | collective-permute-start | bytes 786440 | tf_op jit(solution)/shard_map/ppermute | solution.py:41
  150.5 13.8 %collective-permute-start.11 = (bf16[4,16,16,512]{3,2,1,0:T(8,128)(2,1)}, bf16[4,16,16,512]{3,2,1,0:T(8,128)(2,1)}, u32[]{:S(2)}, u32[]{:S(2)}) collective-permute-start(bf16[4,16,16,512]{3,2,1,0:T(8,128)(2,1)} %pad_maximum_fusion.own_ref), channel_id=1, source_target_pairs={{0,4},{4,0},{1,5},{5,1},{2,6},{6,2},{3,7},{7,3},{8,12},{12,8},{9,1... | collective-permute-start | bytes 3145736 | tf_op jit(solution)/shard_map/ppermute | solution.py:32
  159.7 27.3 %collective-permute-start.16 = (bf16[4,16,16,512]{3,2,1,0:T(8,128)(2,1)S(1)}, bf16[4,16,16,512]{3,2,1,0:T(8,128)(2,1)}, u32[]{:S(2)}, u32[]{:S(2)}) collective-permute-start(bf16[4,16,16,512]{3,2,1,0:T(8,128)(2,1)S(1)} %pad_maximum_fusion.1.own_ref), channel_id=1, source_target_pairs={{0,4},{4,0},{1,5},{5,1},{2,6},{6,2},{3,7},{7,3},{8,12},{12,8},{9,1... | collective-permute-start | bytes 3145736 | tf_op jit(solution)/shard_map/ppermute | solution.py:32
  164.0 9.3 %copy-start.24 = (f32[1,256]{1,0:T(1,128)S(1)}, f32[1,256]{1,0:T(1,128)}, u32[]{:S(2)}) copy-start(f32[1,256]{1,0:T(1,128)} %get-tuple-element.116) | copy-start | bytes 3076
  164.0 9.3 %copy-start.25 = (f32[1,256]{1,0:T(1,128)S(1)}, f32[1,256]{1,0:T(1,128)}, u32[]{:S(2)}) copy-start(f32[1,256]{1,0:T(1,128)} %get-tuple-element.117) | copy-start | bytes 3076
  164.0 9.3 %copy-start.26 = (f32[1,256]{1,0:T(1,128)S(1)}, f32[1,256]{1,0:T(1,128)}, u32[]{:S(2)}) copy-start(f32[1,256]{1,0:T(1,128)} %get-tuple-element.118) | copy-start | bytes 3076
  164.0 9.3 %copy-start.27 = (f32[1,256]{1,0:T(1,128)S(1)}, f32[1,256]{1,0:T(1,128)}, u32[]{:S(2)}) copy-start(f32[1,256]{1,0:T(1,128)} %get-tuple-element.119) | copy-start | bytes 3076
  164.0 9.3 %copy-start.28 = (f32[1,256]{1,0:T(1,128)S(1)}, f32[1,256]{1,0:T(1,128)}, u32[]{:S(2)}) copy-start(f32[1,256]{1,0:T(1,128)} %get-tuple-element.120) | copy-start | bytes 3076
  164.0 9.3 %copy-start.29 = (f32[1,256]{1,0:T(1,128)S(1)}, f32[1,256]{1,0:T(1,128)}, u32[]{:S(2)}) copy-start(f32[1,256]{1,0:T(1,128)} %get-tuple-element.121) | copy-start | bytes 3076
  164.0 9.3 %copy-start.30 = (f32[1,256]{1,0:T(1,128)S(1)}, f32[1,256]{1,0:T(1,128)}, u32[]{:S(2)}) copy-start(f32[1,256]{1,0:T(1,128)} %get-tuple-element.122) | copy-start | bytes 3076
  164.1 9.3 %copy-start.31 = (f32[1,256]{1,0:T(1,128)S(1)}, f32[1,256]{1,0:T(1,128)}, u32[]{:S(2)}) copy-start(f32[1,256]{1,0:T(1,128)} %get-tuple-element.123) | copy-start | bytes 3076
  164.1 9.3 %copy-start.32 = (f32[1,256]{1,0:T(1,128)S(1)}, f32[1,256]{1,0:T(1,128)}, u32[]{:S(2)}) copy-start(f32[1,256]{1,0:T(1,128)} %get-tuple-element.124) | copy-start | bytes 3076
  164.1 9.3 %copy-start.33 = (f32[1,256]{1,0:T(1,128)S(1)}, f32[1,256]{1,0:T(1,128)}, u32[]{:S(2)}) copy-start(f32[1,256]{1,0:T(1,128)} %get-tuple-element.125) | copy-start | bytes 3076
  164.1 9.3 %copy-start.34 = (f32[1,256]{1,0:T(1,128)S(1)}, f32[1,256]{1,0:T(1,128)}, u32[]{:S(2)}) copy-start(f32[1,256]{1,0:T(1,128)} %get-tuple-element.126) | copy-start | bytes 3076
  164.1 9.3 %copy-start.35 = (f32[1,256]{1,0:T(1,128)S(1)}, f32[1,256]{1,0:T(1,128)}, u32[]{:S(2)}) copy-start(f32[1,256]{1,0:T(1,128)} %get-tuple-element.127) | copy-start | bytes 3076
  164.1 9.3 %copy-start.36 = (f32[1,256]{1,0:T(1,128)S(1)}, f32[1,256]{1,0:T(1,128)}, u32[]{:S(2)}) copy-start(f32[1,256]{1,0:T(1,128)} %get-tuple-element.128) | copy-start | bytes 3076
  164.1 9.3 %copy-start.37 = (f32[1,256]{1,0:T(1,128)S(1)}, f32[1,256]{1,0:T(1,128)}, u32[]{:S(2)}) copy-start(f32[1,256]{1,0:T(1,128)} %get-tuple-element.129) | copy-start | bytes 3076
  164.1 9.3 %copy-start.38 = (f32[1,256]{1,0:T(1,128)S(1)}, f32[1,256]{1,0:T(1,128)}, u32[]{:S(2)}) copy-start(f32[1,256]{1,0:T(1,128)} %get-tuple-element.130) | copy-start | bytes 3076
  164.1 9.3 %copy-start.39 = (f32[1,256]{1,0:T(1,128)S(1)}, f32[1,256]{1,0:T(1,128)}, u32[]{:S(2)}) copy-start(f32[1,256]{1,0:T(1,128)} %get-tuple-element.131) | copy-start | bytes 3076
  164.1 9.3 %copy-start.40 = (f32[1,256]{1,0:T(1,128)S(1)}, f32[1,256]{1,0:T(1,128)}, u32[]{:S(2)}) copy-start(f32[1,256]{1,0:T(1,128)} %get-tuple-element.132) | copy-start | bytes 3076
  164.2 9.3 %copy-start.41 = (f32[1,256]{1,0:T(1,128)S(1)}, f32[1,256]{1,0:T(1,128)}, u32[]{:S(2)}) copy-start(f32[1,256]{1,0:T(1,128)} %get-tuple-element.133) | copy-start | bytes 3076
  164.2 9.3 %copy-start.42 = (f32[1,256]{1,0:T(1,128)S(1)}, f32[1,256]{1,0:T(1,128)}, u32[]{:S(2)}) copy-start(f32[1,256]{1,0:T(1,128)} %get-tuple-element.134) | copy-start | bytes 3076
  164.2 9.3 %copy-start.43 = (f32[1,256]{1,0:T(1,128)S(1)}, f32[1,256]{1,0:T(1,128)}, u32[]{:S(2)}) copy-start(f32[1,256]{1,0:T(1,128)} %get-tuple-element.136) | copy-start | bytes 3076
  164.2 9.3 %copy-start.44 = (f32[1,256]{1,0:T(1,128)S(1)}, f32[1,256]{1,0:T(1,128)}, u32[]{:S(2)}) copy-start(f32[1,256]{1,0:T(1,128)} %get-tuple-element.137) | copy-start | bytes 3076
  164.2 9.3 %copy-start.45 = (f32[1,256]{1,0:T(1,128)S(1)}, f32[1,256]{1,0:T(1,128)}, u32[]{:S(2)}) copy-start(f32[1,256]{1,0:T(1,128)} %get-tuple-element.138) | copy-start | bytes 3076
  164.2 9.3 %copy-start.46 = (f32[1,256]{1,0:T(1,128)S(1)}, f32[1,256]{1,0:T(1,128)}, u32[]{:S(2)}) copy-start(f32[1,256]{1,0:T(1,128)} %get-tuple-element.139) | copy-start | bytes 3076
  164.2 9.3 %copy-start.47 = (f32[1,256]{1,0:T(1,128)S(1)}, f32[1,256]{1,0:T(1,128)}, u32[]{:S(2)}) copy-start(f32[1,256]{1,0:T(1,128)} %get-tuple-element.140) | copy-start | bytes 3076
  164.2 9.3 %copy-start.48 = (f32[1,256]{1,0:T(1,128)S(1)}, f32[1,256]{1,0:T(1,128)}, u32[]{:S(2)}) copy-start(f32[1,256]{1,0:T(1,128)} %get-tuple-element.141) | copy-start | bytes 3076
  164.2 9.3 %copy-start.49 = (f32[1,256]{1,0:T(1,128)S(1)}, f32[1,256]{1,0:T(1,128)}, u32[]{:S(2)}) copy-start(f32[1,256]{1,0:T(1,128)} %get-tuple-element.142) | copy-start | bytes 3076
  164.2 9.3 %copy-start.50 = (f32[1,256]{1,0:T(1,128)S(1)}, f32[1,256]{1,0:T(1,128)}, u32[]{:S(2)}) copy-start(f32[1,256]{1,0:T(1,128)} %get-tuple-element.143) | copy-start | bytes 3076
  164.3 9.3 %copy-start.51 = (f32[1,256]{1,0:T(1,128)S(1)}, f32[1,256]{1,0:T(1,128)}, u32[]{:S(2)}) copy-start(f32[1,256]{1,0:T(1,128)} %get-tuple-element.144) | copy-start | bytes 3076
  168.1 5.1 %collective-permute-start.12 = (bf16[32,256]{1,0:T(8,128)(2,1)S(1)}, bf16[32,256]{1,0:T(8,128)(2,1)S(1)}, u32[]{:S(2)}, u32[]{:S(2)}) collective-permute-start(bf16[32,256]{1,0:T(8,128)(2,1)S(1)} %slice.1126), channel_id=1, source_target_pairs={{0,4},{4,8},{8,12},{12,16},{16,20},{20,24},{24,28},{28,32},{32,36}... | collective-permute-start | bytes 49160 | tf_op jit(solution)/shard_map/ppermute | solution.py:28
  173.5 12.2 %copy-start.54 = (f32[256]{0:T(256)S(1)}, f32[256]{0:T(256)}, u32[]{:S(2)}) copy-start(f32[256]{0:T(256)} %param.31) | copy-start | bytes 3076
  173.6 13.5 %copy-start.1 = (bf16[512,2048]{1,0:T(8,128)(2,1)S(1)}, bf16[512,2048]{1,0:T(8,128)(2,1)}, u32[]{:S(2)}) copy-start(bf16[512,2048]{1,0:T(8,128)(2,1)} %copy-done) | copy-start | bytes 6291460
  177.2 8.6 %all-to-all-start.4 = ((f32[4,8,128]{2,1,0:T(8,128)}), f32[4,8,128]{2,1,0:T(8,128)S(1)}, u32[]{:S(2)}, u32[]{:S(2)}) async-start(f32[4,8,128]{2,1,0:T(8,128)} %broadcast_in_dim.25), calls=%async_computation.4 | async-start | bytes 32768 | tf_op jit(solution)/shard_map/all_to_all | solution.py:21
  (14 other events, 46.1 us)

commit v3 on v2

--- a/solution.py
+++ b/solution.py
@@ -5,6 +5,7 @@
 from jax.experimental.pallas import tpu as pltpu
 from jax.sharding import Mesh
 from jax.sharding import PartitionSpec as P
+
 
 CONV_W = 1024
 SP = ("z", "x", "c")
@@ -32,22 +33,14 @@
     return lax.ppermute(block, "c", [(0, 1), (1, 0)])
 
 
-def after(value, *others):
-    return lax.optimization_barrier((value, *others))[0]
-
-
 def from_ahead(block, axis, distance):
     count = lax.axis_size(axis)
     return lax.ppermute(block, axis, [(i, (i - distance) % count) for i in range(count)])
 
 
-def along_z(piece):
-    return copies(piece, "z")
-
-
-def along_x(planes):
-    peers = lax.axis_size("x")
-    return jnp.stack([planes] + [from_ahead(planes, "x", d) for d in range(1, peers)])
+def from_own_on(planes, axis):
+    peers = lax.axis_size(axis)
+    return jnp.stack([planes] + [from_ahead(planes, axis, d) for d in range(1, peers)])
 
 
 def whole_specs(arrays):
@@ -66,17 +59,21 @@
     )(*scalars, *arrays)
 
 
-def natural_order(place_ref, own_ref, other_ref, into_ref, turned):
+def natural_order(place_ref, own_ref, other_ref, into_ref, turned, first_lane=0, from_own_x=False):
     peers_x, _, rows, _ = own_ref.shape
     blocks = into_ref.shape[0] // rows
-    core, place_x, part = place_ref[0], place_ref[1], place_ref[2]
+    lanes = slice(first_lane, first_lane + into_ref.shape[1])
+    core, part = place_ref[0], place_ref[2]
+    place_x = place_ref[1] if from_own_x else 0
     first = part * turned
 
     def place(by_core):
         for k in range(blocks):
             at = lax.rem(first + k, blocks)
             x = lax.rem(lax.div(at, 2) - place_x + 2 * peers_x, peers_x)
-            into_ref[k * rows : (k + 1) * rows, :] = by_core[k % 2][x, lax.div(at, 2 * peers_x)]
+            into_ref[k * rows : (k + 1) * rows, :] = by_core[k % 2][
+                x, lax.div(at, 2 * peers_x), :, lanes
+            ]
 
     @pl.when(core == 0)
     def _():
@@ -134,8 +131,8 @@
 def glu_kernel(place_ref, normed_ref, own_ref, other_ref, out_ref, weight_ref):
     parts = normed_ref.shape[0]
     turned = weight_ref.shape[0] // own_ref.shape[2] // parts
-    natural_order(place_ref, own_ref, other_ref, weight_ref, turned)
     width = out_ref.shape[1]
+    natural_order(place_ref, own_ref, other_ref, weight_ref, turned, first_lane=width)
     both = projected(normed_ref, weight_ref)
     value = both[:, :width].astype(BF16).astype(F32)
     gate = both[:, width:].astype(BF16).astype(F32)
@@ -266,7 +263,7 @@
     end_re_ref,
     end_im_ref,
 ):
-    count, width = u_ref.shape
+    count, _ = u_ref.shape
     states = fwd_re_ref.shape[1]
     chunks = count // CHUNK
     block = lower_ref.shape[0]
@@ -348,7 +345,7 @@
     out_ref,
     weight_ref,
 ):
-    natural_order(place_ref, own_ref, other_ref, weight_ref, 0)
+    natural_order(place_ref, own_ref, other_ref, weight_ref, 0, from_own_x=True)
     lanes = h_re_ref.shape[1]
     h_re, h_im = h_re_ref[...], h_im_ref[...]
     c_re, c_im = read_ref[:, :lanes].astype(F32), read_ref[:, lanes:].astype(F32)
@@ -487,7 +484,8 @@
 
 def summed_over(arrays, axis):
     line = jnp.concatenate([a.reshape(-1) for a in arrays]).reshape(-1, 128)
-    total = jnp.sum(copies(line, axis), axis=0).reshape(-1)
+    others = [from_ahead(line, axis, d) for d in range(1, lax.axis_size(axis))]
+    total = sum(others, line).reshape(-1)
     done, at = [], 0
     for a in arrays:
         done.append(total[at : at + a.size].reshape(a.shape))
@@ -498,7 +496,8 @@
 def conv_branch(glu, conv_taps, channel_gain):
     reach = conv_taps.shape[0] - 1
     count = glu.shape[0]
-    before = next_along(glu[count - 32 :], SP)[32 - reach :]
+    before = next_along(glu[count - 32 :], SP)
+    before = before[32 - reach :]
     extended = jnp.concatenate([before, glu], axis=0).astype(F32)
     raw = jnp.zeros(glu.shape, F32)
     for offset in range(reach + 1):
@@ -512,7 +511,7 @@
     return jax.nn.silu(scaled).astype(BF16)
 
 
-def per_device(
+def mixer(
     tokens,
     norm_gain,
     proj_state,
@@ -537,17 +536,14 @@
     depth = depth_part * parts
     half = count // 2
     width = proj_state.shape[1]
+    merged = jnp.concatenate([merge_state, merge_conv]).T
+    planes = copies(
+        jnp.concatenate([proj_state, proj_value, proj_gate, merged], axis=1), "z"
+    )
     ahead = from_ahead(tokens, "tp", 1)
     behind = from_ahead(tokens, "tp", -1)
-    in_z = along_z(proj_state)
-    vg_z = along_z(jnp.concatenate([proj_value, proj_gate], axis=1))
-    merge_z = along_z(jnp.concatenate([merge_state.T, merge_conv.T], axis=1))
     top = from_ahead(ahead[:half], "tp", 1)
     bottom = from_ahead(behind[half:], "tp", -1)
-    in_x = along_x(in_z)
-    vg_x = along_x(vg_z)
-    merge_x = along_x(merge_z)
-
     scan_tables, power, reads, device = tables(
         eigen_real, eigen_imag, log_step, decay_shift, state_input, readout, width
     )
@@ -561,11 +557,16 @@
         bytes_accessed=4 * count * depth,
         transcendentals=count,
     )
+    planes, normed, _ = lax.optimization_barrier((planes, normed, device["shift"]))
+    project_x = copies(planes[:, :, : 3 * width], "x")
+    merge_x = from_own_on(planes[:, :, 3 * width :], "x")
+    project_other = partner(project_x)
+    merge_other = partner(merge_x)
 
     u_in = call(
         state_in_kernel,
         jax.ShapeDtypeStruct((count, width), BF16),
-        (normed, in_x, partner(in_x)),
+        (normed, project_x, project_other),
         scalars=(place,),
         scratch=(pltpu.VMEM((depth, width), BF16),),
         mib=12,
@@ -598,7 +599,7 @@
     glu = call(
         glu_kernel,
         jax.ShapeDtypeStruct((count, width), BF16),
-        (normed, vg_x, partner(vg_x)),
+        (normed, project_x, project_other),
         scalars=(place,),
         scratch=(pltpu.VMEM((depth, 2 * width), BF16),),
         flops=4 * count * depth * width,
@@ -618,7 +619,7 @@
             reads,
             conv_out,
             merge_x,
-            partner(merge_x),
+            merge_other,
         ),
         scalars=(place,),
         scratch=(pltpu.VMEM((depth, 2 * width), BF16),),
@@ -639,7 +640,7 @@
 
 def solution(mesh):
     return jax.shard_map(
-        per_device,
+        mixer,
         mesh=finer_mesh(mesh),
         in_specs=(
             P(SP, "tp"),

time: 225 us -> 221 us (0.982)
  the two profiles are of different devices: /device:TPU:6 before, /device:TPU:32 now
where the time goes in v3:
time: 221 us; the launch traced here: 220 us
  starting transfers between devices  71.6 us (32%)
  blocking collectives  52 us (24%)
  waiting for transfers between devices  30.8 us (14%)
  local copies, waits for them, and re-layouts  25.3 us (11%)
  Pallas kernels  22.5 us (10%)
  other arithmetic  16.2 us (7%)
    ppermute x10, starting transfers between devices, from_ahead(): lax.ppermute(block, axis, [(i, (i - distance) % count) for i in range(cou...  33.8 us
    all_to_all x3, starting transfers between devices, copies(): lax.all_to_all(jnp.broadcast_to(value[None], (peers, *value.shape)), axis...  31.3 us
    all_to_all x1, blocking collectives, mixer(): lax.all_to_all(product.reshape(parts, count // parts, depth), 'tp', split...  28.7 us
    all_to_all x1, blocking collectives, copies(): lax.all_to_all(jnp.broadcast_to(value[None], (peers, *value.shape)), axis...  23.3 us
    pallas_call x6, Pallas kernels, call(): pl.pallas_call(body, compiler_params=pltpu.CompilerParams(vmem_limit_byte...  22.5 us
    all_to_all x3, waiting for transfers between devices, copies(): lax.all_to_all(jnp.broadcast_to(value[None], (peers, *value.shape)), axis...  19.2 us
    ppermute x10, waiting for transfers between devices, from_ahead(): lax.ppermute(block, axis, [(i, (i - distance) % count) for i in range(cou...  11.6 us
    unnamed x136, local copies, waits for them, and re-layouts  11 us
  transfers between devices with their start and end apart: 16, of which 5 were waited for; matrix products, arithmetic and copies ran while one was open for 12% of the time, Pallas kernels for 8%

profile of v3, /device:TPU:32, one launch (start us, length us, event | category | flops | bytes accessed | tf_op | source)
XLA Modules:
  0.0 219.7 jit_solution(10227244239500584626)
XLA Ops:
  0.0 0.8 maximum_bitcast_fusion
  0.8 0.7 pad_maximum_fusion.1
  1.6 0.9 broadcast_in_dim.14
  2.5 15.2 %all-to-all-start = ((bf16[16,16,1280]{2,1,0:T(8,128)(2,1)}), bf16[16,16,1280]{2,1,0:T(8,128)(2,1)}, u32[]{:S(2)}, u32[]{:S(2)}) async-start(bf16[16,16,1280]{2,1,0:T(8,128)(2,1)} %broadcast_in_dim.14), calls=%async_computation | async-start | bytes 1310720 | tf_op jit(solution)/shard_map/all_to_all | solution.py:22
  17.7 4.9 %collective-permute-start = (bf16[512,512]{1,0:T(8,128)(2,1)S(1)}, bf16[512,512]{1,0:T(8,128)(2,1)S(1)}, u32[]{:S(2)}, u32[]{:S(2)}) collective-permute-start(bf16[512,512]{1,0:T(8,128)(2,1)S(1)} %copy-done.5), channel_id=1, source_target_pairs={{0,3},{1,0},{2,1},{3,2},{4,7},{5,4},{6,5},{7,6},{8,11},{9,8},{10,9... | collective-permute-start | bytes 1572872 | tf_op jit(solution)/shard_map/ppermute | solution.py:38
  22.6 1.9 collective-permute-start.2
  24.6 0.7 broadcast_multiply_fusion
  25.6 1.2 fusion.37
  26.8 6.4 %collective-permute-done.ahead_ref = bf16[512,512]{1,0:T(8,128)(2,1)S(1)} collective-permute-done((bf16[512,512]{1,0:T(8,128)(2,1)S(1)}, bf16[512,512]{1,0:T(8,128)(2,1)S(1)}, u32[]{:S(2)}, u32[]{:S(2)}) %collective-permute-start) | collective-permute-done | bytes 524320 | tf_op jit(solution)/shard_map/ppermute | solution.py:38
  33.2 5.6 %collective-permute-start.1 = (bf16[256,512]{1,0:T(8,128)(2,1)S(1)}, bf16[256,512]{1,0:T(8,128)(2,1)S(1)}, u32[]{:S(2)}, u32[]{:S(2)}) collective-permute-start(bf16[256,512]{1,0:T(8,128)(2,1)S(1)} %slice.1058), channel_id=1, source_target_pairs={{0,3},{1,0},{2,1},{3,2},{4,7},{5,4},{6,5},{7,6},{8,11},{9,8},{10,9... | collective-permute-start | bytes 786440 | tf_op jit(solution)/shard_map/ppermute | solution.py:38
  38.9 1.9 collective-permute-start.3
  41.1 4.9 %shard_map.164 = (f32[512,256]{1,0:T(8,128)S(1)}, f32[512,256]{1,0:T(8,128)S(1)}, bf16[256,2048]{1,0:T(8,128)(2,1)S(1)}, bf16[256,2048]{1,0:T(8,128)(2,1)S(1)}, ...) custom-call(f32[16,512]{1,0:T(8,128)S(1)} %copy-done.15, ...), custom_call_target="tpu_custom_call" | custom-call | flops 83886080 | bytes 4194304 | tf_op jit(solution)/shard_map/pallas_call | solution.py:51
  46.0 1.3 copy-done
  47.3 1.0 copy-done.2
  48.3 1.0 copy-done.17
  49.3 0.8 copy-done.19
  50.1 0.8 copy-done.21
  50.9 0.7 copy-done.23
  51.6 0.7 copy-done.25
  52.9 1.0 copy-done.6
  54.0 1.3 shard_map.163.normed_ref
  55.3 1.0 slice.818
  56.5 23.3 %all_to_all.25.own_ref = bf16[4,16,16,768]{3,2,1,0:T(8,128)(2,1)} all-to-all(bf16[4,16,16,768]{3,2,1,0:T(8,128)(2,1)S(1)} %broadcast_in_dim.15), channel_id=1, replica_groups=mesh['z'=16,'x'=4,'c'=2,'tp'=4] {'x'}, dimensions={0} | all-to-all | bytes 3145728 | tf_op jit(solution)/shard_map/all_to_all | solution.py:22
  79.8 1.9 collective-permute-start.4
  83.0 0.7 fusion.72
  83.7 0.8 multiply_subtract_fusion.3
  84.4 1.7 slice_bitcast_fusion
  86.2 2.5 %collective-permute-start.11 = (bf16[16,16,512]{2,1,0:T(8,128)(2,1)S(1)}, bf16[16,16,512]{2,1,0:T(8,128)(2,1)S(1)}, u32[]{:S(2)}, u32[]{:S(2)}) collective-permute-start(bf16[16,16,512]{2,1,0:T(8,128)(2,1)S(1)} %get-tuple-element.39), channel_id=1, source_target_pairs={{0,8},{8,16},{16,24},{24,0},{1,9},{9,17},{17,25},{25,1},{2,10},{10... | collective-permute-start | bytes 786440 | tf_op jit(solution)/shard_map/ppermute | solution.py:38
  88.6 4.0 %collective-permute-start.10 = (bf16[16,16,512]{2,1,0:T(8,128)(2,1)S(1)}, bf16[16,16,512]{2,1,0:T(8,128)(2,1)S(1)}, u32[]{:S(2)}, u32[]{:S(2)}) collective-permute-start(bf16[16,16,512]{2,1,0:T(8,128)(2,1)S(1)} %get-tuple-element.39), channel_id=1, source_target_pairs={{0,16},{8,24},{16,0},{24,8},{1,17},{9,25},{17,1},{25,9},{2,18},{10... | collective-permute-start | bytes 786440 | tf_op jit(solution)/shard_map/ppermute | solution.py:38
  92.6 2.7 %collective-permute-start.9 = (bf16[16,16,512]{2,1,0:T(8,128)(2,1)S(1)}, bf16[16,16,512]{2,1,0:T(8,128)(2,1)S(1)}, u32[]{:S(2)}, u32[]{:S(2)}) collective-permute-start(bf16[16,16,512]{2,1,0:T(8,128)(2,1)S(1)} %get-tuple-element.39), channel_id=1, source_target_pairs={{0,24},{8,0},{16,8},{24,16},{1,25},{9,1},{17,9},{25,17},{2,26},{10... | collective-permute-start | bytes 786440 | tf_op jit(solution)/shard_map/ppermute | solution.py:38
  95.9 1.4 mul.1744
  97.3 1.4 reshape_squeeze.17
  98.6 1.4 reshape_squeeze.16
  100.0 0.8 fusion.31.lower_ref
  100.9 2.7 %collective-permute-done.11 = bf16[16,16,512]{2,1,0:T(8,128)(2,1)S(1)} collective-permute-done((bf16[16,16,512]{2,1,0:T(8,128)(2,1)S(1)}, bf16[16,16,512]{2,1,0:T(8,128)(2,1)S(1)}, u32[]{:S(2)}, u32[]{:S(2)}) %collective-permute-start.11) | collective-permute-done | bytes 262176 | tf_op jit(solution)/shard_map/ppermute | solution.py:38
  103.6 2.5 %collective-permute-done.9 = bf16[16,16,512]{2,1,0:T(8,128)(2,1)S(1)} collective-permute-done((bf16[16,16,512]{2,1,0:T(8,128)(2,1)S(1)}, bf16[16,16,512]{2,1,0:T(8,128)(2,1)S(1)}, u32[]{:S(2)}, u32[]{:S(2)}) %collective-permute-start.9) | collective-permute-done | bytes 262176 | tf_op jit(solution)/shard_map/ppermute | solution.py:38
  106.1 0.7 copy-done.31
  106.8 1.3 pad_maximum_fusion.own_ref
  108.1 1.9 collective-permute-start.12
  110.1 4.1 %shard_map.167 = bf16[512,256]{1,0:T(8,128)(2,1)S(1)} custom-call(s32[3]{0:T(128)S(1)} %pad_add_fusion.place_ref, bf16[4,512,512]{2,1,0:T(8,128)(2,1)S(1)} %shard_map.163.normed_ref, bf16[4,16,16,768]{3,2,1,0:T(8,128)(2,1)} %all_to_all.25.own_ref, bf16[4,16,16,768]{3,2,1,0:T(8,128)(2,1)} %collective-permute-done.4.other_ref), custom_call_target="tpu_custom_call" | custom-call | flops 1073741824 | bytes 4194304 | tf_op jit(solution)/shard_map/pallas_call | solution.py:51
  114.3 2.7 %collective-permute-start.5 = (bf16[32,256]{1,0:T(8,128)(2,1)S(1)}, bf16[32,256]{1,0:T(8,128)(2,1)S(1)}, u32[]{:S(2)}, u32[]{:S(2)}) collective-permute-start(bf16[32,256]{1,0:T(8,128)(2,1)S(1)} %slice.1134), channel_id=1, source_target_pairs={{0,4},{4,8},{8,12},{12,16},{16,20},{20,24},{24,28},{28,32},{32,36}... | collective-permute-start | bytes 49160 | tf_op jit(solution)/shard_map/ppermute | solution.py:29
  117.0 3.7 %shard_map.165.u_ref = bf16[512,256]{1,0:T(8,128)(2,1)S(1)} custom-call(s32[3]{0:T(128)S(1)} %pad_add_fusion.place_ref, bf16[4,512,512]{2,1,0:T(8,128)(2,1)S(1)} %shard_map.163.normed_ref, bf16[4,16,16,768]{3,2,1,0:T(8,128)(2,1)} %all_to_all.25.own_ref, bf16[4,16,16,768]{3,2,1,0:T(8,128)(2,1)} %collective-permute-done.4.other_ref), custom_call_target="tpu_custom_call" | custom-call | flops 536870912 | bytes 4194304 | tf_op jit(solution)/shard_map/pallas_call | solution.py:51
  121.1 4.1 %shard_map.166 = (f32[512,256]{1,0:T(8,128)S(1)}, f32[16,128]{1,0:T(8,128)S(1)}) custom-call(bf16[512,256]{1,0:T(8,128)(2,1)S(1)} %shard_map.165.u_ref, f32[512,256]{1,0:T(8,128)S(1)} %copy-done.20, f32[512,256]{1,0:T(8,128)S(1)} %copy-done.22, bf16[256,2048]{1,0:T(8,128)(2,1)S(1)} %copy-done.18, bf16[256,2048]{1,0:T(8,128)(2,1)S(1)} %copy-done.3, ...), custom_call_target="tpu_custom_call" | custom-call | flops 1610612736 | bytes 4194304 | tf_op jit(solution)/shard_map/pallas_call | solution.py:51
  125.6 3.6 %fusion.63 = (f32[512]{0:T(512)S(1)}, f32[512]{0:T(512)S(1)}, f32[512,256]{1,0:T(8,128)}) fusion(f32[542,256]{1,0:T(8,128)S(1)} %maximum_convert_fusion, f32[256]{0:T(256)S(1)} %bitcast.506, f32[256]{0:T(256)S(1)} %bitcast.507, f32[256]{0:T(256)S(1)} %bitcast.509, f32[256]{0:T(256)S(1)} %bitcast.510, f32[256]{0:T(256)S(1)} %bitcast.511, ...), kind=kLoop, calls=%fused_computation.281 | loop fusion | flops 8387584 | bytes 16813056 | tf_op jit(solution)/shard_map/reduce_sum | solution.py:506
  129.2 2.1 collective-permute-start.8
  131.3 6.3 %collective-permute-start.7 = (f32[8,128]{1,0:T(8,128)S(1)}, f32[8,128]{1,0:T(8,128)S(1)}, u32[]{:S(2)}, u32[]{:S(2)}) collective-permute-start(f32[8,128]{1,0:T(8,128)S(1)} %pad_maximum_fusion.4), channel_id=1, source_target_pairs={{0,2},{1,3},{2,0},{3,1},{4,6},{5,7},{6,4},{7,5},{8,10},{9,11},{10,... | collective-permute-start | bytes 12296 | tf_op jit(solution)/shard_map/ppermute | solution.py:38
  137.6 1.9 collective-permute-start.6
  140.2 4.1 %all-to-all-start.2 = ((f32[8,24,128]{2,1,0:T(8,128)}), f32[8,24,128]{2,1,0:T(8,128)S(1)}, u32[]{:S(2)}, u32[]{:S(2)}) async-start(f32[8,24,128]{2,1,0:T(8,128)} %broadcast_in_dim.16), calls=%async_computation.2 | async-start | bytes 196608 | tf_op jit(solution)/shard_map/all_to_all | solution.py:22
  144.3 5.7 %all-to-all-done.2 = f32[8,24,128]{2,1,0:T(8,128)S(1)} async-done(((f32[8,24,128]{2,1,0:T(8,128)}), f32[8,24,128]{2,1,0:T(8,128)S(1)}, u32[]{:S(2)}, u32[]{:S(2)}) %all-to-all-start.2) | async-done | bytes 98336 | tf_op jit(solution)/shard_map/all_to_all | solution.py:22
  150.1 0.7 broadcast_in_dim.20
  150.8 12.0 %all-to-all-start.3 = ((f32[16,24,128]{2,1,0:T(8,128)}), f32[16,24,128]{2,1,0:T(8,128)}, u32[]{:S(2)}, u32[]{:S(2)}) async-start(f32[16,24,128]{2,1,0:T(8,128)} %broadcast_in_dim.20), calls=%async_computation.3 | async-start | bytes 393216 | tf_op jit(solution)/shard_map/all_to_all | solution.py:22
  162.8 1.3 multiply_convert_fusion.conv_ref
  164.1 0.7 fusion.70
  164.8 13.5 %all-to-all-done.3 = f32[16,24,128]{2,1,0:T(8,128)} async-done(((f32[16,24,128]{2,1,0:T(8,128)}), f32[16,24,128]{2,1,0:T(8,128)}, u32[]{:S(2)}, u32[]{:S(2)}) %all-to-all-start.3) | async-done | bytes 196640 | tf_op jit(solution)/shard_map/all_to_all | solution.py:22
  178.2 0.7 fusion.69
  179.0 0.8 fusion.67
  179.8 0.8 fusion.68
  180.5 1.5 fusion.46
  182.0 1.0 fusion.45.h_re_ref
  183.1 1.2 copy-done.4
  184.3 1.0 copy-done.8
  185.3 4.4 %shard_map.168 = bf16[512,2048]{1,0:T(8,128)(2,1)S(1)} custom-call(s32[3]{0:T(128)S(1)} %pad_add_fusion.place_ref, f32[512,256]{1,0:T(8,128)S(1)} %copy-done.8, bf16[512,2048]{1,0:T(8,128)(2,1)S(1)} %copy-done.1, f32[1,1024]{1,0:T(1,128)S(1)} %fusion.45.h_re_ref, f32[1,1024]{1,0:T(1,128)S(1)} %get-tuple-element.32.h_im_ref, bf16[256,2048]{1,0:T(8,128)(2,1)S(1)} %copy-done.4, ...), custom_call_target="tpu_custom_call" | custom-call | flops 1073741824 | bytes 4194304 | tf_op jit(solution)/shard_map/pallas_call | solution.py:51
  189.7 28.7 %all_to_all.26 = bf16[4,128,2048]{2,1,0:T(8,128)(2,1)S(1)} all-to-all(bf16[4,128,2048]{2,1,0:T(8,128)(2,1)S(1)} %bitcast.386), channel_id=1, replica_groups=mesh['z'=16,'x'=4,'c'=2,'tp'=4] {'tp'}, dimensions={0} | all-to-all | bytes 4194304 | tf_op jit(solution)/shard_map/all_to_all | solution.py:630
  218.3 1.3 reduce_sum.32
  (166 shorter events, 4.2 us)
Async XLA Ops:
  0.0 17.7 %copy-start.5 = (bf16[512,512]{1,0:T(8,128)(2,1)S(1)}, bf16[512,512]{1,0:T(8,128)(2,1)}, u32[]{:S(2)}) copy-start(bf16[512,512]{1,0:T(8,128)(2,1)} %own_ref.1) | copy-start | bytes 1572868
  0.0 24.5 %copy-start.67 = (f32[16]{0:T(128)S(1)}, f32[16]{0:T(128)}, u32[]{:S(2)}) copy-start(f32[16]{0:T(128)} %param.24) | copy-start | bytes 196
  0.0 24.6 %copy-start.35 = (f32[16,64]{1,0:T(8,128)S(1)}, f32[16,64]{1,0:T(8,128)}, u32[]{:S(2)}) copy-start(f32[16,64]{1,0:T(8,128)} %param.22) | copy-start | bytes 12292
  0.0 24.6 %copy-start.36 = (f32[16,64]{1,0:T(8,128)S(1)}, f32[16,64]{1,0:T(8,128)}, u32[]{:S(2)}) copy-start(f32[16,64]{1,0:T(8,128)} %param.23) | copy-start | bytes 12292
  0.0 25.2 %copy-start.27 = (f32[2,16,16,64]{3,2,1,0:T(8,128)S(1)}, f32[2,16,16,64]{3,2,1,0:T(8,128)}, u32[]{:S(2)}) copy-start(f32[2,16,16,64]{3,2,1,0:T(8,128)} %param.26) | copy-start | bytes 393220
  0.0 25.5 %copy-start.28 = (f32[2,16,16,64]{3,2,1,0:T(8,128)S(1)}, f32[2,16,16,64]{3,2,1,0:T(8,128)}, u32[]{:S(2)}) copy-start(f32[2,16,16,64]{3,2,1,0:T(8,128)} %param.27) | copy-start | bytes 393220
  2.5 52.9 %all-to-all-start = ((bf16[16,16,1280]{2,1,0:T(8,128)(2,1)}), bf16[16,16,1280]{2,1,0:T(8,128)(2,1)}, u32[]{:S(2)}, u32[]{:S(2)}) async-start(bf16[16,16,1280]{2,1,0:T(8,128)(2,1)} %broadcast_in_dim.14), calls=%async_computation | async-start | bytes 1310720 | tf_op jit(solution)/shard_map/all_to_all | solution.py:22
  17.7 23.5 %copy-start.15 = (f32[16,512]{1,0:T(8,128)S(1)}, f32[16,512]{1,0:T(8,128)}, u32[]{:S(2)}) copy-start(f32[16,512]{1,0:T(8,128)} %shift_ref.1) | copy-start | bytes 98308
  17.7 15.5 %collective-permute-start = (bf16[512,512]{1,0:T(8,128)(2,1)S(1)}, bf16[512,512]{1,0:T(8,128)(2,1)S(1)}, u32[]{:S(2)}, u32[]{:S(2)}) collective-permute-start(bf16[512,512]{1,0:T(8,128)(2,1)S(1)} %copy-done.5), channel_id=1, source_target_pairs={{0,3},{1,0},{2,1},{3,2},{4,7},{5,4},{6,5},{7,6},{8,11},{9,8},{10,9... | collective-permute-start | bytes 1572872 | tf_op jit(solution)/shard_map/ppermute | solution.py:38
  22.6 16.2 %collective-permute-start.2 = (bf16[512,512]{1,0:T(8,128)(2,1)S(1)}, bf16[512,512]{1,0:T(8,128)(2,1)S(1)}, u32[]{:S(2)}, u32[]{:S(2)}) collective-permute-start(bf16[512,512]{1,0:T(8,128)(2,1)S(1)} %copy-done.5), channel_id=1, source_target_pairs={{0,1},{1,2},{2,3},{3,0},{4,5},{5,6},{6,7},{7,4},{8,9},{9,10},{10,1... | collective-permute-start | bytes 1572872 | tf_op jit(solution)/shard_map/ppermute | solution.py:38
  25.3 27.6 %copy-start.12 = (f32[2048]{0:T(1024)S(1)}, f32[2048]{0:T(1024)}, u32[]{:S(2)}) copy-start(f32[2048]{0:T(1024)} %param.18) | copy-start | bytes 24580
  33.2 19.2 %collective-permute-start.1 = (bf16[256,512]{1,0:T(8,128)(2,1)S(1)}, bf16[256,512]{1,0:T(8,128)(2,1)S(1)}, u32[]{:S(2)}, u32[]{:S(2)}) collective-permute-start(bf16[256,512]{1,0:T(8,128)(2,1)S(1)} %slice.1058), channel_id=1, source_target_pairs={{0,3},{1,0},{2,1},{3,2},{4,7},{5,4},{6,5},{7,6},{8,11},{9,8},{10,9... | collective-permute-start | bytes 786440 | tf_op jit(solution)/shard_map/ppermute | solution.py:38
  38.9 13.5 %collective-permute-start.3 = (bf16[256,512]{1,0:T(8,128)(2,1)S(1)}, bf16[256,512]{1,0:T(8,128)(2,1)S(1)}, u32[]{:S(2)}, u32[]{:S(2)}) collective-permute-start(bf16[256,512]{1,0:T(8,128)(2,1)S(1)} %slice.1059), channel_id=1, source_target_pairs={{0,1},{1,2},{2,3},{3,0},{4,5},{5,6},{6,7},{7,4},{8,9},{9,10},{10,1... | collective-permute-start | bytes 786440 | tf_op jit(solution)/shard_map/ppermute | solution.py:38
  41.1 11.3 %copy-start.10 = (f32[16,1024]{1,0:T(8,128)}, f32[16,1024]{1,0:T(8,128)S(1)}, u32[]{:S(2)}) copy-start(f32[16,1024]{1,0:T(8,128)S(1)} %get-tuple-element.168.start_sin_ref) | copy-start | bytes 196612
  41.1 11.3 %copy-start.11 = (f32[16,1024]{1,0:T(8,128)}, f32[16,1024]{1,0:T(8,128)S(1)}, u32[]{:S(2)}) copy-start(f32[16,1024]{1,0:T(8,128)S(1)} %get-tuple-element.169.start_cos_ref) | copy-start | bytes 196612
  56.4 25.4 %copy-start.33 = (f32[31,256]{1,0:T(8,128)S(1)}, f32[31,256]{1,0:T(8,128)}, u32[]{:S(2)}) copy-start(f32[31,256]{1,0:T(8,128)} %param.30) | copy-start | bytes 95236
  56.4 26.0 %copy-start.34 = (f32[2,16,64]{2,1,0:T(8,128)S(1)}, f32[2,16,64]{2,1,0:T(8,128)}, u32[]{:S(2)}) copy-start(f32[2,16,64]{2,1,0:T(8,128)} %param.29) | copy-start | bytes 24580
  79.8 30.3 %collective-permute-start.4 = (bf16[4,16,16,768]{3,2,1,0:T(8,128)(2,1)}, bf16[4,16,16,768]{3,2,1,0:T(8,128)(2,1)}, u32[]{:S(2)}, u32[]{:S(2)}) collective-permute-start(bf16[4,16,16,768]{3,2,1,0:T(8,128)(2,1)} %all_to_all.25.own_ref), channel_id=1, source_target_pairs={{0,4},{4,0},{1,5},{5,1},{2,6},{6,2},{3,7},{7,3},{8,12},{12,8},{9,1... | collective-permute-start | bytes 4718600 | tf_op jit(solution)/shard_map/ppermute | solution.py:33
  86.2 17.4 %collective-permute-start.11 = (bf16[16,16,512]{2,1,0:T(8,128)(2,1)S(1)}, bf16[16,16,512]{2,1,0:T(8,128)(2,1)S(1)}, u32[]{:S(2)}, u32[]{:S(2)}) collective-permute-start(bf16[16,16,512]{2,1,0:T(8,128)(2,1)S(1)} %get-tuple-element.39), channel_id=1, source_target_pairs={{0,8},{8,16},{16,24},{24,0},{1,9},{9,17},{17,25},{25,1},{2,10},{10... | collective-permute-start | bytes 786440 | tf_op jit(solution)/shard_map/ppermute | solution.py:38
  88.6 15.0 %collective-permute-start.10 = (bf16[16,16,512]{2,1,0:T(8,128)(2,1)S(1)}, bf16[16,16,512]{2,1,0:T(8,128)(2,1)S(1)}, u32[]{:S(2)}, u32[]{:S(2)}) collective-permute-start(bf16[16,16,512]{2,1,0:T(8,128)(2,1)S(1)} %get-tuple-element.39), channel_id=1, source_target_pairs={{0,16},{8,24},{16,0},{24,8},{1,17},{9,25},{17,1},{25,9},{2,18},{10... | collective-permute-start | bytes 786440 | tf_op jit(solution)/shard_map/ppermute | solution.py:38
  92.6 13.5 %collective-permute-start.9 = (bf16[16,16,512]{2,1,0:T(8,128)(2,1)S(1)}, bf16[16,16,512]{2,1,0:T(8,128)(2,1)S(1)}, u32[]{:S(2)}, u32[]{:S(2)}) collective-permute-start(bf16[16,16,512]{2,1,0:T(8,128)(2,1)S(1)} %get-tuple-element.39), channel_id=1, source_target_pairs={{0,24},{8,0},{16,8},{24,16},{1,25},{9,1},{17,9},{25,17},{2,26},{10... | collective-permute-start | bytes 786440 | tf_op jit(solution)/shard_map/ppermute | solution.py:38
  108.1 74.9 %collective-permute-start.12 = (bf16[4,16,16,512]{3,2,1,0:T(8,128)(2,1)S(1)}, bf16[4,16,16,512]{3,2,1,0:T(8,128)(2,1)}, u32[]{:S(2)}, u32[]{:S(2)}) collective-permute-start(bf16[4,16,16,512]{3,2,1,0:T(8,128)(2,1)S(1)} %pad_maximum_fusion.own_ref), channel_id=1, source_target_pairs={{0,4},{4,0},{1,5},{5,1},{2,6},{6,2},{3,7},{7,3},{8,12},{12,8},{9,1... | collective-permute-start | bytes 3145736 | tf_op jit(solution)/shard_map/ppermute | solution.py:33
  114.2 6.5 %copy-start.3 = (bf16[256,2048]{1,0:T(8,128)(2,1)S(1)}, bf16[256,2048]{1,0:T(8,128)(2,1)}, u32[]{:S(2)}) copy-start(bf16[256,2048]{1,0:T(8,128)(2,1)} %copy-done.2) | copy-start | bytes 3145732
  114.2 6.5 %copy-start.9 = (f32[32,1024]{1,0:T(8,128)S(1)}, f32[32,1024]{1,0:T(8,128)}, u32[]{:S(2)}) copy-start(f32[32,1024]{1,0:T(8,128)} %get-tuple-element.165.fwd_re_ref) | copy-start | bytes 393220
  114.2 6.5 %copy-start.16 = (f32[256]{0:T(256)S(1)}, f32[256]{0:T(256)}, u32[]{:S(2)}) copy-start(f32[256]{0:T(256)} %param.28) | copy-start | bytes 3076
  114.2 6.5 %copy-start.18 = (bf16[256,2048]{1,0:T(8,128)(2,1)S(1)}, bf16[256,2048]{1,0:T(8,128)(2,1)}, u32[]{:S(2)}) copy-start(bf16[256,2048]{1,0:T(8,128)(2,1)} %copy-done.17) | copy-start | bytes 3145732
  114.2 6.5 %copy-start.20 = (f32[512,256]{1,0:T(8,128)S(1)}, f32[512,256]{1,0:T(8,128)}, u32[]{:S(2)}) copy-start(f32[512,256]{1,0:T(8,128)} %copy-done.19) | copy-start | bytes 1572868
  114.3 6.5 %copy-start.22 = (f32[512,256]{1,0:T(8,128)S(1)}, f32[512,256]{1,0:T(8,128)}, u32[]{:S(2)}) copy-start(f32[512,256]{1,0:T(8,128)} %copy-done.21) | copy-start | bytes 1572868
  114.3 6.5 %copy-start.24 = (f32[5,16,1024]{2,1,0:T(8,128)S(1)}, f32[5,16,1024]{2,1,0:T(8,128)}, u32[]{:S(2)}) copy-start(f32[5,16,1024]{2,1,0:T(8,128)} %copy-done.23) | copy-start | bytes 983044
  114.3 6.5 %copy-start.26 = (f32[5,16,1024]{2,1,0:T(8,128)S(1)}, f32[5,16,1024]{2,1,0:T(8,128)}, u32[]{:S(2)}) copy-start(f32[5,16,1024]{2,1,0:T(8,128)} %copy-done.25) | copy-start | bytes 983044
  114.3 10.9 %collective-permute-start.5 = (bf16[32,256]{1,0:T(8,128)(2,1)S(1)}, bf16[32,256]{1,0:T(8,128)(2,1)S(1)}, u32[]{:S(2)}, u32[]{:S(2)}) collective-permute-start(bf16[32,256]{1,0:T(8,128)(2,1)S(1)} %slice.1134), channel_id=1, source_target_pairs={{0,4},{4,8},{8,12},{12,16},{16,20},{20,24},{24,28},{28,32},{32,36}... | collective-permute-start | bytes 49160 | tf_op jit(solution)/shard_map/ppermute | solution.py:29
  120.8 4.5 %copy-start.37 = (f32[1,256]{1,0:T(1,128)S(1)}, f32[1,256]{1,0:T(1,128)}, u32[]{:S(2)}) copy-start(f32[1,256]{1,0:T(1,128)} %get-tuple-element.141) | copy-start | bytes 3076
  120.8 4.5 %copy-start.38 = (f32[1,256]{1,0:T(1,128)S(1)}, f32[1,256]{1,0:T(1,128)}, u32[]{:S(2)}) copy-start(f32[1,256]{1,0:T(1,128)} %get-tuple-element.142) | copy-start | bytes 3076
  120.8 4.5 %copy-start.39 = (f32[1,256]{1,0:T(1,128)S(1)}, f32[1,256]{1,0:T(1,128)}, u32[]{:S(2)}) copy-start(f32[1,256]{1,0:T(1,128)} %get-tuple-element.143) | copy-start | bytes 3076
  120.8 4.5 %copy-start.40 = (f32[1,256]{1,0:T(1,128)S(1)}, f32[1,256]{1,0:T(1,128)}, u32[]{:S(2)}) copy-start(f32[1,256]{1,0:T(1,128)} %get-tuple-element.144) | copy-start | bytes 3076
  120.8 4.5 %copy-start.41 = (f32[1,256]{1,0:T(1,128)S(1)}, f32[1,256]{1,0:T(1,128)}, u32[]{:S(2)}) copy-start(f32[1,256]{1,0:T(1,128)} %get-tuple-element.145) | copy-start | bytes 3076
  120.8 4.5 %copy-start.42 = (f32[1,256]{1,0:T(1,128)S(1)}, f32[1,256]{1,0:T(1,128)}, u32[]{:S(2)}) copy-start(f32[1,256]{1,0:T(1,128)} %get-tuple-element.146) | copy-start | bytes 3076
  120.8 4.5 %copy-start.43 = (f32[1,256]{1,0:T(1,128)S(1)}, f32[1,256]{1,0:T(1,128)}, u32[]{:S(2)}) copy-start(f32[1,256]{1,0:T(1,128)} %get-tuple-element.147) | copy-start | bytes 3076
  120.9 4.5 %copy-start.44 = (f32[1,256]{1,0:T(1,128)S(1)}, f32[1,256]{1,0:T(1,128)}, u32[]{:S(2)}) copy-start(f32[1,256]{1,0:T(1,128)} %get-tuple-element.148) | copy-start | bytes 3076
  120.9 4.5 %copy-start.45 = (f32[1,256]{1,0:T(1,128)S(1)}, f32[1,256]{1,0:T(1,128)}, u32[]{:S(2)}) copy-start(f32[1,256]{1,0:T(1,128)} %get-tuple-element.149) | copy-start | bytes 3076
  120.9 4.5 %copy-start.46 = (f32[1,256]{1,0:T(1,128)S(1)}, f32[1,256]{1,0:T(1,128)}, u32[]{:S(2)}) copy-start(f32[1,256]{1,0:T(1,128)} %get-tuple-element.150) | copy-start | bytes 3076
  120.9 4.5 %copy-start.47 = (f32[1,256]{1,0:T(1,128)S(1)}, f32[1,256]{1,0:T(1,128)}, u32[]{:S(2)}) copy-start(f32[1,256]{1,0:T(1,128)} %get-tuple-element.151) | copy-start | bytes 3076
  120.9 4.5 %copy-start.48 = (f32[1,256]{1,0:T(1,128)S(1)}, f32[1,256]{1,0:T(1,128)}, u32[]{:S(2)}) copy-start(f32[1,256]{1,0:T(1,128)} %get-tuple-element.152) | copy-start | bytes 3076
  120.9 4.5 %copy-start.49 = (f32[1,256]{1,0:T(1,128)S(1)}, f32[1,256]{1,0:T(1,128)}, u32[]{:S(2)}) copy-start(f32[1,256]{1,0:T(1,128)} %get-tuple-element.122) | copy-start | bytes 3076
  120.9 4.5 %copy-start.50 = (f32[1,256]{1,0:T(1,128)S(1)}, f32[1,256]{1,0:T(1,128)}, u32[]{:S(2)}) copy-start(f32[1,256]{1,0:T(1,128)} %get-tuple-element.123) | copy-start | bytes 3076
  120.9 4.5 %copy-start.51 = (f32[1,256]{1,0:T(1,128)S(1)}, f32[1,256]{1,0:T(1,128)}, u32[]{:S(2)}) copy-start(f32[1,256]{1,0:T(1,128)} %get-tuple-element.124) | copy-start | bytes 3076
  120.9 4.5 %copy-start.52 = (f32[1,256]{1,0:T(1,128)S(1)}, f32[1,256]{1,0:T(1,128)}, u32[]{:S(2)}) copy-start(f32[1,256]{1,0:T(1,128)} %get-tuple-element.125) | copy-start | bytes 3076
  120.9 4.5 %copy-start.53 = (f32[1,256]{1,0:T(1,128)S(1)}, f32[1,256]{1,0:T(1,128)}, u32[]{:S(2)}) copy-start(f32[1,256]{1,0:T(1,128)} %get-tuple-element.126) | copy-start | bytes 3076
  121.0 4.5 %copy-start.54 = (f32[1,256]{1,0:T(1,128)S(1)}, f32[1,256]{1,0:T(1,128)}, u32[]{:S(2)}) copy-start(f32[1,256]{1,0:T(1,128)} %get-tuple-element.127) | copy-start | bytes 3076
  121.0 4.5 %copy-start.55 = (f32[1,256]{1,0:T(1,128)S(1)}, f32[1,256]{1,0:T(1,128)}, u32[]{:S(2)}) copy-start(f32[1,256]{1,0:T(1,128)} %get-tuple-element.128) | copy-start | bytes 3076
  121.0 4.5 %copy-start.56 = (f32[1,256]{1,0:T(1,128)S(1)}, f32[1,256]{1,0:T(1,128)}, u32[]{:S(2)}) copy-start(f32[1,256]{1,0:T(1,128)} %get-tuple-element.129) | copy-start | bytes 3076
  121.0 4.5 %copy-start.57 = (f32[1,256]{1,0:T(1,128)S(1)}, f32[1,256]{1,0:T(1,128)}, u32[]{:S(2)}) copy-start(f32[1,256]{1,0:T(1,128)} %get-tuple-element.130) | copy-start | bytes 3076
  121.0 4.5 %copy-start.58 = (f32[1,256]{1,0:T(1,128)S(1)}, f32[1,256]{1,0:T(1,128)}, u32[]{:S(2)}) copy-start(f32[1,256]{1,0:T(1,128)} %get-tuple-element.131) | copy-start | bytes 3076
  121.0 4.5 %copy-start.59 = (f32[1,256]{1,0:T(1,128)S(1)}, f32[1,256]{1,0:T(1,128)}, u32[]{:S(2)}) copy-start(f32[1,256]{1,0:T(1,128)} %get-tuple-element.132) | copy-start | bytes 3076
  121.0 4.5 %copy-start.60 = (f32[1,256]{1,0:T(1,128)S(1)}, f32[1,256]{1,0:T(1,128)}, u32[]{:S(2)}) copy-start(f32[1,256]{1,0:T(1,128)} %get-tuple-element.133) | copy-start | bytes 3076
  121.0 4.5 %copy-start.61 = (f32[1,256]{1,0:T(1,128)S(1)}, f32[1,256]{1,0:T(1,128)}, u32[]{:S(2)}) copy-start(f32[1,256]{1,0:T(1,128)} %get-tuple-element.134) | copy-start | bytes 3076
  125.6 13.9 %copy-start.14 = (f32[8,128]{1,0:T(8,128)S(1)}, f32[8,128]{1,0:T(8,128)}, u32[]{:S(2)}) copy-start(f32[8,128]{1,0:T(8,128)} %copy-done.13) | copy-start | bytes 12292
  125.6 24.4 %copy-start.32 = (f32[8,128]{1,0:T(8,128)S(1)}, f32[8,128]{1,0:T(8,128)}, u32[]{:S(2)}) copy-start(f32[8,128]{1,0:T(8,128)} %mul.1744) | copy-start | bytes 12292
  129.2 53.8 %copy-start.1 = (bf16[512,2048]{1,0:T(8,128)(2,1)S(1)}, bf16[512,2048]{1,0:T(8,128)(2,1)}, u32[]{:S(2)}) copy-start(bf16[512,2048]{1,0:T(8,128)(2,1)} %copy-done) | copy-start | bytes 6291460
  129.2 15.0 %collective-permute-start.8 = (f32[8,128]{1,0:T(8,128)S(1)}, f32[8,128]{1,0:T(8,128)S(1)}, u32[]{:S(2)}, u32[]{:S(2)}) collective-permute-start(f32[8,128]{1,0:T(8,128)S(1)} %pad_maximum_fusion.4), channel_id=1, source_target_pairs={{0,1},{1,2},{2,3},{3,0},{4,5},{5,6},{6,7},{7,4},{8,9},{9,10},{10,1... | collective-permute-start | bytes 12296 | tf_op jit(solution)/shard_map/ppermute | solution.py:38
  131.3 13.0 %collective-permute-start.7 = (f32[8,128]{1,0:T(8,128)S(1)}, f32[8,128]{1,0:T(8,128)S(1)}, u32[]{:S(2)}, u32[]{:S(2)}) collective-permute-start(f32[8,128]{1,0:T(8,128)S(1)} %pad_maximum_fusion.4), channel_id=1, source_target_pairs={{0,2},{1,3},{2,0},{3,1},{4,6},{5,7},{6,4},{7,5},{8,10},{9,11},{10,... | collective-permute-start | bytes 12296 | tf_op jit(solution)/shard_map/ppermute | solution.py:38
  137.6 6.7 %collective-permute-start.6 = (f32[8,128]{1,0:T(8,128)S(1)}, f32[8,128]{1,0:T(8,128)S(1)}, u32[]{:S(2)}, u32[]{:S(2)}) collective-permute-start(f32[8,128]{1,0:T(8,128)S(1)} %pad_maximum_fusion.4), channel_id=1, source_target_pairs={{0,3},{1,0},{2,1},{3,2},{4,7},{5,4},{6,5},{7,6},{8,11},{9,8},{10,9... | collective-permute-start | bytes 12296 | tf_op jit(solution)/shard_map/ppermute | solution.py:38
  140.2 9.9 %all-to-all-start.2 = ((f32[8,24,128]{2,1,0:T(8,128)}), f32[8,24,128]{2,1,0:T(8,128)S(1)}, u32[]{:S(2)}, u32[]{:S(2)}) async-start(f32[8,24,128]{2,1,0:T(8,128)} %broadcast_in_dim.16), calls=%async_computation.2 | async-start | bytes 196608 | tf_op jit(solution)/shard_map/all_to_all | solution.py:22
  150.8 27.4 %all-to-all-start.3 = ((f32[16,24,128]{2,1,0:T(8,128)}), f32[16,24,128]{2,1,0:T(8,128)}, u32[]{:S(2)}, u32[]{:S(2)}) async-start(f32[16,24,128]{2,1,0:T(8,128)} %broadcast_in_dim.20), calls=%async_computation.3 | async-start | bytes 393216 | tf_op jit(solution)/shard_map/all_to_all | solution.py:22
  (20 other events, 42.7 us)

commit v4 on v3

--- a/solution.py
+++ b/solution.py
@@ -11,6 +11,7 @@
 SP = ("z", "x", "c")
 SP_TP = ("z", "x", "c", "tp")
 CHUNK = 32
+HALO = 32
 EPS = 1e-06
 EXACT = lax.Precision.HIGHEST
 F32 = jnp.float32
@@ -43,17 +44,21 @@
     return jnp.stack([planes] + [from_ahead(planes, axis, d) for d in range(1, peers)])
 
 
+def far_from_core(*arrays):
+    return [pltpu.with_memory_space_constraint(array, pltpu.HBM) for array in arrays]
+
+
 def whole_specs(arrays):
     return [pl.BlockSpec(memory_space=pltpu.VMEM) for _ in arrays]
 
 
-def call(body, outs, arrays, scalars=(), scratch=(), mib=16, **costs):
+def call(body, outs, arrays, scalars=(), scratch=(), mib=16, space=pltpu.VMEM, **costs):
     return pl.pallas_call(
         body,
         compiler_params=pltpu.CompilerParams(vmem_limit_bytes=mib * 2**20),
         out_shape=outs,
         in_specs=[pl.BlockSpec(memory_space=pltpu.SMEM) for _ in scalars] + whole_specs(arrays),
-        out_specs=jax.tree.map(lambda _: pl.BlockSpec(memory_space=pltpu.VMEM), outs),
+        out_specs=jax.tree.map(lambda _: pl.BlockSpec(memory_space=space), outs),
         scratch_shapes=list(scratch),
         cost_estimate=pl.CostEstimate(**costs) if costs else None,
     )(*scalars, *arrays)
@@ -96,8 +101,8 @@
     def rows_of(at, opposite_ref):
         rows = pl.ds(at, half)
         blocks = [
-            ref.astype(F32)
-            for ref in (own_ref[rows], ahead_ref[rows], opposite_ref[...], behind_ref[rows])
+            block.astype(F32)
+            for block in (own_ref[rows], ahead_ref[rows], opposite_ref[...], behind_ref[rows])
         ]
         power = sum(jnp.sum(block * block, axis=1, keepdims=True) for block in blocks)
         scale = lax.rsqrt(power / (parts * depth) + EPS)
@@ -109,11 +114,11 @@
     rows_of(half, bottom_ref)
 
 
-def projected(normed_ref, weight_ref):
+def projected(normed_ref, weight_ref, rows):
     parts, _, depth = normed_ref.shape
     return sum(
         jnp.dot(
-            normed_ref[p],
+            normed_ref[p, rows],
             weight_ref[p * depth : (p + 1) * depth],
             preferred_element_type=F32,
         )
@@ -122,21 +127,51 @@
 
 
 def state_in_kernel(place_ref, normed_ref, own_ref, other_ref, out_ref, weight_ref):
-    parts = normed_ref.shape[0]
+    parts, rows, _ = normed_ref.shape
     turned = weight_ref.shape[0] // own_ref.shape[2] // parts
     natural_order(place_ref, own_ref, other_ref, weight_ref, turned)
-    out_ref[...] = projected(normed_ref, weight_ref).astype(BF16)
-
-
-def glu_kernel(place_ref, normed_ref, own_ref, other_ref, out_ref, weight_ref):
-    parts = normed_ref.shape[0]
+    out_ref[...] = projected(normed_ref, weight_ref, slice(HALO, rows)).astype(BF16)
+
+
+def conv_kernel(
+    place_ref, normed_ref, own_ref, other_ref, taps_ref, raw_ref, sums_ref, weight_ref, glu_ref, shifted_ref
+):
+    parts, rows, _ = normed_ref.shape
+    count, width = raw_ref.shape
     turned = weight_ref.shape[0] // own_ref.shape[2] // parts
-    width = out_ref.shape[1]
     natural_order(place_ref, own_ref, other_ref, weight_ref, turned, first_lane=width)
-    both = projected(normed_ref, weight_ref)
+    both = projected(normed_ref, weight_ref, slice(0, rows))
     value = both[:, :width].astype(BF16).astype(F32)
     gate = both[:, width:].astype(BF16).astype(F32)
-    out_ref[...] = (value * jax.nn.sigmoid(gate)).astype(BF16)
+    glu_ref[:rows] = (value * jax.nn.sigmoid(gate)).astype(BF16).astype(F32)
+    glu_ref[rows:] = jnp.zeros((glu_ref.shape[0] - rows, width), F32)
+    taps = taps_ref.shape[0]
+    sublanes = 8
+    for k in range(sublanes):
+        shifted_ref[k] = glu_ref[k : k + rows]
+    first = HALO - (taps - 1)
+    step = 64
+
+    def some_rows(n, _):
+        at = pl.multiple_of(n * step, step)
+        total = jnp.zeros((step, width), F32)
+        for k in range(taps):
+            shift, whole = (first + k) % sublanes, (first + k) // sublanes * sublanes
+            total = total + taps_ref[k : k + 1] * shifted_ref[shift, pl.ds(at + whole, step)]
+        raw_ref[pl.ds(at, step)] = total
+        return 0
+
+    lax.fori_loop(0, count // step, some_rows, 0)
+    raw = raw_ref[...]
+    ones = jnp.ones((8, width), F32)
+
+    def across(value):
+        return lax.dot_general(
+            ones, value, (((1,), (1,)), ((), ())), precision=EXACT, preferred_element_type=F32
+        )[:1]
+
+    sums_ref[0:1] = across(raw)
+    sums_ref[1:2] = across(raw * raw)
 
 
 def squared(re, im):
@@ -167,7 +202,20 @@
         out_ref[:, at + 2 * k * cols : at + 2 * (k + 1) * cols] = jnp.where(mine, pair, 0.0).astype(BF16)
 
 
-def table_kernel(
+def table_kernel(*refs):
+    inputs, hbm, vmem, done = refs[:10], refs[10:18], refs[18:26], refs[26]
+
+    def send(*which):
+        for k in which:
+            pltpu.make_async_copy(vmem[k], hbm[k], done.at[k]).start()
+
+    fill_tables(send, *inputs, *vmem)
+    for k in range(len(vmem)):
+        pltpu.make_async_copy(vmem[k], hbm[k], done.at[k]).wait()
+
+
+def fill_tables(
+    send,
     shift_ref,
     base_ref,
     cos_ref,
@@ -213,6 +261,7 @@
     spread = spread_over(groups, lanes // groups)
     wide = exact_dot(whole, spread)
     wide_last = wide[count - 1 :]
+    send(0, 1)
     for k in range(lanes // 128):
         total_ref[k : k + 1, :] = wide_last[:, k * 128 : (k + 1) * 128]
     sums = jnp.concatenate([partial[(c + 1) * CHUNK - 1 : (c + 1) * CHUNK] for c in range(chunks)])
@@ -228,6 +277,7 @@
         hop_re_ref[level], hop_im_ref[level] = size * turn[0], size * turn[1]
         near = near + jnp.where(index >= distance, pltpu.roll(near, distance, 0), 0.0)
         distance, level = distance * 2, level + 1
+    send(4, 5, 7)
     counts = lax.broadcasted_iota(jnp.int32, (CHUNK, 1), 0).astype(F32)
     inner = (cos_ref[...], sin_ref[...])
     for c in range(chunks):
@@ -236,10 +286,13 @@
         turn = times((start_cos_ref[c : c + 1], start_sin_ref[c : c + 1]), inner)
         power_ref[at, :lanes] = (size * turn[0]).astype(BF16)
         power_ref[at, lanes:] = (size * turn[1]).astype(BF16)
+    send(6)
     write_diagonal(into_ref, 0, b_re_ref[...], groups)
     write_diagonal(into_ref, lanes, b_im_ref[...], groups)
+    send(2)
     write_diagonal(out_ref, 0, c_re_ref[...], groups)
     write_diagonal(out_ref, lanes, -c_im_ref[...], groups)
+    send(3)
 
 
 def scan_kernel(
@@ -400,18 +453,19 @@
     lower_block = (
         (at[:, None] >= at[None, :]) & (at[:, None] // CHUNK == at[None, :] // CHUNK)
     ).astype(BF16)
+    outs = (
+        pltpu.HBM((count, width), F32),
+        pltpu.HBM((count, width), F32),
+        pltpu.HBM((width, 2 * lanes), BF16),
+        pltpu.HBM((width, 2 * lanes), BF16),
+        pltpu.HBM((levels, chunks, lanes), F32),
+        pltpu.HBM((levels, chunks, lanes), F32),
+        pltpu.HBM((count, 2 * lanes), BF16),
+        pltpu.HBM((lanes // 128, 128), F32),
+    )
     grow, shrink, into, out, hop_re, hop_im, power, total = call(
         table_kernel,
-        (
-            jax.ShapeDtypeStruct((count, width), F32),
-            jax.ShapeDtypeStruct((count, width), F32),
-            jax.ShapeDtypeStruct((width, 2 * lanes), BF16),
-            jax.ShapeDtypeStruct((width, 2 * lanes), BF16),
-            jax.ShapeDtypeStruct((levels, chunks, lanes), F32),
-            jax.ShapeDtypeStruct((levels, chunks, lanes), F32),
-            jax.ShapeDtypeStruct((count, 2 * lanes), BF16),
-            jax.ShapeDtypeStruct((lanes // 128, 128), F32),
-        ),
+        outs,
         (
             decay_shift,
             base,
@@ -424,7 +478,9 @@
             readout[0].reshape(rows),
             readout[1].reshape(rows),
         ),
+        scratch=[pltpu.VMEM(o.shape, o.dtype) for o in outs] + [pltpu.SemaphoreType.DMA((len(outs),))],
         mib=24,
+        space=pltpu.HBM,
         flops=20 * count * count * groups,
         bytes_accessed=8 * count * lanes,
         transcendentals=count * lanes,
@@ -442,7 +498,7 @@
     return packed[:rows], packed[rows : 2 * rows], packed[2 * rows :]
 
 
-def carry_in(last, device, count, init_state):
+def carry_in(last, device, count, h):
     rows = device["base"].shape[0]
     base, turn = device["base"], device["turn"]
     plane = ("x", "c")
@@ -466,7 +522,6 @@
     plane_turn, at = turn, 1
     while at < peers:
         plane_turn, at = squared(*plane_turn), at * 2
-    h = tuple(s.reshape(-1, 128) for s in (init_state[0], init_state[1]))
     for k in range(lax.axis_size("z")):
         re, im, shift = pulled(far[k], rows)
         size = jnp.exp(peers * count * base + shift)
@@ -482,29 +537,9 @@
     return moved[0] + before[0], moved[1] + before[1]
 
 
-def summed_over(arrays, axis):
-    line = jnp.concatenate([a.reshape(-1) for a in arrays]).reshape(-1, 128)
-    others = [from_ahead(line, axis, d) for d in range(1, lax.axis_size(axis))]
-    total = sum(others, line).reshape(-1)
-    done, at = [], 0
-    for a in arrays:
-        done.append(total[at : at + a.size].reshape(a.shape))
-        at += a.size
-    return done
-
-
-def conv_branch(glu, conv_taps, channel_gain):
-    reach = conv_taps.shape[0] - 1
-    count = glu.shape[0]
-    before = next_along(glu[count - 32 :], SP)
-    before = before[32 - reach :]
-    extended = jnp.concatenate([before, glu], axis=0).astype(F32)
-    raw = jnp.zeros(glu.shape, F32)
-    for offset in range(reach + 1):
-        raw = raw + conv_taps[offset] * extended[offset : offset + count]
-    first, second = summed_over(
-        (jnp.sum(raw, axis=1, keepdims=True), jnp.sum(raw * raw, axis=1, keepdims=True)), "tp"
-    )
+def conv_finish(raw, sums, channel_gain):
+    others = [from_ahead(sums, "tp", d) for d in range(1, lax.axis_size("tp"))]
+    first, second = (row[:, None] for row in sum(others, sums))
     middle = first / CONV_W
     spread = second / CONV_W - middle * middle
     scaled = (raw - middle) * lax.rsqrt(spread + EPS) * channel_gain
@@ -534,35 +569,39 @@
     parts = lax.axis_size("tp")
     count, depth_part = tokens.shape
     depth = depth_part * parts
-    half = count // 2
+    rows = count + HALO
+    half = rows // 2
     width = proj_state.shape[1]
     merged = jnp.concatenate([merge_state, merge_conv]).T
     planes = copies(
         jnp.concatenate([proj_state, proj_value, proj_gate, merged], axis=1), "z"
     )
-    ahead = from_ahead(tokens, "tp", 1)
-    behind = from_ahead(tokens, "tp", -1)
+    extended = jnp.concatenate([next_along(tokens[count - HALO :], SP), tokens])
+    ahead = from_ahead(extended, "tp", 1)
+    behind = from_ahead(extended, "tp", -1)
     top = from_ahead(ahead[:half], "tp", 1)
     bottom = from_ahead(behind[half:], "tp", -1)
     scan_tables, power, reads, device = tables(
         eigen_real, eigen_imag, log_step, decay_shift, state_input, readout, width
     )
+    start = tuple(s.reshape(-1, 128) for s in (init_state[0], init_state[1]))
+    planes, total, start = lax.optimization_barrier((planes, device["shift"], start))
+    device["shift"] = total
+    project_x = copies(planes[:, :, : 3 * width], "x")
+    merge_x = from_own_on(planes[:, :, 3 * width :], "x")
+    project_other = partner(project_x)
+    merge_other = partner(merge_x)
+
     normed = call(
         norm_kernel,
-        jax.ShapeDtypeStruct((parts, count, depth_part), BF16),
-        (tokens, ahead, top, bottom, behind, norm_gain.reshape(parts, 1, depth_part)),
+        jax.ShapeDtypeStruct((parts, rows, depth_part), BF16),
+        (*far_from_core(extended, ahead, top, bottom, behind), norm_gain.reshape(parts, 1, depth_part)),
         scalars=(place,),
         mib=12,
         flops=8 * count * depth,
         bytes_accessed=4 * count * depth,
         transcendentals=count,
     )
-    planes, normed, _ = lax.optimization_barrier((planes, normed, device["shift"]))
-    project_x = copies(planes[:, :, : 3 * width], "x")
-    merge_x = from_own_on(planes[:, :, 3 * width :], "x")
-    project_other = partner(project_x)
-    merge_other = partner(merge_x)
-
     u_in = call(
         state_in_kernel,
         jax.ShapeDtypeStruct((count, width), BF16),
@@ -579,7 +618,7 @@
     y_local, last = call(
         scan_kernel,
         (
-            jax.ShapeDtypeStruct((count, width), F32),
+            pltpu.HBM((count, width), F32),
             jax.ShapeDtypeStruct((2 * lanes // 128, 128), F32),
         ),
         (u_in, *scan_tables, skip_gain.reshape(1, -1)),
@@ -594,19 +633,27 @@
         bytes_accessed=8 * count * lanes,
         transcendentals=0,
     )
-    h_re, h_im = carry_in(last, device, count, init_state)
-
-    glu = call(
-        glu_kernel,
-        jax.ShapeDtypeStruct((count, width), BF16),
-        (normed, project_x, project_other),
+    h_re, h_im = carry_in(last, device, count, start)
+
+    raw, sums = call(
+        conv_kernel,
+        (
+            pltpu.HBM((count, width), F32),
+            jax.ShapeDtypeStruct((2, count), F32),
+        ),
+        (normed, project_x, project_other, conv_taps),
         scalars=(place,),
-        scratch=(pltpu.VMEM((depth, 2 * width), BF16),),
+        scratch=(
+            pltpu.VMEM((depth, 2 * width), BF16),
+            pltpu.VMEM((rows + 8, width), F32),
+            pltpu.VMEM((8, rows, width), F32),
+        ),
+        mib=20,
         flops=4 * count * depth * width,
         bytes_accessed=4 * depth * count,
         transcendentals=0,
     )
-    conv_out = conv_branch(glu, conv_taps, channel_gain)
+    conv_out = conv_finish(raw, sums, channel_gain)
 
     product = call(
         merge_kernel,

time: 221 us -> 229 us (1.036)
  waiting for transfers between devices: 30.8 us -> 68.2 us
  blocking collectives: 52 us -> 28.6 us
  local copies, waits for them, and re-layouts: 25.3 us -> 12.2 us
  Pallas kernels: 22.5 us -> 30.2 us
  other arithmetic: 16.2 us -> 11.6 us
  starting transfers between devices: 71.6 us -> 75.6 us
    all_to_all x3 -> x4, waiting for transfers between devices: 19.2 us -> 52.2 us  [copies(): lax.all_to_all(jnp.broadcast_to(value[None], (peers, *value.shape)), axis...]
    all_to_all x1 -> x0, blocking collectives: 23.3 us -> none  [copies(): lax.all_to_all(jnp.broadcast_to(value[None], (peers, *value.shape)), axis...]
    pallas_call x6, Pallas kernels: 22.5 us -> 30.2 us  [call(): pl.pallas_call(body, compiler_params=pltpu.CompilerParams(vmem_limit_byte...]
    unnamed x136 -> x67, local copies, waits for them, and re-layouts: 11 us -> 4.7 us
    slice x10 -> x2, local copies, waits for them, and re-layouts: 4.86 us -> 0.01 us  [the longest x1 0.01 us: mixer(): extended = jnp.concatenate([next_along(tokens[count - HALO:], SP), tokens])]
    all_to_all x3 -> x4, starting transfers between devices: 31.3 us -> 36 us  [copies(): lax.all_to_all(jnp.broadcast_to(value[None], (peers, *value.shape)), axis...]
    ppermute x10, waiting for transfers between devices: 11.6 us -> 15.9 us  [from_ahead(): lax.ppermute(block, axis, [(i, (i - distance) % count) for i in range(cou...]
    reduce_sum x1 -> x0, other arithmetic: 3.57 us -> none  [conv_branch(): jnp.sum(raw, axis=1, keepdims=True)]
  transfers between devices with their start and end apart: 16 -> 17, of which waited for: 5 -> 6; matrix products, arithmetic and copies ran while one was open for 12% -> 6% of each run, Pallas kernels for 8% -> 11%
where the time goes in v4:
time: 229 us; the launch traced here: 227 us
  starting transfers between devices  75.6 us (33%)
  waiting for transfers between devices  68.2 us (30%)
  Pallas kernels  30.2 us (13%)
  blocking collectives  28.6 us (12%)
  local copies, waits for them, and re-layouts  12.2 us (5%)
  other arithmetic  11.6 us (5%)
    all_to_all x4, waiting for transfers between devices, copies(): lax.all_to_all(jnp.broadcast_to(value[None], (peers, *value.shape)), axis...  52.2 us
    all_to_all x4, starting transfers between devices, copies(): lax.all_to_all(jnp.broadcast_to(value[None], (peers, *value.shape)), axis...  36 us
    ppermute x10, starting transfers between devices, from_ahead(): lax.ppermute(block, axis, [(i, (i - distance) % count) for i in range(cou...  33.6 us
    pallas_call x6, Pallas kernels, call(): pl.pallas_call(body, compiler_params=pltpu.CompilerParams(vmem_limit_byte...  30.2 us
    all_to_all x1, blocking collectives, mixer(): lax.all_to_all(product.reshape(parts, count // parts, depth), 'tp', split...  28.6 us
    ppermute x10, waiting for transfers between devices, from_ahead(): lax.ppermute(block, axis, [(i, (i - distance) % count) for i in range(cou...  15.9 us
    unnamed x67, local copies, waits for them, and re-layouts  4.7 us
  transfers between devices with their start and end apart: 17, of which 6 were waited for; matrix products, arithmetic and copies ran while one was open for 6% of the time, Pallas kernels for 11%

profile of v4, /device:TPU:32, one launch (start us, length us, event | category | flops | bytes accessed | tf_op | source)
XLA Modules:
  0.0 227.1 jit_solution(3004610891865954091)
XLA Ops:
  0.0 0.8 maximum_bitcast_fusion
  0.8 0.7 pad_maximum_fusion.1
  1.6 0.9 broadcast_in_dim.12
  2.5 15.3 %all-to-all-start = ((bf16[16,16,1280]{2,1,0:T(8,128)(2,1)}), bf16[16,16,1280]{2,1,0:T(8,128)(2,1)S(1)}, u32[]{:S(2)}, u32[]{:S(2)}) async-start(bf16[16,16,1280]{2,1,0:T(8,128)(2,1)} %broadcast_in_dim.12), calls=%async_computation | async-start | bytes 1310720 | tf_op jit(solution)/shard_map/all_to_all | solution.py:23
  17.8 0.1 broadcast_multiply_fusion.1
  18.0 0.1 reshape.237.refs_1_
  18.0 0.1 mul.833
  18.1 0.1 mul.810
  18.2 0.7 reshape_squeeze.16
  18.9 0.7 reshape_squeeze.17
  19.6 0.3 multiply_sine_fusion.1
  20.0 1.3 fusion.7
  21.3 7.4 %shard_map.164 = (f32[512,256]{1,0:T(8,128)}, f32[512,256]{1,0:T(8,128)}, bf16[256,2048]{1,0:T(8,128)(2,1)}, bf16[256,2048]{1,0:T(8,128)(2,1)}, f32[5,16,1024]{2...) custom-call(f32[16,512]{1,0:T(8,128)S(1)} %copy-done.8, ...), custom_call_target="tpu_custom_call" | custom-call | flops 83886080 | bytes 4194304 | tf_op jit(solution)/shard_map/pallas_call | solution.py:56
  28.7 22.9 %all-to-all-done = bf16[16,16,1280]{2,1,0:T(8,128)(2,1)S(1)} async-done(((bf16[16,16,1280]{2,1,0:T(8,128)(2,1)}), bf16[16,16,1280]{2,1,0:T(8,128)(2,1)S(1)}, u32[]{:S(2)}, u32[]{:S(2)}) %all-to-all-start) | async-done | bytes 655392 | tf_op jit(solution)/shard_map/all_to_all | solution.py:23
  51.6 1.3 broadcast_in_dim.13
  52.9 4.3 %all-to-all-start.1 = ((bf16[4,16,16,768]{3,2,1,0:T(8,128)(2,1)}), bf16[4,16,16,768]{3,2,1,0:T(8,128)(2,1)}, u32[]{:S(2)}, u32[]{:S(2)}) async-start(bf16[4,16,16,768]{3,2,1,0:T(8,128)(2,1)} %broadcast_in_dim.13), calls=%async_computation.1 | async-start | bytes 3145728 | tf_op jit(solution)/shard_map/all_to_all | solution.py:23
  57.3 1.9 collective-permute-start
  59.2 14.5 %all-to-all-done.1.own_ref = bf16[4,16,16,768]{3,2,1,0:T(8,128)(2,1)} async-done(((bf16[4,16,16,768]{3,2,1,0:T(8,128)(2,1)}), bf16[4,16,16,768]{3,2,1,0:T(8,128)(2,1)}, u32[]{:S(2)}, u32[]{:S(2)}) %all-to-all-start.1) | async-done | bytes 1572896 | tf_op jit(solution)/shard_map/all_to_all | solution.py:23
  73.8 1.9 collective-permute-start.5
  75.8 4.9 %collective-permute-start.1 = (bf16[544,512]{1,0:T(8,128)(2,1)S(1)}, bf16[544,512]{1,0:T(8,128)(2,1)S(1)}, u32[]{:S(2)}, u32[]{:S(2)}) collective-permute-start(bf16[544,512]{1,0:T(8,128)(2,1)S(1)} %constant_dynamic-update-slice_fusion.own_ref), channel_id=1, source_target_pairs={{0,3},{1,0},{2,1},{3,2},{4,7},{5,4},{6,5},{7,6},{8,11},{9,8},{10,9... | collective-permute-start | bytes 1671176 | tf_op jit(solution)/shard_map/ppermute | solution.py:39
  80.7 1.9 collective-permute-start.3
  82.6 10.6 %collective-permute-done.1.ahead_ref = bf16[544,512]{1,0:T(8,128)(2,1)S(1)} collective-permute-done((bf16[544,512]{1,0:T(8,128)(2,1)S(1)}, bf16[544,512]{1,0:T(8,128)(2,1)S(1)}, u32[]{:S(2)}, u32[]{:S(2)}) %collective-permute-start.1) | collective-permute-done | bytes 557088 | tf_op jit(solution)/shard_map/ppermute | solution.py:39
  93.2 0.9 copy-done.16
  94.1 5.6 %collective-permute-start.2 = (bf16[272,512]{1,0:T(8,128)(2,1)S(1)}, bf16[272,512]{1,0:T(8,128)(2,1)S(1)}, u32[]{:S(2)}, u32[]{:S(2)}) collective-permute-start(bf16[272,512]{1,0:T(8,128)(2,1)S(1)} %slice.724), channel_id=1, source_target_pairs={{0,3},{1,0},{2,1},{3,2},{4,7},{5,4},{6,5},{7,6},{8,11},{9,8},{10,9... | collective-permute-start | bytes 835592 | tf_op jit(solution)/shard_map/ppermute | solution.py:39
  99.8 1.9 collective-permute-start.4
  101.7 0.9 slice_bitcast_fusion.72
  102.5 2.1 collective-permute-start.11
  104.7 4.0 %collective-permute-start.10 = (bf16[16,16,512]{2,1,0:T(8,128)(2,1)}, bf16[16,16,512]{2,1,0:T(8,128)(2,1)S(1)}, u32[]{:S(2)}, u32[]{:S(2)}) collective-permute-start(bf16[16,16,512]{2,1,0:T(8,128)(2,1)} %get-tuple-element.51), channel_id=1, source_target_pairs={{0,16},{8,24},{16,0},{24,8},{1,17},{9,25},{17,1},{25,9},{2,18},{10... | collective-permute-start | bytes 786440 | tf_op jit(solution)/shard_map/ppermute | solution.py:39
  108.7 2.9 %collective-permute-start.9 = (bf16[16,16,512]{2,1,0:T(8,128)(2,1)}, bf16[16,16,512]{2,1,0:T(8,128)(2,1)}, u32[]{:S(2)}, u32[]{:S(2)}) collective-permute-start(bf16[16,16,512]{2,1,0:T(8,128)(2,1)} %get-tuple-element.51), channel_id=1, source_target_pairs={{0,24},{8,0},{16,8},{24,16},{1,25},{9,1},{17,9},{25,17},{2,26},{10... | collective-permute-start | bytes 786440 | tf_op jit(solution)/shard_map/ppermute | solution.py:39
  111.6 0.1 pad_add_fusion.place_ref
  111.6 0.1 mul.880
  111.7 0.7 mul.844
  112.4 0.7 mul.878
  113.0 0.1 fusion.1.lower_ref
  113.2 0.7 copy-done.22
  113.9 2.5 %shard_map.163.normed_ref = bf16[4,544,512]{2,1,0:T(8,128)(2,1)S(1)} custom-call(s32[3]{0:T(128)S(1)} %pad_add_fusion.place_ref, bf16[544,512]{1,0:T(8,128)(2,1)} %copy-done.19, bf16[544,512]{1,0:T(8,128)(2,1)} %copy-done.16, bf16[272,512]{1,0:T(8,128)(2,1)} %copy-done.21, bf16[272,512]{1,0:T(8,128)(2,1)} %copy-done.22, bf16[544,512]{1,0:T(8,128)(2,1)} %copy-done.17, ...), custom_call_target="tpu_custom_call" | custom-call | flops 8388608 | bytes 4194304 | tf_op jit(solution)/shard_map/pallas_call | solution.py:56
  116.3 2.7 %collective-permute-done.11 = bf16[16,16,512]{2,1,0:T(8,128)(2,1)S(1)} collective-permute-done((bf16[16,16,512]{2,1,0:T(8,128)(2,1)}, bf16[16,16,512]{2,1,0:T(8,128)(2,1)S(1)}, u32[]{:S(2)}, u32[]{:S(2)}) %collective-permute-start.11) | collective-permute-done | bytes 262176 | tf_op jit(solution)/shard_map/ppermute | solution.py:39
  119.0 2.6 %collective-permute-done.9 = bf16[16,16,512]{2,1,0:T(8,128)(2,1)} collective-permute-done((bf16[16,16,512]{2,1,0:T(8,128)(2,1)}, bf16[16,16,512]{2,1,0:T(8,128)(2,1)}, u32[]{:S(2)}, u32[]{:S(2)}) %collective-permute-start.9) | collective-permute-done | bytes 262176 | tf_op jit(solution)/shard_map/ppermute | solution.py:39
  121.7 1.2 pad_maximum_fusion.own_ref
  123.0 2.2 collective-permute-start.12
  125.2 3.7 %shard_map.165.u_ref = bf16[512,256]{1,0:T(8,128)(2,1)S(1)} custom-call(s32[3]{0:T(128)S(1)} %pad_add_fusion.place_ref, bf16[4,544,512]{2,1,0:T(8,128)(2,1)S(1)} %shard_map.163.normed_ref, bf16[4,16,16,768]{3,2,1,0:T(8,128)(2,1)} %all-to-all-done.1.own_ref, bf16[4,16,16,768]{3,2,1,0:T(8,128)(2,1)} %collective-permute-done.5.other_ref), custom_call_target="tpu_custom_call" | custom-call | flops 536870912 | bytes 4194304 | tf_op jit(solution)/shard_map/pallas_call | solution.py:56
  129.1 5.0 %shard_map.166 = (f32[512,256]{1,0:T(8,128)}, f32[16,128]{1,0:T(8,128)S(1)}) custom-call(bf16[512,256]{1,0:T(8,128)(2,1)S(1)} %shard_map.165.u_ref, f32[512,256]{1,0:T(8,128)S(1)} %copy-done.11, f32[512,256]{1,0:T(8,128)S(1)} %copy-done.12, bf16[256,2048]{1,0:T(8,128)(2,1)S(1)} %copy-done.10, bf16[256,2048]{1,0:T(8,128)(2,1)S(1)} %copy-done.1, ...), custom_call_target="tpu_custom_call" | custom-call | flops 1610612736 | bytes 4194304 | tf_op jit(solution)/shard_map/pallas_call | solution.py:56
  134.1 0.7 broadcast_in_dim.14
  134.7 4.0 %all-to-all-start.2 = ((f32[8,24,128]{2,1,0:T(8,128)}), f32[8,24,128]{2,1,0:T(8,128)S(1)}, u32[]{:S(2)}, u32[]{:S(2)}) async-start(f32[8,24,128]{2,1,0:T(8,128)} %broadcast_in_dim.14), calls=%async_computation.2 | async-start | bytes 196608 | tf_op jit(solution)/shard_map/all_to_all | solution.py:23
  138.7 0.8 copy-done.6
  139.5 7.3 %shard_map.167 = (f32[512,256]{1,0:T(8,128)}, f32[2,512]{1,0:T(2,128)S(1)}) custom-call(s32[3]{0:T(128)S(1)} %pad_add_fusion.place_ref, bf16[4,544,512]{2,1,0:T(8,128)(2,1)S(1)} %shard_map.163.normed_ref, bf16[4,16,16,768]{3,2,1,0:T(8,128)(2,1)} %all-to-all-done.1.own_ref, bf16[4,16,16,768]{3,2,1,0:T(8,128)(2,1)} %collective-permute-done.5.other_ref, ...), custom_call_target="tpu_custom_call" | custom-call | flops 1073741824 | bytes 4194304 | tf_op jit(solution)/shard_map/pallas_call | solution.py:56
  146.8 0.0 copy-start.27
  146.8 2.1 collective-permute-start.8
  148.8 6.3 %collective-permute-start.7 = (f32[2,512]{1,0:T(2,128)S(1)}, f32[2,512]{1,0:T(2,128)S(1)}, u32[]{:S(2)}, u32[]{:S(2)}) collective-permute-start(f32[2,512]{1,0:T(2,128)S(1)} %get-tuple-element.36), channel_id=1, source_target_pairs={{0,2},{1,3},{2,0},{3,1},{4,6},{5,7},{6,4},{7,5},{8,10},{9,11},{10,... | collective-permute-start | bytes 12296 | tf_op jit(solution)/shard_map/ppermute | solution.py:39
  155.1 1.9 collective-permute-start.6
  157.2 0.7 broadcast_in_dim.17
  157.9 12.3 %all-to-all-start.3 = ((f32[16,24,128]{2,1,0:T(8,128)}), f32[16,24,128]{2,1,0:T(8,128)}, u32[]{:S(2)}, u32[]{:S(2)}) async-start(f32[16,24,128]{2,1,0:T(8,128)} %broadcast_in_dim.17), calls=%async_computation.3 | async-start | bytes 393216 | tf_op jit(solution)/shard_map/all_to_all | solution.py:23
  170.2 1.3 multiply_convert_fusion.conv_ref
  171.5 14.8 %all-to-all-done.3 = f32[16,24,128]{2,1,0:T(8,128)} async-done(((f32[16,24,128]{2,1,0:T(8,128)}), f32[16,24,128]{2,1,0:T(8,128)}, u32[]{:S(2)}, u32[]{:S(2)}) %all-to-all-start.3) | async-done | bytes 196640 | tf_op jit(solution)/shard_map/all_to_all | solution.py:23
  186.3 0.7 fusion.64
  187.1 0.9 fusion.40
  187.9 0.8 fusion.18
  188.8 0.9 select_add_fusion
  189.7 0.8 select_add_fusion.1
  190.6 1.2 copy-done.2
  191.8 1.0 copy-done.3
  192.8 4.4 %shard_map.168 = bf16[512,2048]{1,0:T(8,128)(2,1)S(1)} custom-call(s32[3]{0:T(128)S(1)} %pad_add_fusion.place_ref, f32[512,256]{1,0:T(8,128)S(1)} %copy-done.3, bf16[512,2048]{1,0:T(8,128)(2,1)S(1)} %copy-done, f32[1,1024]{1,0:T(1,128)S(1)} %bitcast.1076, f32[1,1024]{1,0:T(1,128)S(1)} %bitcast.1075, bf16[256,2048]{1,0:T(8,128)(2,1)S(1)} %copy-done.2, ...), custom_call_target="tpu_custom_call" | custom-call | flops 1073741824 | bytes 4194304 | tf_op jit(solution)/shard_map/pallas_call | solution.py:56
  197.2 28.6 %all_to_all.25 = bf16[4,128,2048]{2,1,0:T(8,128)(2,1)S(1)} all-to-all(bf16[4,128,2048]{2,1,0:T(8,128)(2,1)S(1)} %bitcast.1072), channel_id=1, replica_groups=mesh['z'=16,'x'=4,'c'=2,'tp'=4] {'tp'}, dimensions={0} | all-to-all | bytes 4194304 | tf_op jit(solution)/shard_map/all_to_all | solution.py:677
  225.8 1.3 reduce_sum.12
  (94 shorter events, 0.5 us)
Async XLA Ops:
  0.0 17.8 %copy-start.32 = (f32[16]{0:T(128)S(1)}, f32[16]{0:T(128)}, u32[]{:S(2)}) copy-start(f32[16]{0:T(128)} %param.24) | copy-start | bytes 196
  0.0 17.8 %copy-start.29 = (f32[16,64]{1,0:T(8,128)S(1)}, f32[16,64]{1,0:T(8,128)}, u32[]{:S(2)}) copy-start(f32[16,64]{1,0:T(8,128)} %param.22) | copy-start | bytes 12292
  0.0 17.8 %copy-start.30 = (f32[16,64]{1,0:T(8,128)S(1)}, f32[16,64]{1,0:T(8,128)}, u32[]{:S(2)}) copy-start(f32[16,64]{1,0:T(8,128)} %param.23) | copy-start | bytes 12292
  0.0 18.2 %copy-start.28 = (f32[2,16,64]{2,1,0:T(8,128)S(1)}, f32[2,16,64]{2,1,0:T(8,128)}, u32[]{:S(2)}) copy-start(f32[2,16,64]{2,1,0:T(8,128)} %param.29) | copy-start | bytes 24580
  0.0 19.5 %copy-start.23 = (f32[2,16,16,64]{3,2,1,0:T(8,128)S(1)}, f32[2,16,16,64]{3,2,1,0:T(8,128)}, u32[]{:S(2)}) copy-start(f32[2,16,16,64]{3,2,1,0:T(8,128)} %param.26) | copy-start | bytes 393220
  0.0 19.9 %copy-start.24 = (f32[2,16,16,64]{3,2,1,0:T(8,128)S(1)}, f32[2,16,16,64]{3,2,1,0:T(8,128)}, u32[]{:S(2)}) copy-start(f32[2,16,16,64]{3,2,1,0:T(8,128)} %param.27) | copy-start | bytes 393220
  2.4 18.8 %copy-start.8 = (f32[16,512]{1,0:T(8,128)S(1)}, f32[16,512]{1,0:T(8,128)}, u32[]{:S(2)}) copy-start(f32[16,512]{1,0:T(8,128)} %refs_0_.1) | copy-start | bytes 98308
  2.5 49.2 %all-to-all-start = ((bf16[16,16,1280]{2,1,0:T(8,128)(2,1)}), bf16[16,16,1280]{2,1,0:T(8,128)(2,1)S(1)}, u32[]{:S(2)}, u32[]{:S(2)}) async-start(bf16[16,16,1280]{2,1,0:T(8,128)(2,1)} %broadcast_in_dim.12), calls=%async_computation | async-start | bytes 1310720 | tf_op jit(solution)/shard_map/all_to_all | solution.py:23
  51.6 5.7 %copy-start.20 = (bf16[512,512]{1,0:T(8,128)(2,1)S(1)}, bf16[512,512]{1,0:T(8,128)(2,1)}, u32[]{:S(2)}) copy-start(bf16[512,512]{1,0:T(8,128)(2,1)} %param.17) | copy-start | bytes 1572868
  52.9 20.8 %all-to-all-start.1 = ((bf16[4,16,16,768]{3,2,1,0:T(8,128)(2,1)}), bf16[4,16,16,768]{3,2,1,0:T(8,128)(2,1)}, u32[]{:S(2)}, u32[]{:S(2)}) async-start(bf16[4,16,16,768]{3,2,1,0:T(8,128)(2,1)} %broadcast_in_dim.13), calls=%async_computation.1 | async-start | bytes 3145728 | tf_op jit(solution)/shard_map/all_to_all | solution.py:23
  57.3 56.6 %copy-start.7 = (f32[2048]{0:T(1024)S(1)}, f32[2048]{0:T(1024)}, u32[]{:S(2)}) copy-start(f32[2048]{0:T(1024)} %param.18) | copy-start | bytes 24580
  57.3 18.4 %collective-permute-start = (bf16[32,512]{1,0:T(8,128)(2,1)S(1)}, bf16[32,512]{1,0:T(8,128)(2,1)S(1)}, u32[]{:S(2)}, u32[]{:S(2)}) collective-permute-start(bf16[32,512]{1,0:T(8,128)(2,1)S(1)} %slice.567), channel_id=1, source_target_pairs={{0,4},{4,8},{8,12},{12,16},{16,20},{20,24},{24,28},{28,32},{32,36}... | collective-permute-start | bytes 98312 | tf_op jit(solution)/shard_map/ppermute | solution.py:30
  73.8 51.5 %collective-permute-start.5 = (bf16[4,16,16,768]{3,2,1,0:T(8,128)(2,1)}, bf16[4,16,16,768]{3,2,1,0:T(8,128)(2,1)}, u32[]{:S(2)}, u32[]{:S(2)}) collective-permute-start(bf16[4,16,16,768]{3,2,1,0:T(8,128)(2,1)} %all-to-all-done.1.own_ref), channel_id=1, source_target_pairs={{0,4},{4,0},{1,5},{5,1},{2,6},{6,2},{3,7},{7,3},{8,12},{12,8},{9,1... | collective-permute-start | bytes 4718600 | tf_op jit(solution)/shard_map/ppermute | solution.py:34
  75.7 37.4 %copy-start.19 = (bf16[544,512]{1,0:T(8,128)(2,1)}, bf16[544,512]{1,0:T(8,128)(2,1)S(1)}, u32[]{:S(2)}) copy-start(bf16[544,512]{1,0:T(8,128)(2,1)S(1)} %constant_dynamic-update-slice_fusion.own_ref) | copy-start | bytes 1671172
  75.8 17.5 %collective-permute-start.1 = (bf16[544,512]{1,0:T(8,128)(2,1)S(1)}, bf16[544,512]{1,0:T(8,128)(2,1)S(1)}, u32[]{:S(2)}, u32[]{:S(2)}) collective-permute-start(bf16[544,512]{1,0:T(8,128)(2,1)S(1)} %constant_dynamic-update-slice_fusion.own_ref), channel_id=1, source_target_pairs={{0,3},{1,0},{2,1},{3,2},{4,7},{5,4},{6,5},{7,6},{8,11},{9,8},{10,9... | collective-permute-start | bytes 1671176 | tf_op jit(solution)/shard_map/ppermute | solution.py:39
  80.7 19.0 %collective-permute-start.3 = (bf16[544,512]{1,0:T(8,128)(2,1)S(1)}, bf16[544,512]{1,0:T(8,128)(2,1)S(1)}, u32[]{:S(2)}, u32[]{:S(2)}) collective-permute-start(bf16[544,512]{1,0:T(8,128)(2,1)S(1)} %constant_dynamic-update-slice_fusion.own_ref), channel_id=1, source_target_pairs={{0,1},{1,2},{2,3},{3,0},{4,5},{5,6},{6,7},{7,4},{8,9},{9,10},{10,1... | collective-permute-start | bytes 1671176 | tf_op jit(solution)/shard_map/ppermute | solution.py:39
  93.2 0.9 copy-start.16
  94.1 14.6 %collective-permute-start.2 = (bf16[272,512]{1,0:T(8,128)(2,1)S(1)}, bf16[272,512]{1,0:T(8,128)(2,1)S(1)}, u32[]{:S(2)}, u32[]{:S(2)}) collective-permute-start(bf16[272,512]{1,0:T(8,128)(2,1)S(1)} %slice.724), channel_id=1, source_target_pairs={{0,3},{1,0},{2,1},{3,2},{4,7},{5,4},{6,5},{7,6},{8,11},{9,8},{10,9... | collective-permute-start | bytes 835592 | tf_op jit(solution)/shard_map/ppermute | solution.py:39
  99.7 13.4 %copy-start.17 = (bf16[544,512]{1,0:T(8,128)(2,1)}, bf16[544,512]{1,0:T(8,128)(2,1)S(1)}, u32[]{:S(2)}) copy-start(bf16[544,512]{1,0:T(8,128)(2,1)S(1)} %collective-permute-done.3.behind_ref) | copy-start | bytes 1671172
  99.8 13.4 %collective-permute-start.4 = (bf16[272,512]{1,0:T(8,128)(2,1)S(1)}, bf16[272,512]{1,0:T(8,128)(2,1)S(1)}, u32[]{:S(2)}, u32[]{:S(2)}) collective-permute-start(bf16[272,512]{1,0:T(8,128)(2,1)S(1)} %slice.725), channel_id=1, source_target_pairs={{0,1},{1,2},{2,3},{3,0},{4,5},{5,6},{6,7},{7,4},{8,9},{9,10},{10,1... | collective-permute-start | bytes 835592 | tf_op jit(solution)/shard_map/ppermute | solution.py:39
  102.5 16.5 %collective-permute-start.11 = (bf16[16,16,512]{2,1,0:T(8,128)(2,1)}, bf16[16,16,512]{2,1,0:T(8,128)(2,1)S(1)}, u32[]{:S(2)}, u32[]{:S(2)}) collective-permute-start(bf16[16,16,512]{2,1,0:T(8,128)(2,1)} %get-tuple-element.51), channel_id=1, source_target_pairs={{0,8},{8,16},{16,24},{24,0},{1,9},{9,17},{17,25},{25,1},{2,10},{10... | collective-permute-start | bytes 786440 | tf_op jit(solution)/shard_map/ppermute | solution.py:39
  104.7 14.4 %collective-permute-start.10 = (bf16[16,16,512]{2,1,0:T(8,128)(2,1)}, bf16[16,16,512]{2,1,0:T(8,128)(2,1)S(1)}, u32[]{:S(2)}, u32[]{:S(2)}) collective-permute-start(bf16[16,16,512]{2,1,0:T(8,128)(2,1)} %get-tuple-element.51), channel_id=1, source_target_pairs={{0,16},{8,24},{16,0},{24,8},{1,17},{9,25},{17,1},{25,9},{2,18},{10... | collective-permute-start | bytes 786440 | tf_op jit(solution)/shard_map/ppermute | solution.py:39
  108.7 5.2 %copy-start.21 = (bf16[272,512]{1,0:T(8,128)(2,1)}, bf16[272,512]{1,0:T(8,128)(2,1)S(1)}, u32[]{:S(2)}) copy-start(bf16[272,512]{1,0:T(8,128)(2,1)S(1)} %collective-permute-done.2.top_ref) | copy-start | bytes 835588
  108.7 13.0 %collective-permute-start.9 = (bf16[16,16,512]{2,1,0:T(8,128)(2,1)}, bf16[16,16,512]{2,1,0:T(8,128)(2,1)}, u32[]{:S(2)}, u32[]{:S(2)}) collective-permute-start(bf16[16,16,512]{2,1,0:T(8,128)(2,1)} %get-tuple-element.51), channel_id=1, source_target_pairs={{0,24},{8,0},{16,8},{24,16},{1,25},{9,1},{17,9},{25,17},{2,26},{10... | collective-permute-start | bytes 786440 | tf_op jit(solution)/shard_map/ppermute | solution.py:39
  113.1 0.7 copy-start.22
  113.9 7.8 %copy-start.18 = (bf16[1,16,16,512]{3,2,1,0:T(8,128)(2,1)S(1)}, bf16[1,16,16,512]{3,2,1,0:T(8,128)(2,1)}, u32[]{:S(2)}) copy-start(bf16[1,16,16,512]{3,2,1,0:T(8,128)(2,1)} %get-tuple-element.50) | copy-start | bytes 786436
  119.0 2.6 %copy-start.25 = (bf16[16,16,512]{2,1,0:T(8,128)(2,1)}, bf16[16,16,512]{2,1,0:T(8,128)(2,1)S(1)}, u32[]{:S(2)}) copy-start(bf16[16,16,512]{2,1,0:T(8,128)(2,1)S(1)} %collective-permute-done.11) | copy-start | bytes 786436
  119.0 2.6 %copy-start.26 = (bf16[16,16,512]{2,1,0:T(8,128)(2,1)}, bf16[16,16,512]{2,1,0:T(8,128)(2,1)S(1)}, u32[]{:S(2)}) copy-start(bf16[16,16,512]{2,1,0:T(8,128)(2,1)S(1)} %collective-permute-done.10) | copy-start | bytes 786436
  122.9 6.0 %copy-start.1 = (bf16[256,2048]{1,0:T(8,128)(2,1)S(1)}, bf16[256,2048]{1,0:T(8,128)(2,1)}, u32[]{:S(2)}) copy-start(bf16[256,2048]{1,0:T(8,128)(2,1)} %get-tuple-element.26.out_mat_ref.read_ref) | copy-start | bytes 3145732
  122.9 6.0 %copy-start.4 = (f32[32,1024]{1,0:T(8,128)S(1)}, f32[32,1024]{1,0:T(8,128)}, u32[]{:S(2)}) copy-start(f32[32,1024]{1,0:T(8,128)} %get-tuple-element.73.fwd_im_ref) | copy-start | bytes 393220
  123.0 6.0 %copy-start.5 = (f32[32,1024]{1,0:T(8,128)S(1)}, f32[32,1024]{1,0:T(8,128)}, u32[]{:S(2)}) copy-start(f32[32,1024]{1,0:T(8,128)} %get-tuple-element.74.fwd_re_ref) | copy-start | bytes 393220
  123.0 6.0 %copy-start.9 = (f32[256]{0:T(256)S(1)}, f32[256]{0:T(256)}, u32[]{:S(2)}) copy-start(f32[256]{0:T(256)} %param.28) | copy-start | bytes 3076
  123.0 6.0 %copy-start.10 = (bf16[256,2048]{1,0:T(8,128)(2,1)S(1)}, bf16[256,2048]{1,0:T(8,128)(2,1)}, u32[]{:S(2)}) copy-start(bf16[256,2048]{1,0:T(8,128)(2,1)} %get-tuple-element.25.in_ref) | copy-start | bytes 3145732
  123.0 6.0 %copy-start.11 = (f32[512,256]{1,0:T(8,128)S(1)}, f32[512,256]{1,0:T(8,128)}, u32[]{:S(2)}) copy-start(f32[512,256]{1,0:T(8,128)} %get-tuple-element.23.grow_ref) | copy-start | bytes 1572868
  123.0 6.0 %copy-start.12 = (f32[512,256]{1,0:T(8,128)S(1)}, f32[512,256]{1,0:T(8,128)}, u32[]{:S(2)}) copy-start(f32[512,256]{1,0:T(8,128)} %get-tuple-element.24.shrink_ref) | copy-start | bytes 1572868
  123.0 6.0 %copy-start.13 = (f32[5,16,1024]{2,1,0:T(8,128)S(1)}, f32[5,16,1024]{2,1,0:T(8,128)}, u32[]{:S(2)}) copy-start(f32[5,16,1024]{2,1,0:T(8,128)} %get-tuple-element.27.hop_re_ref) | copy-start | bytes 983044
  123.0 6.0 %copy-start.14 = (f32[5,16,1024]{2,1,0:T(8,128)S(1)}, f32[5,16,1024]{2,1,0:T(8,128)}, u32[]{:S(2)}) copy-start(f32[5,16,1024]{2,1,0:T(8,128)} %get-tuple-element.28.hop_im_ref) | copy-start | bytes 983044
  123.0 67.5 %collective-permute-start.12 = (bf16[4,16,16,512]{3,2,1,0:T(8,128)(2,1)S(1)}, bf16[4,16,16,512]{3,2,1,0:T(8,128)(2,1)}, u32[]{:S(2)}, u32[]{:S(2)}) collective-permute-start(bf16[4,16,16,512]{3,2,1,0:T(8,128)(2,1)S(1)} %pad_maximum_fusion.own_ref), channel_id=1, source_target_pairs={{0,4},{4,0},{1,5},{5,1},{2,6},{6,2},{3,7},{7,3},{8,12},{12,8},{9,1... | collective-permute-start | bytes 3145736 | tf_op jit(solution)/shard_map/ppermute | solution.py:34
  129.1 5.0 %copy-start.31 = (f32[8,128]{1,0:T(8,128)S(1)}, f32[8,128]{1,0:T(8,128)}, u32[]{:S(2)}) copy-start(f32[8,128]{1,0:T(8,128)} %get-tuple-element.32) | copy-start | bytes 12292
  134.7 22.4 %all-to-all-start.2 = ((f32[8,24,128]{2,1,0:T(8,128)}), f32[8,24,128]{2,1,0:T(8,128)S(1)}, u32[]{:S(2)}, u32[]{:S(2)}) async-start(f32[8,24,128]{2,1,0:T(8,128)} %broadcast_in_dim.14), calls=%async_computation.2 | async-start | bytes 196608 | tf_op jit(solution)/shard_map/all_to_all | solution.py:23
  138.7 0.8 copy-start.6
  146.8 42.0 %copy-start.27 = (f32[8,128]{1,0:T(8,128)S(1)}, f32[8,128]{1,0:T(8,128)}, u32[]{:S(2)}) copy-start(f32[8,128]{1,0:T(8,128)} %mul.878) | copy-start | bytes 12292
  146.8 43.8 %copy-start = (bf16[512,2048]{1,0:T(8,128)(2,1)S(1)}, bf16[512,2048]{1,0:T(8,128)(2,1)}, u32[]{:S(2)}) copy-start(bf16[512,2048]{1,0:T(8,128)(2,1)} %get-tuple-element.30.power_ref) | copy-start | bytes 6291460
  146.8 23.4 %collective-permute-start.8 = (f32[2,512]{1,0:T(2,128)S(1)}, f32[2,512]{1,0:T(2,128)S(1)}, u32[]{:S(2)}, u32[]{:S(2)}) collective-permute-start(f32[2,512]{1,0:T(2,128)S(1)} %get-tuple-element.36), channel_id=1, source_target_pairs={{0,1},{1,2},{2,3},{3,0},{4,5},{5,6},{6,7},{7,4},{8,9},{9,10},{10,1... | collective-permute-start | bytes 12296 | tf_op jit(solution)/shard_map/ppermute | solution.py:39
  148.8 21.3 %collective-permute-start.7 = (f32[2,512]{1,0:T(2,128)S(1)}, f32[2,512]{1,0:T(2,128)S(1)}, u32[]{:S(2)}, u32[]{:S(2)}) collective-permute-start(f32[2,512]{1,0:T(2,128)S(1)} %get-tuple-element.36), channel_id=1, source_target_pairs={{0,2},{1,3},{2,0},{3,1},{4,6},{5,7},{6,4},{7,5},{8,10},{9,11},{10,... | collective-permute-start | bytes 12296 | tf_op jit(solution)/shard_map/ppermute | solution.py:39
  155.1 15.0 %collective-permute-start.6 = (f32[2,512]{1,0:T(2,128)S(1)}, f32[2,512]{1,0:T(2,128)S(1)}, u32[]{:S(2)}, u32[]{:S(2)}) collective-permute-start(f32[2,512]{1,0:T(2,128)S(1)} %get-tuple-element.36), channel_id=1, source_target_pairs={{0,3},{1,0},{2,1},{3,2},{4,7},{5,4},{6,5},{7,6},{8,11},{9,8},{10,9... | collective-permute-start | bytes 12296 | tf_op jit(solution)/shard_map/ppermute | solution.py:39
  157.1 13.1 %copy-start.15 = (f32[8,24,128]{2,1,0:T(8,128)}, f32[8,24,128]{2,1,0:T(8,128)S(1)}, u32[]{:S(2)}) copy-start(f32[8,24,128]{2,1,0:T(8,128)S(1)} %all-to-all-done.2) | copy-start | bytes 294916
  157.9 28.4 %all-to-all-start.3 = ((f32[16,24,128]{2,1,0:T(8,128)}), f32[16,24,128]{2,1,0:T(8,128)}, u32[]{:S(2)}, u32[]{:S(2)}) async-start(f32[16,24,128]{2,1,0:T(8,128)} %broadcast_in_dim.17), calls=%async_computation.3 | async-start | bytes 393216 | tf_op jit(solution)/shard_map/all_to_all | solution.py:23
  190.5 1.2 copy-start.2
  191.8 1.0 copy-start.3

commit v5 on v4

--- a/solution.py
+++ b/solution.py
@@ -1,3 +1,5 @@
+import functools
+
 import jax
 import jax.numpy as jnp
 from jax import lax
@@ -386,6 +388,7 @@
 
 
 def merge_kernel(
+    distances,
     place_ref,
     y_ref,
     power_ref,
@@ -400,16 +403,22 @@
 ):
     natural_order(place_ref, own_ref, other_ref, weight_ref, 0, from_own_x=True)
     lanes = h_re_ref.shape[1]
+    block = out_ref.shape[1]
+    parts = y_ref.shape[0] // block
     h_re, h_im = h_re_ref[...], h_im_ref[...]
     c_re, c_im = read_ref[:, :lanes].astype(F32), read_ref[:, lanes:].astype(F32)
-    total = (
-        y_ref[...]
-        + dot_rows(power_ref[:, :lanes], (c_re * h_re + c_im * h_im).astype(BF16))
-        + dot_rows(power_ref[:, lanes:], (c_im * h_re - c_re * h_im).astype(BF16))
-    )
-    ssm = jax.nn.gelu(total).astype(BF16)
-    both = jnp.concatenate([ssm, conv_ref[...]], axis=1)
-    out_ref[...] = dot_rows(both, weight_ref[...]).astype(BF16)
+    blend_re = (c_re * h_re + c_im * h_im).astype(BF16)
+    blend_im = (c_im * h_re - c_re * h_im).astype(BF16)
+    for k, distance in enumerate(distances):
+        rows = pl.ds(pl.multiple_of(lax.rem(place_ref[2] + distance, parts) * block, block), block)
+        total = (
+            y_ref[rows]
+            + dot_rows(power_ref[rows, :lanes], blend_re)
+            + dot_rows(power_ref[rows, lanes:], blend_im)
+        )
+        ssm = jax.nn.gelu(total).astype(BF16)
+        both = jnp.concatenate([ssm, conv_ref[rows]], axis=1)
+        out_ref[k] = dot_rows(both, weight_ref[...]).astype(BF16)
 
 
 def input_matrix(eigen_real, eigen_imag, step, state_input):
@@ -655,29 +664,40 @@
     )
     conv_out = conv_finish(raw, sums, channel_gain)
 
-    product = call(
-        merge_kernel,
-        jax.ShapeDtypeStruct((count, depth), BF16),
-        (
-            y_local,
-            power,
-            h_re.reshape(1, -1),
-            h_im.reshape(1, -1),
-            reads,
-            conv_out,
-            merge_x,
-            merge_other,
-        ),
-        scalars=(place,),
-        scratch=(pltpu.VMEM((depth, 2 * width), BF16),),
-        flops=4 * count * depth * width,
-        bytes_accessed=4 * depth * count,
-        transcendentals=0,
-    )
-    arrived = lax.all_to_all(
-        product.reshape(parts, count // parts, depth), "tp", split_axis=0, concat_axis=0, tiled=True
-    )
-    return arrived.astype(F32).sum(axis=0).astype(BF16)
+    block = count // parts
+    merge_inputs = (
+        y_local,
+        power,
+        h_re.reshape(1, -1),
+        h_im.reshape(1, -1),
+        reads,
+        conv_out,
+        merge_x,
+        merge_other,
+    )
+
+    def products(*distances):
+        return call(
+            functools.partial(merge_kernel, distances),
+            jax.ShapeDtypeStruct((len(distances), block, depth), BF16),
+            merge_inputs,
+            scalars=(place,),
+            scratch=(pltpu.VMEM((depth, 2 * width), BF16),),
+            flops=4 * block * len(distances) * depth * width,
+            bytes_accessed=4 * depth * count,
+            transcendentals=0,
+        )
+
+    opposite = products(2)[0]
+    through_ahead = from_ahead(opposite[: block // 2], "tp", 1)
+    through_behind = from_ahead(opposite[block // 2 :], "tp", -1)
+    mine, to_ahead, to_behind = products(0, 1, 3)
+    empty = jnp.zeros((block // 2, depth), F32)
+    to_behind = to_behind.astype(F32) + jnp.concatenate([through_ahead.astype(F32), empty])
+    to_ahead = to_ahead.astype(F32) + jnp.concatenate([empty, through_behind.astype(F32)])
+    from_next = from_ahead(to_behind.astype(BF16), "tp", 1)
+    from_last = from_ahead(to_ahead.astype(BF16), "tp", -1)
+    return (mine.astype(F32) + from_next.astype(F32) + from_last.astype(F32)).astype(BF16)
 
 
 def finer_mesh(mesh):

time: 229 us -> 229 us (level)
  the two profiles are of different devices: /device:TPU:32 before, /device:TPU:56 now
where the time goes in v5:
time: 229 us; the launch traced here: 227 us
  starting transfers between devices  86.8 us (38%)
  waiting for transfers between devices  81.4 us (36%)
  Pallas kernels  33.8 us (15%)
  local copies, waits for them, and re-layouts  12.9 us (6%)
  other arithmetic  11.5 us (5%)
    all_to_all x4, waiting for transfers between devices, copies(): lax.all_to_all(jnp.broadcast_to(value[None], (peers, *value.shape)), axis...  52.3 us
    ppermute x14, starting transfers between devices, from_ahead(): lax.ppermute(block, axis, [(i, (i - distance) % count) for i in range(cou...  44.9 us
    all_to_all x4, starting transfers between devices, copies(): lax.all_to_all(jnp.broadcast_to(value[None], (peers, *value.shape)), axis...  36 us
    pallas_call x7, Pallas kernels, call(): pl.pallas_call(body, compiler_params=pltpu.CompilerParams(vmem_limit_byte...  33.8 us
    ppermute x14, waiting for transfers between devices, from_ahead(): lax.ppermute(block, axis, [(i, (i - distance) % count) for i in range(cou...  29.1 us
    unnamed x67, local copies, waits for them, and re-layouts  5.37 us
  transfers between devices with their start and end apart: 21, of which 9 were waited for; matrix products, arithmetic and copies ran while one was open for 6% of the time, Pallas kernels for 14%

profile of v5, /device:TPU:56, one launch (start us, length us, event | category | flops | bytes accessed | tf_op | source)
XLA Modules:
  0.0 227.3 jit_solution(2253175310589041950)
XLA Ops:
  0.0 0.8 maximum_bitcast_fusion
  0.8 0.7 pad_maximum_fusion.1
  1.5 0.9 broadcast_in_dim.12
  2.4 15.2 %all-to-all-start = ((bf16[16,16,1280]{2,1,0:T(8,128)(2,1)}), bf16[16,16,1280]{2,1,0:T(8,128)(2,1)S(1)}, u32[]{:S(2)}, u32[]{:S(2)}) async-start(bf16[16,16,1280]{2,1,0:T(8,128)(2,1)} %broadcast_in_dim.12), calls=%async_computation | async-start | bytes 1310720 | tf_op jit(solution)/shard_map/all_to_all | solution.py:25
  18.0 0.7 reshape_squeeze.16
  18.7 0.7 reshape_squeeze.17
  19.4 0.3 multiply_sine_fusion.1
  19.8 1.3 fusion.11
  21.1 7.4 %shard_map.164 = (f32[512,256]{1,0:T(8,128)}, f32[512,256]{1,0:T(8,128)}, bf16[256,2048]{1,0:T(8,128)(2,1)}, bf16[256,2048]{1,0:T(8,128)(2,1)}, f32[5,16,1024]{2...) custom-call(f32[16,512]{1,0:T(8,128)S(1)} %copy-done.8, ...), custom_call_target="tpu_custom_call" | custom-call | flops 83886080 | bytes 4194304 | tf_op jit(solution)/shard_map/pallas_call | solution.py:58
  28.5 23.0 %all-to-all-done = bf16[16,16,1280]{2,1,0:T(8,128)(2,1)S(1)} async-done(((bf16[16,16,1280]{2,1,0:T(8,128)(2,1)}), bf16[16,16,1280]{2,1,0:T(8,128)(2,1)S(1)}, u32[]{:S(2)}, u32[]{:S(2)}) %all-to-all-start) | async-done | bytes 655392 | tf_op jit(solution)/shard_map/all_to_all | solution.py:25
  51.5 1.3 broadcast_in_dim.13
  52.7 4.5 %all-to-all-start.1 = ((bf16[4,16,16,768]{3,2,1,0:T(8,128)(2,1)}), bf16[4,16,16,768]{3,2,1,0:T(8,128)(2,1)}, u32[]{:S(2)}, u32[]{:S(2)}) async-start(bf16[4,16,16,768]{3,2,1,0:T(8,128)(2,1)} %broadcast_in_dim.13), calls=%async_computation.1 | async-start | bytes 3145728 | tf_op jit(solution)/shard_map/all_to_all | solution.py:25
  57.3 1.9 collective-permute-start
  59.2 14.5 %all-to-all-done.1.own_ref = bf16[4,16,16,768]{3,2,1,0:T(8,128)(2,1)} async-done(((bf16[4,16,16,768]{3,2,1,0:T(8,128)(2,1)}), bf16[4,16,16,768]{3,2,1,0:T(8,128)(2,1)}, u32[]{:S(2)}, u32[]{:S(2)}) %all-to-all-start.1) | async-done | bytes 1572896 | tf_op jit(solution)/shard_map/all_to_all | solution.py:25
  73.7 1.9 collective-permute-start.5
  75.7 2.7 %collective-permute-start.1 = (bf16[544,512]{1,0:T(8,128)(2,1)S(1)}, bf16[544,512]{1,0:T(8,128)(2,1)S(1)}, u32[]{:S(2)}, u32[]{:S(2)}) collective-permute-start(bf16[544,512]{1,0:T(8,128)(2,1)S(1)} %constant_dynamic-update-slice_fusion.own_ref), channel_id=1, source_target_pairs={{0,3},{1,0},{2,1},{3,2},{4,7},{5,4},{6,5},{7,6},{8,11},{9,8},{10,9... | collective-permute-start | bytes 1671176 | tf_op jit(solution)/shard_map/ppermute | solution.py:41
  78.4 4.4 %collective-permute-start.3 = (bf16[544,512]{1,0:T(8,128)(2,1)S(1)}, bf16[544,512]{1,0:T(8,128)(2,1)S(1)}, u32[]{:S(2)}, u32[]{:S(2)}) collective-permute-start(bf16[544,512]{1,0:T(8,128)(2,1)S(1)} %constant_dynamic-update-slice_fusion.own_ref), channel_id=1, source_target_pairs={{0,1},{1,2},{2,3},{3,0},{4,5},{5,6},{6,7},{7,4},{8,9},{9,10},{10,1... | collective-permute-start | bytes 1671176 | tf_op jit(solution)/shard_map/ppermute | solution.py:41
  82.8 11.0 %collective-permute-done.1.ahead_ref = bf16[544,512]{1,0:T(8,128)(2,1)S(1)} collective-permute-done((bf16[544,512]{1,0:T(8,128)(2,1)S(1)}, bf16[544,512]{1,0:T(8,128)(2,1)S(1)}, u32[]{:S(2)}, u32[]{:S(2)}) %collective-permute-start.1) | collective-permute-done | bytes 557088 | tf_op jit(solution)/shard_map/ppermute | solution.py:41
  93.8 0.8 copy-done.16
  94.7 1.9 collective-permute-start.2
  96.7 5.1 %collective-permute-start.4 = (bf16[272,512]{1,0:T(8,128)(2,1)S(1)}, bf16[272,512]{1,0:T(8,128)(2,1)S(1)}, u32[]{:S(2)}, u32[]{:S(2)}) collective-permute-start(bf16[272,512]{1,0:T(8,128)(2,1)S(1)} %slice.741), channel_id=1, source_target_pairs={{0,1},{1,2},{2,3},{3,0},{4,5},{5,6},{6,7},{7,4},{8,9},{9,10},{10,1... | collective-permute-start | bytes 835592 | tf_op jit(solution)/shard_map/ppermute | solution.py:41
  101.8 0.9 slice_bitcast_fusion.77
  102.7 2.1 collective-permute-start.11
  104.8 4.0 %collective-permute-start.10 = (bf16[16,16,512]{2,1,0:T(8,128)(2,1)}, bf16[16,16,512]{2,1,0:T(8,128)(2,1)S(1)}, u32[]{:S(2)}, u32[]{:S(2)}) collective-permute-start(bf16[16,16,512]{2,1,0:T(8,128)(2,1)} %get-tuple-element.53), channel_id=1, source_target_pairs={{0,16},{8,24},{16,0},{24,8},{1,17},{9,25},{17,1},{25,9},{2,18},{10... | collective-permute-start | bytes 786440 | tf_op jit(solution)/shard_map/ppermute | solution.py:41
  108.8 2.9 %collective-permute-start.9 = (bf16[16,16,512]{2,1,0:T(8,128)(2,1)}, bf16[16,16,512]{2,1,0:T(8,128)(2,1)S(1)}, u32[]{:S(2)}, u32[]{:S(2)}) collective-permute-start(bf16[16,16,512]{2,1,0:T(8,128)(2,1)} %get-tuple-element.53), channel_id=1, source_target_pairs={{0,24},{8,0},{16,8},{24,16},{1,25},{9,1},{17,9},{25,17},{2,26},{10... | collective-permute-start | bytes 786440 | tf_op jit(solution)/shard_map/ppermute | solution.py:41
  111.8 0.6 mul.844
  112.5 0.7 mul.878
  113.3 0.7 copy-done.22
  114.0 2.5 %shard_map.163.normed_ref = bf16[4,544,512]{2,1,0:T(8,128)(2,1)S(1)} custom-call(s32[3]{0:T(128)S(1)} %pad_add_fusion.place_ref, bf16[544,512]{1,0:T(8,128)(2,1)} %copy-done.19, bf16[544,512]{1,0:T(8,128)(2,1)} %copy-done.16, bf16[272,512]{1,0:T(8,128)(2,1)} %copy-done.21, bf16[272,512]{1,0:T(8,128)(2,1)} %copy-done.22, bf16[544,512]{1,0:T(8,128)(2,1)} %copy-done.17, ...), custom_call_target="tpu_custom_call" | custom-call | flops 8388608 | bytes 4194304 | tf_op jit(solution)/shard_map/pallas_call | solution.py:58
  116.5 2.5 %collective-permute-done.11 = bf16[16,16,512]{2,1,0:T(8,128)(2,1)} collective-permute-done((bf16[16,16,512]{2,1,0:T(8,128)(2,1)}, bf16[16,16,512]{2,1,0:T(8,128)(2,1)}, u32[]{:S(2)}, u32[]{:S(2)}) %collective-permute-start.11) | collective-permute-done | bytes 262176 | tf_op jit(solution)/shard_map/ppermute | solution.py:41
  119.0 2.4 %collective-permute-done.9 = bf16[16,16,512]{2,1,0:T(8,128)(2,1)S(1)} collective-permute-done((bf16[16,16,512]{2,1,0:T(8,128)(2,1)}, bf16[16,16,512]{2,1,0:T(8,128)(2,1)S(1)}, u32[]{:S(2)}, u32[]{:S(2)}) %collective-permute-start.9) | collective-permute-done | bytes 262176 | tf_op jit(solution)/shard_map/ppermute | solution.py:41
  121.4 0.7 copy-done.26
  122.1 1.2 pad_maximum_fusion.own_ref
  123.5 2.2 collective-permute-start.12
  125.7 3.7 %shard_map.165.u_ref = bf16[512,256]{1,0:T(8,128)(2,1)S(1)} custom-call(s32[3]{0:T(128)S(1)} %pad_add_fusion.place_ref, bf16[4,544,512]{2,1,0:T(8,128)(2,1)S(1)} %shard_map.163.normed_ref, bf16[4,16,16,768]{3,2,1,0:T(8,128)(2,1)} %all-to-all-done.1.own_ref, bf16[4,16,16,768]{3,2,1,0:T(8,128)(2,1)} %collective-permute-done.5.other_ref), custom_call_target="tpu_custom_call" | custom-call | flops 536870912 | bytes 4194304 | tf_op jit(solution)/shard_map/pallas_call | solution.py:58
  129.5 4.9 %shard_map.166 = (f32[512,256]{1,0:T(8,128)}, f32[16,128]{1,0:T(8,128)S(1)}) custom-call(bf16[512,256]{1,0:T(8,128)(2,1)S(1)} %shard_map.165.u_ref, f32[512,256]{1,0:T(8,128)S(1)} %copy-done.11, f32[512,256]{1,0:T(8,128)S(1)} %copy-done.12, bf16[256,2048]{1,0:T(8,128)(2,1)S(1)} %copy-done.10, bf16[256,2048]{1,0:T(8,128)(2,1)S(1)} %copy-done.1, ...), custom_call_target="tpu_custom_call" | custom-call | flops 1610612736 | bytes 4194304 | tf_op jit(solution)/shard_map/pallas_call | solution.py:58
  134.4 0.7 broadcast_in_dim.14
  135.1 4.0 %all-to-all-start.2 = ((f32[8,24,128]{2,1,0:T(8,128)}), f32[8,24,128]{2,1,0:T(8,128)S(1)}, u32[]{:S(2)}, u32[]{:S(2)}) async-start(f32[8,24,128]{2,1,0:T(8,128)} %broadcast_in_dim.14), calls=%async_computation.2 | async-start | bytes 196608 | tf_op jit(solution)/shard_map/all_to_all | solution.py:25
  139.1 0.8 copy-done.6
  139.8 7.0 %shard_map.167 = (f32[512,256]{1,0:T(8,128)}, f32[2,512]{1,0:T(2,128)S(1)}) custom-call(s32[3]{0:T(128)S(1)} %pad_add_fusion.place_ref, bf16[4,544,512]{2,1,0:T(8,128)(2,1)S(1)} %shard_map.163.normed_ref, bf16[4,16,16,768]{3,2,1,0:T(8,128)(2,1)} %all-to-all-done.1.own_ref, bf16[4,16,16,768]{3,2,1,0:T(8,128)(2,1)} %collective-permute-done.5.other_ref, ...), custom_call_target="tpu_custom_call" | custom-call | flops 1073741824 | bytes 4194304 | tf_op jit(solution)/shard_map/pallas_call | solution.py:58
  146.9 2.3 %collective-permute-start.8 = (f32[2,512]{1,0:T(2,128)S(1)}, f32[2,512]{1,0:T(2,128)S(1)}, u32[]{:S(2)}, u32[]{:S(2)}) collective-permute-start(f32[2,512]{1,0:T(2,128)S(1)} %get-tuple-element.36), channel_id=1, source_target_pairs={{0,1},{1,2},{2,3},{3,0},{4,5},{5,6},{6,7},{7,4},{8,9},{9,10},{10,1... | collective-permute-start | bytes 12296 | tf_op jit(solution)/shard_map/ppermute | solution.py:41
  149.2 2.8 %collective-permute-start.7 = (f32[2,512]{1,0:T(2,128)S(1)}, f32[2,512]{1,0:T(2,128)S(1)}, u32[]{:S(2)}, u32[]{:S(2)}) collective-permute-start(f32[2,512]{1,0:T(2,128)S(1)} %get-tuple-element.36), channel_id=1, source_target_pairs={{0,2},{1,3},{2,0},{3,1},{4,6},{5,7},{6,4},{7,5},{8,10},{9,11},{10,... | collective-permute-start | bytes 12296 | tf_op jit(solution)/shard_map/ppermute | solution.py:41
  152.0 2.8 %collective-permute-start.6 = (f32[2,512]{1,0:T(2,128)S(1)}, f32[2,512]{1,0:T(2,128)S(1)}, u32[]{:S(2)}, u32[]{:S(2)}) collective-permute-start(f32[2,512]{1,0:T(2,128)S(1)} %get-tuple-element.36), channel_id=1, source_target_pairs={{0,3},{1,0},{2,1},{3,2},{4,7},{5,4},{6,5},{7,6},{8,11},{9,8},{10,9... | collective-permute-start | bytes 12296 | tf_op jit(solution)/shard_map/ppermute | solution.py:41
  154.9 0.7 broadcast_in_dim.17
  155.7 12.3 %all-to-all-start.3 = ((f32[16,24,128]{2,1,0:T(8,128)}), f32[16,24,128]{2,1,0:T(8,128)}, u32[]{:S(2)}, u32[]{:S(2)}) async-start(f32[16,24,128]{2,1,0:T(8,128)} %broadcast_in_dim.17), calls=%async_computation.3 | async-start | bytes 393216 | tf_op jit(solution)/shard_map/all_to_all | solution.py:25
  168.0 1.3 multiply_convert_fusion.conv_ref
  169.3 14.8 %all-to-all-done.3 = f32[16,24,128]{2,1,0:T(8,128)} async-done(((f32[16,24,128]{2,1,0:T(8,128)}), f32[16,24,128]{2,1,0:T(8,128)}, u32[]{:S(2)}, u32[]{:S(2)}) %all-to-all-start.3) | async-done | bytes 196640 | tf_op jit(solution)/shard_map/all_to_all | solution.py:25
  184.1 0.8 fusion.68
  184.9 0.9 fusion.44
  185.7 0.9 fusion.22
  186.6 0.9 select_add_fusion
  187.5 0.8 select_add_fusion.1
  188.3 1.2 copy-done.2
  189.6 1.0 copy-done.3
  190.6 3.1 %shard_map.169 = bf16[1,128,2048]{2,1,0:T(8,128)(2,1)S(1)} custom-call(s32[3]{0:T(128)S(1)} %pad_add_fusion.place_ref, f32[512,256]{1,0:T(8,128)S(1)} %copy-done.3, bf16[512,2048]{1,0:T(8,128)(2,1)S(1)} %copy-done, f32[1,1024]{1,0:T(1,128)S(1)} %bitcast.1094, f32[1,1024]{1,0:T(1,128)S(1)} %bitcast.1092, bf16[256,2048]{1,0:T(8,128)(2,1)S(1)} %copy-done.2, ...), custom_call_target="tpu_custom_call" | custom-call | flops 268435456 | bytes 4194304 | tf_op jit(solution)/shard_map/pallas_call | solution.py:58
  193.8 2.9 %collective-permute-start.13 = (bf16[64,2048]{1,0:T(8,128)(2,1)S(1)}, bf16[64,2048]{1,0:T(8,128)(2,1)S(1)}, u32[]{:S(2)}, u32[]{:S(2)}) collective-permute-start(bf16[64,2048]{1,0:T(8,128)(2,1)S(1)} %get-tuple-element.54), channel_id=1, source_target_pairs={{0,3},{1,0},{2,1},{3,2},{4,7},{5,4},{6,5},{7,6},{8,11},{9,8},{10,9... | collective-permute-start | bytes 786440 | tf_op jit(solution)/shard_map/ppermute | solution.py:41
  196.6 4.2 %collective-permute-start.15 = (bf16[64,2048]{1,0:T(8,128)(2,1)S(1)}, bf16[64,2048]{1,0:T(8,128)(2,1)S(1)}, u32[]{:S(2)}, u32[]{:S(2)}) collective-permute-start(bf16[64,2048]{1,0:T(8,128)(2,1)S(1)} %get-tuple-element.55), channel_id=1, source_target_pairs={{0,1},{1,2},{2,3},{3,0},{4,5},{5,6},{6,7},{7,4},{8,9},{9,10},{10,1... | collective-permute-start | bytes 786440 | tf_op jit(solution)/shard_map/ppermute | solution.py:41
  200.8 5.3 %shard_map.168 = bf16[3,128,2048]{2,1,0:T(8,128)(2,1)S(1)} custom-call(s32[3]{0:T(128)S(1)} %pad_add_fusion.place_ref, f32[512,256]{1,0:T(8,128)S(1)} %copy-done.3, bf16[512,2048]{1,0:T(8,128)(2,1)S(1)} %copy-done, f32[1,1024]{1,0:T(1,128)S(1)} %bitcast.1095, f32[1,1024]{1,0:T(1,128)S(1)} %bitcast.1093, bf16[256,2048]{1,0:T(8,128)(2,1)S(1)} %copy-done.2, ...), custom_call_target="tpu_custom_call" | custom-call | flops 805306368 | bytes 4194304 | tf_op jit(solution)/shard_map/pallas_call | solution.py:58
  206.3 0.2 fusion.1
  206.5 4.9 %collective-permute-start.16 = (bf16[128,2048]{1,0:T(8,128)(2,1)S(1)}, bf16[128,2048]{1,0:T(8,128)(2,1)S(1)}, u32[]{:S(2)}, u32[]{:S(2)}) collective-permute-start(bf16[128,2048]{1,0:T(8,128)(2,1)S(1)} %get-tuple-element.51), channel_id=1, source_target_pairs={{0,1},{1,2},{2,3},{3,0},{4,5},{5,6},{6,7},{7,4},{8,9},{9,10},{10,1... | collective-permute-start | bytes 1572872 | tf_op jit(solution)/shard_map/ppermute | solution.py:41
  211.4 1.9 collective-permute-start.14
  213.3 7.6 %collective-permute-done.16 = bf16[128,2048]{1,0:T(8,128)(2,1)S(1)} collective-permute-done((bf16[128,2048]{1,0:T(8,128)(2,1)S(1)}, bf16[128,2048]{1,0:T(8,128)(2,1)S(1)}, u32[]{:S(2)}, u32[]{:S(2)}) %collective-permute-start.16) | collective-permute-done | bytes 524320 | tf_op jit(solution)/shard_map/ppermute | solution.py:41
  220.9 5.3 %collective-permute-done.14 = bf16[128,2048]{1,0:T(8,128)(2,1)S(1)} collective-permute-done((bf16[128,2048]{1,0:T(8,128)(2,1)S(1)}, bf16[128,2048]{1,0:T(8,128)(2,1)S(1)}, u32[]{:S(2)}, u32[]{:S(2)}) %collective-permute-start.14) | collective-permute-done | bytes 524320 | tf_op jit(solution)/shard_map/ppermute | solution.py:41
  226.3 1.0 fusion.3
  (104 shorter events, 1.3 us)
Async XLA Ops:
  0.0 17.6 %copy-start.32 = (f32[16]{0:T(128)S(1)}, f32[16]{0:T(128)}, u32[]{:S(2)}) copy-start(f32[16]{0:T(128)} %param.24) | copy-start | bytes 196
  0.0 17.7 %copy-start.29 = (f32[16,64]{1,0:T(8,128)S(1)}, f32[16,64]{1,0:T(8,128)}, u32[]{:S(2)}) copy-start(f32[16,64]{1,0:T(8,128)} %param.22) | copy-start | bytes 12292
  0.0 17.7 %copy-start.30 = (f32[16,64]{1,0:T(8,128)S(1)}, f32[16,64]{1,0:T(8,128)}, u32[]{:S(2)}) copy-start(f32[16,64]{1,0:T(8,128)} %param.23) | copy-start | bytes 12292
  0.0 18.0 %copy-start.28 = (f32[2,16,64]{2,1,0:T(8,128)S(1)}, f32[2,16,64]{2,1,0:T(8,128)}, u32[]{:S(2)}) copy-start(f32[2,16,64]{2,1,0:T(8,128)} %param.29) | copy-start | bytes 24580
  0.0 19.3 %copy-start.23 = (f32[2,16,16,64]{3,2,1,0:T(8,128)S(1)}, f32[2,16,16,64]{3,2,1,0:T(8,128)}, u32[]{:S(2)}) copy-start(f32[2,16,16,64]{3,2,1,0:T(8,128)} %param.26) | copy-start | bytes 393220
  1.5 18.2 %copy-start.24 = (f32[2,16,16,64]{3,2,1,0:T(8,128)S(1)}, f32[2,16,16,64]{3,2,1,0:T(8,128)}, u32[]{:S(2)}) copy-start(f32[2,16,16,64]{3,2,1,0:T(8,128)} %param.27) | copy-start | bytes 393220
  2.4 49.0 %all-to-all-start = ((bf16[16,16,1280]{2,1,0:T(8,128)(2,1)}), bf16[16,16,1280]{2,1,0:T(8,128)(2,1)S(1)}, u32[]{:S(2)}, u32[]{:S(2)}) async-start(bf16[16,16,1280]{2,1,0:T(8,128)(2,1)} %broadcast_in_dim.12), calls=%async_computation | async-start | bytes 1310720 | tf_op jit(solution)/shard_map/all_to_all | solution.py:25
  17.6 3.5 %copy-start.8 = (f32[16,512]{1,0:T(8,128)S(1)}, f32[16,512]{1,0:T(8,128)}, u32[]{:S(2)}) copy-start(f32[16,512]{1,0:T(8,128)} %refs_0_.1) | copy-start | bytes 98308
  52.7 4.5 %copy-start.20 = (bf16[512,512]{1,0:T(8,128)(2,1)S(1)}, bf16[512,512]{1,0:T(8,128)(2,1)}, u32[]{:S(2)}) copy-start(bf16[512,512]{1,0:T(8,128)(2,1)} %param.17) | copy-start | bytes 1572868
  52.7 21.0 %all-to-all-start.1 = ((bf16[4,16,16,768]{3,2,1,0:T(8,128)(2,1)}), bf16[4,16,16,768]{3,2,1,0:T(8,128)(2,1)}, u32[]{:S(2)}, u32[]{:S(2)}) async-start(bf16[4,16,16,768]{3,2,1,0:T(8,128)(2,1)} %broadcast_in_dim.13), calls=%async_computation.1 | async-start | bytes 3145728 | tf_op jit(solution)/shard_map/all_to_all | solution.py:25
  57.3 18.4 %collective-permute-start = (bf16[32,512]{1,0:T(8,128)(2,1)S(1)}, bf16[32,512]{1,0:T(8,128)(2,1)S(1)}, u32[]{:S(2)}, u32[]{:S(2)}) collective-permute-start(bf16[32,512]{1,0:T(8,128)(2,1)S(1)} %slice.579), channel_id=1, source_target_pairs={{0,4},{4,8},{8,12},{12,16},{16,20},{20,24},{24,28},{28,32},{32,36}... | collective-permute-start | bytes 98312 | tf_op jit(solution)/shard_map/ppermute | solution.py:32
  73.7 52.0 %collective-permute-start.5 = (bf16[4,16,16,768]{3,2,1,0:T(8,128)(2,1)}, bf16[4,16,16,768]{3,2,1,0:T(8,128)(2,1)}, u32[]{:S(2)}, u32[]{:S(2)}) collective-permute-start(bf16[4,16,16,768]{3,2,1,0:T(8,128)(2,1)} %all-to-all-done.1.own_ref), channel_id=1, source_target_pairs={{0,4},{4,0},{1,5},{5,1},{2,6},{6,2},{3,7},{7,3},{8,12},{12,8},{9,1... | collective-permute-start | bytes 4718600 | tf_op jit(solution)/shard_map/ppermute | solution.py:36
  75.6 38.4 %copy-start.7 = (f32[2048]{0:T(1024)S(1)}, f32[2048]{0:T(1024)}, u32[]{:S(2)}) copy-start(f32[2048]{0:T(1024)} %param.18) | copy-start | bytes 24580
  75.7 37.6 %copy-start.19 = (bf16[544,512]{1,0:T(8,128)(2,1)}, bf16[544,512]{1,0:T(8,128)(2,1)S(1)}, u32[]{:S(2)}) copy-start(bf16[544,512]{1,0:T(8,128)(2,1)S(1)} %constant_dynamic-update-slice_fusion.own_ref) | copy-start | bytes 1671172
  75.7 18.1 %collective-permute-start.1 = (bf16[544,512]{1,0:T(8,128)(2,1)S(1)}, bf16[544,512]{1,0:T(8,128)(2,1)S(1)}, u32[]{:S(2)}, u32[]{:S(2)}) collective-permute-start(bf16[544,512]{1,0:T(8,128)(2,1)S(1)} %constant_dynamic-update-slice_fusion.own_ref), channel_id=1, source_target_pairs={{0,3},{1,0},{2,1},{3,2},{4,7},{5,4},{6,5},{7,6},{8,11},{9,8},{10,9... | collective-permute-start | bytes 1671176 | tf_op jit(solution)/shard_map/ppermute | solution.py:41
  78.4 18.3 %collective-permute-start.3 = (bf16[544,512]{1,0:T(8,128)(2,1)S(1)}, bf16[544,512]{1,0:T(8,128)(2,1)S(1)}, u32[]{:S(2)}, u32[]{:S(2)}) collective-permute-start(bf16[544,512]{1,0:T(8,128)(2,1)S(1)} %constant_dynamic-update-slice_fusion.own_ref), channel_id=1, source_target_pairs={{0,1},{1,2},{2,3},{3,0},{4,5},{5,6},{6,7},{7,4},{8,9},{9,10},{10,1... | collective-permute-start | bytes 1671176 | tf_op jit(solution)/shard_map/ppermute | solution.py:41
  93.8 0.8 copy-start.16
  94.7 14.1 %collective-permute-start.2 = (bf16[272,512]{1,0:T(8,128)(2,1)S(1)}, bf16[272,512]{1,0:T(8,128)(2,1)S(1)}, u32[]{:S(2)}, u32[]{:S(2)}) collective-permute-start(bf16[272,512]{1,0:T(8,128)(2,1)S(1)} %slice.740), channel_id=1, source_target_pairs={{0,3},{1,0},{2,1},{3,2},{4,7},{5,4},{6,5},{7,6},{8,11},{9,8},{10,9... | collective-permute-start | bytes 835592 | tf_op jit(solution)/shard_map/ppermute | solution.py:41
  96.6 16.6 %copy-start.17 = (bf16[544,512]{1,0:T(8,128)(2,1)}, bf16[544,512]{1,0:T(8,128)(2,1)S(1)}, u32[]{:S(2)}) copy-start(bf16[544,512]{1,0:T(8,128)(2,1)S(1)} %collective-permute-done.3.behind_ref) | copy-start | bytes 1671172
  96.7 16.6 %collective-permute-start.4 = (bf16[272,512]{1,0:T(8,128)(2,1)S(1)}, bf16[272,512]{1,0:T(8,128)(2,1)S(1)}, u32[]{:S(2)}, u32[]{:S(2)}) collective-permute-start(bf16[272,512]{1,0:T(8,128)(2,1)S(1)} %slice.741), channel_id=1, source_target_pairs={{0,1},{1,2},{2,3},{3,0},{4,5},{5,6},{6,7},{7,4},{8,9},{9,10},{10,1... | collective-permute-start | bytes 835592 | tf_op jit(solution)/shard_map/ppermute | solution.py:41
  102.7 16.3 %collective-permute-start.11 = (bf16[16,16,512]{2,1,0:T(8,128)(2,1)}, bf16[16,16,512]{2,1,0:T(8,128)(2,1)}, u32[]{:S(2)}, u32[]{:S(2)}) collective-permute-start(bf16[16,16,512]{2,1,0:T(8,128)(2,1)} %get-tuple-element.53), channel_id=1, source_target_pairs={{0,8},{8,16},{16,24},{24,0},{1,9},{9,17},{17,25},{25,1},{2,10},{10... | collective-permute-start | bytes 786440 | tf_op jit(solution)/shard_map/ppermute | solution.py:41
  104.8 14.2 %collective-permute-start.10 = (bf16[16,16,512]{2,1,0:T(8,128)(2,1)}, bf16[16,16,512]{2,1,0:T(8,128)(2,1)S(1)}, u32[]{:S(2)}, u32[]{:S(2)}) collective-permute-start(bf16[16,16,512]{2,1,0:T(8,128)(2,1)} %get-tuple-element.53), channel_id=1, source_target_pairs={{0,16},{8,24},{16,0},{24,8},{1,17},{9,25},{17,1},{25,9},{2,18},{10... | collective-permute-start | bytes 786440 | tf_op jit(solution)/shard_map/ppermute | solution.py:41
  108.8 4.5 %copy-start.21 = (bf16[272,512]{1,0:T(8,128)(2,1)}, bf16[272,512]{1,0:T(8,128)(2,1)S(1)}, u32[]{:S(2)}) copy-start(bf16[272,512]{1,0:T(8,128)(2,1)S(1)} %collective-permute-done.2.top_ref) | copy-start | bytes 835588
  108.8 12.6 %collective-permute-start.9 = (bf16[16,16,512]{2,1,0:T(8,128)(2,1)}, bf16[16,16,512]{2,1,0:T(8,128)(2,1)S(1)}, u32[]{:S(2)}, u32[]{:S(2)}) collective-permute-start(bf16[16,16,512]{2,1,0:T(8,128)(2,1)} %get-tuple-element.53), channel_id=1, source_target_pairs={{0,24},{8,0},{16,8},{24,16},{1,25},{9,1},{17,9},{25,17},{2,26},{10... | collective-permute-start | bytes 786440 | tf_op jit(solution)/shard_map/ppermute | solution.py:41
  113.3 0.7 copy-start.22
  114.0 8.1 %copy-start.18 = (bf16[1,16,16,512]{3,2,1,0:T(8,128)(2,1)S(1)}, bf16[1,16,16,512]{3,2,1,0:T(8,128)(2,1)}, u32[]{:S(2)}) copy-start(bf16[1,16,16,512]{3,2,1,0:T(8,128)(2,1)} %get-tuple-element.52) | copy-start | bytes 786436
  119.0 2.4 %copy-start.25 = (bf16[16,16,512]{2,1,0:T(8,128)(2,1)}, bf16[16,16,512]{2,1,0:T(8,128)(2,1)S(1)}, u32[]{:S(2)}) copy-start(bf16[16,16,512]{2,1,0:T(8,128)(2,1)S(1)} %collective-permute-done.10) | copy-start | bytes 786436
  121.4 0.7 copy-start.26
  123.4 6.0 %copy-start.1 = (bf16[256,2048]{1,0:T(8,128)(2,1)S(1)}, bf16[256,2048]{1,0:T(8,128)(2,1)}, u32[]{:S(2)}) copy-start(bf16[256,2048]{1,0:T(8,128)(2,1)} %get-tuple-element.26.out_mat_ref.read_ref) | copy-start | bytes 3145732
  123.4 6.0 %copy-start.4 = (f32[32,1024]{1,0:T(8,128)S(1)}, f32[32,1024]{1,0:T(8,128)}, u32[]{:S(2)}) copy-start(f32[32,1024]{1,0:T(8,128)} %get-tuple-element.77.fwd_im_ref) | copy-start | bytes 393220
  123.4 6.0 %copy-start.5 = (f32[32,1024]{1,0:T(8,128)S(1)}, f32[32,1024]{1,0:T(8,128)}, u32[]{:S(2)}) copy-start(f32[32,1024]{1,0:T(8,128)} %get-tuple-element.78.fwd_re_ref) | copy-start | bytes 393220
  123.4 6.0 %copy-start.9 = (f32[256]{0:T(256)S(1)}, f32[256]{0:T(256)}, u32[]{:S(2)}) copy-start(f32[256]{0:T(256)} %param.28) | copy-start | bytes 3076
  123.4 6.0 %copy-start.10 = (bf16[256,2048]{1,0:T(8,128)(2,1)S(1)}, bf16[256,2048]{1,0:T(8,128)(2,1)}, u32[]{:S(2)}) copy-start(bf16[256,2048]{1,0:T(8,128)(2,1)} %get-tuple-element.25.in_ref) | copy-start | bytes 3145732
  123.4 6.0 %copy-start.11 = (f32[512,256]{1,0:T(8,128)S(1)}, f32[512,256]{1,0:T(8,128)}, u32[]{:S(2)}) copy-start(f32[512,256]{1,0:T(8,128)} %get-tuple-element.23.grow_ref) | copy-start | bytes 1572868
  123.4 6.0 %copy-start.12 = (f32[512,256]{1,0:T(8,128)S(1)}, f32[512,256]{1,0:T(8,128)}, u32[]{:S(2)}) copy-start(f32[512,256]{1,0:T(8,128)} %get-tuple-element.24.shrink_ref) | copy-start | bytes 1572868
  123.4 6.0 %copy-start.13 = (f32[5,16,1024]{2,1,0:T(8,128)S(1)}, f32[5,16,1024]{2,1,0:T(8,128)}, u32[]{:S(2)}) copy-start(f32[5,16,1024]{2,1,0:T(8,128)} %get-tuple-element.27.hop_re_ref) | copy-start | bytes 983044
  123.5 6.0 %copy-start.14 = (f32[5,16,1024]{2,1,0:T(8,128)S(1)}, f32[5,16,1024]{2,1,0:T(8,128)}, u32[]{:S(2)}) copy-start(f32[5,16,1024]{2,1,0:T(8,128)} %get-tuple-element.28.hop_im_ref) | copy-start | bytes 983044
  123.5 64.9 %collective-permute-start.12 = (bf16[4,16,16,512]{3,2,1,0:T(8,128)(2,1)S(1)}, bf16[4,16,16,512]{3,2,1,0:T(8,128)(2,1)}, u32[]{:S(2)}, u32[]{:S(2)}) collective-permute-start(bf16[4,16,16,512]{3,2,1,0:T(8,128)(2,1)S(1)} %pad_maximum_fusion.own_ref), channel_id=1, source_target_pairs={{0,4},{4,0},{1,5},{5,1},{2,6},{6,2},{3,7},{7,3},{8,12},{12,8},{9,1... | collective-permute-start | bytes 3145736 | tf_op jit(solution)/shard_map/ppermute | solution.py:36
  129.5 4.9 %copy-start.31 = (f32[8,128]{1,0:T(8,128)S(1)}, f32[8,128]{1,0:T(8,128)}, u32[]{:S(2)}) copy-start(f32[8,128]{1,0:T(8,128)} %get-tuple-element.32) | copy-start | bytes 12292
  135.1 19.8 %all-to-all-start.2 = ((f32[8,24,128]{2,1,0:T(8,128)}), f32[8,24,128]{2,1,0:T(8,128)S(1)}, u32[]{:S(2)}, u32[]{:S(2)}) async-start(f32[8,24,128]{2,1,0:T(8,128)} %broadcast_in_dim.14), calls=%async_computation.2 | async-start | bytes 196608 | tf_op jit(solution)/shard_map/all_to_all | solution.py:25
  139.1 0.8 copy-start.6
  146.9 39.7 %copy-start.27 = (f32[8,128]{1,0:T(8,128)S(1)}, f32[8,128]{1,0:T(8,128)}, u32[]{:S(2)}) copy-start(f32[8,128]{1,0:T(8,128)} %mul.878) | copy-start | bytes 12292
  146.9 41.4 %copy-start = (bf16[512,2048]{1,0:T(8,128)(2,1)S(1)}, bf16[512,2048]{1,0:T(8,128)(2,1)}, u32[]{:S(2)}) copy-start(bf16[512,2048]{1,0:T(8,128)(2,1)} %get-tuple-element.30.power_ref) | copy-start | bytes 6291460
  146.9 21.0 %collective-permute-start.8 = (f32[2,512]{1,0:T(2,128)S(1)}, f32[2,512]{1,0:T(2,128)S(1)}, u32[]{:S(2)}, u32[]{:S(2)}) collective-permute-start(f32[2,512]{1,0:T(2,128)S(1)} %get-tuple-element.36), channel_id=1, source_target_pairs={{0,1},{1,2},{2,3},{3,0},{4,5},{5,6},{6,7},{7,4},{8,9},{9,10},{10,1... | collective-permute-start | bytes 12296 | tf_op jit(solution)/shard_map/ppermute | solution.py:41
  149.2 18.7 %collective-permute-start.7 = (f32[2,512]{1,0:T(2,128)S(1)}, f32[2,512]{1,0:T(2,128)S(1)}, u32[]{:S(2)}, u32[]{:S(2)}) collective-permute-start(f32[2,512]{1,0:T(2,128)S(1)} %get-tuple-element.36), channel_id=1, source_target_pairs={{0,2},{1,3},{2,0},{3,1},{4,6},{5,7},{6,4},{7,5},{8,10},{9,11},{10,... | collective-permute-start | bytes 12296 | tf_op jit(solution)/shard_map/ppermute | solution.py:41
  152.0 15.9 %collective-permute-start.6 = (f32[2,512]{1,0:T(2,128)S(1)}, f32[2,512]{1,0:T(2,128)S(1)}, u32[]{:S(2)}, u32[]{:S(2)}) collective-permute-start(f32[2,512]{1,0:T(2,128)S(1)} %get-tuple-element.36), channel_id=1, source_target_pairs={{0,3},{1,0},{2,1},{3,2},{4,7},{5,4},{6,5},{7,6},{8,11},{9,8},{10,9... | collective-permute-start | bytes 12296 | tf_op jit(solution)/shard_map/ppermute | solution.py:41
  154.8 13.2 %copy-start.15 = (f32[8,24,128]{2,1,0:T(8,128)}, f32[8,24,128]{2,1,0:T(8,128)S(1)}, u32[]{:S(2)}) copy-start(f32[8,24,128]{2,1,0:T(8,128)S(1)} %all-to-all-done.2) | copy-start | bytes 294916
  155.7 28.4 %all-to-all-start.3 = ((f32[16,24,128]{2,1,0:T(8,128)}), f32[16,24,128]{2,1,0:T(8,128)}, u32[]{:S(2)}, u32[]{:S(2)}) async-start(f32[16,24,128]{2,1,0:T(8,128)} %broadcast_in_dim.17), calls=%async_computation.3 | async-start | bytes 393216 | tf_op jit(solution)/shard_map/all_to_all | solution.py:25
  188.3 1.2 copy-start.2
  189.6 1.0 copy-start.3
  193.8 12.3 %collective-permute-start.13 = (bf16[64,2048]{1,0:T(8,128)(2,1)S(1)}, bf16[64,2048]{1,0:T(8,128)(2,1)S(1)}, u32[]{:S(2)}, u32[]{:S(2)}) collective-permute-start(bf16[64,2048]{1,0:T(8,128)(2,1)S(1)} %get-tuple-element.54), channel_id=1, source_target_pairs={{0,3},{1,0},{2,1},{3,2},{4,7},{5,4},{6,5},{7,6},{8,11},{9,8},{10,9... | collective-permute-start | bytes 786440 | tf_op jit(solution)/shard_map/ppermute | solution.py:41
  196.6 9.6 %collective-permute-start.15 = (bf16[64,2048]{1,0:T(8,128)(2,1)S(1)}, bf16[64,2048]{1,0:T(8,128)(2,1)S(1)}, u32[]{:S(2)}, u32[]{:S(2)}) collective-permute-start(bf16[64,2048]{1,0:T(8,128)(2,1)S(1)} %get-tuple-element.55), channel_id=1, source_target_pairs={{0,1},{1,2},{2,3},{3,0},{4,5},{5,6},{6,7},{7,4},{8,9},{9,10},{10,1... | collective-permute-start | bytes 786440 | tf_op jit(solution)/shard_map/ppermute | solution.py:41
  206.5 14.5 %collective-permute-start.16 = (bf16[128,2048]{1,0:T(8,128)(2,1)S(1)}, bf16[128,2048]{1,0:T(8,128)(2,1)S(1)}, u32[]{:S(2)}, u32[]{:S(2)}) collective-permute-start(bf16[128,2048]{1,0:T(8,128)(2,1)S(1)} %get-tuple-element.51), channel_id=1, source_target_pairs={{0,1},{1,2},{2,3},{3,0},{4,5},{5,6},{6,7},{7,4},{8,9},{9,10},{10,1... | collective-permute-start | bytes 1572872 | tf_op jit(solution)/shard_map/ppermute | solution.py:41
  211.4 14.8 %collective-permute-start.14 = (bf16[128,2048]{1,0:T(8,128)(2,1)S(1)}, bf16[128,2048]{1,0:T(8,128)(2,1)S(1)}, u32[]{:S(2)}, u32[]{:S(2)}) collective-permute-start(bf16[128,2048]{1,0:T(8,128)(2,1)S(1)} %get-tuple-element.50), channel_id=1, source_target_pairs={{0,3},{1,0},{2,1},{3,2},{4,7},{5,4},{6,5},{7,6},{8,11},{9,8},{10,9... | collective-permute-start | bytes 1572872 | tf_op jit(solution)/shard_map/ppermute | solution.py:41

commit v6 on v5

--- a/solution.py
+++ b/solution.py
@@ -39,11 +39,6 @@
 def from_ahead(block, axis, distance):
     count = lax.axis_size(axis)
     return lax.ppermute(block, axis, [(i, (i - distance) % count) for i in range(count)])
-
-
-def from_own_on(planes, axis):
-    peers = lax.axis_size(axis)
-    return jnp.stack([planes] + [from_ahead(planes, axis, d) for d in range(1, peers)])
 
 
 def far_from_core(*arrays):
@@ -66,18 +61,17 @@
     )(*scalars, *arrays)
 
 
-def natural_order(place_ref, own_ref, other_ref, into_ref, turned, first_lane=0, from_own_x=False):
+def natural_order(place_ref, own_ref, other_ref, into_ref, turned, first_lane=0):
     peers_x, _, rows, _ = own_ref.shape
     blocks = into_ref.shape[0] // rows
     lanes = slice(first_lane, first_lane + into_ref.shape[1])
     core, part = place_ref[0], place_ref[2]
-    place_x = place_ref[1] if from_own_x else 0
     first = part * turned
 
     def place(by_core):
         for k in range(blocks):
             at = lax.rem(first + k, blocks)
-            x = lax.rem(lax.div(at, 2) - place_x + 2 * peers_x, peers_x)
+            x = lax.rem(lax.div(at, 2), peers_x)
             into_ref[k * rows : (k + 1) * rows, :] = by_core[k % 2][
                 x, lax.div(at, 2 * peers_x), :, lanes
             ]
@@ -262,10 +256,10 @@
     shrink_ref[...] = jnp.exp(-narrow)
     spread = spread_over(groups, lanes // groups)
     wide = exact_dot(whole, spread)
-    wide_last = wide[count - 1 :]
     send(0, 1)
-    for k in range(lanes // 128):
-        total_ref[k : k + 1, :] = wide_last[:, k * 128 : (k + 1) * 128]
+    same = lax.broadcasted_iota(jnp.int32, (groups, 128), 0)
+    same = same == lax.broadcasted_iota(jnp.int32, (groups, 128), 1)
+    total_ref[...] = exact_dot(whole[count - 8 :], same.astype(F32))[7:]
     sums = jnp.concatenate([partial[(c + 1) * CHUNK - 1 : (c + 1) * CHUNK] for c in range(chunks)])
     near = exact_dot(sums, spread)
     index = lax.broadcasted_iota(jnp.int32, (chunks, lanes), 0)
@@ -311,6 +305,7 @@
     hop_im_ref,
     lower_ref,
     skip_ref,
+    shift_ref,
     y_ref,
     last_ref,
     cum_re_ref,
@@ -362,11 +357,9 @@
         h_re, h_im = hop_re_ref[level], hop_im_ref[level]
         p_re, p_im = pltpu.roll(s_re, 1 << (level - 1), 0), pltpu.roll(s_im, 1 << (level - 1), 0)
         s_re, s_im = s_re + h_re * p_re - h_im * p_im, s_im + h_re * p_im + h_im * p_re
-    lanes = last_ref.shape[1]
-    for k in range(states // lanes):
-        last_ref[k : k + 1, :] = s_re[chunks - 1 :, k * lanes : (k + 1) * lanes]
-        row = states // lanes + k
-        last_ref[row : row + 1, :] = s_im[chunks - 1 :, k * lanes : (k + 1) * lanes]
+    last_ref[:, :states] = s_re[chunks - 1 :]
+    last_ref[:, states : 2 * states] = s_im[chunks - 1 :]
+    last_ref[:, 2 * states :] = shift_ref[...]
     begins = lax.broadcasted_iota(jnp.int32, s_re.shape, 0) > 0
     end_re_ref[...] = jnp.where(begins, pltpu.roll(s_re, 1, 0), 0.0)
     end_im_ref[...] = jnp.where(begins, pltpu.roll(s_im, 1, 0), 0.0)
@@ -387,25 +380,43 @@
     y_ref[...] = y_ref[...] * grow_ref[...] + skip_ref[...] * u
 
 
-def merge_kernel(
-    distances,
-    place_ref,
-    y_ref,
-    power_ref,
-    h_re_ref,
-    h_im_ref,
-    read_ref,
-    conv_ref,
-    own_ref,
-    other_ref,
-    out_ref,
-    weight_ref,
-):
-    natural_order(place_ref, own_ref, other_ref, weight_ref, 0, from_own_x=True)
-    lanes = h_re_ref.shape[1]
+def shares(rows_ref, rates_ref, count):
+    peers, lanes = rows_ref.shape[0], rates_ref.shape[1]
+    shifts = jnp.concatenate([rows_ref[k][:, 2 * lanes :] for k in range(peers)])
+    groups = lanes // 64
+    sizes = jnp.exp(
+        count * rates_ref[0:1] + exact_dot(shifts[:, :groups], spread_over(groups, lanes // groups))
+    )
+    states = [(rows_ref[k][:, :lanes], rows_ref[k][:, lanes : 2 * lanes]) for k in range(peers)]
+    return shifts, sizes, states
+
+
+def near_kernel(count, place_ref, near_ref, rates_ref, packed_ref, prefix_ref):
+    peers, lanes = near_ref.shape[0], rates_ref.shape[1]
+    place = place_ref[1] * 2 + place_ref[0]
+    shifts, sizes, states = shares(near_ref, rates_ref, count)
+    turn = (rates_ref[1:2], rates_ref[2:3])
+    zero = jnp.zeros((1, lanes), F32)
+    run = before = (zero, zero)
+    decay = (zero + 1.0, zero)
+    for k in range(peers):
+        step = (sizes[k : k + 1] * turn[0], sizes[k : k + 1] * turn[1])
+        passed = k < place
+        decay = tuple(jnp.where(passed, n, o) for n, o in zip(times(step, decay), decay))
+        run = tuple(m + s for m, s in zip(times(step, run), states[k]))
+        before = tuple(jnp.where(passed, n, o) for n, o in zip(run, before))
+    packed_ref[:, :lanes], packed_ref[:, lanes : 2 * lanes] = run
+    packed_ref[:, 2 * lanes :] = jnp.sum(shifts, axis=0, keepdims=True)
+    for k, row in enumerate((*before, *decay)):
+        prefix_ref[k : k + 1] = row
+
+
+def merge_rows(distances, place_ref, h, y_ref, power_ref, read_ref, conv_ref, own_ref, other_ref, out_ref, weight_ref):
+    natural_order(place_ref, own_ref, other_ref, weight_ref, 0)
+    h_re, h_im = h
+    lanes = h_re.shape[1]
     block = out_ref.shape[1]
     parts = y_ref.shape[0] // block
-    h_re, h_im = h_re_ref[...], h_im_ref[...]
     c_re, c_im = read_ref[:, :lanes].astype(F32), read_ref[:, lanes:].astype(F32)
     blend_re = (c_re * h_re + c_im * h_im).astype(BF16)
     blend_im = (c_im * h_re - c_re * h_im).astype(BF16)
@@ -419,6 +430,29 @@
         ssm = jax.nn.gelu(total).astype(BF16)
         both = jnp.concatenate([ssm, conv_ref[rows]], axis=1)
         out_ref[k] = dot_rows(both, weight_ref[...]).astype(BF16)
+
+
+def opposite_kernel(count, place_ref, far_ref, rates_ref, prefix_ref, start_ref, *refs):
+    *inputs, out_ref, h_ref, weight_ref = refs
+    peers_z, peers_near = far_ref.shape[0], 2 * inputs[-1].shape[0]
+    _, sizes, states = shares(far_ref, rates_ref, peers_near * count)
+    turn = (rates_ref[1:2], rates_ref[2:3])
+    for _ in range(peers_near.bit_length() - 1):
+        turn = squared(*turn)
+    h = (start_ref[0:1], start_ref[1:2])
+    for k in range(peers_z):
+        passed = k < place_ref[3]
+        step = (sizes[k : k + 1] * turn[0], sizes[k : k + 1] * turn[1])
+        moved = times(step, h)
+        h = tuple(jnp.where(passed, m + s, o) for m, s, o in zip(moved, states[k], h))
+    moved = times((prefix_ref[2:3], prefix_ref[3:4]), h)
+    h = (moved[0] + prefix_ref[0:1], moved[1] + prefix_ref[1:2])
+    h_ref[0:1], h_ref[1:2] = h
+    merge_rows((2,), place_ref, h, *inputs, out_ref, weight_ref)
+
+
+def rest_kernel(place_ref, h_ref, *refs):
+    merge_rows((0, 1, 3), place_ref, (h_ref[0:1], h_ref[1:2]), *refs)
 
 
 def input_matrix(eigen_real, eigen_imag, step, state_input):
@@ -470,7 +504,7 @@
         pltpu.HBM((levels, chunks, lanes), F32),
         pltpu.HBM((levels, chunks, lanes), F32),
         pltpu.HBM((count, 2 * lanes), BF16),
-        pltpu.HBM((lanes // 128, 128), F32),
+        pltpu.HBM((1, 128), F32),
     )
     grow, shrink, into, out, hop_re, hop_im, power, total = call(
         table_kernel,
@@ -494,61 +528,17 @@
         bytes_accessed=8 * count * lanes,
         transcendentals=count * lanes,
     )
-    device = dict(
-        base=base.reshape(-1, 128),
-        turn=squared(*(r.reshape(-1, 128) for r in whole_turn)),
-        shift=total,
-    )
+    turn = squared(*(r.reshape(1, -1) for r in whole_turn))
+    device = dict(rates=jnp.concatenate([base, *turn]), shift=total)
     scan = (grow, shrink, into, out, *forward, *inverse, hop_re, hop_im, lower_block)
     return scan, power, out, device
 
 
-def pulled(packed, rows):
-    return packed[:rows], packed[rows : 2 * rows], packed[2 * rows :]
-
-
-def carry_in(last, device, count, h):
-    rows = device["base"].shape[0]
-    base, turn = device["base"], device["turn"]
-    plane = ("x", "c")
-    packed = jnp.concatenate([last, device["shift"]])
-    near = copies(packed, plane)
-    peers, place = lax.axis_size(plane), lax.axis_index(plane)
-    zero = jnp.zeros_like(base)
-    run = (zero, zero)
-    before, shift_before = run, zero
-    shift_run = zero
-    for k in range(peers):
-        re, im, shift = pulled(near[k], rows)
-        size = jnp.exp(count * base + shift)
-        moved = times((size * turn[0], size * turn[1]), run)
-        run = (moved[0] + re, moved[1] + im)
-        shift_run = shift_run + shift
-        passed = k < place
-        before = jax.tree.map(lambda new, old: jnp.where(passed, new, old), run, before)
-        shift_before = jnp.where(passed, shift_run, shift_before)
-    far = copies(jnp.concatenate([*run, shift_run]), "z")
-    plane_turn, at = turn, 1
-    while at < peers:
-        plane_turn, at = squared(*plane_turn), at * 2
-    for k in range(lax.axis_size("z")):
-        re, im, shift = pulled(far[k], rows)
-        size = jnp.exp(peers * count * base + shift)
-        moved = times((size * plane_turn[0], size * plane_turn[1]), h)
-        passed = k < lax.axis_index("z")
-        h = tuple(jnp.where(passed, m + s, o) for m, s, o in zip(moved, (re, im), h))
-    turns = (jnp.ones_like(base), zero)
-    for k in range(peers):
-        passed = k < place
-        turns = tuple(jnp.where(passed, new, old) for new, old in zip(times(turns, turn), turns))
-    size = jnp.exp(place * count * base + shift_before)
-    moved = times((size * turns[0], size * turns[1]), h)
-    return moved[0] + before[0], moved[1] + before[1]
-
-
 def conv_finish(raw, sums, channel_gain):
-    others = [from_ahead(sums, "tp", d) for d in range(1, lax.axis_size("tp"))]
-    first, second = (row[:, None] for row in sum(others, sums))
+    for pairs in (((0, 1), (2, 3)), ((0, 3), (1, 2))):
+        route = [*pairs, *((b, a) for a, b in pairs)]
+        sums = sums + lax.ppermute(sums, "tp", route)
+    first, second = (row[:, None] for row in sums)
     middle = first / CONV_W
     spread = second / CONV_W - middle * middle
     scaled = (raw - middle) * lax.rsqrt(spread + EPS) * channel_gain
@@ -574,7 +564,7 @@
     merge_state,
     merge_conv,
 ):
-    place = jnp.stack([lax.axis_index("c"), lax.axis_index("x"), lax.axis_index("tp")]).astype(jnp.int32)
+    place = jnp.stack([lax.axis_index(axis) for axis in ("c", "x", "tp", "z")]).astype(jnp.int32)
     parts = lax.axis_size("tp")
     count, depth_part = tokens.shape
     depth = depth_part * parts
@@ -593,14 +583,11 @@
     scan_tables, power, reads, device = tables(
         eigen_real, eigen_imag, log_step, decay_shift, state_input, readout, width
     )
-    start = tuple(s.reshape(-1, 128) for s in (init_state[0], init_state[1]))
-    planes, total, start = lax.optimization_barrier((planes, device["shift"], start))
-    device["shift"] = total
+    planes, total, rates, start = lax.optimization_barrier(
+        (planes, device["shift"], device["rates"], init_state.reshape(2, -1))
+    )
+    device = dict(shift=total, rates=rates)
     project_x = copies(planes[:, :, : 3 * width], "x")
-    merge_x = from_own_on(planes[:, :, 3 * width :], "x")
-    project_other = partner(project_x)
-    merge_other = partner(merge_x)
-
     normed = call(
         norm_kernel,
         jax.ShapeDtypeStruct((parts, rows, depth_part), BF16),
@@ -611,6 +598,9 @@
         bytes_accessed=4 * count * depth,
         transcendentals=count,
     )
+    project_x, normed = lax.optimization_barrier((project_x, normed))
+    project_other = partner(project_x)
+    merge_x = copies(planes[:, :, 3 * width :], "x")
     u_in = call(
         state_in_kernel,
         jax.ShapeDtypeStruct((count, width), BF16),
@@ -628,9 +618,9 @@
         scan_kernel,
         (
             pltpu.HBM((count, width), F32),
-            jax.ShapeDtypeStruct((2 * lanes // 128, 128), F32),
+            jax.ShapeDtypeStruct((1, 2 * lanes + 128), F32),
         ),
-        (u_in, *scan_tables, skip_gain.reshape(1, -1)),
+        (u_in, *scan_tables, skip_gain.reshape(1, -1), device["shift"]),
         scratch=(
             pltpu.VMEM((count, lanes), F32),
             pltpu.VMEM((count, lanes), F32),
@@ -642,7 +632,23 @@
         bytes_accessed=8 * count * lanes,
         transcendentals=0,
     )
-    h_re, h_im = carry_in(last, device, count, start)
+    last, merge_x = lax.optimization_barrier((last, merge_x))
+    near = copies(last, ("x", "c"))
+    merge_other = partner(merge_x)
+    packed, prefix = call(
+        functools.partial(near_kernel, count),
+        (
+            jax.ShapeDtypeStruct((1, 2 * lanes + 128), F32),
+            jax.ShapeDtypeStruct((4, lanes), F32),
+        ),
+        (near, device["rates"]),
+        scalars=(place,),
+        mib=4,
+        flops=100 * lanes,
+        bytes_accessed=64 * lanes,
+        transcendentals=8 * lanes,
+    )
+    far = copies(packed, "z")
 
     raw, sums = call(
         conv_kernel,
@@ -665,33 +671,30 @@
     conv_out = conv_finish(raw, sums, channel_gain)
 
     block = count // parts
-    merge_inputs = (
-        y_local,
-        power,
-        h_re.reshape(1, -1),
-        h_im.reshape(1, -1),
-        reads,
-        conv_out,
-        merge_x,
-        merge_other,
-    )
-
-    def products(*distances):
+    merge_inputs = (y_local, power, reads, conv_out, merge_x, merge_other)
+
+    def products(kernel, blocks, more, arrays):
         return call(
-            functools.partial(merge_kernel, distances),
-            jax.ShapeDtypeStruct((len(distances), block, depth), BF16),
-            merge_inputs,
+            kernel,
+            (jax.ShapeDtypeStruct((blocks, block, depth), BF16), *more),
+            (*arrays, *merge_inputs),
             scalars=(place,),
             scratch=(pltpu.VMEM((depth, 2 * width), BF16),),
-            flops=4 * block * len(distances) * depth * width,
+            flops=4 * block * blocks * depth * width,
             bytes_accessed=4 * depth * count,
             transcendentals=0,
         )
 
-    opposite = products(2)[0]
+    opposite, h = products(
+        functools.partial(opposite_kernel, count),
+        1,
+        (jax.ShapeDtypeStruct((2, lanes), F32),),
+        (far, device["rates"], prefix, start),
+    )
+    opposite = opposite[0]
     through_ahead = from_ahead(opposite[: block // 2], "tp", 1)
     through_behind = from_ahead(opposite[block // 2 :], "tp", -1)
-    mine, to_ahead, to_behind = products(0, 1, 3)
+    ((mine, to_ahead, to_behind),) = products(rest_kernel, 3, (), (h,))
     empty = jnp.zeros((block // 2, depth), F32)
     to_behind = to_behind.astype(F32) + jnp.concatenate([through_ahead.astype(F32), empty])
     to_ahead = to_ahead.astype(F32) + jnp.concatenate([empty, through_behind.astype(F32)])

time: 229 us -> 218 us (0.952)
  the two profiles are of different devices: /device:TPU:56 before, /device:TPU:6 now
where the time goes in v6:
time: 218 us; the launch traced here: 217 us
  starting transfers between devices  84.6 us (39%)
  waiting for transfers between devices  79.6 us (37%)
  Pallas kernels  35.4 us (16%)
  local copies, waits for them, and re-layouts  10.4 us (5%)
  other arithmetic  6.07 us (3%)
    all_to_all x5, starting transfers between devices, copies(): lax.all_to_all(jnp.broadcast_to(value[None], (peers, *value.shape)), axis...  47.4 us
    all_to_all x5, waiting for transfers between devices, copies(): lax.all_to_all(jnp.broadcast_to(value[None], (peers, *value.shape)), axis...  40.5 us
    pallas_call x8, Pallas kernels, call(): pl.pallas_call(body, compiler_params=pltpu.CompilerParams(vmem_limit_byte...  35.4 us
    ppermute x8, starting transfers between devices, from_ahead(): lax.ppermute(block, axis, [(i, (i - distance) % count) for i in range(cou...  27.5 us
    ppermute x8, waiting for transfers between devices, from_ahead(): lax.ppermute(block, axis, [(i, (i - distance) % count) for i in range(cou...  25 us
    ppermute x2, waiting for transfers between devices, conv_finish(): sums = sums + lax.ppermute(sums, 'tp', route)  8.36 us
    ppermute x1, waiting for transfers between devices, next_along(): return lax.ppermute(block, axis, [(i, i + 1) for i in range(count - 1)])  5.75 us
    unnamed x61, local copies, waits for them, and re-layouts  5.13 us
  transfers between devices with their start and end apart: 18, of which 11 were waited for; matrix products, arithmetic and copies ran while one was open for 3% of the time, Pallas kernels for 15%

profile of v6, /device:TPU:6, one launch (start us, length us, event | category | flops | bytes accessed | tf_op | source)
XLA Modules:
  0.0 216.8 jit_solution(8258888169251188308)
XLA Ops:
  0.0 0.8 maximum_bitcast_fusion
  0.8 0.7 pad_maximum_fusion
  1.5 0.9 broadcast_in_dim.14
  2.4 15.2 %all-to-all-start = ((bf16[16,16,1280]{2,1,0:T(8,128)(2,1)}), bf16[16,16,1280]{2,1,0:T(8,128)(2,1)S(1)}, u32[]{:S(2)}, u32[]{:S(2)}) async-start(bf16[16,16,1280]{2,1,0:T(8,128)(2,1)} %broadcast_in_dim.14), calls=%async_computation | async-start | bytes 1310720 | tf_op jit(solution)/shard_map/all_to_all | solution.py:25
  17.7 0.1 fusion.14
  17.8 0.1 mul.220
  17.9 0.1 reshape.159.refs_1_
  18.0 0.1 mul.192
  18.0 0.1 reshape.160.start_ref
  18.2 0.3 multiply_sine_fusion.1
  18.6 1.3 fusion.11
  19.8 7.4 %shard_map.163 = (f32[512,256]{1,0:T(8,128)}, f32[512,256]{1,0:T(8,128)}, bf16[256,2048]{1,0:T(8,128)(2,1)}, bf16[256,2048]{1,0:T(8,128)(2,1)}, f32[5,16,1024]{2...) custom-call(f32[16,512]{1,0:T(8,128)S(1)} %copy-done.9, ...), custom_call_target="tpu_custom_call" | custom-call | flops 83886080 | bytes 4194304 | tf_op jit(solution)/shard_map/pallas_call | solution.py:53
  27.3 24.0 %all-to-all-done = bf16[16,16,1280]{2,1,0:T(8,128)(2,1)S(1)} async-done(((bf16[16,16,1280]{2,1,0:T(8,128)(2,1)}), bf16[16,16,1280]{2,1,0:T(8,128)(2,1)S(1)}, u32[]{:S(2)}, u32[]{:S(2)}) %all-to-all-start) | async-done | bytes 655392 | tf_op jit(solution)/shard_map/all_to_all | solution.py:25
  51.4 1.3 broadcast_in_dim.15
  52.7 4.9 %all-to-all-start.1 = ((bf16[4,16,16,768]{3,2,1,0:T(8,128)(2,1)}), bf16[4,16,16,768]{3,2,1,0:T(8,128)(2,1)}, u32[]{:S(2)}, u32[]{:S(2)}) async-start(bf16[4,16,16,768]{3,2,1,0:T(8,128)(2,1)} %broadcast_in_dim.15), calls=%async_computation.1 | async-start | bytes 3145728 | tf_op jit(solution)/shard_map/all_to_all | solution.py:25
  57.6 1.9 collective-permute-start
  59.5 5.8 %collective-permute-done = bf16[32,512]{1,0:T(8,128)(2,1)S(1)} collective-permute-done((bf16[32,512]{1,0:T(8,128)(2,1)S(1)}, bf16[32,512]{1,0:T(8,128)(2,1)S(1)}, u32[]{:S(2)}, u32[]{:S(2)}) %collective-permute-start) | collective-permute-done | bytes 32800 | tf_op jit(solution)/shard_map/ppermute | solution.py:32
  65.3 4.9 %collective-permute-start.1 = (bf16[544,512]{1,0:T(8,128)(2,1)S(1)}, bf16[544,512]{1,0:T(8,128)(2,1)S(1)}, u32[]{:S(2)}, u32[]{:S(2)}) collective-permute-start(bf16[544,512]{1,0:T(8,128)(2,1)S(1)} %constant_dynamic-update-slice_fusion.own_ref), channel_id=1, source_target_pairs={{0,3},{1,0},{2,1},{3,2},{4,7},{5,4},{6,5},{7,6},{8,11},{9,8},{10,9... | collective-permute-start | bytes 1671176 | tf_op jit(solution)/shard_map/ppermute | solution.py:41
  70.2 1.9 collective-permute-start.3
  72.2 7.0 %collective-permute-done.1.ahead_ref = bf16[544,512]{1,0:T(8,128)(2,1)S(1)} collective-permute-done((bf16[544,512]{1,0:T(8,128)(2,1)S(1)}, bf16[544,512]{1,0:T(8,128)(2,1)S(1)}, u32[]{:S(2)}, u32[]{:S(2)}) %collective-permute-start.1) | collective-permute-done | bytes 557088 | tf_op jit(solution)/shard_map/ppermute | solution.py:41
  79.2 0.9 copy-done.17
  80.1 5.6 %collective-permute-start.2 = (bf16[272,512]{1,0:T(8,128)(2,1)S(1)}, bf16[272,512]{1,0:T(8,128)(2,1)S(1)}, u32[]{:S(2)}, u32[]{:S(2)}) collective-permute-start(bf16[272,512]{1,0:T(8,128)(2,1)S(1)} %slice.62), channel_id=1, source_target_pairs={{0,3},{1,0},{2,1},{3,2},{4,7},{5,4},{6,5},{7,6},{8,11},{9,8},{10,9... | collective-permute-start | bytes 835592 | tf_op jit(solution)/shard_map/ppermute | solution.py:41
  85.7 0.8 copy-done.18
  86.5 1.9 collective-permute-start.4
  88.5 0.1 pad_add_fusion.place_ref
  88.5 1.2 collective-permute-done.2.top_ref
  89.7 6.4 %collective-permute-done.4.bottom_ref = bf16[272,512]{1,0:T(8,128)(2,1)S(1)} collective-permute-done((bf16[272,512]{1,0:T(8,128)(2,1)S(1)}, bf16[272,512]{1,0:T(8,128)(2,1)S(1)}, u32[]{:S(2)}, u32[]{:S(2)}) %collective-permute-start.4) | collective-permute-done | bytes 278560 | tf_op jit(solution)/shard_map/ppermute | solution.py:41
  96.2 0.7 copy-done.22
  96.9 2.4 %shard_map.164.normed_ref = bf16[4,544,512]{2,1,0:T(8,128)(2,1)S(1)} custom-call(s32[4]{0:T(128)S(1)} %pad_add_fusion.place_ref, bf16[544,512]{1,0:T(8,128)(2,1)} %copy-done.19, bf16[544,512]{1,0:T(8,128)(2,1)} %copy-done.17, bf16[272,512]{1,0:T(8,128)(2,1)} %copy-done.21, bf16[272,512]{1,0:T(8,128)(2,1)} %copy-done.22, bf16[544,512]{1,0:T(8,128)(2,1)} %copy-done.18, ...), custom_call_target="tpu_custom_call" | custom-call | flops 8388608 | bytes 4194304 | tf_op jit(solution)/shard_map/pallas_call | solution.py:53
  99.3 1.9 collective-permute-start.5
  101.3 1.2 broadcast_in_dim.16
  102.5 7.8 %all-to-all-start.2 = ((bf16[4,16,16,512]{3,2,1,0:T(8,128)(2,1)}), bf16[4,16,16,512]{3,2,1,0:T(8,128)(2,1)S(1)}, u32[]{:S(2)}, u32[]{:S(2)}) async-start(bf16[4,16,16,512]{3,2,1,0:T(8,128)(2,1)} %broadcast_in_dim.16), calls=%async_computation.2 | async-start | bytes 2097152 | tf_op jit(solution)/shard_map/all_to_all | solution.py:25
  110.3 0.1 fusion.5.lower_ref
  110.4 0.0 copy-start.12
  110.5 3.9 %shard_map.165.u_ref = bf16[512,256]{1,0:T(8,128)(2,1)S(1)} custom-call(s32[4]{0:T(128)S(1)} %pad_add_fusion.place_ref, bf16[4,544,512]{2,1,0:T(8,128)(2,1)S(1)} %shard_map.164.normed_ref, bf16[4,16,16,768]{3,2,1,0:T(8,128)(2,1)} %all-to-all-done.1.own_ref, bf16[4,16,16,768]{3,2,1,0:T(8,128)(2,1)} %collective-permute-done.5.other_ref), custom_call_target="tpu_custom_call" | custom-call | flops 536870912 | bytes 4194304 | tf_op jit(solution)/shard_map/pallas_call | solution.py:53
  114.5 0.0 copy-start.7
  114.5 5.0 %shard_map.166 = (f32[512,256]{1,0:T(8,128)}, f32[1,2176]{1,0:T(1,128)S(1)}) custom-call(bf16[512,256]{1,0:T(8,128)(2,1)S(1)} %shard_map.165.u_ref, f32[512,256]{1,0:T(8,128)S(1)} %copy-done.12, f32[512,256]{1,0:T(8,128)S(1)} %copy-done.13, bf16[256,2048]{1,0:T(8,128)(2,1)S(1)} %copy-done.11, bf16[256,2048]{1,0:T(8,128)(2,1)S(1)} %copy-done.1, ...), custom_call_target="tpu_custom_call" | custom-call | flops 1610612736 | bytes 4194304 | tf_op jit(solution)/shard_map/pallas_call | solution.py:53
  119.5 4.5 %all-to-all-done.2.refs_4_ = bf16[4,16,16,512]{3,2,1,0:T(8,128)(2,1)S(1)} async-done(((bf16[4,16,16,512]{3,2,1,0:T(8,128)(2,1)}), bf16[4,16,16,512]{3,2,1,0:T(8,128)(2,1)S(1)}, u32[]{:S(2)}, u32[]{:S(2)}) %all-to-all-start.2) | async-done | bytes 1048608 | tf_op jit(solution)/shard_map/all_to_all | solution.py:25
  124.0 1.9 collective-permute-start.8
  125.9 0.7 broadcast_in_dim.18
  126.6 5.4 %all-to-all-start.3 = ((f32[8,1,2176]{2,1,0:T(1,128)}), f32[8,1,2176]{2,1,0:T(1,128)S(1)}, u32[]{:S(2)}, u32[]{:S(2)}) async-start(f32[8,1,2176]{2,1,0:T(1,128)} %broadcast_in_dim.18), calls=%async_computation.3 | async-start | bytes 139264 | tf_op jit(solution)/shard_map/all_to_all | solution.py:25
  131.9 7.2 %shard_map.168 = (f32[512,256]{1,0:T(8,128)}, f32[2,512]{1,0:T(2,128)S(1)}) custom-call(s32[4]{0:T(128)S(1)} %pad_add_fusion.place_ref, bf16[4,544,512]{2,1,0:T(8,128)(2,1)S(1)} %shard_map.164.normed_ref, bf16[4,16,16,768]{3,2,1,0:T(8,128)(2,1)} %all-to-all-done.1.own_ref, bf16[4,16,16,768]{3,2,1,0:T(8,128)(2,1)} %collective-permute-done.5.other_ref, ...), custom_call_target="tpu_custom_call" | custom-call | flops 1073741824 | bytes 4194304 | tf_op jit(solution)/shard_map/pallas_call | solution.py:53
  139.1 0.0 copy-start.2
  139.1 2.1 collective-permute-start.6
  141.2 3.6 %collective-permute-done.6 = f32[2,512]{1,0:T(2,128)S(1)} collective-permute-done((f32[2,512]{1,0:T(2,128)S(1)}, f32[2,512]{1,0:T(2,128)S(1)}, u32[]{:S(2)}, u32[]{:S(2)}) %collective-permute-start.6) | collective-permute-done | bytes 4128 | tf_op jit(solution)/shard_map/ppermute | solution.py:540
  144.8 1.9 collective-permute-start.7
  146.7 4.8 %collective-permute-done.7 = f32[2,512]{1,0:T(2,128)S(1)} collective-permute-done((f32[2,512]{1,0:T(2,128)S(1)}, f32[2,512]{1,0:T(2,128)S(1)}, u32[]{:S(2)}, u32[]{:S(2)}) %collective-permute-start.7) | collective-permute-done | bytes 4128 | tf_op jit(solution)/shard_map/ppermute | solution.py:540
  151.5 0.9 shard_map.167
  152.4 0.7 broadcast_in_dim.20
  153.2 14.1 %all-to-all-start.4 = ((f32[16,1,2176]{2,1,0:T(1,128)}), f32[16,1,2176]{2,1,0:T(1,128)S(1)}, u32[]{:S(2)}, u32[]{:S(2)}) async-start(f32[16,1,2176]{2,1,0:T(1,128)} %broadcast_in_dim.20), calls=%async_computation.4 | async-start | bytes 278528 | tf_op jit(solution)/shard_map/all_to_all | solution.py:25
  167.3 1.3 multiply_convert_fusion.refs_3_
  168.6 12.0 %all-to-all-done.4.far_ref = f32[16,1,2176]{2,1,0:T(1,128)S(1)} async-done(((f32[16,1,2176]{2,1,0:T(1,128)}), f32[16,1,2176]{2,1,0:T(1,128)S(1)}, u32[]{:S(2)}, u32[]{:S(2)}) %all-to-all-start.4) | async-done | bytes 139296 | tf_op jit(solution)/shard_map/all_to_all | solution.py:25
  180.6 1.6 copy-done
  182.2 1.0 copy-done.3
  183.2 3.5 %shard_map.169 = (bf16[1,128,2048]{2,1,0:T(8,128)(2,1)S(1)}, f32[2,1024]{1,0:T(2,128)S(1)}) custom-call(s32[4]{0:T(128)S(1)} %pad_add_fusion.place_ref, f32[16,1,2176]{2,1,0:T(1,128)S(1)} %all-to-all-done.4.far_ref, f32[3,1024]{1,0:T(4,128)S(1)} %pad_maximum_fusion.1.rates_ref, f32[4,1024]{1,0:T(4,128)S(1)} %get-tuple-element.44.prefix_ref, ...), custom_call_target="tpu_custom_call" | custom-call | flops 268435456 | bytes 4194304 | tf_op jit(solution)/shard_map/pallas_call | solution.py:53
  186.8 1.9 collective-permute-start.11
  188.7 5.1 %collective-permute-start.9 = (bf16[64,2048]{1,0:T(8,128)(2,1)S(1)}, bf16[64,2048]{1,0:T(8,128)(2,1)S(1)}, u32[]{:S(2)}, u32[]{:S(2)}) collective-permute-start(bf16[64,2048]{1,0:T(8,128)(2,1)S(1)} %get-tuple-element.55), channel_id=1, source_target_pairs={{0,3},{1,0},{2,1},{3,2},{4,7},{5,4},{6,5},{7,6},{8,11},{9,8},{10,9... | collective-permute-start | bytes 786440 | tf_op jit(solution)/shard_map/ppermute | solution.py:41
  193.8 5.2 %shard_map.170 = bf16[3,128,2048]{2,1,0:T(8,128)(2,1)S(1)} custom-call(s32[4]{0:T(128)S(1)} %pad_add_fusion.place_ref, f32[2,1024]{1,0:T(2,128)S(1)} %get-tuple-element.51.h_ref, f32[512,256]{1,0:T(8,128)S(1)} %copy-done.3, bf16[512,2048]{1,0:T(8,128)(2,1)S(1)} %copy-done, bf16[256,2048]{1,0:T(8,128)(2,1)S(1)} %copy-done.2, ...), custom_call_target="tpu_custom_call" | custom-call | flops 805306368 | bytes 4194304 | tf_op jit(solution)/shard_map/pallas_call | solution.py:53
  199.1 0.2 fusion.1
  199.3 4.2 %collective-permute-start.10 = (bf16[128,2048]{1,0:T(8,128)(2,1)S(1)}, bf16[128,2048]{1,0:T(8,128)(2,1)S(1)}, u32[]{:S(2)}, u32[]{:S(2)}) collective-permute-start(bf16[128,2048]{1,0:T(8,128)(2,1)S(1)} %get-tuple-element.53), channel_id=1, source_target_pairs={{0,3},{1,0},{2,1},{3,2},{4,7},{5,4},{6,5},{7,6},{8,11},{9,8},{10,9... | collective-permute-start | bytes 1572872 | tf_op jit(solution)/shard_map/ppermute | solution.py:41
  203.5 1.9 collective-permute-start.12
  205.4 5.3 %collective-permute-done.10 = bf16[128,2048]{1,0:T(8,128)(2,1)S(1)} collective-permute-done((bf16[128,2048]{1,0:T(8,128)(2,1)S(1)}, bf16[128,2048]{1,0:T(8,128)(2,1)S(1)}, u32[]{:S(2)}, u32[]{:S(2)}) %collective-permute-start.10) | collective-permute-done | bytes 524320 | tf_op jit(solution)/shard_map/ppermute | solution.py:41
  210.7 5.1 %collective-permute-done.12 = bf16[128,2048]{1,0:T(8,128)(2,1)S(1)} collective-permute-done((bf16[128,2048]{1,0:T(8,128)(2,1)S(1)}, bf16[128,2048]{1,0:T(8,128)(2,1)S(1)}, u32[]{:S(2)}, u32[]{:S(2)}) %collective-permute-start.12) | collective-permute-done | bytes 524320 | tf_op jit(solution)/shard_map/ppermute | solution.py:41
  215.8 1.0 fusion.3
  (82 shorter events, 0.5 us)
Async XLA Ops:
  0.0 17.6 %copy-start.29 = (f32[16]{0:T(128)S(1)}, f32[16]{0:T(128)}, u32[]{:S(2)}) copy-start(f32[16]{0:T(128)} %param.24) | copy-start | bytes 196
  0.0 17.7 %copy-start.27 = (f32[16,64]{1,0:T(8,128)S(1)}, f32[16,64]{1,0:T(8,128)}, u32[]{:S(2)}) copy-start(f32[16,64]{1,0:T(8,128)} %param.22) | copy-start | bytes 12292
  0.0 17.7 %copy-start.26 = (f32[16,64]{1,0:T(8,128)S(1)}, f32[16,64]{1,0:T(8,128)}, u32[]{:S(2)}) copy-start(f32[16,64]{1,0:T(8,128)} %param.23) | copy-start | bytes 12292
  0.0 18.0 %copy-start.25 = (f32[2,16,64]{2,1,0:T(8,128)S(1)}, f32[2,16,64]{2,1,0:T(8,128)}, u32[]{:S(2)}) copy-start(f32[2,16,64]{2,1,0:T(8,128)} %param.29) | copy-start | bytes 24580
  0.0 18.1 %copy-start.23 = (f32[2,16,16,64]{3,2,1,0:T(8,128)S(1)}, f32[2,16,16,64]{3,2,1,0:T(8,128)}, u32[]{:S(2)}) copy-start(f32[2,16,16,64]{3,2,1,0:T(8,128)} %param.26) | copy-start | bytes 393220
  1.5 17.0 %copy-start.24 = (f32[2,16,16,64]{3,2,1,0:T(8,128)S(1)}, f32[2,16,16,64]{3,2,1,0:T(8,128)}, u32[]{:S(2)}) copy-start(f32[2,16,16,64]{3,2,1,0:T(8,128)} %param.27) | copy-start | bytes 393220
  2.4 48.9 %all-to-all-start = ((bf16[16,16,1280]{2,1,0:T(8,128)(2,1)}), bf16[16,16,1280]{2,1,0:T(8,128)(2,1)S(1)}, u32[]{:S(2)}, u32[]{:S(2)}) async-start(bf16[16,16,1280]{2,1,0:T(8,128)(2,1)} %broadcast_in_dim.14), calls=%async_computation | async-start | bytes 1310720 | tf_op jit(solution)/shard_map/all_to_all | solution.py:25
  17.6 2.2 %copy-start.9 = (f32[16,512]{1,0:T(8,128)S(1)}, f32[16,512]{1,0:T(8,128)}, u32[]{:S(2)}) copy-start(f32[16,512]{1,0:T(8,128)} %refs_0_.1) | copy-start | bytes 98308
  52.6 4.9 %copy-start.20 = (bf16[512,512]{1,0:T(8,128)(2,1)S(1)}, bf16[512,512]{1,0:T(8,128)(2,1)}, u32[]{:S(2)}) copy-start(bf16[512,512]{1,0:T(8,128)(2,1)} %param.17) | copy-start | bytes 1572868
  52.7 46.6 %all-to-all-start.1 = ((bf16[4,16,16,768]{3,2,1,0:T(8,128)(2,1)}), bf16[4,16,16,768]{3,2,1,0:T(8,128)(2,1)}, u32[]{:S(2)}, u32[]{:S(2)}) async-start(bf16[4,16,16,768]{3,2,1,0:T(8,128)(2,1)} %broadcast_in_dim.15), calls=%async_computation.1 | async-start | bytes 3145728 | tf_op jit(solution)/shard_map/all_to_all | solution.py:25
  57.6 39.3 %copy-start.8 = (f32[2048]{0:T(1024)S(1)}, f32[2048]{0:T(1024)}, u32[]{:S(2)}) copy-start(f32[2048]{0:T(1024)} %param.18) | copy-start | bytes 24580
  57.6 7.7 %collective-permute-start = (bf16[32,512]{1,0:T(8,128)(2,1)S(1)}, bf16[32,512]{1,0:T(8,128)(2,1)S(1)}, u32[]{:S(2)}, u32[]{:S(2)}) collective-permute-start(bf16[32,512]{1,0:T(8,128)(2,1)S(1)} %slice.52), channel_id=1, source_target_pairs={{0,4},{4,8},{8,12},{12,16},{16,20},{20,24},{24,28},{28,32},{32,36}... | collective-permute-start | bytes 98312 | tf_op jit(solution)/shard_map/ppermute | solution.py:32
  65.3 21.2 %copy-start.19 = (bf16[544,512]{1,0:T(8,128)(2,1)}, bf16[544,512]{1,0:T(8,128)(2,1)S(1)}, u32[]{:S(2)}) copy-start(bf16[544,512]{1,0:T(8,128)(2,1)S(1)} %constant_dynamic-update-slice_fusion.own_ref) | copy-start | bytes 1671172
  65.3 13.8 %collective-permute-start.1 = (bf16[544,512]{1,0:T(8,128)(2,1)S(1)}, bf16[544,512]{1,0:T(8,128)(2,1)S(1)}, u32[]{:S(2)}, u32[]{:S(2)}) collective-permute-start(bf16[544,512]{1,0:T(8,128)(2,1)S(1)} %constant_dynamic-update-slice_fusion.own_ref), channel_id=1, source_target_pairs={{0,3},{1,0},{2,1},{3,2},{4,7},{5,4},{6,5},{7,6},{8,11},{9,8},{10,9... | collective-permute-start | bytes 1671176 | tf_op jit(solution)/shard_map/ppermute | solution.py:41
  70.2 15.4 %collective-permute-start.3 = (bf16[544,512]{1,0:T(8,128)(2,1)S(1)}, bf16[544,512]{1,0:T(8,128)(2,1)S(1)}, u32[]{:S(2)}, u32[]{:S(2)}) collective-permute-start(bf16[544,512]{1,0:T(8,128)(2,1)S(1)} %constant_dynamic-update-slice_fusion.own_ref), channel_id=1, source_target_pairs={{0,1},{1,2},{2,3},{3,0},{4,5},{5,6},{6,7},{7,4},{8,9},{9,10},{10,1... | collective-permute-start | bytes 1671176 | tf_op jit(solution)/shard_map/ppermute | solution.py:41
  79.2 0.9 copy-start.17
  80.1 9.7 %collective-permute-start.2 = (bf16[272,512]{1,0:T(8,128)(2,1)S(1)}, bf16[272,512]{1,0:T(8,128)(2,1)S(1)}, u32[]{:S(2)}, u32[]{:S(2)}) collective-permute-start(bf16[272,512]{1,0:T(8,128)(2,1)S(1)} %slice.62), channel_id=1, source_target_pairs={{0,3},{1,0},{2,1},{3,2},{4,7},{5,4},{6,5},{7,6},{8,11},{9,8},{10,9... | collective-permute-start | bytes 835592 | tf_op jit(solution)/shard_map/ppermute | solution.py:41
  85.7 0.8 copy-start.18
  86.5 9.7 %collective-permute-start.4 = (bf16[272,512]{1,0:T(8,128)(2,1)S(1)}, bf16[272,512]{1,0:T(8,128)(2,1)S(1)}, u32[]{:S(2)}, u32[]{:S(2)}) collective-permute-start(bf16[272,512]{1,0:T(8,128)(2,1)S(1)} %slice.63), channel_id=1, source_target_pairs={{0,1},{1,2},{2,3},{3,0},{4,5},{5,6},{6,7},{7,4},{8,9},{9,10},{10,1... | collective-permute-start | bytes 835592 | tf_op jit(solution)/shard_map/ppermute | solution.py:41
  89.7 7.2 %copy-start.21 = (bf16[272,512]{1,0:T(8,128)(2,1)}, bf16[272,512]{1,0:T(8,128)(2,1)S(1)}, u32[]{:S(2)}) copy-start(bf16[272,512]{1,0:T(8,128)(2,1)S(1)} %collective-permute-done.2.top_ref) | copy-start | bytes 835588
  96.2 0.7 copy-start.22
  99.3 11.2 %collective-permute-start.5 = (bf16[4,16,16,768]{3,2,1,0:T(8,128)(2,1)}, bf16[4,16,16,768]{3,2,1,0:T(8,128)(2,1)}, u32[]{:S(2)}, u32[]{:S(2)}) collective-permute-start(bf16[4,16,16,768]{3,2,1,0:T(8,128)(2,1)} %all-to-all-done.1.own_ref), channel_id=1, source_target_pairs={{0,4},{4,0},{1,5},{5,1},{2,6},{6,2},{3,7},{7,3},{8,12},{12,8},{9,1... | collective-permute-start | bytes 4718600 | tf_op jit(solution)/shard_map/ppermute | solution.py:36
  102.5 21.5 %all-to-all-start.2 = ((bf16[4,16,16,512]{3,2,1,0:T(8,128)(2,1)}), bf16[4,16,16,512]{3,2,1,0:T(8,128)(2,1)S(1)}, u32[]{:S(2)}, u32[]{:S(2)}) async-start(bf16[4,16,16,512]{3,2,1,0:T(8,128)(2,1)} %broadcast_in_dim.16), calls=%async_computation.2 | async-start | bytes 2097152 | tf_op jit(solution)/shard_map/all_to_all | solution.py:25
  110.4 4.0 %copy-start.1 = (bf16[256,2048]{1,0:T(8,128)(2,1)S(1)}, bf16[256,2048]{1,0:T(8,128)(2,1)}, u32[]{:S(2)}) copy-start(bf16[256,2048]{1,0:T(8,128)(2,1)} %get-tuple-element.36.out_mat_ref.refs_2_) | copy-start | bytes 3145732
  110.4 4.0 %copy-start.4 = (f32[32,1024]{1,0:T(8,128)S(1)}, f32[32,1024]{1,0:T(8,128)}, u32[]{:S(2)}) copy-start(f32[32,1024]{1,0:T(8,128)} %get-tuple-element.68.inv_re_ref) | copy-start | bytes 393220
  110.4 4.0 %copy-start.5 = (f32[32,1024]{1,0:T(8,128)S(1)}, f32[32,1024]{1,0:T(8,128)}, u32[]{:S(2)}) copy-start(f32[32,1024]{1,0:T(8,128)} %get-tuple-element.69.fwd_im_ref) | copy-start | bytes 393220
  110.4 4.0 %copy-start.6 = (f32[32,1024]{1,0:T(8,128)S(1)}, f32[32,1024]{1,0:T(8,128)}, u32[]{:S(2)}) copy-start(f32[32,1024]{1,0:T(8,128)} %get-tuple-element.70.fwd_re_ref) | copy-start | bytes 393220
  110.4 4.0 %copy-start.10 = (f32[256]{0:T(256)S(1)}, f32[256]{0:T(256)}, u32[]{:S(2)}) copy-start(f32[256]{0:T(256)} %param.28) | copy-start | bytes 3076
  110.4 4.0 %copy-start.11 = (bf16[256,2048]{1,0:T(8,128)(2,1)S(1)}, bf16[256,2048]{1,0:T(8,128)(2,1)}, u32[]{:S(2)}) copy-start(bf16[256,2048]{1,0:T(8,128)(2,1)} %get-tuple-element.35.in_ref) | copy-start | bytes 3145732
  110.4 4.0 %copy-start.12 = (f32[512,256]{1,0:T(8,128)S(1)}, f32[512,256]{1,0:T(8,128)}, u32[]{:S(2)}) copy-start(f32[512,256]{1,0:T(8,128)} %get-tuple-element.33.grow_ref) | copy-start | bytes 1572868
  110.5 4.0 %copy-start.13 = (f32[512,256]{1,0:T(8,128)S(1)}, f32[512,256]{1,0:T(8,128)}, u32[]{:S(2)}) copy-start(f32[512,256]{1,0:T(8,128)} %get-tuple-element.34.shrink_ref) | copy-start | bytes 1572868
  110.5 4.0 %copy-start.14 = (f32[5,16,1024]{2,1,0:T(8,128)S(1)}, f32[5,16,1024]{2,1,0:T(8,128)}, u32[]{:S(2)}) copy-start(f32[5,16,1024]{2,1,0:T(8,128)} %get-tuple-element.37.hop_re_ref) | copy-start | bytes 983044
  110.5 4.0 %copy-start.15 = (f32[5,16,1024]{2,1,0:T(8,128)S(1)}, f32[5,16,1024]{2,1,0:T(8,128)}, u32[]{:S(2)}) copy-start(f32[5,16,1024]{2,1,0:T(8,128)} %get-tuple-element.38.hop_im_ref) | copy-start | bytes 983044
  110.5 4.0 %copy-start.16 = (f32[1,128]{1,0:T(1,128)S(1)}, f32[1,128]{1,0:T(1,128)}, u32[]{:S(2)}) copy-start(f32[1,128]{1,0:T(1,128)} %get-tuple-element.39.shift_ref) | copy-start | bytes 1540
  114.5 17.5 %copy-start.7 = (f32[31,256]{1,0:T(8,128)S(1)}, f32[31,256]{1,0:T(8,128)}, u32[]{:S(2)}) copy-start(f32[31,256]{1,0:T(8,128)} %taps_ref.1) | copy-start | bytes 95236
  124.0 56.6 %collective-permute-start.8 = (bf16[4,16,16,512]{3,2,1,0:T(8,128)(2,1)S(1)}, bf16[4,16,16,512]{3,2,1,0:T(8,128)(2,1)}, u32[]{:S(2)}, u32[]{:S(2)}) collective-permute-start(bf16[4,16,16,512]{3,2,1,0:T(8,128)(2,1)S(1)} %all-to-all-done.2.refs_4_), channel_id=1, source_target_pairs={{0,4},{4,0},{1,5},{5,1},{2,6},{6,2},{3,7},{7,3},{8,12},{12,8},{9,1... | collective-permute-start | bytes 3145736 | tf_op jit(solution)/shard_map/ppermute | solution.py:36
  126.6 24.9 %all-to-all-start.3 = ((f32[8,1,2176]{2,1,0:T(1,128)}), f32[8,1,2176]{2,1,0:T(1,128)S(1)}, u32[]{:S(2)}, u32[]{:S(2)}) async-start(f32[8,1,2176]{2,1,0:T(1,128)} %broadcast_in_dim.18), calls=%async_computation.3 | async-start | bytes 139264 | tf_op jit(solution)/shard_map/all_to_all | solution.py:25
  131.9 35.3 %copy-start.28 = (f32[256]{0:T(256)S(1)}, f32[256]{0:T(256)}, u32[]{:S(2)}) copy-start(f32[256]{0:T(256)} %param.31) | copy-start | bytes 3076
  139.1 41.5 %copy-start.2 = (bf16[256,2048]{1,0:T(8,128)(2,1)S(1)}, bf16[256,2048]{1,0:T(8,128)(2,1)}, u32[]{:S(2)}) copy-start(bf16[256,2048]{1,0:T(8,128)(2,1)} %get-tuple-element.36.out_mat_ref.refs_2_) | copy-start | bytes 3145732
  139.1 5.6 %collective-permute-start.6 = (f32[2,512]{1,0:T(2,128)S(1)}, f32[2,512]{1,0:T(2,128)S(1)}, u32[]{:S(2)}, u32[]{:S(2)}) collective-permute-start(f32[2,512]{1,0:T(2,128)S(1)} %get-tuple-element.49), channel_id=1, source_target_pairs={{0,1},{2,3},{1,0},{3,2},{4,5},{6,7},{5,4},{7,6},{8,9},{10,11},{9,8... | collective-permute-start | bytes 12296 | tf_op jit(solution)/shard_map/ppermute | solution.py:540
  144.8 6.7 %collective-permute-start.7 = (f32[2,512]{1,0:T(2,128)S(1)}, f32[2,512]{1,0:T(2,128)S(1)}, u32[]{:S(2)}, u32[]{:S(2)}) collective-permute-start(f32[2,512]{1,0:T(2,128)S(1)} %add.77), channel_id=1, source_target_pairs={{0,3},{1,2},{3,0},{2,1},{4,7},{5,6},{7,4},{6,5},{8,11},{9,10},{11,... | collective-permute-start | bytes 12296 | tf_op jit(solution)/shard_map/ppermute | solution.py:540
  153.2 27.4 %all-to-all-start.4 = ((f32[16,1,2176]{2,1,0:T(1,128)}), f32[16,1,2176]{2,1,0:T(1,128)S(1)}, u32[]{:S(2)}, u32[]{:S(2)}) async-start(f32[16,1,2176]{2,1,0:T(1,128)} %broadcast_in_dim.20), calls=%async_computation.4 | async-start | bytes 278528 | tf_op jit(solution)/shard_map/all_to_all | solution.py:25
  180.6 1.6 copy-start
  182.2 1.0 copy-start.3
  186.8 12.3 %collective-permute-start.11 = (bf16[64,2048]{1,0:T(8,128)(2,1)S(1)}, bf16[64,2048]{1,0:T(8,128)(2,1)S(1)}, u32[]{:S(2)}, u32[]{:S(2)}) collective-permute-start(bf16[64,2048]{1,0:T(8,128)(2,1)S(1)} %get-tuple-element.56), channel_id=1, source_target_pairs={{0,1},{1,2},{2,3},{3,0},{4,5},{5,6},{6,7},{7,4},{8,9},{9,10},{10,1... | collective-permute-start | bytes 786440 | tf_op jit(solution)/shard_map/ppermute | solution.py:41
  188.7 10.4 %collective-permute-start.9 = (bf16[64,2048]{1,0:T(8,128)(2,1)S(1)}, bf16[64,2048]{1,0:T(8,128)(2,1)S(1)}, u32[]{:S(2)}, u32[]{:S(2)}) collective-permute-start(bf16[64,2048]{1,0:T(8,128)(2,1)S(1)} %get-tuple-element.55), channel_id=1, source_target_pairs={{0,3},{1,0},{2,1},{3,2},{4,7},{5,4},{6,5},{7,6},{8,11},{9,8},{10,9... | collective-permute-start | bytes 786440 | tf_op jit(solution)/shard_map/ppermute | solution.py:41
  199.3 11.4 %collective-permute-start.10 = (bf16[128,2048]{1,0:T(8,128)(2,1)S(1)}, bf16[128,2048]{1,0:T(8,128)(2,1)S(1)}, u32[]{:S(2)}, u32[]{:S(2)}) collective-permute-start(bf16[128,2048]{1,0:T(8,128)(2,1)S(1)} %get-tuple-element.53), channel_id=1, source_target_pairs={{0,3},{1,0},{2,1},{3,2},{4,7},{5,4},{6,5},{7,6},{8,11},{9,8},{10,9... | collective-permute-start | bytes 1572872 | tf_op jit(solution)/shard_map/ppermute | solution.py:41
  203.5 12.3 %collective-permute-start.12 = (bf16[128,2048]{1,0:T(8,128)(2,1)S(1)}, bf16[128,2048]{1,0:T(8,128)(2,1)S(1)}, u32[]{:S(2)}, u32[]{:S(2)}) collective-permute-start(bf16[128,2048]{1,0:T(8,128)(2,1)S(1)} %get-tuple-element.54), channel_id=1, source_target_pairs={{0,1},{1,2},{2,3},{3,0},{4,5},{5,6},{6,7},{7,4},{8,9},{9,10},{10,1... | collective-permute-start | bytes 1572872 | tf_op jit(solution)/shard_map/ppermute | solution.py:41

commit v7 on v6

--- a/solution.py
+++ b/solution.py
@@ -41,6 +41,11 @@
     return lax.ppermute(block, axis, [(i, (i - distance) % count) for i in range(count)])
 
 
+def from_own_on(planes, axis):
+    peers = lax.axis_size(axis)
+    return [planes] + [from_ahead(planes, axis, d) for d in range(1, peers)]
+
+
 def far_from_core(*arrays):
     return [pltpu.with_memory_space_constraint(array, pltpu.HBM) for array in arrays]
 
@@ -49,40 +54,49 @@
     return [pl.BlockSpec(memory_space=pltpu.VMEM) for _ in arrays]
 
 
-def call(body, outs, arrays, scalars=(), scratch=(), mib=16, space=pltpu.VMEM, **costs):
+def call(body, outs, arrays, apart=(), scalars=(), scratch=(), mib=16, space=pltpu.VMEM, **costs):
     return pl.pallas_call(
         body,
         compiler_params=pltpu.CompilerParams(vmem_limit_bytes=mib * 2**20),
         out_shape=outs,
-        in_specs=[pl.BlockSpec(memory_space=pltpu.SMEM) for _ in scalars] + whole_specs(arrays),
+        in_specs=[pl.BlockSpec(memory_space=pltpu.SMEM) for _ in scalars]
+        + whole_specs(arrays)
+        + [pl.BlockSpec(memory_space=pl.ANY) for _ in apart],
         out_specs=jax.tree.map(lambda _: pl.BlockSpec(memory_space=space), outs),
         scratch_shapes=list(scratch),
         cost_estimate=pl.CostEstimate(**costs) if costs else None,
-    )(*scalars, *arrays)
-
-
-def natural_order(place_ref, own_ref, other_ref, into_ref, turned, first_lane=0):
-    peers_x, _, rows, _ = own_ref.shape
-    blocks = into_ref.shape[0] // rows
-    lanes = slice(first_lane, first_lane + into_ref.shape[1])
-    core, part = place_ref[0], place_ref[2]
-    first = part * turned
-
-    def place(by_core):
-        for k in range(blocks):
-            at = lax.rem(first + k, blocks)
-            x = lax.rem(lax.div(at, 2), peers_x)
-            into_ref[k * rows : (k + 1) * rows, :] = by_core[k % 2][
-                x, lax.div(at, 2 * peers_x), :, lanes
-            ]
-
-    @pl.when(core == 0)
-    def _():
-        place((own_ref, other_ref))
-
-    @pl.when(core == 1)
-    def _():
-        place((other_ref, own_ref))
+    )(*scalars, *arrays, *apart)
+
+
+def fetch(source, target, done):
+    copy = pltpu.make_async_copy(source, target, done)
+    copy.start()
+    return copy
+
+
+def natural_order(place_ref, own_ref, other_ref, into_ref, done, first_lane=0, from_own_x=False):
+    peers_x, width = own_ref.shape[0], into_ref.shape[-1]
+    begun = []
+    for side, ref in enumerate((own_ref, other_ref)):
+        core = lax.rem(place_ref[0] + side, 2)
+        for x in range(peers_x):
+            at = lax.rem(x - place_ref[1] + peers_x, peers_x) if from_own_x else x
+            source = ref.at[at, :, :, pl.ds(first_lane, width)]
+            begun.append(fetch(source, into_ref.at[:, x, core], done.at[side * peers_x + x]))
+    return begun
+
+
+def arrived(copies_begun):
+    for copy in copies_begun:
+        copy.wait()
+
+
+def weight_scratch(merged, width):
+    peers_x, peers_z, rows, _ = merged.shape
+    return [
+        pltpu.VMEM((peers_z, peers_x, 2, rows, width), BF16),
+        pltpu.SemaphoreType.DMA((2 * peers_x,)),
+    ]
 
 
 def dot_rows(a, b):
@@ -104,7 +118,7 @@
         scale = lax.rsqrt(power / (parts * depth) + EPS)
         for p, block in enumerate(blocks):
             gain = gain_ref[lax.rem(part + p, parts)]
-            out_ref[p, rows] = (block * scale * gain).astype(BF16)
+            out_ref[lax.rem(part + p, parts), rows] = (block * scale * gain).astype(BF16)
 
     rows_of(0, top_ref)
     rows_of(half, bottom_ref)
@@ -112,30 +126,39 @@
 
 def projected(normed_ref, weight_ref, rows):
     parts, _, depth = normed_ref.shape
+    weights = weight_ref[...].reshape(parts * depth, -1)
     return sum(
         jnp.dot(
             normed_ref[p, rows],
-            weight_ref[p * depth : (p + 1) * depth],
+            weights[p * depth : (p + 1) * depth],
             preferred_element_type=F32,
         )
         for p in range(parts)
     )
 
 
-def state_in_kernel(place_ref, normed_ref, own_ref, other_ref, out_ref, weight_ref):
-    parts, rows, _ = normed_ref.shape
-    turned = weight_ref.shape[0] // own_ref.shape[2] // parts
-    natural_order(place_ref, own_ref, other_ref, weight_ref, turned)
+def state_in_kernel(place_ref, normed_ref, own_ref, other_ref, out_ref, weight_ref, done):
+    rows = normed_ref.shape[1]
+    arrived(natural_order(place_ref, own_ref, other_ref, weight_ref, done))
     out_ref[...] = projected(normed_ref, weight_ref, slice(HALO, rows)).astype(BF16)
 
 
 def conv_kernel(
-    place_ref, normed_ref, own_ref, other_ref, taps_ref, raw_ref, sums_ref, weight_ref, glu_ref, shifted_ref
+    place_ref,
+    normed_ref,
+    taps_ref,
+    own_ref,
+    other_ref,
+    raw_ref,
+    sums_ref,
+    weight_ref,
+    done,
+    glu_ref,
+    shifted_ref,
 ):
-    parts, rows, _ = normed_ref.shape
+    _, rows, _ = normed_ref.shape
     count, width = raw_ref.shape
-    turned = weight_ref.shape[0] // own_ref.shape[2] // parts
-    natural_order(place_ref, own_ref, other_ref, weight_ref, turned, first_lane=width)
+    arrived(natural_order(place_ref, own_ref, other_ref, weight_ref, done, first_lane=width))
     both = projected(normed_ref, weight_ref, slice(0, rows))
     value = both[:, :width].astype(BF16).astype(F32)
     gate = both[:, width:].astype(BF16).astype(F32)
@@ -411,48 +434,72 @@
         prefix_ref[k : k + 1] = row
 
 
-def merge_rows(distances, place_ref, h, y_ref, power_ref, read_ref, conv_ref, own_ref, other_ref, out_ref, weight_ref):
-    natural_order(place_ref, own_ref, other_ref, weight_ref, 0)
-    h_re, h_im = h
+def merge_rows(distances, carried, place_ref, conv_ref, refs):
+    (y_all, power_all, read_all, own_ref, other_ref, out_ref) = refs[:6]
+    weight_ref, weight_done, y_ref, power_ref, read_ref, done = refs[6:]
+    block = out_ref.shape[1]
+    parts = conv_ref.shape[0] // block
+    places = [
+        pl.ds(pl.multiple_of(lax.rem(place_ref[2] + distance, parts) * block, block), block)
+        for distance in distances
+    ]
+    begun = [fetch(read_all, read_ref, done.at[0])]
+    for k, rows in enumerate(places):
+        begun.append(fetch(power_all.at[rows], power_ref.at[k], done.at[1 + 2 * k]))
+        begun.append(fetch(y_all.at[rows], y_ref.at[k], done.at[2 + 2 * k]))
+    weights_begun = natural_order(
+        place_ref, own_ref, other_ref, weight_ref, weight_done, from_own_x=True
+    )
+    h_re, h_im = carried()
     lanes = h_re.shape[1]
-    block = out_ref.shape[1]
-    parts = y_ref.shape[0] // block
+    arrived(begun)
     c_re, c_im = read_ref[:, :lanes].astype(F32), read_ref[:, lanes:].astype(F32)
     blend_re = (c_re * h_re + c_im * h_im).astype(BF16)
     blend_im = (c_im * h_re - c_re * h_im).astype(BF16)
-    for k, distance in enumerate(distances):
-        rows = pl.ds(pl.multiple_of(lax.rem(place_ref[2] + distance, parts) * block, block), block)
+    arrived(weights_begun)
+    weights = weight_ref[...].reshape(out_ref.shape[2], -1)
+    for k, rows in enumerate(places):
         total = (
-            y_ref[rows]
-            + dot_rows(power_ref[rows, :lanes], blend_re)
-            + dot_rows(power_ref[rows, lanes:], blend_im)
+            y_ref[k]
+            + dot_rows(power_ref[k, :, :lanes], blend_re)
+            + dot_rows(power_ref[k, :, lanes:], blend_im)
         )
         ssm = jax.nn.gelu(total).astype(BF16)
         both = jnp.concatenate([ssm, conv_ref[rows]], axis=1)
-        out_ref[k] = dot_rows(both, weight_ref[...]).astype(BF16)
-
-
-def opposite_kernel(count, place_ref, far_ref, rates_ref, prefix_ref, start_ref, *refs):
-    *inputs, out_ref, h_ref, weight_ref = refs
+        out_ref[k] = dot_rows(both, weights).astype(BF16)
+
+
+def opposite_kernel(count, place_ref, conv_ref, far_ref, rates_ref, prefix_ref, start_ref, *refs):
+    *inputs, out_ref, h_ref, weight_ref, weight_done, y_ref, power_ref, read_ref, done = refs
     peers_z, peers_near = far_ref.shape[0], 2 * inputs[-1].shape[0]
-    _, sizes, states = shares(far_ref, rates_ref, peers_near * count)
-    turn = (rates_ref[1:2], rates_ref[2:3])
-    for _ in range(peers_near.bit_length() - 1):
-        turn = squared(*turn)
-    h = (start_ref[0:1], start_ref[1:2])
-    for k in range(peers_z):
-        passed = k < place_ref[3]
-        step = (sizes[k : k + 1] * turn[0], sizes[k : k + 1] * turn[1])
-        moved = times(step, h)
-        h = tuple(jnp.where(passed, m + s, o) for m, s, o in zip(moved, states[k], h))
-    moved = times((prefix_ref[2:3], prefix_ref[3:4]), h)
-    h = (moved[0] + prefix_ref[0:1], moved[1] + prefix_ref[1:2])
-    h_ref[0:1], h_ref[1:2] = h
-    merge_rows((2,), place_ref, h, *inputs, out_ref, weight_ref)
-
-
-def rest_kernel(place_ref, h_ref, *refs):
-    merge_rows((0, 1, 3), place_ref, (h_ref[0:1], h_ref[1:2]), *refs)
+
+    def carried():
+        _, sizes, states = shares(far_ref, rates_ref, peers_near * count)
+        turn = (rates_ref[1:2], rates_ref[2:3])
+        for _ in range(peers_near.bit_length() - 1):
+            turn = squared(*turn)
+        h = (start_ref[0:1], start_ref[1:2])
+        for k in range(peers_z):
+            passed = k < place_ref[3]
+            step = (sizes[k : k + 1] * turn[0], sizes[k : k + 1] * turn[1])
+            moved = times(step, h)
+            h = tuple(jnp.where(passed, m + s, o) for m, s, o in zip(moved, states[k], h))
+        moved = times((prefix_ref[2:3], prefix_ref[3:4]), h)
+        h = (moved[0] + prefix_ref[0:1], moved[1] + prefix_ref[1:2])
+        h_ref[0:1], h_ref[1:2] = h
+        return h
+
+    merge_rows(
+        (2,),
+        carried,
+        place_ref,
+        conv_ref,
+        (*inputs, out_ref, weight_ref, weight_done, y_ref, power_ref, read_ref, done),
+    )
+
+
+def rest_kernel(place_ref, conv_ref, h_ref, *refs):
+    merge_rows((0, 1, 3), lambda: (h_ref[0:1], h_ref[1:2]), place_ref, conv_ref, refs)
 
 
 def input_matrix(eigen_real, eigen_imag, step, state_input):
@@ -535,10 +582,8 @@
 
 
 def conv_finish(raw, sums, channel_gain):
-    for pairs in (((0, 1), (2, 3)), ((0, 3), (1, 2))):
-        route = [*pairs, *((b, a) for a, b in pairs)]
-        sums = sums + lax.ppermute(sums, "tp", route)
-    first, second = (row[:, None] for row in sums)
+    others = [from_ahead(sums, "tp", d) for d in range(1, lax.axis_size("tp"))]
+    first, second = (row[:, None] for row in sum(others, sums))
     middle = first / CONV_W
     spread = second / CONV_W - middle * middle
     scaled = (raw - middle) * lax.rsqrt(spread + EPS) * channel_gain
@@ -598,15 +643,15 @@
         bytes_accessed=4 * count * depth,
         transcendentals=count,
     )
-    project_x, normed = lax.optimization_barrier((project_x, normed))
+    merge_pieces = from_own_on(planes[:, :, 3 * width :], "x")
     project_other = partner(project_x)
-    merge_x = copies(planes[:, :, 3 * width :], "x")
     u_in = call(
         state_in_kernel,
         jax.ShapeDtypeStruct((count, width), BF16),
-        (normed, project_x, project_other),
+        (normed,),
+        apart=far_from_core(project_x, project_other),
         scalars=(place,),
-        scratch=(pltpu.VMEM((depth, width), BF16),),
+        scratch=weight_scratch(project_x, width),
         mib=12,
         flops=2 * count * depth * width,
         bytes_accessed=4 * depth * count,
@@ -632,8 +677,9 @@
         bytes_accessed=8 * count * lanes,
         transcendentals=0,
     )
-    last, merge_x = lax.optimization_barrier((last, merge_x))
     near = copies(last, ("x", "c"))
+    *merge_pieces, _ = lax.optimization_barrier((*merge_pieces, last))
+    merge_x = jnp.stack(merge_pieces)
     merge_other = partner(merge_x)
     packed, prefix = call(
         functools.partial(near_kernel, count),
@@ -656,10 +702,11 @@
             pltpu.HBM((count, width), F32),
             jax.ShapeDtypeStruct((2, count), F32),
         ),
-        (normed, project_x, project_other, conv_taps),
+        (normed, conv_taps),
+        apart=far_from_core(project_x, project_other),
         scalars=(place,),
         scratch=(
-            pltpu.VMEM((depth, 2 * width), BF16),
+            *weight_scratch(project_x, 2 * width),
             pltpu.VMEM((rows + 8, width), F32),
             pltpu.VMEM((8, rows, width), F32),
         ),
@@ -671,15 +718,21 @@
     conv_out = conv_finish(raw, sums, channel_gain)
 
     block = count // parts
-    merge_inputs = (y_local, power, reads, conv_out, merge_x, merge_other)
 
     def products(kernel, blocks, more, arrays):
         return call(
             kernel,
             (jax.ShapeDtypeStruct((blocks, block, depth), BF16), *more),
-            (*arrays, *merge_inputs),
+            (conv_out, *arrays),
+            apart=(*far_from_core(y_local, power, reads), merge_x, merge_other),
             scalars=(place,),
-            scratch=(pltpu.VMEM((depth, 2 * width), BF16),),
+            scratch=(
+                *weight_scratch(merge_x, 2 * width),
+                pltpu.VMEM((blocks, block, width), F32),
+                pltpu.VMEM((blocks, block, 2 * lanes), BF16),
+                pltpu.VMEM((width, 2 * lanes), BF16),
+                pltpu.SemaphoreType.DMA((1 + 2 * blocks,)),
+            ),
             flops=4 * block * blocks * depth * width,
             bytes_accessed=4 * depth * count,
             transcendentals=0,

time: 218 us -> 216 us (level)
  blocking collectives: 0 us -> 18.4 us
  waiting for transfers between devices: 79.6 us -> 64.4 us
  local copies, waits for them, and re-layouts: 10.4 us -> 3.71 us
    ppermute x8 -> x14, starting transfers between devices: 27.5 us -> 46 us  [from_ahead(): lax.ppermute(block, axis, [(i, (i - distance) % count) for i in range(cou...]
    all_to_all x0 -> x1, blocking collectives: none -> 18.4 us  [copies(): lax.all_to_all(jnp.broadcast_to(value[None], (peers, *value.shape)), axis...]
    all_to_all x5 -> x3, starting transfers between devices: 47.4 us -> 31.8 us  [copies(): lax.all_to_all(jnp.broadcast_to(value[None], (peers, *value.shape)), axis...]
    ppermute x2 -> x0, waiting for transfers between devices: 8.36 us -> none  [conv_finish(): sums = sums + lax.ppermute(sums, 'tp', route)]
    ppermute x8 -> x14, waiting for transfers between devices: 25 us -> 19.8 us  [from_ahead(): lax.ppermute(block, axis, [(i, (i - distance) % count) for i in range(cou...]
    unnamed x61 -> x49, local copies, waits for them, and re-layouts: 5.13 us -> 0.79 us
    ppermute x2 -> x0, starting transfers between devices: 3.96 us -> none  [conv_finish(): sums = sums + lax.ppermute(sums, 'tp', route)]
    ppermute x1, waiting for transfers between devices: 5.75 us -> 2.82 us  [next_along(): return lax.ppermute(block, axis, [(i, i + 1) for i in range(count - 1)])]
  transfers between devices with their start and end apart: 18 -> 20, of which waited for: 11 -> 9; matrix products, arithmetic and copies ran while one was open for 3% -> 2% of each run, Pallas kernels for 15% -> 15%
where the time goes in v7:
time: 216 us; the launch traced here: 213 us
  starting transfers between devices  84.4 us (39%)
  waiting for transfers between devices  64.4 us (30%)
  Pallas kernels  36 us (17%)
  blocking collectives  18.4 us (9%)
  other arithmetic  5.47 us (3%)
  local copies, waits for them, and re-layouts  3.71 us (2%)
    ppermute x14, starting transfers between devices, from_ahead(): lax.ppermute(block, axis, [(i, (i - distance) % count) for i in range(cou...  46 us
    all_to_all x3, waiting for transfers between devices, copies(): lax.all_to_all(jnp.broadcast_to(value[None], (peers, *value.shape)), axis...  41.8 us
    pallas_call x8, Pallas kernels, call(): pl.pallas_call(body, compiler_params=pltpu.CompilerParams(vmem_limit_byte...  36 us
    all_to_all x3, starting transfers between devices, copies(): lax.all_to_all(jnp.broadcast_to(value[None], (peers, *value.shape)), axis...  31.8 us
    ppermute x14, waiting for transfers between devices, from_ahead(): lax.ppermute(block, axis, [(i, (i - distance) % count) for i in range(cou...  19.8 us
    all_to_all x1, blocking collectives, copies(): lax.all_to_all(jnp.broadcast_to(value[None], (peers, *value.shape)), axis...  18.4 us
  transfers between devices with their start and end apart: 20, of which 9 were waited for; matrix products, arithmetic and copies ran while one was open for 2% of the time, Pallas kernels for 15%

profile of v7, /device:TPU:6, one launch (start us, length us, event | category | flops | bytes accessed | tf_op | source)
XLA Modules:
  0.0 213.0 jit_solution(17459372198268977411)
XLA Ops:
  0.0 0.8 maximum_bitcast_fusion
  0.8 0.7 pad_maximum_fusion.1
  1.5 0.9 broadcast_in_dim.12
  2.4 15.2 %all-to-all-start = ((bf16[16,16,1280]{2,1,0:T(8,128)(2,1)}), bf16[16,16,1280]{2,1,0:T(8,128)(2,1)S(1)}, u32[]{:S(2)}, u32[]{:S(2)}) async-start(bf16[16,16,1280]{2,1,0:T(8,128)(2,1)} %broadcast_in_dim.12), calls=%async_computation | async-start | bytes 1310720 | tf_op jit(solution)/shard_map/all_to_all | solution.py:25
  17.6 0.0 copy-start.3
  17.7 0.1 fusion.14
  17.8 0.1 reshape.159.refs_1_
  17.9 0.1 mul.226
  17.9 0.1 mul.192
  18.0 0.1 reshape.160.start_ref
  18.2 0.3 multiply_sine_fusion.1
  18.5 0.6 fusion.11
  19.1 7.4 %shard_map.164 = (f32[512,256]{1,0:T(8,128)}, f32[512,256]{1,0:T(8,128)}, bf16[256,2048]{1,0:T(8,128)(2,1)}, bf16[256,2048]{1,0:T(8,128)(2,1)}, f32[5,16,1024]{2...) custom-call(f32[16,512]{1,0:T(8,128)S(1)} %copy-done.3, ...), custom_call_target="tpu_custom_call" | custom-call | flops 83886080 | bytes 4194304 | tf_op jit(solution)/shard_map/pallas_call | solution.py:58
  26.6 24.7 %all-to-all-done = bf16[16,16,1280]{2,1,0:T(8,128)(2,1)S(1)} async-done(((bf16[16,16,1280]{2,1,0:T(8,128)(2,1)}), bf16[16,16,1280]{2,1,0:T(8,128)(2,1)S(1)}, u32[]{:S(2)}, u32[]{:S(2)}) %all-to-all-start) | async-done | bytes 655392 | tf_op jit(solution)/shard_map/all_to_all | solution.py:25
  51.4 0.1 broadcast_in_dim.13
  51.5 0.0 copy-start.14
  51.5 18.4 %all_to_all.20.own_ref = bf16[4,16,16,768]{3,2,1,0:T(8,128)(2,1)} all-to-all(bf16[4,16,16,768]{3,2,1,0:T(8,128)(2,1)S(1)} %broadcast_in_dim.13), channel_id=1, replica_groups=mesh['z'=16,'x'=4,'c'=2,'tp'=4] {'x'}, dimensions={0} | all-to-all | bytes 3145728 | tf_op jit(solution)/shard_map/all_to_all | solution.py:25
  69.9 2.0 collective-permute-start.5
  71.9 2.4 %collective-permute-start = (bf16[32,512]{1,0:T(8,128)(2,1)S(1)}, bf16[32,512]{1,0:T(8,128)(2,1)S(1)}, u32[]{:S(2)}, u32[]{:S(2)}) collective-permute-start(bf16[32,512]{1,0:T(8,128)(2,1)S(1)} %slice.45), channel_id=1, source_target_pairs={{0,4},{4,8},{8,12},{12,16},{16,20},{20,24},{24,28},{28,32},{32,36}... | collective-permute-start | bytes 98312 | tf_op jit(solution)/shard_map/ppermute | solution.py:32
  74.3 2.8 %collective-permute-done = bf16[32,512]{1,0:T(8,128)(2,1)S(1)} collective-permute-done((bf16[32,512]{1,0:T(8,128)(2,1)S(1)}, bf16[32,512]{1,0:T(8,128)(2,1)S(1)}, u32[]{:S(2)}, u32[]{:S(2)}) %collective-permute-start) | collective-permute-done | bytes 32800 | tf_op jit(solution)/shard_map/ppermute | solution.py:32
  77.2 4.9 %collective-permute-start.1 = (bf16[544,512]{1,0:T(8,128)(2,1)S(1)}, bf16[544,512]{1,0:T(8,128)(2,1)S(1)}, u32[]{:S(2)}, u32[]{:S(2)}) collective-permute-start(bf16[544,512]{1,0:T(8,128)(2,1)S(1)} %constant_dynamic-update-slice_fusion.own_ref), channel_id=1, source_target_pairs={{0,3},{1,0},{2,1},{3,2},{4,7},{5,4},{6,5},{7,6},{8,11},{9,8},{10,9... | collective-permute-start | bytes 1671176 | tf_op jit(solution)/shard_map/ppermute | solution.py:41
  82.1 1.9 collective-permute-start.3
  84.1 10.5 %collective-permute-done.1.ahead_ref = bf16[544,512]{1,0:T(8,128)(2,1)S(1)} collective-permute-done((bf16[544,512]{1,0:T(8,128)(2,1)S(1)}, bf16[544,512]{1,0:T(8,128)(2,1)S(1)}, u32[]{:S(2)}, u32[]{:S(2)}) %collective-permute-start.1) | collective-permute-done | bytes 557088 | tf_op jit(solution)/shard_map/ppermute | solution.py:41
  94.6 5.6 %collective-permute-start.2 = (bf16[272,512]{1,0:T(8,128)(2,1)S(1)}, bf16[272,512]{1,0:T(8,128)(2,1)S(1)}, u32[]{:S(2)}, u32[]{:S(2)}) collective-permute-start(bf16[272,512]{1,0:T(8,128)(2,1)S(1)} %slice.60), channel_id=1, source_target_pairs={{0,3},{1,0},{2,1},{3,2},{4,7},{5,4},{6,5},{7,6},{8,11},{9,8},{10,9... | collective-permute-start | bytes 835592 | tf_op jit(solution)/shard_map/ppermute | solution.py:41
  100.3 0.2 collective-permute-done.3.behind_ref
  100.5 1.9 collective-permute-start.4
  102.4 0.1 fusion.5.lower_ref
  102.6 1.9 collective-permute-start.9
  104.5 3.2 %collective-permute-start.10 = (bf16[16,16,512]{2,1,0:T(8,128)(2,1)S(1)}, bf16[16,16,512]{2,1,0:T(8,128)(2,1)S(1)}, u32[]{:S(2)}, u32[]{:S(2)}) collective-permute-start(bf16[16,16,512]{2,1,0:T(8,128)(2,1)S(1)} %slice.55), channel_id=1, source_target_pairs={{0,16},{8,24},{16,0},{24,8},{1,17},{9,25},{17,1},{25,9},{2,18},{10... | collective-permute-start | bytes 786440 | tf_op jit(solution)/shard_map/ppermute | solution.py:41
  107.8 0.0 collective-permute-done.2.top_ref
  107.8 3.8 %collective-permute-start.11 = (bf16[16,16,512]{2,1,0:T(8,128)(2,1)S(1)}, bf16[16,16,512]{2,1,0:T(8,128)(2,1)S(1)}, u32[]{:S(2)}, u32[]{:S(2)}) collective-permute-start(bf16[16,16,512]{2,1,0:T(8,128)(2,1)S(1)} %slice.55), channel_id=1, source_target_pairs={{0,8},{8,16},{16,24},{24,0},{1,9},{9,17},{17,25},{25,1},{2,10},{10... | collective-permute-start | bytes 786440 | tf_op jit(solution)/shard_map/ppermute | solution.py:41
  111.6 0.1 pad_add_fusion.place_ref
  111.7 0.6 collective-permute-done.4.bottom_ref
  112.3 0.7 copy-done.16
  113.0 2.4 %shard_map.163.normed_ref = bf16[4,544,512]{2,1,0:T(8,128)(2,1)S(1)} custom-call(s32[4]{0:T(128)S(1)} %pad_add_fusion.place_ref, bf16[544,512]{1,0:T(8,128)(2,1)} %copy-done.13, bf16[544,512]{1,0:T(8,128)(2,1)} %copy-done.11, bf16[272,512]{1,0:T(8,128)(2,1)} %copy-done.15, bf16[272,512]{1,0:T(8,128)(2,1)} %copy-done.16, bf16[544,512]{1,0:T(8,128)(2,1)} %copy-done.12, ...), custom_call_target="tpu_custom_call" | custom-call | flops 8388608 | bytes 4194304 | tf_op jit(solution)/shard_map/pallas_call | solution.py:58
  115.4 0.0 copy-start.4
  115.5 0.0 copy-start.6
  115.5 2.9 %shard_map.166.u_ref = bf16[512,256]{1,0:T(8,128)(2,1)S(1)} custom-call(s32[4]{0:T(128)S(1)} %pad_add_fusion.place_ref, bf16[4,544,512]{2,1,0:T(8,128)(2,1)S(1)} %shard_map.163.normed_ref, bf16[4,16,16,768]{3,2,1,0:T(8,128)(2,1)} %all_to_all.20.own_ref, bf16[4,16,16,768]{3,2,1,0:T(8,128)(2,1)} %collective-permute-done.5.other_ref), custom_call_target="tpu_custom_call" | custom-call | flops 536870912 | bytes 4194304 | tf_op jit(solution)/shard_map/pallas_call | solution.py:58
  118.6 4.9 %shard_map.167 = (f32[512,256]{1,0:T(8,128)}, f32[1,2176]{1,0:T(1,128)S(1)}) custom-call(bf16[512,256]{1,0:T(8,128)(2,1)S(1)} %shard_map.166.u_ref, f32[512,256]{1,0:T(8,128)S(1)} %copy-done.6, f32[512,256]{1,0:T(8,128)S(1)} %copy-done.7, bf16[256,2048]{1,0:T(8,128)(2,1)S(1)} %copy-done.5, bf16[256,2048]{1,0:T(8,128)(2,1)S(1)} %copy-done, ...), custom_call_target="tpu_custom_call" | custom-call | flops 1610612736 | bytes 4194304 | tf_op jit(solution)/shard_map/pallas_call | solution.py:58
  123.5 0.1 pad_maximum_fusion.refs_3_
  123.6 0.0 copy-start.22
  123.6 2.1 collective-permute-start.12
  125.8 6.3 %shard_map.165 = (f32[512,256]{1,0:T(8,128)}, f32[2,512]{1,0:T(2,128)S(1)}) custom-call(s32[4]{0:T(128)S(1)} %pad_add_fusion.place_ref, bf16[4,544,512]{2,1,0:T(8,128)(2,1)S(1)} %shard_map.163.normed_ref, f32[31,256]{1,0:T(8,128)S(1)} %copy-done.1, bf16[4,16,16,768]{3,2,1,0:T(8,128)(2,1)} %all_to_all.20.own_ref, ...), custom_call_target="tpu_custom_call" | custom-call | flops 1073741824 | bytes 4194304 | tf_op jit(solution)/shard_map/pallas_call | solution.py:58
  132.1 1.9 collective-permute-start.8
  134.0 6.0 %collective-permute-start.7 = (f32[2,512]{1,0:T(2,128)S(1)}, f32[2,512]{1,0:T(2,128)S(1)}, u32[]{:S(2)}, u32[]{:S(2)}) collective-permute-start(f32[2,512]{1,0:T(2,128)S(1)} %get-tuple-element.32), channel_id=1, source_target_pairs={{0,2},{1,3},{2,0},{3,1},{4,6},{5,7},{6,4},{7,5},{8,10},{9,11},{10,... | collective-permute-start | bytes 12296 | tf_op jit(solution)/shard_map/ppermute | solution.py:41
  140.0 1.9 collective-permute-start.6
  141.9 0.7 broadcast_in_dim.15
  142.6 4.9 %all-to-all-start.2 = ((f32[8,1,2176]{2,1,0:T(1,128)}), f32[8,1,2176]{2,1,0:T(1,128)S(1)}, u32[]{:S(2)}, u32[]{:S(2)}) async-start(f32[8,1,2176]{2,1,0:T(1,128)} %broadcast_in_dim.15), calls=%async_computation.2 | async-start | bytes 139264 | tf_op jit(solution)/shard_map/all_to_all | solution.py:25
  147.6 3.5 %all-to-all-done.2.near_ref = f32[8,1,2176]{2,1,0:T(1,128)S(1)} async-done(((f32[8,1,2176]{2,1,0:T(1,128)}), f32[8,1,2176]{2,1,0:T(1,128)S(1)}, u32[]{:S(2)}, u32[]{:S(2)}) %all-to-all-start.2) | async-done | bytes 69664 | tf_op jit(solution)/shard_map/all_to_all | solution.py:25
  151.1 0.9 shard_map.168
  152.0 0.7 broadcast_in_dim.17
  152.8 11.7 %all-to-all-start.3 = ((f32[16,1,2176]{2,1,0:T(1,128)}), f32[16,1,2176]{2,1,0:T(1,128)S(1)}, u32[]{:S(2)}, u32[]{:S(2)}) async-start(f32[16,1,2176]{2,1,0:T(1,128)} %broadcast_in_dim.17), calls=%async_computation.3 | async-start | bytes 278528 | tf_op jit(solution)/shard_map/all_to_all | solution.py:25
  164.5 1.3 multiply_convert_fusion.conv_ref
  165.8 13.5 %all-to-all-done.3.far_ref = f32[16,1,2176]{2,1,0:T(1,128)S(1)} async-done(((f32[16,1,2176]{2,1,0:T(1,128)}), f32[16,1,2176]{2,1,0:T(1,128)S(1)}, u32[]{:S(2)}, u32[]{:S(2)}) %all-to-all-start.3) | async-done | bytes 139296 | tf_op jit(solution)/shard_map/all_to_all | solution.py:25
  179.3 4.3 %shard_map.169 = (bf16[1,128,2048]{2,1,0:T(8,128)(2,1)S(1)}, f32[2,1024]{1,0:T(2,128)S(1)}) custom-call(s32[4]{0:T(128)S(1)} %pad_add_fusion.place_ref, bf16[512,256]{1,0:T(8,128)(2,1)S(1)} %multiply_convert_fusion.conv_ref, f32[16,1,2176]{2,1,0:T(1,128)S(1)} %all-to-all-done.3.far_ref, f32[3,1024]{1,0:T(4,128)S(1)} %pad_maximum_fusion.2.rates_ref, ...), custom_call_target="tpu_custom_call" | custom-call | flops 268435456 | bytes 4194304 | tf_op jit(solution)/shard_map/pallas_call | solution.py:58
  183.6 2.5 %collective-permute-start.13 = (bf16[64,2048]{1,0:T(8,128)(2,1)S(1)}, bf16[64,2048]{1,0:T(8,128)(2,1)S(1)}, u32[]{:S(2)}, u32[]{:S(2)}) collective-permute-start(bf16[64,2048]{1,0:T(8,128)(2,1)S(1)} %get-tuple-element.55), channel_id=1, source_target_pairs={{0,3},{1,0},{2,1},{3,2},{4,7},{5,4},{6,5},{7,6},{8,11},{9,8},{10,9... | collective-permute-start | bytes 786440 | tf_op jit(solution)/shard_map/ppermute | solution.py:41
  186.1 3.4 %collective-permute-start.15 = (bf16[64,2048]{1,0:T(8,128)(2,1)S(1)}, bf16[64,2048]{1,0:T(8,128)(2,1)S(1)}, u32[]{:S(2)}, u32[]{:S(2)}) collective-permute-start(bf16[64,2048]{1,0:T(8,128)(2,1)S(1)} %get-tuple-element.56), channel_id=1, source_target_pairs={{0,1},{1,2},{2,3},{3,0},{4,5},{5,6},{6,7},{7,4},{8,9},{9,10},{10,1... | collective-permute-start | bytes 786440 | tf_op jit(solution)/shard_map/ppermute | solution.py:41
  189.5 6.9 %shard_map.170 = bf16[3,128,2048]{2,1,0:T(8,128)(2,1)S(1)} custom-call(s32[4]{0:T(128)S(1)} %pad_add_fusion.place_ref, bf16[512,256]{1,0:T(8,128)(2,1)S(1)} %multiply_convert_fusion.conv_ref, f32[2,1024]{1,0:T(2,128)S(1)} %get-tuple-element.51.h_ref, f32[512,256]{1,0:T(8,128)} %get-tuple-element.45.refs_0_, bf16[512,2048]{1,0:T(8,128)(2,1)} %get-tuple-element.46.refs_1_, ...), custom_call_target="tpu_custom_call" | custom-call | flops 805306368 | bytes 4194304 | tf_op jit(solution)/shard_map/pallas_call | solution.py:58
  196.4 0.2 fusion.1
  196.6 3.9 %collective-permute-start.16 = (bf16[128,2048]{1,0:T(8,128)(2,1)S(1)}, bf16[128,2048]{1,0:T(8,128)(2,1)S(1)}, u32[]{:S(2)}, u32[]{:S(2)}) collective-permute-start(bf16[128,2048]{1,0:T(8,128)(2,1)S(1)} %get-tuple-element.54), channel_id=1, source_target_pairs={{0,1},{1,2},{2,3},{3,0},{4,5},{5,6},{6,7},{7,4},{8,9},{9,10},{10,1... | collective-permute-start | bytes 1572872 | tf_op jit(solution)/shard_map/ppermute | solution.py:41
  200.5 3.1 %collective-permute-start.14 = (bf16[128,2048]{1,0:T(8,128)(2,1)S(1)}, bf16[128,2048]{1,0:T(8,128)(2,1)S(1)}, u32[]{:S(2)}, u32[]{:S(2)}) collective-permute-start(bf16[128,2048]{1,0:T(8,128)(2,1)S(1)} %get-tuple-element.53), channel_id=1, source_target_pairs={{0,3},{1,0},{2,1},{3,2},{4,7},{5,4},{6,5},{7,6},{8,11},{9,8},{10,9... | collective-permute-start | bytes 1572872 | tf_op jit(solution)/shard_map/ppermute | solution.py:41
  203.7 6.2 %collective-permute-done.16 = bf16[128,2048]{1,0:T(8,128)(2,1)S(1)} collective-permute-done((bf16[128,2048]{1,0:T(8,128)(2,1)S(1)}, bf16[128,2048]{1,0:T(8,128)(2,1)S(1)}, u32[]{:S(2)}, u32[]{:S(2)}) %collective-permute-start.16) | collective-permute-done | bytes 524320 | tf_op jit(solution)/shard_map/ppermute | solution.py:41
  209.8 2.2 %collective-permute-done.14 = bf16[128,2048]{1,0:T(8,128)(2,1)S(1)} collective-permute-done((bf16[128,2048]{1,0:T(8,128)(2,1)S(1)}, bf16[128,2048]{1,0:T(8,128)(2,1)S(1)}, u32[]{:S(2)}, u32[]{:S(2)}) %collective-permute-start.14) | collective-permute-done | bytes 524320 | tf_op jit(solution)/shard_map/ppermute | solution.py:41
  212.0 1.0 fusion.3
  (74 shorter events, 0.5 us)
Async XLA Ops:
  0.0 17.6 %copy-start.23 = (f32[16]{0:T(128)S(1)}, f32[16]{0:T(128)}, u32[]{:S(2)}) copy-start(f32[16]{0:T(128)} %param.24) | copy-start | bytes 196
  0.0 17.7 %copy-start.20 = (f32[16,64]{1,0:T(8,128)S(1)}, f32[16,64]{1,0:T(8,128)}, u32[]{:S(2)}) copy-start(f32[16,64]{1,0:T(8,128)} %param.23) | copy-start | bytes 12292
  0.0 17.7 %copy-start.21 = (f32[16,64]{1,0:T(8,128)S(1)}, f32[16,64]{1,0:T(8,128)}, u32[]{:S(2)}) copy-start(f32[16,64]{1,0:T(8,128)} %param.22) | copy-start | bytes 12292
  0.0 18.0 %copy-start.19 = (f32[2,16,64]{2,1,0:T(8,128)S(1)}, f32[2,16,64]{2,1,0:T(8,128)}, u32[]{:S(2)}) copy-start(f32[2,16,64]{2,1,0:T(8,128)} %param.29) | copy-start | bytes 24580
  0.0 18.1 %copy-start.17 = (f32[2,16,16,64]{3,2,1,0:T(8,128)S(1)}, f32[2,16,16,64]{3,2,1,0:T(8,128)}, u32[]{:S(2)}) copy-start(f32[2,16,16,64]{3,2,1,0:T(8,128)} %param.26) | copy-start | bytes 393220
  1.5 17.0 %copy-start.18 = (f32[2,16,16,64]{3,2,1,0:T(8,128)S(1)}, f32[2,16,16,64]{3,2,1,0:T(8,128)}, u32[]{:S(2)}) copy-start(f32[2,16,16,64]{3,2,1,0:T(8,128)} %param.27) | copy-start | bytes 393220
  2.4 48.9 %all-to-all-start = ((bf16[16,16,1280]{2,1,0:T(8,128)(2,1)}), bf16[16,16,1280]{2,1,0:T(8,128)(2,1)S(1)}, u32[]{:S(2)}, u32[]{:S(2)}) async-start(bf16[16,16,1280]{2,1,0:T(8,128)(2,1)} %broadcast_in_dim.12), calls=%async_computation | async-start | bytes 1310720 | tf_op jit(solution)/shard_map/all_to_all | solution.py:25
  17.6 1.5 copy-start.3
  51.5 20.4 %copy-start.14 = (bf16[512,512]{1,0:T(8,128)(2,1)S(1)}, bf16[512,512]{1,0:T(8,128)(2,1)}, u32[]{:S(2)}) copy-start(bf16[512,512]{1,0:T(8,128)(2,1)} %param.17) | copy-start | bytes 1572868
  69.8 43.2 %copy-start.2 = (f32[2048]{0:T(1024)S(1)}, f32[2048]{0:T(1024)}, u32[]{:S(2)}) copy-start(f32[2048]{0:T(1024)} %param.18) | copy-start | bytes 24580
  69.9 45.7 %collective-permute-start.5 = (bf16[4,16,16,768]{3,2,1,0:T(8,128)(2,1)}, bf16[4,16,16,768]{3,2,1,0:T(8,128)(2,1)}, u32[]{:S(2)}, u32[]{:S(2)}) collective-permute-start(bf16[4,16,16,768]{3,2,1,0:T(8,128)(2,1)} %all_to_all.20.own_ref), channel_id=1, source_target_pairs={{0,4},{4,0},{1,5},{5,1},{2,6},{6,2},{3,7},{7,3},{8,12},{12,8},{9,1... | collective-permute-start | bytes 4718600 | tf_op jit(solution)/shard_map/ppermute | solution.py:36
  71.9 5.2 %collective-permute-start = (bf16[32,512]{1,0:T(8,128)(2,1)S(1)}, bf16[32,512]{1,0:T(8,128)(2,1)S(1)}, u32[]{:S(2)}, u32[]{:S(2)}) collective-permute-start(bf16[32,512]{1,0:T(8,128)(2,1)S(1)} %slice.45), channel_id=1, source_target_pairs={{0,4},{4,8},{8,12},{12,16},{16,20},{20,24},{24,28},{28,32},{32,36}... | collective-permute-start | bytes 98312 | tf_op jit(solution)/shard_map/ppermute | solution.py:32
  77.2 35.1 %copy-start.13 = (bf16[544,512]{1,0:T(8,128)(2,1)}, bf16[544,512]{1,0:T(8,128)(2,1)S(1)}, u32[]{:S(2)}) copy-start(bf16[544,512]{1,0:T(8,128)(2,1)S(1)} %constant_dynamic-update-slice_fusion.own_ref) | copy-start | bytes 1671172
  77.2 17.4 %collective-permute-start.1 = (bf16[544,512]{1,0:T(8,128)(2,1)S(1)}, bf16[544,512]{1,0:T(8,128)(2,1)S(1)}, u32[]{:S(2)}, u32[]{:S(2)}) collective-permute-start(bf16[544,512]{1,0:T(8,128)(2,1)S(1)} %constant_dynamic-update-slice_fusion.own_ref), channel_id=1, source_target_pairs={{0,3},{1,0},{2,1},{3,2},{4,7},{5,4},{6,5},{7,6},{8,11},{9,8},{10,9... | collective-permute-start | bytes 1671176 | tf_op jit(solution)/shard_map/ppermute | solution.py:41
  82.1 18.4 %collective-permute-start.3 = (bf16[544,512]{1,0:T(8,128)(2,1)S(1)}, bf16[544,512]{1,0:T(8,128)(2,1)S(1)}, u32[]{:S(2)}, u32[]{:S(2)}) collective-permute-start(bf16[544,512]{1,0:T(8,128)(2,1)S(1)} %constant_dynamic-update-slice_fusion.own_ref), channel_id=1, source_target_pairs={{0,1},{1,2},{2,3},{3,0},{4,5},{5,6},{6,7},{7,4},{8,9},{9,10},{10,1... | collective-permute-start | bytes 1671176 | tf_op jit(solution)/shard_map/ppermute | solution.py:41
  94.6 17.7 %copy-start.11 = (bf16[544,512]{1,0:T(8,128)(2,1)}, bf16[544,512]{1,0:T(8,128)(2,1)S(1)}, u32[]{:S(2)}) copy-start(bf16[544,512]{1,0:T(8,128)(2,1)S(1)} %collective-permute-done.1.ahead_ref) | copy-start | bytes 1671172
  94.6 13.1 %collective-permute-start.2 = (bf16[272,512]{1,0:T(8,128)(2,1)S(1)}, bf16[272,512]{1,0:T(8,128)(2,1)S(1)}, u32[]{:S(2)}, u32[]{:S(2)}) collective-permute-start(bf16[272,512]{1,0:T(8,128)(2,1)S(1)} %slice.60), channel_id=1, source_target_pairs={{0,3},{1,0},{2,1},{3,2},{4,7},{5,4},{6,5},{7,6},{8,11},{9,8},{10,9... | collective-permute-start | bytes 835592 | tf_op jit(solution)/shard_map/ppermute | solution.py:41
  100.5 11.8 %copy-start.12 = (bf16[544,512]{1,0:T(8,128)(2,1)}, bf16[544,512]{1,0:T(8,128)(2,1)S(1)}, u32[]{:S(2)}) copy-start(bf16[544,512]{1,0:T(8,128)(2,1)S(1)} %collective-permute-done.3.behind_ref) | copy-start | bytes 1671172
  100.5 11.8 %collective-permute-start.4 = (bf16[272,512]{1,0:T(8,128)(2,1)S(1)}, bf16[272,512]{1,0:T(8,128)(2,1)S(1)}, u32[]{:S(2)}, u32[]{:S(2)}) collective-permute-start(bf16[272,512]{1,0:T(8,128)(2,1)S(1)} %slice.61), channel_id=1, source_target_pairs={{0,1},{1,2},{2,3},{3,0},{4,5},{5,6},{6,7},{7,4},{8,9},{9,10},{10,1... | collective-permute-start | bytes 835592 | tf_op jit(solution)/shard_map/ppermute | solution.py:41
  102.6 20.9 %collective-permute-start.9 = (bf16[16,16,512]{2,1,0:T(8,128)(2,1)S(1)}, bf16[16,16,512]{2,1,0:T(8,128)(2,1)S(1)}, u32[]{:S(2)}, u32[]{:S(2)}) collective-permute-start(bf16[16,16,512]{2,1,0:T(8,128)(2,1)S(1)} %slice.55), channel_id=1, source_target_pairs={{0,24},{8,0},{16,8},{24,16},{1,25},{9,1},{17,9},{25,17},{2,26},{10... | collective-permute-start | bytes 786440 | tf_op jit(solution)/shard_map/ppermute | solution.py:41
  104.5 19.0 %collective-permute-start.10 = (bf16[16,16,512]{2,1,0:T(8,128)(2,1)S(1)}, bf16[16,16,512]{2,1,0:T(8,128)(2,1)S(1)}, u32[]{:S(2)}, u32[]{:S(2)}) collective-permute-start(bf16[16,16,512]{2,1,0:T(8,128)(2,1)S(1)} %slice.55), channel_id=1, source_target_pairs={{0,16},{8,24},{16,0},{24,8},{1,17},{9,25},{17,1},{25,9},{2,18},{10... | collective-permute-start | bytes 786440 | tf_op jit(solution)/shard_map/ppermute | solution.py:41
  107.8 4.5 %copy-start.15 = (bf16[272,512]{1,0:T(8,128)(2,1)}, bf16[272,512]{1,0:T(8,128)(2,1)S(1)}, u32[]{:S(2)}) copy-start(bf16[272,512]{1,0:T(8,128)(2,1)S(1)} %collective-permute-done.2.top_ref) | copy-start | bytes 835588
  107.8 15.7 %collective-permute-start.11 = (bf16[16,16,512]{2,1,0:T(8,128)(2,1)S(1)}, bf16[16,16,512]{2,1,0:T(8,128)(2,1)S(1)}, u32[]{:S(2)}, u32[]{:S(2)}) collective-permute-start(bf16[16,16,512]{2,1,0:T(8,128)(2,1)S(1)} %slice.55), channel_id=1, source_target_pairs={{0,8},{8,16},{16,24},{24,0},{1,9},{9,17},{17,25},{25,1},{2,10},{10... | collective-permute-start | bytes 786440 | tf_op jit(solution)/shard_map/ppermute | solution.py:41
  112.3 0.7 copy-start.16
  115.4 3.1 %copy-start = (bf16[256,2048]{1,0:T(8,128)(2,1)S(1)}, bf16[256,2048]{1,0:T(8,128)(2,1)}, u32[]{:S(2)}) copy-start(bf16[256,2048]{1,0:T(8,128)(2,1)} %get-tuple-element.36.out_mat_ref.refs_2_) | copy-start | bytes 3145732
  115.4 3.1 %copy-start.4 = (f32[256]{0:T(256)S(1)}, f32[256]{0:T(256)}, u32[]{:S(2)}) copy-start(f32[256]{0:T(256)} %param.28) | copy-start | bytes 3076
  115.4 3.1 %copy-start.5 = (bf16[256,2048]{1,0:T(8,128)(2,1)S(1)}, bf16[256,2048]{1,0:T(8,128)(2,1)}, u32[]{:S(2)}) copy-start(bf16[256,2048]{1,0:T(8,128)(2,1)} %get-tuple-element.35.in_ref) | copy-start | bytes 3145732
  115.5 3.1 %copy-start.6 = (f32[512,256]{1,0:T(8,128)S(1)}, f32[512,256]{1,0:T(8,128)}, u32[]{:S(2)}) copy-start(f32[512,256]{1,0:T(8,128)} %get-tuple-element.33.grow_ref) | copy-start | bytes 1572868
  115.5 3.0 %copy-start.7 = (f32[512,256]{1,0:T(8,128)S(1)}, f32[512,256]{1,0:T(8,128)}, u32[]{:S(2)}) copy-start(f32[512,256]{1,0:T(8,128)} %get-tuple-element.34.shrink_ref) | copy-start | bytes 1572868
  115.5 3.0 %copy-start.8 = (f32[5,16,1024]{2,1,0:T(8,128)S(1)}, f32[5,16,1024]{2,1,0:T(8,128)}, u32[]{:S(2)}) copy-start(f32[5,16,1024]{2,1,0:T(8,128)} %get-tuple-element.37.hop_re_ref) | copy-start | bytes 983044
  115.5 3.0 %copy-start.9 = (f32[5,16,1024]{2,1,0:T(8,128)S(1)}, f32[5,16,1024]{2,1,0:T(8,128)}, u32[]{:S(2)}) copy-start(f32[5,16,1024]{2,1,0:T(8,128)} %get-tuple-element.38.hop_im_ref) | copy-start | bytes 983044
  115.5 3.0 %copy-start.10 = (f32[1,128]{1,0:T(1,128)S(1)}, f32[1,128]{1,0:T(1,128)}, u32[]{:S(2)}) copy-start(f32[1,128]{1,0:T(1,128)} %get-tuple-element.39.shift_ref) | copy-start | bytes 1540
  123.5 2.3 %copy-start.1 = (f32[31,256]{1,0:T(8,128)S(1)}, f32[31,256]{1,0:T(8,128)}, u32[]{:S(2)}) copy-start(f32[31,256]{1,0:T(8,128)} %taps_ref.1) | copy-start | bytes 95236
  123.6 40.9 %copy-start.22 = (f32[256]{0:T(256)S(1)}, f32[256]{0:T(256)}, u32[]{:S(2)}) copy-start(f32[256]{0:T(256)} %param.31) | copy-start | bytes 3076
  123.6 55.7 %collective-permute-start.12 = (bf16[4,16,16,512]{3,2,1,0:T(8,128)(2,1)S(1)}, bf16[4,16,16,512]{3,2,1,0:T(8,128)(2,1)S(1)}, u32[]{:S(2)}, u32[]{:S(2)}) collective-permute-start(bf16[4,16,16,512]{3,2,1,0:T(8,128)(2,1)S(1)} %pad_maximum_fusion.refs_3_), channel_id=1, source_target_pairs={{0,4},{4,0},{1,5},{5,1},{2,6},{6,2},{3,7},{7,3},{8,12},{12,8},{9,1... | collective-permute-start | bytes 3145736 | tf_op jit(solution)/shard_map/ppermute | solution.py:36
  132.1 15.5 %collective-permute-start.8 = (f32[2,512]{1,0:T(2,128)S(1)}, f32[2,512]{1,0:T(2,128)S(1)}, u32[]{:S(2)}, u32[]{:S(2)}) collective-permute-start(f32[2,512]{1,0:T(2,128)S(1)} %get-tuple-element.32), channel_id=1, source_target_pairs={{0,1},{1,2},{2,3},{3,0},{4,5},{5,6},{6,7},{7,4},{8,9},{9,10},{10,1... | collective-permute-start | bytes 12296 | tf_op jit(solution)/shard_map/ppermute | solution.py:41
  134.0 13.5 %collective-permute-start.7 = (f32[2,512]{1,0:T(2,128)S(1)}, f32[2,512]{1,0:T(2,128)S(1)}, u32[]{:S(2)}, u32[]{:S(2)}) collective-permute-start(f32[2,512]{1,0:T(2,128)S(1)} %get-tuple-element.32), channel_id=1, source_target_pairs={{0,2},{1,3},{2,0},{3,1},{4,6},{5,7},{6,4},{7,5},{8,10},{9,11},{10,... | collective-permute-start | bytes 12296 | tf_op jit(solution)/shard_map/ppermute | solution.py:41
  140.0 7.6 %collective-permute-start.6 = (f32[2,512]{1,0:T(2,128)S(1)}, f32[2,512]{1,0:T(2,128)S(1)}, u32[]{:S(2)}, u32[]{:S(2)}) collective-permute-start(f32[2,512]{1,0:T(2,128)S(1)} %get-tuple-element.32), channel_id=1, source_target_pairs={{0,3},{1,0},{2,1},{3,2},{4,7},{5,4},{6,5},{7,6},{8,11},{9,8},{10,9... | collective-permute-start | bytes 12296 | tf_op jit(solution)/shard_map/ppermute | solution.py:41
  142.6 8.5 %all-to-all-start.2 = ((f32[8,1,2176]{2,1,0:T(1,128)}), f32[8,1,2176]{2,1,0:T(1,128)S(1)}, u32[]{:S(2)}, u32[]{:S(2)}) async-start(f32[8,1,2176]{2,1,0:T(1,128)} %broadcast_in_dim.15), calls=%async_computation.2 | async-start | bytes 139264 | tf_op jit(solution)/shard_map/all_to_all | solution.py:25
  152.8 26.5 %all-to-all-start.3 = ((f32[16,1,2176]{2,1,0:T(1,128)}), f32[16,1,2176]{2,1,0:T(1,128)S(1)}, u32[]{:S(2)}, u32[]{:S(2)}) async-start(f32[16,1,2176]{2,1,0:T(1,128)} %broadcast_in_dim.17), calls=%async_computation.3 | async-start | bytes 278528 | tf_op jit(solution)/shard_map/all_to_all | solution.py:25
  183.6 12.7 %collective-permute-start.13 = (bf16[64,2048]{1,0:T(8,128)(2,1)S(1)}, bf16[64,2048]{1,0:T(8,128)(2,1)S(1)}, u32[]{:S(2)}, u32[]{:S(2)}) collective-permute-start(bf16[64,2048]{1,0:T(8,128)(2,1)S(1)} %get-tuple-element.55), channel_id=1, source_target_pairs={{0,3},{1,0},{2,1},{3,2},{4,7},{5,4},{6,5},{7,6},{8,11},{9,8},{10,9... | collective-permute-start | bytes 786440 | tf_op jit(solution)/shard_map/ppermute | solution.py:41
  186.1 10.3 %collective-permute-start.15 = (bf16[64,2048]{1,0:T(8,128)(2,1)S(1)}, bf16[64,2048]{1,0:T(8,128)(2,1)S(1)}, u32[]{:S(2)}, u32[]{:S(2)}) collective-permute-start(bf16[64,2048]{1,0:T(8,128)(2,1)S(1)} %get-tuple-element.56), channel_id=1, source_target_pairs={{0,1},{1,2},{2,3},{3,0},{4,5},{5,6},{6,7},{7,4},{8,9},{9,10},{10,1... | collective-permute-start | bytes 786440 | tf_op jit(solution)/shard_map/ppermute | solution.py:41
  196.6 13.3 %collective-permute-start.16 = (bf16[128,2048]{1,0:T(8,128)(2,1)S(1)}, bf16[128,2048]{1,0:T(8,128)(2,1)S(1)}, u32[]{:S(2)}, u32[]{:S(2)}) collective-permute-start(bf16[128,2048]{1,0:T(8,128)(2,1)S(1)} %get-tuple-element.54), channel_id=1, source_target_pairs={{0,1},{1,2},{2,3},{3,0},{4,5},{5,6},{6,7},{7,4},{8,9},{9,10},{10,1... | collective-permute-start | bytes 1572872 | tf_op jit(solution)/shard_map/ppermute | solution.py:41
  200.5 11.5 %collective-permute-start.14 = (bf16[128,2048]{1,0:T(8,128)(2,1)S(1)}, bf16[128,2048]{1,0:T(8,128)(2,1)S(1)}, u32[]{:S(2)}, u32[]{:S(2)}) collective-permute-start(bf16[128,2048]{1,0:T(8,128)(2,1)S(1)} %get-tuple-element.53), channel_id=1, source_target_pairs={{0,3},{1,0},{2,1},{3,2},{4,7},{5,4},{6,5},{7,6},{8,11},{9,8},{10,9... | collective-permute-start | bytes 1572872 | tf_op jit(solution)/shard_map/ppermute | solution.py:41

commit v8 on v7

--- a/solution.py
+++ b/solution.py
@@ -39,11 +39,6 @@
 def from_ahead(block, axis, distance):
     count = lax.axis_size(axis)
     return lax.ppermute(block, axis, [(i, (i - distance) % count) for i in range(count)])
-
-
-def from_own_on(planes, axis):
-    peers = lax.axis_size(axis)
-    return [planes] + [from_ahead(planes, axis, d) for d in range(1, peers)]
 
 
 def far_from_core(*arrays):
@@ -434,19 +429,35 @@
         prefix_ref[k : k + 1] = row
 
 
-def merge_rows(distances, carried, place_ref, conv_ref, refs):
-    (y_all, power_all, read_all, own_ref, other_ref, out_ref) = refs[:6]
-    weight_ref, weight_done, y_ref, power_ref, read_ref, done = refs[6:]
+def channel_norm(raw, first, second, gain):
+    row = lax.broadcasted_iota(jnp.int32, (raw.shape[0], raw.shape[0]), 0)
+    same = row == lax.broadcasted_iota(jnp.int32, row.shape, 1)
+
+    def upright(line):
+        return jnp.sum(jnp.where(same, line, 0.0), axis=1, keepdims=True)
+
+    middle = upright(first) / CONV_W
+    spread = upright(second) / CONV_W - middle * middle
+    scaled = (raw - middle) * lax.rsqrt(spread + EPS) * gain
+    return jax.nn.silu(scaled).astype(BF16)
+
+
+def merge_rows(distances, carried, place_ref, channel, refs):
+    gain_ref, *sums_refs = channel
+    raw_all, y_all, power_all, read_all, own_ref, other_ref, out_ref = refs[:7]
+    weight_ref, weight_done, raw_ref, y_ref, power_ref, read_ref, done = refs[7:]
     block = out_ref.shape[1]
-    parts = conv_ref.shape[0] // block
+    parts = len(sums_refs)
+    sums = sum((ref[...] for ref in sums_refs[1:]), sums_refs[0][...])
     places = [
         pl.ds(pl.multiple_of(lax.rem(place_ref[2] + distance, parts) * block, block), block)
         for distance in distances
     ]
     begun = [fetch(read_all, read_ref, done.at[0])]
     for k, rows in enumerate(places):
-        begun.append(fetch(power_all.at[rows], power_ref.at[k], done.at[1 + 2 * k]))
-        begun.append(fetch(y_all.at[rows], y_ref.at[k], done.at[2 + 2 * k]))
+        begun.append(fetch(power_all.at[rows], power_ref.at[k], done.at[1 + 3 * k]))
+        begun.append(fetch(y_all.at[rows], y_ref.at[k], done.at[2 + 3 * k]))
+        begun.append(fetch(raw_all.at[rows], raw_ref.at[k], done.at[3 + 3 * k]))
     weights_begun = natural_order(
         place_ref, own_ref, other_ref, weight_ref, weight_done, from_own_x=True
     )
@@ -458,19 +469,27 @@
     blend_im = (c_im * h_re - c_re * h_im).astype(BF16)
     arrived(weights_begun)
     weights = weight_ref[...].reshape(out_ref.shape[2], -1)
-    for k, rows in enumerate(places):
+    for k, distance in enumerate(distances):
+        mine = lax.rem(place_ref[2] + distance, parts)
+        first, second = jnp.zeros((1, block), F32), jnp.zeros((1, block), F32)
+        for part in range(parts):
+            lines = sums[:, part * block : (part + 1) * block]
+            first = jnp.where(mine == part, lines[0:1], first)
+            second = jnp.where(mine == part, lines[1:2], second)
+        conv = channel_norm(raw_ref[k], first, second, gain_ref[...])
         total = (
             y_ref[k]
             + dot_rows(power_ref[k, :, :lanes], blend_re)
             + dot_rows(power_ref[k, :, lanes:], blend_im)
         )
         ssm = jax.nn.gelu(total).astype(BF16)
-        both = jnp.concatenate([ssm, conv_ref[rows]], axis=1)
+        both = jnp.concatenate([ssm, conv], axis=1)
         out_ref[k] = dot_rows(both, weights).astype(BF16)
 
 
-def opposite_kernel(count, place_ref, conv_ref, far_ref, rates_ref, prefix_ref, start_ref, *refs):
-    *inputs, out_ref, h_ref, weight_ref, weight_done, y_ref, power_ref, read_ref, done = refs
+def opposite_kernel(count, place_ref, *refs):
+    channel, (far_ref, rates_ref, prefix_ref, start_ref) = refs[:5], refs[5:9]
+    *inputs, out_ref, h_ref, weight_ref, weight_done, raw_ref, y_ref, power_ref, read_ref, done = refs[9:]
     peers_z, peers_near = far_ref.shape[0], 2 * inputs[-1].shape[0]
 
     def carried():
@@ -493,13 +512,14 @@
         (2,),
         carried,
         place_ref,
-        conv_ref,
-        (*inputs, out_ref, weight_ref, weight_done, y_ref, power_ref, read_ref, done),
-    )
-
-
-def rest_kernel(place_ref, conv_ref, h_ref, *refs):
-    merge_rows((0, 1, 3), lambda: (h_ref[0:1], h_ref[1:2]), place_ref, conv_ref, refs)
+        channel,
+        (*inputs, out_ref, weight_ref, weight_done, raw_ref, y_ref, power_ref, read_ref, done),
+    )
+
+
+def rest_kernel(place_ref, *refs):
+    channel, h_ref = refs[:5], refs[5]
+    merge_rows((0, 1, 3), lambda: (h_ref[0:1], h_ref[1:2]), place_ref, channel, refs[6:])
 
 
 def input_matrix(eigen_real, eigen_imag, step, state_input):
@@ -581,15 +601,6 @@
     return scan, power, out, device
 
 
-def conv_finish(raw, sums, channel_gain):
-    others = [from_ahead(sums, "tp", d) for d in range(1, lax.axis_size("tp"))]
-    first, second = (row[:, None] for row in sum(others, sums))
-    middle = first / CONV_W
-    spread = second / CONV_W - middle * middle
-    scaled = (raw - middle) * lax.rsqrt(spread + EPS) * channel_gain
-    return jax.nn.silu(scaled).astype(BF16)
-
-
 def mixer(
     tokens,
     norm_gain,
@@ -643,7 +654,11 @@
         bytes_accessed=4 * count * depth,
         transcendentals=count,
     )
-    merge_pieces = from_own_on(planes[:, :, 3 * width :], "x")
+    merge_planes, normed = lax.optimization_barrier((planes[:, :, 3 * width :], normed))
+    merge_ahead = from_ahead(merge_planes, "x", 1)
+    merge_behind = from_ahead(merge_planes, "x", -1)
+    merge_across = from_ahead(merge_planes, "x", 2)
+    merge_pieces = (merge_planes, merge_ahead, merge_across, merge_behind)
     project_other = partner(project_x)
     u_in = call(
         state_in_kernel,
@@ -715,7 +730,7 @@
         bytes_accessed=4 * depth * count,
         transcendentals=0,
     )
-    conv_out = conv_finish(raw, sums, channel_gain)
+    all_sums = [sums] + [from_ahead(sums, "tp", d) for d in range(1, parts)]
 
     block = count // parts
 
@@ -723,15 +738,16 @@
         return call(
             kernel,
             (jax.ShapeDtypeStruct((blocks, block, depth), BF16), *more),
-            (conv_out, *arrays),
-            apart=(*far_from_core(y_local, power, reads), merge_x, merge_other),
+            (channel_gain.reshape(1, -1), *all_sums, *arrays),
+            apart=(*far_from_core(raw, y_local, power, reads), merge_x, merge_other),
             scalars=(place,),
             scratch=(
                 *weight_scratch(merge_x, 2 * width),
                 pltpu.VMEM((blocks, block, width), F32),
+                pltpu.VMEM((blocks, block, width), F32),
                 pltpu.VMEM((blocks, block, 2 * lanes), BF16),
                 pltpu.VMEM((width, 2 * lanes), BF16),
-                pltpu.SemaphoreType.DMA((1 + 2 * blocks,)),
+                pltpu.SemaphoreType.DMA((1 + 3 * blocks,)),
             ),
             flops=4 * block * blocks * depth * width,
             bytes_accessed=4 * depth * count,

time: 216 us -> 215 us (level)
  blocking collectives: 18.4 us -> 26.9 us
  starting transfers between devices: 84.4 us -> 76.4 us
    all_to_all x3 -> x2, waiting for transfers between devices: 41.8 us -> 24.7 us  [copies(): lax.all_to_all(jnp.broadcast_to(value[None], (peers, *value.shape)), axis...]
    ppermute x14, waiting for transfers between devices: 19.8 us -> 34.8 us  [from_ahead(): lax.ppermute(block, axis, [(i, (i - distance) % count) for i in range(cou...]
    all_to_all x1 -> x2, blocking collectives: 18.4 us -> 26.9 us  [copies(): lax.all_to_all(jnp.broadcast_to(value[None], (peers, *value.shape)), axis...]
    all_to_all x3 -> x2, starting transfers between devices: 31.8 us -> 26 us  [copies(): lax.all_to_all(jnp.broadcast_to(value[None], (peers, *value.shape)), axis...]
  transfers between devices with their start and end apart: 20 -> 19, of which waited for: 9 -> 12; matrix products, arithmetic and copies ran while one was open for 2% -> 2% of each run, Pallas kernels for 15% -> 15%
where the time goes in v8:
time: 215 us; the launch traced here: 212 us
  starting transfers between devices  76.4 us (36%)
  waiting for transfers between devices  62.4 us (29%)
  Pallas kernels  36.4 us (17%)
  blocking collectives  26.9 us (13%)
  local copies, waits for them, and re-layouts  4.81 us (2%)
  other arithmetic  4.15 us (2%)
    ppermute x14, starting transfers between devices, from_ahead(): lax.ppermute(block, axis, [(i, (i - distance) % count) for i in range(cou...  44 us
    pallas_call x8, Pallas kernels, call(): pl.pallas_call(body, compiler_params=pltpu.CompilerParams(vmem_limit_byte...  36.4 us
    ppermute x14, waiting for transfers between devices, from_ahead(): lax.ppermute(block, axis, [(i, (i - distance) % count) for i in range(cou...  34.8 us
    all_to_all x2, blocking collectives, copies(): lax.all_to_all(jnp.broadcast_to(value[None], (peers, *value.shape)), axis...  26.9 us
    all_to_all x2, starting transfers between devices, copies(): lax.all_to_all(jnp.broadcast_to(value[None], (peers, *value.shape)), axis...  26 us
    all_to_all x2, waiting for transfers between devices, copies(): lax.all_to_all(jnp.broadcast_to(value[None], (peers, *value.shape)), axis...  24.7 us
  transfers between devices with their start and end apart: 19, of which 12 were waited for; matrix products, arithmetic and copies ran while one was open for 2% of the time, Pallas kernels for 15%

profile of v8, /device:TPU:6, one launch (start us, length us, event | category | flops | bytes accessed | tf_op | source)
XLA Modules:
  0.0 211.7 jit_solution(9339012544773989299)
XLA Ops:
  0.0 0.8 maximum_bitcast_fusion
  0.8 0.7 pad_maximum_fusion.1
  1.5 0.9 broadcast_in_dim.12
  2.4 15.2 %all-to-all-start = ((bf16[16,16,1280]{2,1,0:T(8,128)(2,1)}), bf16[16,16,1280]{2,1,0:T(8,128)(2,1)S(1)}, u32[]{:S(2)}, u32[]{:S(2)}) async-start(bf16[16,16,1280]{2,1,0:T(8,128)(2,1)} %broadcast_in_dim.12), calls=%async_computation | async-start | bytes 1310720 | tf_op jit(solution)/shard_map/all_to_all | solution.py:25
  17.6 0.0 copy-start.4
  17.7 0.1 fusion.14
  17.8 0.1 reshape.133.refs_1_
  17.9 0.1 mul.192
  17.9 0.1 mul.164
  18.0 0.1 reshape.134.refs_8_
  18.2 0.3 multiply_sine_fusion.1
  18.5 0.6 fusion.11
  19.1 7.4 %shard_map.163 = (f32[512,256]{1,0:T(8,128)}, f32[512,256]{1,0:T(8,128)}, bf16[256,2048]{1,0:T(8,128)(2,1)}, bf16[256,2048]{1,0:T(8,128)(2,1)}, f32[5,16,1024]{2...) custom-call(f32[16,512]{1,0:T(8,128)S(1)} %copy-done.4, ...), custom_call_target="tpu_custom_call" | custom-call | flops 83886080 | bytes 4194304 | tf_op jit(solution)/shard_map/pallas_call | solution.py:53
  26.6 24.7 %all-to-all-done = bf16[16,16,1280]{2,1,0:T(8,128)(2,1)S(1)} async-done(((bf16[16,16,1280]{2,1,0:T(8,128)(2,1)}), bf16[16,16,1280]{2,1,0:T(8,128)(2,1)S(1)}, u32[]{:S(2)}, u32[]{:S(2)}) %all-to-all-start) | async-done | bytes 655392 | tf_op jit(solution)/shard_map/all_to_all | solution.py:25
  51.3 0.1 broadcast_in_dim.13
  51.5 0.0 copy-start.16
  51.5 18.4 %all_to_all.20.own_ref = bf16[4,16,16,768]{3,2,1,0:T(8,128)(2,1)} all-to-all(bf16[4,16,16,768]{3,2,1,0:T(8,128)(2,1)S(1)} %broadcast_in_dim.13), channel_id=1, replica_groups=mesh['z'=16,'x'=4,'c'=2,'tp'=4] {'x'}, dimensions={0} | all-to-all | bytes 3145728 | tf_op jit(solution)/shard_map/all_to_all | solution.py:25
  69.8 2.0 collective-permute-start.5
  71.9 2.4 %collective-permute-start = (bf16[32,512]{1,0:T(8,128)(2,1)S(1)}, bf16[32,512]{1,0:T(8,128)(2,1)S(1)}, u32[]{:S(2)}, u32[]{:S(2)}) collective-permute-start(bf16[32,512]{1,0:T(8,128)(2,1)S(1)} %slice.52), channel_id=1, source_target_pairs={{0,4},{4,8},{8,12},{12,16},{16,20},{20,24},{24,28},{28,32},{32,36}... | collective-permute-start | bytes 98312 | tf_op jit(solution)/shard_map/ppermute | solution.py:32
  74.3 2.8 %collective-permute-done = bf16[32,512]{1,0:T(8,128)(2,1)S(1)} collective-permute-done((bf16[32,512]{1,0:T(8,128)(2,1)S(1)}, bf16[32,512]{1,0:T(8,128)(2,1)S(1)}, u32[]{:S(2)}, u32[]{:S(2)}) %collective-permute-start) | collective-permute-done | bytes 32800 | tf_op jit(solution)/shard_map/ppermute | solution.py:32
  77.2 4.9 %collective-permute-start.1 = (bf16[544,512]{1,0:T(8,128)(2,1)S(1)}, bf16[544,512]{1,0:T(8,128)(2,1)S(1)}, u32[]{:S(2)}, u32[]{:S(2)}) collective-permute-start(bf16[544,512]{1,0:T(8,128)(2,1)S(1)} %constant_dynamic-update-slice_fusion.own_ref), channel_id=1, source_target_pairs={{0,3},{1,0},{2,1},{3,2},{4,7},{5,4},{6,5},{7,6},{8,11},{9,8},{10,9... | collective-permute-start | bytes 1671176 | tf_op jit(solution)/shard_map/ppermute | solution.py:41
  82.1 1.9 collective-permute-start.3
  84.1 10.5 %collective-permute-done.1.ahead_ref = bf16[544,512]{1,0:T(8,128)(2,1)S(1)} collective-permute-done((bf16[544,512]{1,0:T(8,128)(2,1)S(1)}, bf16[544,512]{1,0:T(8,128)(2,1)S(1)}, u32[]{:S(2)}, u32[]{:S(2)}) %collective-permute-start.1) | collective-permute-done | bytes 557088 | tf_op jit(solution)/shard_map/ppermute | solution.py:41
  94.6 5.6 %collective-permute-start.2 = (bf16[272,512]{1,0:T(8,128)(2,1)S(1)}, bf16[272,512]{1,0:T(8,128)(2,1)S(1)}, u32[]{:S(2)}, u32[]{:S(2)}) collective-permute-start(bf16[272,512]{1,0:T(8,128)(2,1)S(1)} %slice.62), channel_id=1, source_target_pairs={{0,3},{1,0},{2,1},{3,2},{4,7},{5,4},{6,5},{7,6},{8,11},{9,8},{10,9... | collective-permute-start | bytes 835592 | tf_op jit(solution)/shard_map/ppermute | solution.py:41
  100.2 0.3 collective-permute-done.3.behind_ref
  100.5 0.8 copy-done.14
  101.3 1.9 collective-permute-start.4
  103.2 0.1 pad_add_fusion.place_ref
  103.3 3.3 %collective-permute-done.2.top_ref = bf16[272,512]{1,0:T(8,128)(2,1)S(1)} collective-permute-done((bf16[272,512]{1,0:T(8,128)(2,1)S(1)}, bf16[272,512]{1,0:T(8,128)(2,1)S(1)}, u32[]{:S(2)}, u32[]{:S(2)}) %collective-permute-start.2) | collective-permute-done | bytes 278560 | tf_op jit(solution)/shard_map/ppermute | solution.py:41
  106.6 6.4 %collective-permute-done.4.bottom_ref = bf16[272,512]{1,0:T(8,128)(2,1)S(1)} collective-permute-done((bf16[272,512]{1,0:T(8,128)(2,1)S(1)}, bf16[272,512]{1,0:T(8,128)(2,1)S(1)}, u32[]{:S(2)}, u32[]{:S(2)}) %collective-permute-start.4) | collective-permute-done | bytes 278560 | tf_op jit(solution)/shard_map/ppermute | solution.py:41
  113.1 0.7 copy-done.18
  113.8 2.4 %shard_map.164.normed_ref = bf16[4,544,512]{2,1,0:T(8,128)(2,1)S(1)} custom-call(s32[4]{0:T(128)S(1)} %pad_add_fusion.place_ref, bf16[544,512]{1,0:T(8,128)(2,1)} %copy-done.15, bf16[544,512]{1,0:T(8,128)(2,1)} %copy-done.13, bf16[272,512]{1,0:T(8,128)(2,1)} %copy-done.17, bf16[272,512]{1,0:T(8,128)(2,1)} %copy-done.18, bf16[544,512]{1,0:T(8,128)(2,1)} %copy-done.14, ...), custom_call_target="tpu_custom_call" | custom-call | flops 8388608 | bytes 4194304 | tf_op jit(solution)/shard_map/pallas_call | solution.py:53
  116.2 1.0 slice.51
  117.2 1.9 collective-permute-start.9
  119.1 2.3 %collective-permute-start.10 = (bf16[16,16,512]{2,1,0:T(8,128)(2,1)S(1)}, bf16[16,16,512]{2,1,0:T(8,128)(2,1)S(1)}, u32[]{:S(2)}, u32[]{:S(2)}) collective-permute-start(bf16[16,16,512]{2,1,0:T(8,128)(2,1)S(1)} %slice.51), channel_id=1, source_target_pairs={{0,16},{8,24},{16,0},{24,8},{1,17},{9,25},{17,1},{25,9},{2,18},{10... | collective-permute-start | bytes 786440 | tf_op jit(solution)/shard_map/ppermute | solution.py:41
  121.5 4.7 %collective-permute-start.11 = (bf16[16,16,512]{2,1,0:T(8,128)(2,1)S(1)}, bf16[16,16,512]{2,1,0:T(8,128)(2,1)S(1)}, u32[]{:S(2)}, u32[]{:S(2)}) collective-permute-start(bf16[16,16,512]{2,1,0:T(8,128)(2,1)S(1)} %slice.51), channel_id=1, source_target_pairs={{0,8},{8,16},{16,24},{24,0},{1,9},{9,17},{17,25},{25,1},{2,10},{10... | collective-permute-start | bytes 786440 | tf_op jit(solution)/shard_map/ppermute | solution.py:41
  126.2 0.1 fusion.5.lower_ref
  126.3 0.0 copy-start.7
  126.4 2.9 %shard_map.166.u_ref = bf16[512,256]{1,0:T(8,128)(2,1)S(1)} custom-call(s32[4]{0:T(128)S(1)} %pad_add_fusion.place_ref, bf16[4,544,512]{2,1,0:T(8,128)(2,1)S(1)} %shard_map.164.normed_ref, bf16[4,16,16,768]{3,2,1,0:T(8,128)(2,1)} %all_to_all.20.own_ref, bf16[4,16,16,768]{3,2,1,0:T(8,128)(2,1)} %collective-permute-done.5.other_ref), custom_call_target="tpu_custom_call" | custom-call | flops 536870912 | bytes 4194304 | tf_op jit(solution)/shard_map/pallas_call | solution.py:53
  129.4 5.0 %shard_map.167 = (f32[512,256]{1,0:T(8,128)}, f32[1,2176]{1,0:T(1,128)S(1)}) custom-call(bf16[512,256]{1,0:T(8,128)(2,1)S(1)} %shard_map.166.u_ref, f32[512,256]{1,0:T(8,128)S(1)} %copy-done.7, f32[512,256]{1,0:T(8,128)S(1)} %copy-done.8, bf16[256,2048]{1,0:T(8,128)(2,1)S(1)} %copy-done.6, bf16[256,2048]{1,0:T(8,128)(2,1)S(1)} %copy-done, ...), custom_call_target="tpu_custom_call" | custom-call | flops 1610612736 | bytes 4194304 | tf_op jit(solution)/shard_map/pallas_call | solution.py:53
  134.4 1.5 collective-permute-done.11
  135.9 0.1 pad_maximum_fusion.refs_13_.refs_10_
  136.1 1.9 collective-permute-start.12
  138.1 8.6 %all_to_all.21.near_ref = f32[8,1,2176]{2,1,0:T(1,128)S(1)} all-to-all(f32[8,1,2176]{2,1,0:T(1,128)S(1)} %broadcast_in_dim.15), channel_id=1, replica_groups=mesh['z'=16,'x'=4,'c'=2,'tp'=4] {'x','c'}, dimensions={0} | all-to-all | bytes 139264 | tf_op jit(solution)/shard_map/all_to_all | solution.py:25
  146.7 0.9 shard_map.168
  147.6 0.7 broadcast_in_dim.17
  148.3 10.8 %all-to-all-start.3 = ((f32[16,1,2176]{2,1,0:T(1,128)}), f32[16,1,2176]{2,1,0:T(1,128)S(1)}, u32[]{:S(2)}, u32[]{:S(2)}) async-start(f32[16,1,2176]{2,1,0:T(1,128)} %broadcast_in_dim.17), calls=%async_computation.3 | async-start | bytes 278528 | tf_op jit(solution)/shard_map/all_to_all | solution.py:25
  159.2 6.3 %shard_map.165 = (f32[512,256]{1,0:T(8,128)}, f32[2,512]{1,0:T(2,128)S(1)}) custom-call(s32[4]{0:T(128)S(1)} %pad_add_fusion.place_ref, bf16[4,544,512]{2,1,0:T(8,128)(2,1)S(1)} %shard_map.164.normed_ref, f32[31,256]{1,0:T(8,128)S(1)} %copy-done.1, bf16[4,16,16,768]{3,2,1,0:T(8,128)(2,1)} %all_to_all.20.own_ref, ...), custom_call_target="tpu_custom_call" | custom-call | flops 1073741824 | bytes 4194304 | tf_op jit(solution)/shard_map/pallas_call | solution.py:53
  165.6 1.9 collective-permute-start.6
  167.5 3.3 %collective-permute-start.7 = (f32[2,512]{1,0:T(2,128)S(1)}, f32[2,512]{1,0:T(2,128)S(1)}, u32[]{:S(2)}, u32[]{:S(2)}) collective-permute-start(f32[2,512]{1,0:T(2,128)S(1)} %get-tuple-element.34.refs_1_), channel_id=1, source_target_pairs={{0,2},{1,3},{2,0},{3,1},{4,6},{5,7},{6,4},{7,5},{8,10},{9,11},{10,... | collective-permute-start | bytes 12296 | tf_op jit(solution)/shard_map/ppermute | solution.py:41
  170.8 2.5 %collective-permute-start.8 = (f32[2,512]{1,0:T(2,128)S(1)}, f32[2,512]{1,0:T(2,128)S(1)}, u32[]{:S(2)}, u32[]{:S(2)}) collective-permute-start(f32[2,512]{1,0:T(2,128)S(1)} %get-tuple-element.34.refs_1_), channel_id=1, source_target_pairs={{0,1},{1,2},{2,3},{3,0},{4,5},{5,6},{6,7},{7,4},{8,9},{9,10},{10,1... | collective-permute-start | bytes 12296 | tf_op jit(solution)/shard_map/ppermute | solution.py:41
  173.3 1.1 collective-permute-done.7.refs_3_
  174.5 3.1 %collective-permute-done.8.refs_4_ = f32[2,512]{1,0:T(2,128)S(1)} collective-permute-done((f32[2,512]{1,0:T(2,128)S(1)}, f32[2,512]{1,0:T(2,128)S(1)}, u32[]{:S(2)}, u32[]{:S(2)}) %collective-permute-start.8) | collective-permute-done | bytes 4128 | tf_op jit(solution)/shard_map/ppermute | solution.py:41
  177.6 4.3 %shard_map.169 = (bf16[1,128,2048]{2,1,0:T(8,128)(2,1)S(1)}, f32[2,1024]{1,0:T(2,128)S(1)}) custom-call(s32[4]{0:T(128)S(1)} %pad_add_fusion.place_ref, f32[1,256]{1,0:T(1,128)S(1)} %bitcast.57, f32[2,512]{1,0:T(2,128)S(1)} %get-tuple-element.34.refs_1_, f32[2,512]{1,0:T(2,128)S(1)} %collective-permute-done.6.refs_2_, ...), custom_call_target="tpu_custom_call" | custom-call | flops 268435456 | bytes 4194304 | tf_op jit(solution)/shard_map/pallas_call | solution.py:53
  182.0 3.9 %collective-permute-start.13 = (bf16[64,2048]{1,0:T(8,128)(2,1)S(1)}, bf16[64,2048]{1,0:T(8,128)(2,1)S(1)}, u32[]{:S(2)}, u32[]{:S(2)}) collective-permute-start(bf16[64,2048]{1,0:T(8,128)(2,1)S(1)} %get-tuple-element.59), channel_id=1, source_target_pairs={{0,3},{1,0},{2,1},{3,2},{4,7},{5,4},{6,5},{7,6},{8,11},{9,8},{10,9... | collective-permute-start | bytes 786440 | tf_op jit(solution)/shard_map/ppermute | solution.py:41
  185.9 1.9 collective-permute-start.15
  187.8 7.0 %shard_map.170 = bf16[3,128,2048]{2,1,0:T(8,128)(2,1)S(1)} custom-call(s32[4]{0:T(128)S(1)} %pad_add_fusion.place_ref, f32[1,256]{1,0:T(1,128)S(1)} %bitcast.58, f32[2,512]{1,0:T(2,128)S(1)} %get-tuple-element.34.refs_1_, f32[2,512]{1,0:T(2,128)S(1)} %collective-permute-done.6.refs_2_, f32[2,512]{1,0:T(2,128)S(1)} %collective-permute-done.7.refs_3_, ...), custom_call_target="tpu_custom_call" | custom-call | flops 805306368 | bytes 4194304 | tf_op jit(solution)/shard_map/pallas_call | solution.py:53
  194.9 0.5 collective-permute-done.15
  195.4 0.2 fusion.1
  195.6 1.9 collective-permute-start.16
  197.5 5.1 %collective-permute-start.14 = (bf16[128,2048]{1,0:T(8,128)(2,1)S(1)}, bf16[128,2048]{1,0:T(8,128)(2,1)S(1)}, u32[]{:S(2)}, u32[]{:S(2)}) collective-permute-start(bf16[128,2048]{1,0:T(8,128)(2,1)S(1)} %get-tuple-element.57), channel_id=1, source_target_pairs={{0,3},{1,0},{2,1},{3,2},{4,7},{5,4},{6,5},{7,6},{8,11},{9,8},{10,9... | collective-permute-start | bytes 1572872 | tf_op jit(solution)/shard_map/ppermute | solution.py:41
  202.6 6.9 %collective-permute-done.16 = bf16[128,2048]{1,0:T(8,128)(2,1)S(1)} collective-permute-done((bf16[128,2048]{1,0:T(8,128)(2,1)S(1)}, bf16[128,2048]{1,0:T(8,128)(2,1)S(1)}, u32[]{:S(2)}, u32[]{:S(2)}) %collective-permute-start.16) | collective-permute-done | bytes 524320 | tf_op jit(solution)/shard_map/ppermute | solution.py:41
  209.5 1.2 collective-permute-done.14
  210.7 1.0 fusion.3
  (71 shorter events, 0.5 us)
Async XLA Ops:
  0.0 17.6 %copy-start.24 = (f32[16]{0:T(128)S(1)}, f32[16]{0:T(128)}, u32[]{:S(2)}) copy-start(f32[16]{0:T(128)} %param.24) | copy-start | bytes 196
  0.0 17.6 %copy-start.22 = (f32[16,64]{1,0:T(8,128)S(1)}, f32[16,64]{1,0:T(8,128)}, u32[]{:S(2)}) copy-start(f32[16,64]{1,0:T(8,128)} %param.23) | copy-start | bytes 12292
  0.0 17.7 %copy-start.23 = (f32[16,64]{1,0:T(8,128)S(1)}, f32[16,64]{1,0:T(8,128)}, u32[]{:S(2)}) copy-start(f32[16,64]{1,0:T(8,128)} %param.22) | copy-start | bytes 12292
  0.0 18.0 %copy-start.21 = (f32[2,16,64]{2,1,0:T(8,128)S(1)}, f32[2,16,64]{2,1,0:T(8,128)}, u32[]{:S(2)}) copy-start(f32[2,16,64]{2,1,0:T(8,128)} %param.29) | copy-start | bytes 24580
  0.0 18.1 %copy-start.19 = (f32[2,16,16,64]{3,2,1,0:T(8,128)S(1)}, f32[2,16,16,64]{3,2,1,0:T(8,128)}, u32[]{:S(2)}) copy-start(f32[2,16,16,64]{3,2,1,0:T(8,128)} %param.26) | copy-start | bytes 393220
  1.5 17.0 %copy-start.20 = (f32[2,16,16,64]{3,2,1,0:T(8,128)S(1)}, f32[2,16,16,64]{3,2,1,0:T(8,128)}, u32[]{:S(2)}) copy-start(f32[2,16,16,64]{3,2,1,0:T(8,128)} %param.27) | copy-start | bytes 393220
  2.4 48.9 %all-to-all-start = ((bf16[16,16,1280]{2,1,0:T(8,128)(2,1)}), bf16[16,16,1280]{2,1,0:T(8,128)(2,1)S(1)}, u32[]{:S(2)}, u32[]{:S(2)}) async-start(bf16[16,16,1280]{2,1,0:T(8,128)(2,1)} %broadcast_in_dim.12), calls=%async_computation | async-start | bytes 1310720 | tf_op jit(solution)/shard_map/all_to_all | solution.py:25
  17.6 1.5 copy-start.4
  51.3 18.5 %copy-start.12 = (bf16[16,16,1280]{2,1,0:T(8,128)(2,1)}, bf16[16,16,1280]{2,1,0:T(8,128)(2,1)S(1)}, u32[]{:S(2)}) copy-start(bf16[16,16,1280]{2,1,0:T(8,128)(2,1)S(1)} %all-to-all-done) | copy-start | bytes 1966084
  51.5 20.4 %copy-start.16 = (bf16[512,512]{1,0:T(8,128)(2,1)S(1)}, bf16[512,512]{1,0:T(8,128)(2,1)}, u32[]{:S(2)}) copy-start(bf16[512,512]{1,0:T(8,128)(2,1)} %param.17) | copy-start | bytes 1572868
  69.8 44.0 %copy-start.2 = (f32[2048]{0:T(1024)S(1)}, f32[2048]{0:T(1024)}, u32[]{:S(2)}) copy-start(f32[2048]{0:T(1024)} %param.18) | copy-start | bytes 24580
  69.8 56.5 %collective-permute-start.5 = (bf16[4,16,16,768]{3,2,1,0:T(8,128)(2,1)}, bf16[4,16,16,768]{3,2,1,0:T(8,128)(2,1)}, u32[]{:S(2)}, u32[]{:S(2)}) collective-permute-start(bf16[4,16,16,768]{3,2,1,0:T(8,128)(2,1)} %all_to_all.20.own_ref), channel_id=1, source_target_pairs={{0,4},{4,0},{1,5},{5,1},{2,6},{6,2},{3,7},{7,3},{8,12},{12,8},{9,1... | collective-permute-start | bytes 4718600 | tf_op jit(solution)/shard_map/ppermute | solution.py:36
  71.9 5.2 %collective-permute-start = (bf16[32,512]{1,0:T(8,128)(2,1)S(1)}, bf16[32,512]{1,0:T(8,128)(2,1)S(1)}, u32[]{:S(2)}, u32[]{:S(2)}) collective-permute-start(bf16[32,512]{1,0:T(8,128)(2,1)S(1)} %slice.52), channel_id=1, source_target_pairs={{0,4},{4,8},{8,12},{12,16},{16,20},{20,24},{24,28},{28,32},{32,36}... | collective-permute-start | bytes 98312 | tf_op jit(solution)/shard_map/ppermute | solution.py:32
  77.2 24.1 %copy-start.15 = (bf16[544,512]{1,0:T(8,128)(2,1)}, bf16[544,512]{1,0:T(8,128)(2,1)S(1)}, u32[]{:S(2)}) copy-start(bf16[544,512]{1,0:T(8,128)(2,1)S(1)} %constant_dynamic-update-slice_fusion.own_ref) | copy-start | bytes 1671172
  77.2 17.4 %collective-permute-start.1 = (bf16[544,512]{1,0:T(8,128)(2,1)S(1)}, bf16[544,512]{1,0:T(8,128)(2,1)S(1)}, u32[]{:S(2)}, u32[]{:S(2)}) collective-permute-start(bf16[544,512]{1,0:T(8,128)(2,1)S(1)} %constant_dynamic-update-slice_fusion.own_ref), channel_id=1, source_target_pairs={{0,3},{1,0},{2,1},{3,2},{4,7},{5,4},{6,5},{7,6},{8,11},{9,8},{10,9... | collective-permute-start | bytes 1671176 | tf_op jit(solution)/shard_map/ppermute | solution.py:41
  82.1 18.4 %collective-permute-start.3 = (bf16[544,512]{1,0:T(8,128)(2,1)S(1)}, bf16[544,512]{1,0:T(8,128)(2,1)S(1)}, u32[]{:S(2)}, u32[]{:S(2)}) collective-permute-start(bf16[544,512]{1,0:T(8,128)(2,1)S(1)} %constant_dynamic-update-slice_fusion.own_ref), channel_id=1, source_target_pairs={{0,1},{1,2},{2,3},{3,0},{4,5},{5,6},{6,7},{7,4},{8,9},{9,10},{10,1... | collective-permute-start | bytes 1671176 | tf_op jit(solution)/shard_map/ppermute | solution.py:41
  94.6 19.2 %copy-start.13 = (bf16[544,512]{1,0:T(8,128)(2,1)}, bf16[544,512]{1,0:T(8,128)(2,1)S(1)}, u32[]{:S(2)}) copy-start(bf16[544,512]{1,0:T(8,128)(2,1)S(1)} %collective-permute-done.1.ahead_ref) | copy-start | bytes 1671172
  94.6 12.0 %collective-permute-start.2 = (bf16[272,512]{1,0:T(8,128)(2,1)S(1)}, bf16[272,512]{1,0:T(8,128)(2,1)S(1)}, u32[]{:S(2)}, u32[]{:S(2)}) collective-permute-start(bf16[272,512]{1,0:T(8,128)(2,1)S(1)} %slice.62), channel_id=1, source_target_pairs={{0,3},{1,0},{2,1},{3,2},{4,7},{5,4},{6,5},{7,6},{8,11},{9,8},{10,9... | collective-permute-start | bytes 835592 | tf_op jit(solution)/shard_map/ppermute | solution.py:41
  100.5 0.8 copy-start.14
  101.3 11.8 %collective-permute-start.4 = (bf16[272,512]{1,0:T(8,128)(2,1)S(1)}, bf16[272,512]{1,0:T(8,128)(2,1)S(1)}, u32[]{:S(2)}, u32[]{:S(2)}) collective-permute-start(bf16[272,512]{1,0:T(8,128)(2,1)S(1)} %slice.63), channel_id=1, source_target_pairs={{0,1},{1,2},{2,3},{3,0},{4,5},{5,6},{6,7},{7,4},{8,9},{9,10},{10,1... | collective-permute-start | bytes 835592 | tf_op jit(solution)/shard_map/ppermute | solution.py:41
  106.6 6.4 %copy-start.17 = (bf16[272,512]{1,0:T(8,128)(2,1)}, bf16[272,512]{1,0:T(8,128)(2,1)S(1)}, u32[]{:S(2)}) copy-start(bf16[272,512]{1,0:T(8,128)(2,1)S(1)} %collective-permute-done.2.top_ref) | copy-start | bytes 835588
  113.1 0.7 copy-start.18
  117.2 17.2 %collective-permute-start.9 = (bf16[16,16,512]{2,1,0:T(8,128)(2,1)S(1)}, bf16[16,16,512]{2,1,0:T(8,128)(2,1)S(1)}, u32[]{:S(2)}, u32[]{:S(2)}) collective-permute-start(bf16[16,16,512]{2,1,0:T(8,128)(2,1)S(1)} %slice.51), channel_id=1, source_target_pairs={{0,24},{8,0},{16,8},{24,16},{1,25},{9,1},{17,9},{25,17},{2,26},{10... | collective-permute-start | bytes 786440 | tf_op jit(solution)/shard_map/ppermute | solution.py:41
  119.1 15.3 %collective-permute-start.10 = (bf16[16,16,512]{2,1,0:T(8,128)(2,1)S(1)}, bf16[16,16,512]{2,1,0:T(8,128)(2,1)S(1)}, u32[]{:S(2)}, u32[]{:S(2)}) collective-permute-start(bf16[16,16,512]{2,1,0:T(8,128)(2,1)S(1)} %slice.51), channel_id=1, source_target_pairs={{0,16},{8,24},{16,0},{24,8},{1,17},{9,25},{17,1},{25,9},{2,18},{10... | collective-permute-start | bytes 786440 | tf_op jit(solution)/shard_map/ppermute | solution.py:41
  121.5 14.5 %collective-permute-start.11 = (bf16[16,16,512]{2,1,0:T(8,128)(2,1)S(1)}, bf16[16,16,512]{2,1,0:T(8,128)(2,1)S(1)}, u32[]{:S(2)}, u32[]{:S(2)}) collective-permute-start(bf16[16,16,512]{2,1,0:T(8,128)(2,1)S(1)} %slice.51), channel_id=1, source_target_pairs={{0,8},{8,16},{16,24},{24,0},{1,9},{9,17},{17,25},{25,1},{2,10},{10... | collective-permute-start | bytes 786440 | tf_op jit(solution)/shard_map/ppermute | solution.py:41
  126.3 3.1 %copy-start = (bf16[256,2048]{1,0:T(8,128)(2,1)S(1)}, bf16[256,2048]{1,0:T(8,128)(2,1)}, u32[]{:S(2)}) copy-start(bf16[256,2048]{1,0:T(8,128)(2,1)} %get-tuple-element.38.out_mat_ref.refs_12_.refs_9_) | copy-start | bytes 3145732
  126.3 3.1 %copy-start.5 = (f32[256]{0:T(256)S(1)}, f32[256]{0:T(256)}, u32[]{:S(2)}) copy-start(f32[256]{0:T(256)} %param.28) | copy-start | bytes 3076
  126.3 3.1 %copy-start.6 = (bf16[256,2048]{1,0:T(8,128)(2,1)S(1)}, bf16[256,2048]{1,0:T(8,128)(2,1)}, u32[]{:S(2)}) copy-start(bf16[256,2048]{1,0:T(8,128)(2,1)} %get-tuple-element.37.in_ref) | copy-start | bytes 3145732
  126.3 3.1 %copy-start.7 = (f32[512,256]{1,0:T(8,128)S(1)}, f32[512,256]{1,0:T(8,128)}, u32[]{:S(2)}) copy-start(f32[512,256]{1,0:T(8,128)} %get-tuple-element.35.grow_ref) | copy-start | bytes 1572868
  126.4 3.0 %copy-start.8 = (f32[512,256]{1,0:T(8,128)S(1)}, f32[512,256]{1,0:T(8,128)}, u32[]{:S(2)}) copy-start(f32[512,256]{1,0:T(8,128)} %get-tuple-element.36.shrink_ref) | copy-start | bytes 1572868
  126.4 3.0 %copy-start.9 = (f32[5,16,1024]{2,1,0:T(8,128)S(1)}, f32[5,16,1024]{2,1,0:T(8,128)}, u32[]{:S(2)}) copy-start(f32[5,16,1024]{2,1,0:T(8,128)} %get-tuple-element.39.hop_re_ref) | copy-start | bytes 983044
  126.4 3.0 %copy-start.10 = (f32[5,16,1024]{2,1,0:T(8,128)S(1)}, f32[5,16,1024]{2,1,0:T(8,128)}, u32[]{:S(2)}) copy-start(f32[5,16,1024]{2,1,0:T(8,128)} %get-tuple-element.40.hop_im_ref) | copy-start | bytes 983044
  126.4 3.0 %copy-start.11 = (f32[1,128]{1,0:T(1,128)S(1)}, f32[1,128]{1,0:T(1,128)}, u32[]{:S(2)}) copy-start(f32[1,128]{1,0:T(1,128)} %get-tuple-element.41.shift_ref) | copy-start | bytes 1540
  134.4 24.8 %copy-start.1 = (f32[31,256]{1,0:T(8,128)S(1)}, f32[31,256]{1,0:T(8,128)}, u32[]{:S(2)}) copy-start(f32[31,256]{1,0:T(8,128)} %taps_ref.1) | copy-start | bytes 95236
  136.1 41.5 %collective-permute-start.12 = (bf16[4,16,16,512]{3,2,1,0:T(8,128)(2,1)S(1)}, bf16[4,16,16,512]{3,2,1,0:T(8,128)(2,1)}, u32[]{:S(2)}, u32[]{:S(2)}) collective-permute-start(bf16[4,16,16,512]{3,2,1,0:T(8,128)(2,1)S(1)} %pad_maximum_fusion.refs_13_.refs_10_), channel_id=1, source_target_pairs={{0,4},{4,0},{1,5},{5,1},{2,6},{6,2},{3,7},{7,3},{8,12},{12,8},{9,1... | collective-permute-start | bytes 3145736 | tf_op jit(solution)/shard_map/ppermute | solution.py:36
  148.3 29.2 %all-to-all-start.3 = ((f32[16,1,2176]{2,1,0:T(1,128)}), f32[16,1,2176]{2,1,0:T(1,128)S(1)}, u32[]{:S(2)}, u32[]{:S(2)}) async-start(f32[16,1,2176]{2,1,0:T(1,128)} %broadcast_in_dim.17), calls=%async_computation.3 | async-start | bytes 278528 | tf_op jit(solution)/shard_map/all_to_all | solution.py:25
  159.2 18.4 %copy-start.3 = (f32[256]{0:T(256)S(1)}, f32[256]{0:T(256)}, u32[]{:S(2)}) copy-start(f32[256]{0:T(256)} %param.31) | copy-start | bytes 3076
  165.6 7.8 %collective-permute-start.6 = (f32[2,512]{1,0:T(2,128)S(1)}, f32[2,512]{1,0:T(2,128)S(1)}, u32[]{:S(2)}, u32[]{:S(2)}) collective-permute-start(f32[2,512]{1,0:T(2,128)S(1)} %get-tuple-element.34.refs_1_), channel_id=1, source_target_pairs={{0,3},{1,0},{2,1},{3,2},{4,7},{5,4},{6,5},{7,6},{8,11},{9,8},{10,9... | collective-permute-start | bytes 12296 | tf_op jit(solution)/shard_map/ppermute | solution.py:41
  167.5 7.0 %collective-permute-start.7 = (f32[2,512]{1,0:T(2,128)S(1)}, f32[2,512]{1,0:T(2,128)S(1)}, u32[]{:S(2)}, u32[]{:S(2)}) collective-permute-start(f32[2,512]{1,0:T(2,128)S(1)} %get-tuple-element.34.refs_1_), channel_id=1, source_target_pairs={{0,2},{1,3},{2,0},{3,1},{4,6},{5,7},{6,4},{7,5},{8,10},{9,11},{10,... | collective-permute-start | bytes 12296 | tf_op jit(solution)/shard_map/ppermute | solution.py:41
  170.8 6.7 %collective-permute-start.8 = (f32[2,512]{1,0:T(2,128)S(1)}, f32[2,512]{1,0:T(2,128)S(1)}, u32[]{:S(2)}, u32[]{:S(2)}) collective-permute-start(f32[2,512]{1,0:T(2,128)S(1)} %get-tuple-element.34.refs_1_), channel_id=1, source_target_pairs={{0,1},{1,2},{2,3},{3,0},{4,5},{5,6},{6,7},{7,4},{8,9},{9,10},{10,1... | collective-permute-start | bytes 12296 | tf_op jit(solution)/shard_map/ppermute | solution.py:41
  182.0 12.9 %collective-permute-start.13 = (bf16[64,2048]{1,0:T(8,128)(2,1)S(1)}, bf16[64,2048]{1,0:T(8,128)(2,1)S(1)}, u32[]{:S(2)}, u32[]{:S(2)}) collective-permute-start(bf16[64,2048]{1,0:T(8,128)(2,1)S(1)} %get-tuple-element.59), channel_id=1, source_target_pairs={{0,3},{1,0},{2,1},{3,2},{4,7},{5,4},{6,5},{7,6},{8,11},{9,8},{10,9... | collective-permute-start | bytes 786440 | tf_op jit(solution)/shard_map/ppermute | solution.py:41
  185.9 9.5 %collective-permute-start.15 = (bf16[64,2048]{1,0:T(8,128)(2,1)S(1)}, bf16[64,2048]{1,0:T(8,128)(2,1)S(1)}, u32[]{:S(2)}, u32[]{:S(2)}) collective-permute-start(bf16[64,2048]{1,0:T(8,128)(2,1)S(1)} %get-tuple-element.60), channel_id=1, source_target_pairs={{0,1},{1,2},{2,3},{3,0},{4,5},{5,6},{6,7},{7,4},{8,9},{9,10},{10,1... | collective-permute-start | bytes 786440 | tf_op jit(solution)/shard_map/ppermute | solution.py:41
  195.6 13.9 %collective-permute-start.16 = (bf16[128,2048]{1,0:T(8,128)(2,1)S(1)}, bf16[128,2048]{1,0:T(8,128)(2,1)S(1)}, u32[]{:S(2)}, u32[]{:S(2)}) collective-permute-start(bf16[128,2048]{1,0:T(8,128)(2,1)S(1)} %get-tuple-element.58), channel_id=1, source_target_pairs={{0,1},{1,2},{2,3},{3,0},{4,5},{5,6},{6,7},{7,4},{8,9},{9,10},{10,1... | collective-permute-start | bytes 1572872 | tf_op jit(solution)/shard_map/ppermute | solution.py:41
  197.5 13.2 %collective-permute-start.14 = (bf16[128,2048]{1,0:T(8,128)(2,1)S(1)}, bf16[128,2048]{1,0:T(8,128)(2,1)S(1)}, u32[]{:S(2)}, u32[]{:S(2)}) collective-permute-start(bf16[128,2048]{1,0:T(8,128)(2,1)S(1)} %get-tuple-element.57), channel_id=1, source_target_pairs={{0,3},{1,0},{2,1},{3,2},{4,7},{5,4},{6,5},{7,6},{8,11},{9,8},{10,9... | collective-permute-start | bytes 1572872 | tf_op jit(solution)/shard_map/ppermute | solution.py:41

commit v9 on v8

--- a/solution.py
+++ b/solution.py
@@ -443,12 +443,12 @@
 
 
 def merge_rows(distances, carried, place_ref, channel, refs):
-    gain_ref, *sums_refs = channel
+    gain_ref, sums_ref = channel
     raw_all, y_all, power_all, read_all, own_ref, other_ref, out_ref = refs[:7]
     weight_ref, weight_done, raw_ref, y_ref, power_ref, read_ref, done = refs[7:]
     block = out_ref.shape[1]
-    parts = len(sums_refs)
-    sums = sum((ref[...] for ref in sums_refs[1:]), sums_refs[0][...])
+    parts = sums_ref.shape[1] // block
+    sums = sums_ref[...]
     places = [
         pl.ds(pl.multiple_of(lax.rem(place_ref[2] + distance, parts) * block, block), block)
         for distance in distances
@@ -488,8 +488,8 @@
 
 
 def opposite_kernel(count, place_ref, *refs):
-    channel, (far_ref, rates_ref, prefix_ref, start_ref) = refs[:5], refs[5:9]
-    *inputs, out_ref, h_ref, weight_ref, weight_done, raw_ref, y_ref, power_ref, read_ref, done = refs[9:]
+    channel, (far_ref, rates_ref, prefix_ref, start_ref) = refs[:2], refs[2:6]
+    *inputs, out_ref, h_ref, weight_ref, weight_done, raw_ref, y_ref, power_ref, read_ref, done = refs[6:]
     peers_z, peers_near = far_ref.shape[0], 2 * inputs[-1].shape[0]
 
     def carried():
@@ -518,8 +518,8 @@
 
 
 def rest_kernel(place_ref, *refs):
-    channel, h_ref = refs[:5], refs[5]
-    merge_rows((0, 1, 3), lambda: (h_ref[0:1], h_ref[1:2]), place_ref, channel, refs[6:])
+    channel, h_ref = refs[:2], refs[2]
+    merge_rows((0, 1, 3), lambda: (h_ref[0:1], h_ref[1:2]), place_ref, channel, refs[3:])
 
 
 def input_matrix(eigen_real, eigen_imag, step, state_input):
@@ -693,9 +693,6 @@
         transcendentals=0,
     )
     near = copies(last, ("x", "c"))
-    *merge_pieces, _ = lax.optimization_barrier((*merge_pieces, last))
-    merge_x = jnp.stack(merge_pieces)
-    merge_other = partner(merge_x)
     packed, prefix = call(
         functools.partial(near_kernel, count),
         (
@@ -709,6 +706,9 @@
         bytes_accessed=64 * lanes,
         transcendentals=8 * lanes,
     )
+    *merge_pieces, _ = lax.optimization_barrier((*merge_pieces, packed))
+    merge_x = jnp.stack(merge_pieces)
+    merge_other = partner(merge_x)
     far = copies(packed, "z")
 
     raw, sums = call(
@@ -730,7 +730,7 @@
         bytes_accessed=4 * depth * count,
         transcendentals=0,
     )
-    all_sums = [sums] + [from_ahead(sums, "tp", d) for d in range(1, parts)]
+    sums = lax.psum(sums, "tp")
 
     block = count // parts
 
@@ -738,7 +738,7 @@
         return call(
             kernel,
             (jax.ShapeDtypeStruct((blocks, block, depth), BF16), *more),
-            (channel_gain.reshape(1, -1), *all_sums, *arrays),
+            (channel_gain.reshape(1, -1), sums, *arrays),
             apart=(*far_from_core(raw, y_local, power, reads), merge_x, merge_other),
             scalars=(place,),
             scratch=(

time: 215 us -> 211 us (0.981)
  blocking collectives: 26.9 us -> 34.3 us
  starting transfers between devices: 76.4 us -> 69.3 us
  waiting for transfers between devices: 62.4 us -> 58.2 us
    psum x0 -> x1, blocking collectives: none -> 7.75 us  [mixer(): sums = lax.psum(sums, 'tp')]
    ppermute x14 -> x11, starting transfers between devices: 44 us -> 36.5 us  [from_ahead(): lax.ppermute(block, axis, [(i, (i - distance) % count) for i in range(cou...]
    ppermute x14 -> x11, waiting for transfers between devices: 34.8 us -> 30.7 us  [from_ahead(): lax.ppermute(block, axis, [(i, (i - distance) % count) for i in range(cou...]
  transfers between devices with their start and end apart: 19 -> 16, of which waited for: 12 -> 9; matrix products, arithmetic and copies ran while one was open for 2% -> 2% of each run, Pallas kernels for 15% -> 15%
where the time goes in v9:
time: 211 us; the launch traced here: 208 us
  starting transfers between devices  69.3 us (33%)
  waiting for transfers between devices  58.2 us (28%)
  Pallas kernels  36 us (17%)
  blocking collectives  34.3 us (16%)
  other arithmetic  5.35 us (3%)
  local copies, waits for them, and re-layouts  4.03 us (2%)
    ppermute x11, starting transfers between devices, from_ahead(): lax.ppermute(block, axis, [(i, (i - distance) % count) for i in range(cou...  36.5 us
    pallas_call x8, Pallas kernels, call(): pl.pallas_call(body, compiler_params=pltpu.CompilerParams(vmem_limit_byte...  36 us
    ppermute x11, waiting for transfers between devices, from_ahead(): lax.ppermute(block, axis, [(i, (i - distance) % count) for i in range(cou...  30.7 us
    all_to_all x2, blocking collectives, copies(): lax.all_to_all(jnp.broadcast_to(value[None], (peers, *value.shape)), axis...  26.5 us
    all_to_all x2, starting transfers between devices, copies(): lax.all_to_all(jnp.broadcast_to(value[None], (peers, *value.shape)), axis...  26.4 us
    all_to_all x2, waiting for transfers between devices, copies(): lax.all_to_all(jnp.broadcast_to(value[None], (peers, *value.shape)), axis...  24.7 us
    psum x1, blocking collectives, mixer(): sums = lax.psum(sums, 'tp')  7.75 us
  transfers between devices with their start and end apart: 16, of which 9 were waited for; matrix products, arithmetic and copies ran while one was open for 2% of the time, Pallas kernels for 15%

profile of v9, /device:TPU:6, one launch (start us, length us, event | category | flops | bytes accessed | tf_op | source)
XLA Modules:
  0.0 207.9 jit_solution(16224294388025622795)
XLA Ops:
  0.0 0.8 maximum_bitcast_fusion
  0.8 0.7 pad_maximum_fusion.1
  1.5 0.9 broadcast_in_dim.12
  2.4 15.2 %all-to-all-start = ((bf16[16,16,1280]{2,1,0:T(8,128)(2,1)}), bf16[16,16,1280]{2,1,0:T(8,128)(2,1)S(1)}, u32[]{:S(2)}, u32[]{:S(2)}) async-start(bf16[16,16,1280]{2,1,0:T(8,128)(2,1)} %broadcast_in_dim.12), calls=%async_computation | async-start | bytes 1310720 | tf_op jit(solution)/shard_map/all_to_all | solution.py:25
  17.6 0.0 copy-start.4
  17.7 0.1 fusion.14
  17.8 0.1 reshape.133.refs_1_
  17.9 0.1 mul.192
  18.0 0.1 mul.164
  18.0 0.1 reshape.134.refs_5_
  18.2 0.3 multiply_sine_fusion.1
  18.6 0.6 fusion.11
  19.2 7.4 %shard_map.163 = (f32[512,256]{1,0:T(8,128)}, f32[512,256]{1,0:T(8,128)}, bf16[256,2048]{1,0:T(8,128)(2,1)}, bf16[256,2048]{1,0:T(8,128)(2,1)}, f32[5,16,1024]{2...) custom-call(f32[16,512]{1,0:T(8,128)S(1)} %copy-done.4, ...), custom_call_target="tpu_custom_call" | custom-call | flops 83886080 | bytes 4194304 | tf_op jit(solution)/shard_map/pallas_call | solution.py:53
  26.6 24.7 %all-to-all-done = bf16[16,16,1280]{2,1,0:T(8,128)(2,1)S(1)} async-done(((bf16[16,16,1280]{2,1,0:T(8,128)(2,1)}), bf16[16,16,1280]{2,1,0:T(8,128)(2,1)S(1)}, u32[]{:S(2)}, u32[]{:S(2)}) %all-to-all-start) | async-done | bytes 655392 | tf_op jit(solution)/shard_map/all_to_all | solution.py:25
  51.4 0.1 broadcast_in_dim.13
  51.5 0.0 copy-start.17
  51.5 18.4 %all_to_all.20.own_ref = bf16[4,16,16,768]{3,2,1,0:T(8,128)(2,1)} all-to-all(bf16[4,16,16,768]{3,2,1,0:T(8,128)(2,1)S(1)} %broadcast_in_dim.13), channel_id=1, replica_groups=mesh['z'=16,'x'=4,'c'=2,'tp'=4] {'x'}, dimensions={0} | all-to-all | bytes 3145728 | tf_op jit(solution)/shard_map/all_to_all | solution.py:25
  69.9 2.0 collective-permute-start.5
  71.9 2.4 %collective-permute-start = (bf16[32,512]{1,0:T(8,128)(2,1)S(1)}, bf16[32,512]{1,0:T(8,128)(2,1)S(1)}, u32[]{:S(2)}, u32[]{:S(2)}) collective-permute-start(bf16[32,512]{1,0:T(8,128)(2,1)S(1)} %slice.52), channel_id=1, source_target_pairs={{0,4},{4,8},{8,12},{12,16},{16,20},{20,24},{24,28},{28,32},{32,36}... | collective-permute-start | bytes 98312 | tf_op jit(solution)/shard_map/ppermute | solution.py:32
  74.4 2.8 %collective-permute-done = bf16[32,512]{1,0:T(8,128)(2,1)S(1)} collective-permute-done((bf16[32,512]{1,0:T(8,128)(2,1)S(1)}, bf16[32,512]{1,0:T(8,128)(2,1)S(1)}, u32[]{:S(2)}, u32[]{:S(2)}) %collective-permute-start) | collective-permute-done | bytes 32800 | tf_op jit(solution)/shard_map/ppermute | solution.py:32
  77.2 4.9 %collective-permute-start.1 = (bf16[544,512]{1,0:T(8,128)(2,1)S(1)}, bf16[544,512]{1,0:T(8,128)(2,1)S(1)}, u32[]{:S(2)}, u32[]{:S(2)}) collective-permute-start(bf16[544,512]{1,0:T(8,128)(2,1)S(1)} %constant_dynamic-update-slice_fusion.own_ref), channel_id=1, source_target_pairs={{0,3},{1,0},{2,1},{3,2},{4,7},{5,4},{6,5},{7,6},{8,11},{9,8},{10,9... | collective-permute-start | bytes 1671176 | tf_op jit(solution)/shard_map/ppermute | solution.py:41
  82.2 1.9 collective-permute-start.3
  84.1 10.5 %collective-permute-done.1.ahead_ref = bf16[544,512]{1,0:T(8,128)(2,1)S(1)} collective-permute-done((bf16[544,512]{1,0:T(8,128)(2,1)S(1)}, bf16[544,512]{1,0:T(8,128)(2,1)S(1)}, u32[]{:S(2)}, u32[]{:S(2)}) %collective-permute-start.1) | collective-permute-done | bytes 557088 | tf_op jit(solution)/shard_map/ppermute | solution.py:41
  94.6 5.6 %collective-permute-start.2 = (bf16[272,512]{1,0:T(8,128)(2,1)S(1)}, bf16[272,512]{1,0:T(8,128)(2,1)S(1)}, u32[]{:S(2)}, u32[]{:S(2)}) collective-permute-start(bf16[272,512]{1,0:T(8,128)(2,1)S(1)} %slice.62), channel_id=1, source_target_pairs={{0,3},{1,0},{2,1},{3,2},{4,7},{5,4},{6,5},{7,6},{8,11},{9,8},{10,9... | collective-permute-start | bytes 835592 | tf_op jit(solution)/shard_map/ppermute | solution.py:41
  100.3 0.3 collective-permute-done.3.behind_ref
  100.5 1.9 collective-permute-start.4
  102.5 0.1 pad_add_fusion.place_ref
  102.5 0.1 fusion.5.lower_ref
  102.7 4.0 %collective-permute-done.2.top_ref = bf16[272,512]{1,0:T(8,128)(2,1)S(1)} collective-permute-done((bf16[272,512]{1,0:T(8,128)(2,1)S(1)}, bf16[272,512]{1,0:T(8,128)(2,1)S(1)}, u32[]{:S(2)}, u32[]{:S(2)}) %collective-permute-start.2) | collective-permute-done | bytes 278560 | tf_op jit(solution)/shard_map/ppermute | solution.py:41
  106.7 5.6 %collective-permute-done.4.bottom_ref = bf16[272,512]{1,0:T(8,128)(2,1)S(1)} collective-permute-done((bf16[272,512]{1,0:T(8,128)(2,1)S(1)}, bf16[272,512]{1,0:T(8,128)(2,1)S(1)}, u32[]{:S(2)}, u32[]{:S(2)}) %collective-permute-start.4) | collective-permute-done | bytes 278560 | tf_op jit(solution)/shard_map/ppermute | solution.py:41
  112.3 0.7 copy-done.19
  113.0 2.4 %shard_map.164.normed_ref = bf16[4,544,512]{2,1,0:T(8,128)(2,1)S(1)} custom-call(s32[4]{0:T(128)S(1)} %pad_add_fusion.place_ref, bf16[544,512]{1,0:T(8,128)(2,1)} %copy-done.16, bf16[544,512]{1,0:T(8,128)(2,1)} %copy-done.13, bf16[272,512]{1,0:T(8,128)(2,1)} %copy-done.18, bf16[272,512]{1,0:T(8,128)(2,1)} %copy-done.19, bf16[544,512]{1,0:T(8,128)(2,1)} %copy-done.14, ...), custom_call_target="tpu_custom_call" | custom-call | flops 8388608 | bytes 4194304 | tf_op jit(solution)/shard_map/pallas_call | solution.py:53
  115.4 1.0 slice.51
  116.4 0.0 copy-start.5
  116.5 0.0 copy-start.7
  116.5 2.2 %collective-permute-start.6 = (bf16[16,16,512]{2,1,0:T(8,128)(2,1)S(1)}, bf16[16,16,512]{2,1,0:T(8,128)(2,1)}, u32[]{:S(2)}, u32[]{:S(2)}) collective-permute-start(bf16[16,16,512]{2,1,0:T(8,128)(2,1)S(1)} %slice.51), channel_id=1, source_target_pairs={{0,24},{8,0},{16,8},{24,16},{1,25},{9,1},{17,9},{25,17},{2,26},{10... | collective-permute-start | bytes 786440 | tf_op jit(solution)/shard_map/ppermute | solution.py:41
  118.7 2.4 %collective-permute-start.7 = (bf16[16,16,512]{2,1,0:T(8,128)(2,1)S(1)}, bf16[16,16,512]{2,1,0:T(8,128)(2,1)}, u32[]{:S(2)}, u32[]{:S(2)}) collective-permute-start(bf16[16,16,512]{2,1,0:T(8,128)(2,1)S(1)} %slice.51), channel_id=1, source_target_pairs={{0,16},{8,24},{16,0},{24,8},{1,17},{9,25},{17,1},{25,9},{2,18},{10... | collective-permute-start | bytes 786440 | tf_op jit(solution)/shard_map/ppermute | solution.py:41
  121.1 4.7 %collective-permute-start.8 = (bf16[16,16,512]{2,1,0:T(8,128)(2,1)S(1)}, bf16[16,16,512]{2,1,0:T(8,128)(2,1)}, u32[]{:S(2)}, u32[]{:S(2)}) collective-permute-start(bf16[16,16,512]{2,1,0:T(8,128)(2,1)S(1)} %slice.51), channel_id=1, source_target_pairs={{0,8},{8,16},{16,24},{24,0},{1,9},{9,17},{17,25},{25,1},{2,10},{10... | collective-permute-start | bytes 786440 | tf_op jit(solution)/shard_map/ppermute | solution.py:41
  125.8 0.0 collective-permute-done.5.other_ref
  125.8 2.6 %shard_map.166.u_ref = bf16[512,256]{1,0:T(8,128)(2,1)S(1)} custom-call(s32[4]{0:T(128)S(1)} %pad_add_fusion.place_ref, bf16[4,544,512]{2,1,0:T(8,128)(2,1)S(1)} %shard_map.164.normed_ref, bf16[4,16,16,768]{3,2,1,0:T(8,128)(2,1)} %all_to_all.20.own_ref, bf16[4,16,16,768]{3,2,1,0:T(8,128)(2,1)} %collective-permute-done.5.other_ref), custom_call_target="tpu_custom_call" | custom-call | flops 536870912 | bytes 4194304 | tf_op jit(solution)/shard_map/pallas_call | solution.py:53
  128.5 5.0 %shard_map.167 = (f32[512,256]{1,0:T(8,128)}, f32[1,2176]{1,0:T(1,128)S(1)}) custom-call(bf16[512,256]{1,0:T(8,128)(2,1)S(1)} %shard_map.166.u_ref, f32[512,256]{1,0:T(8,128)S(1)} %copy-done.7, f32[512,256]{1,0:T(8,128)S(1)} %copy-done.8, bf16[256,2048]{1,0:T(8,128)(2,1)S(1)} %copy-done.6, bf16[256,2048]{1,0:T(8,128)(2,1)S(1)} %copy-done, ...), custom_call_target="tpu_custom_call" | custom-call | flops 1610612736 | bytes 4194304 | tf_op jit(solution)/shard_map/pallas_call | solution.py:53
  133.6 8.2 %all_to_all.21.near_ref = f32[8,1,2176]{2,1,0:T(1,128)S(1)} all-to-all(f32[8,1,2176]{2,1,0:T(1,128)S(1)} %broadcast_in_dim.15), channel_id=1, replica_groups=mesh['z'=16,'x'=4,'c'=2,'tp'=4] {'x','c'}, dimensions={0} | all-to-all | bytes 139264 | tf_op jit(solution)/shard_map/all_to_all | solution.py:25
  141.7 0.9 shard_map.168
  142.7 0.0 collective-permute-done.6
  142.7 0.0 collective-permute-done.7
  142.7 1.3 pad_maximum_fusion.refs_10_.refs_7_
  144.0 1.9 collective-permute-start.9
  146.0 0.7 broadcast_in_dim.17
  146.7 11.2 %all-to-all-start.3 = ((f32[16,1,2176]{2,1,0:T(1,128)}), f32[16,1,2176]{2,1,0:T(1,128)S(1)}, u32[]{:S(2)}, u32[]{:S(2)}) async-start(f32[16,1,2176]{2,1,0:T(1,128)} %broadcast_in_dim.17), calls=%async_computation.3 | async-start | bytes 278528 | tf_op jit(solution)/shard_map/all_to_all | solution.py:25
  157.9 0.0 copy-start.3
  157.9 6.3 %shard_map.165 = (f32[512,256]{1,0:T(8,128)}, f32[2,512]{1,0:T(2,128)S(1)}) custom-call(s32[4]{0:T(128)S(1)} %pad_add_fusion.place_ref, bf16[4,544,512]{2,1,0:T(8,128)(2,1)S(1)} %shard_map.164.normed_ref, f32[31,256]{1,0:T(8,128)S(1)} %copy-done.1, bf16[4,16,16,768]{3,2,1,0:T(8,128)(2,1)} %all_to_all.20.own_ref, ...), custom_call_target="tpu_custom_call" | custom-call | flops 1073741824 | bytes 4194304 | tf_op jit(solution)/shard_map/pallas_call | solution.py:53
  164.3 7.8 %psum.7.refs_1_ = f32[2,512]{1,0:T(2,128)S(1)} all-reduce(f32[2,512]{1,0:T(2,128)S(1)} %get-tuple-element.34), channel_id=1, replica_groups=mesh['z'=16,'x'=4,'c'=2,'tp'=4] {'tp'}, use_global_device_ids=true, to_apply=%region_0.1 | all-reduce | flops 1024 | bytes 8192 | tf_op jit(solution)/shard_map/psum | solution.py:733
  172.0 0.0 all-to-all-done.3.refs_2_
  172.1 4.3 %shard_map.169 = (bf16[1,128,2048]{2,1,0:T(8,128)(2,1)S(1)}, f32[2,1024]{1,0:T(2,128)S(1)}) custom-call(s32[4]{0:T(128)S(1)} %pad_add_fusion.place_ref, f32[1,256]{1,0:T(1,128)S(1)} %bitcast.57, f32[2,512]{1,0:T(2,128)S(1)} %psum.7.refs_1_, f32[16,1,2176]{2,1,0:T(1,128)S(1)} %all-to-all-done.3.refs_2_, f32[3,1024]{1,0:T(4,128)S(1)} %pad_maximum_fusion.2.rates_ref.refs_3_, ...), custom_call_target="tpu_custom_call" | custom-call | flops 268435456 | bytes 4194304 | tf_op jit(solution)/shard_map/pallas_call | solution.py:53
  176.4 3.9 %collective-permute-start.10 = (bf16[64,2048]{1,0:T(8,128)(2,1)S(1)}, bf16[64,2048]{1,0:T(8,128)(2,1)S(1)}, u32[]{:S(2)}, u32[]{:S(2)}) collective-permute-start(bf16[64,2048]{1,0:T(8,128)(2,1)S(1)} %get-tuple-element.59), channel_id=1, source_target_pairs={{0,3},{1,0},{2,1},{3,2},{4,7},{5,4},{6,5},{7,6},{8,11},{9,8},{10,9... | collective-permute-start | bytes 786440 | tf_op jit(solution)/shard_map/ppermute | solution.py:41
  180.4 1.9 collective-permute-start.12
  182.3 7.0 %shard_map.170 = bf16[3,128,2048]{2,1,0:T(8,128)(2,1)S(1)} custom-call(s32[4]{0:T(128)S(1)} %pad_add_fusion.place_ref, f32[1,256]{1,0:T(1,128)S(1)} %bitcast.58, f32[2,512]{1,0:T(2,128)S(1)} %psum.7.refs_1_, f32[2,1024]{1,0:T(2,128)S(1)} %get-tuple-element.55.refs_2_, f32[512,256]{1,0:T(8,128)} %get-tuple-element.47.refs_6_.refs_3_, ...), custom_call_target="tpu_custom_call" | custom-call | flops 805306368 | bytes 4194304 | tf_op jit(solution)/shard_map/pallas_call | solution.py:53
  189.4 0.5 collective-permute-done.12
  189.8 0.2 fusion.1
  190.0 3.5 %collective-permute-start.13 = (bf16[128,2048]{1,0:T(8,128)(2,1)S(1)}, bf16[128,2048]{1,0:T(8,128)(2,1)S(1)}, u32[]{:S(2)}, u32[]{:S(2)}) collective-permute-start(bf16[128,2048]{1,0:T(8,128)(2,1)S(1)} %get-tuple-element.58), channel_id=1, source_target_pairs={{0,1},{1,2},{2,3},{3,0},{4,5},{5,6},{6,7},{7,4},{8,9},{9,10},{10,1... | collective-permute-start | bytes 1572872 | tf_op jit(solution)/shard_map/ppermute | solution.py:41
  193.5 3.6 %collective-permute-start.11 = (bf16[128,2048]{1,0:T(8,128)(2,1)S(1)}, bf16[128,2048]{1,0:T(8,128)(2,1)S(1)}, u32[]{:S(2)}, u32[]{:S(2)}) collective-permute-start(bf16[128,2048]{1,0:T(8,128)(2,1)S(1)} %get-tuple-element.57), channel_id=1, source_target_pairs={{0,3},{1,0},{2,1},{3,2},{4,7},{5,4},{6,5},{7,6},{8,11},{9,8},{10,9... | collective-permute-start | bytes 1572872 | tf_op jit(solution)/shard_map/ppermute | solution.py:41
  197.1 7.9 %collective-permute-done.13 = bf16[128,2048]{1,0:T(8,128)(2,1)S(1)} collective-permute-done((bf16[128,2048]{1,0:T(8,128)(2,1)S(1)}, bf16[128,2048]{1,0:T(8,128)(2,1)S(1)}, u32[]{:S(2)}, u32[]{:S(2)}) %collective-permute-start.13) | collective-permute-done | bytes 524320 | tf_op jit(solution)/shard_map/ppermute | solution.py:41
  205.0 1.9 collective-permute-done.11
  206.8 1.0 fusion.3
  (68 shorter events, 0.5 us)
Async XLA Ops:
  0.0 17.6 %copy-start.25 = (f32[16]{0:T(128)S(1)}, f32[16]{0:T(128)}, u32[]{:S(2)}) copy-start(f32[16]{0:T(128)} %param.24) | copy-start | bytes 196
  0.0 17.7 %copy-start.23 = (f32[16,64]{1,0:T(8,128)S(1)}, f32[16,64]{1,0:T(8,128)}, u32[]{:S(2)}) copy-start(f32[16,64]{1,0:T(8,128)} %param.23) | copy-start | bytes 12292
  0.0 17.7 %copy-start.24 = (f32[16,64]{1,0:T(8,128)S(1)}, f32[16,64]{1,0:T(8,128)}, u32[]{:S(2)}) copy-start(f32[16,64]{1,0:T(8,128)} %param.22) | copy-start | bytes 12292
  0.0 18.0 %copy-start.22 = (f32[2,16,64]{2,1,0:T(8,128)S(1)}, f32[2,16,64]{2,1,0:T(8,128)}, u32[]{:S(2)}) copy-start(f32[2,16,64]{2,1,0:T(8,128)} %param.29) | copy-start | bytes 24580
  0.0 18.1 %copy-start.20 = (f32[2,16,16,64]{3,2,1,0:T(8,128)S(1)}, f32[2,16,16,64]{3,2,1,0:T(8,128)}, u32[]{:S(2)}) copy-start(f32[2,16,16,64]{3,2,1,0:T(8,128)} %param.26) | copy-start | bytes 393220
  1.5 17.0 %copy-start.21 = (f32[2,16,16,64]{3,2,1,0:T(8,128)S(1)}, f32[2,16,16,64]{3,2,1,0:T(8,128)}, u32[]{:S(2)}) copy-start(f32[2,16,16,64]{3,2,1,0:T(8,128)} %param.27) | copy-start | bytes 393220
  2.4 48.9 %all-to-all-start = ((bf16[16,16,1280]{2,1,0:T(8,128)(2,1)}), bf16[16,16,1280]{2,1,0:T(8,128)(2,1)S(1)}, u32[]{:S(2)}, u32[]{:S(2)}) async-start(bf16[16,16,1280]{2,1,0:T(8,128)(2,1)} %broadcast_in_dim.12), calls=%async_computation | async-start | bytes 1310720 | tf_op jit(solution)/shard_map/all_to_all | solution.py:25
  17.6 1.5 copy-start.4
  51.3 18.5 %copy-start.12 = (bf16[16,16,1280]{2,1,0:T(8,128)(2,1)}, bf16[16,16,1280]{2,1,0:T(8,128)(2,1)S(1)}, u32[]{:S(2)}) copy-start(bf16[16,16,1280]{2,1,0:T(8,128)(2,1)S(1)} %all-to-all-done) | copy-start | bytes 1966084
  51.5 20.4 %copy-start.17 = (bf16[512,512]{1,0:T(8,128)(2,1)S(1)}, bf16[512,512]{1,0:T(8,128)(2,1)}, u32[]{:S(2)}) copy-start(bf16[512,512]{1,0:T(8,128)(2,1)} %param.17) | copy-start | bytes 1572868
  69.9 43.2 %copy-start.2 = (f32[2048]{0:T(1024)S(1)}, f32[2048]{0:T(1024)}, u32[]{:S(2)}) copy-start(f32[2048]{0:T(1024)} %param.18) | copy-start | bytes 24580
  69.9 55.9 %collective-permute-start.5 = (bf16[4,16,16,768]{3,2,1,0:T(8,128)(2,1)}, bf16[4,16,16,768]{3,2,1,0:T(8,128)(2,1)}, u32[]{:S(2)}, u32[]{:S(2)}) collective-permute-start(bf16[4,16,16,768]{3,2,1,0:T(8,128)(2,1)} %all_to_all.20.own_ref), channel_id=1, source_target_pairs={{0,4},{4,0},{1,5},{5,1},{2,6},{6,2},{3,7},{7,3},{8,12},{12,8},{9,1... | collective-permute-start | bytes 4718600 | tf_op jit(solution)/shard_map/ppermute | solution.py:36
  71.9 5.2 %collective-permute-start = (bf16[32,512]{1,0:T(8,128)(2,1)S(1)}, bf16[32,512]{1,0:T(8,128)(2,1)S(1)}, u32[]{:S(2)}, u32[]{:S(2)}) collective-permute-start(bf16[32,512]{1,0:T(8,128)(2,1)S(1)} %slice.52), channel_id=1, source_target_pairs={{0,4},{4,8},{8,12},{12,16},{16,20},{20,24},{24,28},{28,32},{32,36}... | collective-permute-start | bytes 98312 | tf_op jit(solution)/shard_map/ppermute | solution.py:32
  77.2 35.1 %copy-start.16 = (bf16[544,512]{1,0:T(8,128)(2,1)}, bf16[544,512]{1,0:T(8,128)(2,1)S(1)}, u32[]{:S(2)}) copy-start(bf16[544,512]{1,0:T(8,128)(2,1)S(1)} %constant_dynamic-update-slice_fusion.own_ref) | copy-start | bytes 1671172
  77.2 17.4 %collective-permute-start.1 = (bf16[544,512]{1,0:T(8,128)(2,1)S(1)}, bf16[544,512]{1,0:T(8,128)(2,1)S(1)}, u32[]{:S(2)}, u32[]{:S(2)}) collective-permute-start(bf16[544,512]{1,0:T(8,128)(2,1)S(1)} %constant_dynamic-update-slice_fusion.own_ref), channel_id=1, source_target_pairs={{0,3},{1,0},{2,1},{3,2},{4,7},{5,4},{6,5},{7,6},{8,11},{9,8},{10,9... | collective-permute-start | bytes 1671176 | tf_op jit(solution)/shard_map/ppermute | solution.py:41
  82.2 18.4 %collective-permute-start.3 = (bf16[544,512]{1,0:T(8,128)(2,1)S(1)}, bf16[544,512]{1,0:T(8,128)(2,1)S(1)}, u32[]{:S(2)}, u32[]{:S(2)}) collective-permute-start(bf16[544,512]{1,0:T(8,128)(2,1)S(1)} %constant_dynamic-update-slice_fusion.own_ref), channel_id=1, source_target_pairs={{0,1},{1,2},{2,3},{3,0},{4,5},{5,6},{6,7},{7,4},{8,9},{9,10},{10,1... | collective-permute-start | bytes 1671176 | tf_op jit(solution)/shard_map/ppermute | solution.py:41
  94.6 17.7 %copy-start.13 = (bf16[544,512]{1,0:T(8,128)(2,1)}, bf16[544,512]{1,0:T(8,128)(2,1)S(1)}, u32[]{:S(2)}) copy-start(bf16[544,512]{1,0:T(8,128)(2,1)S(1)} %collective-permute-done.1.ahead_ref) | copy-start | bytes 1671172
  94.6 12.0 %collective-permute-start.2 = (bf16[272,512]{1,0:T(8,128)(2,1)S(1)}, bf16[272,512]{1,0:T(8,128)(2,1)S(1)}, u32[]{:S(2)}, u32[]{:S(2)}) collective-permute-start(bf16[272,512]{1,0:T(8,128)(2,1)S(1)} %slice.62), channel_id=1, source_target_pairs={{0,3},{1,0},{2,1},{3,2},{4,7},{5,4},{6,5},{7,6},{8,11},{9,8},{10,9... | collective-permute-start | bytes 835592 | tf_op jit(solution)/shard_map/ppermute | solution.py:41
  100.5 11.8 %copy-start.14 = (bf16[544,512]{1,0:T(8,128)(2,1)}, bf16[544,512]{1,0:T(8,128)(2,1)S(1)}, u32[]{:S(2)}) copy-start(bf16[544,512]{1,0:T(8,128)(2,1)S(1)} %collective-permute-done.3.behind_ref) | copy-start | bytes 1671172
  100.5 11.8 %collective-permute-start.4 = (bf16[272,512]{1,0:T(8,128)(2,1)S(1)}, bf16[272,512]{1,0:T(8,128)(2,1)S(1)}, u32[]{:S(2)}, u32[]{:S(2)}) collective-permute-start(bf16[272,512]{1,0:T(8,128)(2,1)S(1)} %slice.63), channel_id=1, source_target_pairs={{0,1},{1,2},{2,3},{3,0},{4,5},{5,6},{6,7},{7,4},{8,9},{9,10},{10,1... | collective-permute-start | bytes 835592 | tf_op jit(solution)/shard_map/ppermute | solution.py:41
  106.7 5.7 %copy-start.18 = (bf16[272,512]{1,0:T(8,128)(2,1)}, bf16[272,512]{1,0:T(8,128)(2,1)S(1)}, u32[]{:S(2)}) copy-start(bf16[272,512]{1,0:T(8,128)(2,1)S(1)} %collective-permute-done.2.top_ref) | copy-start | bytes 835588
  112.3 0.7 copy-start.19
  116.4 17.1 %copy-start.15 = (bf16[16,16,512]{2,1,0:T(8,128)(2,1)}, bf16[16,16,512]{2,1,0:T(8,128)(2,1)S(1)}, u32[]{:S(2)}) copy-start(bf16[16,16,512]{2,1,0:T(8,128)(2,1)S(1)} %slice.51) | copy-start | bytes 786436
  116.4 12.0 %copy-start = (bf16[256,2048]{1,0:T(8,128)(2,1)S(1)}, bf16[256,2048]{1,0:T(8,128)(2,1)}, u32[]{:S(2)}) copy-start(bf16[256,2048]{1,0:T(8,128)(2,1)} %get-tuple-element.38.out_mat_ref.refs_9_.refs_6_) | copy-start | bytes 3145732
  116.4 12.0 %copy-start.5 = (f32[256]{0:T(256)S(1)}, f32[256]{0:T(256)}, u32[]{:S(2)}) copy-start(f32[256]{0:T(256)} %param.28) | copy-start | bytes 3076
  116.5 12.0 %copy-start.6 = (bf16[256,2048]{1,0:T(8,128)(2,1)S(1)}, bf16[256,2048]{1,0:T(8,128)(2,1)}, u32[]{:S(2)}) copy-start(bf16[256,2048]{1,0:T(8,128)(2,1)} %get-tuple-element.37.in_ref) | copy-start | bytes 3145732
  116.5 12.0 %copy-start.7 = (f32[512,256]{1,0:T(8,128)S(1)}, f32[512,256]{1,0:T(8,128)}, u32[]{:S(2)}) copy-start(f32[512,256]{1,0:T(8,128)} %get-tuple-element.35.grow_ref) | copy-start | bytes 1572868
  116.5 12.0 %copy-start.8 = (f32[512,256]{1,0:T(8,128)S(1)}, f32[512,256]{1,0:T(8,128)}, u32[]{:S(2)}) copy-start(f32[512,256]{1,0:T(8,128)} %get-tuple-element.36.shrink_ref) | copy-start | bytes 1572868
  116.5 12.0 %copy-start.9 = (f32[5,16,1024]{2,1,0:T(8,128)S(1)}, f32[5,16,1024]{2,1,0:T(8,128)}, u32[]{:S(2)}) copy-start(f32[5,16,1024]{2,1,0:T(8,128)} %get-tuple-element.39.hop_re_ref) | copy-start | bytes 983044
  116.5 12.0 %copy-start.10 = (f32[5,16,1024]{2,1,0:T(8,128)S(1)}, f32[5,16,1024]{2,1,0:T(8,128)}, u32[]{:S(2)}) copy-start(f32[5,16,1024]{2,1,0:T(8,128)} %get-tuple-element.40.hop_im_ref) | copy-start | bytes 983044
  116.5 12.0 %copy-start.11 = (f32[1,128]{1,0:T(1,128)S(1)}, f32[1,128]{1,0:T(1,128)}, u32[]{:S(2)}) copy-start(f32[1,128]{1,0:T(1,128)} %get-tuple-element.41.shift_ref) | copy-start | bytes 1540
  116.5 26.1 %collective-permute-start.6 = (bf16[16,16,512]{2,1,0:T(8,128)(2,1)S(1)}, bf16[16,16,512]{2,1,0:T(8,128)(2,1)}, u32[]{:S(2)}, u32[]{:S(2)}) collective-permute-start(bf16[16,16,512]{2,1,0:T(8,128)(2,1)S(1)} %slice.51), channel_id=1, source_target_pairs={{0,24},{8,0},{16,8},{24,16},{1,25},{9,1},{17,9},{25,17},{2,26},{10... | collective-permute-start | bytes 786440 | tf_op jit(solution)/shard_map/ppermute | solution.py:41
  118.7 24.0 %collective-permute-start.7 = (bf16[16,16,512]{2,1,0:T(8,128)(2,1)S(1)}, bf16[16,16,512]{2,1,0:T(8,128)(2,1)}, u32[]{:S(2)}, u32[]{:S(2)}) collective-permute-start(bf16[16,16,512]{2,1,0:T(8,128)(2,1)S(1)} %slice.51), channel_id=1, source_target_pairs={{0,16},{8,24},{16,0},{24,8},{1,17},{9,25},{17,1},{25,9},{2,18},{10... | collective-permute-start | bytes 786440 | tf_op jit(solution)/shard_map/ppermute | solution.py:41
  121.1 21.6 %collective-permute-start.8 = (bf16[16,16,512]{2,1,0:T(8,128)(2,1)S(1)}, bf16[16,16,512]{2,1,0:T(8,128)(2,1)}, u32[]{:S(2)}, u32[]{:S(2)}) collective-permute-start(bf16[16,16,512]{2,1,0:T(8,128)(2,1)S(1)} %slice.51), channel_id=1, source_target_pairs={{0,8},{8,16},{16,24},{24,0},{1,9},{9,17},{17,25},{25,1},{2,10},{10... | collective-permute-start | bytes 786440 | tf_op jit(solution)/shard_map/ppermute | solution.py:41
  133.5 24.4 %copy-start.1 = (f32[31,256]{1,0:T(8,128)S(1)}, f32[31,256]{1,0:T(8,128)}, u32[]{:S(2)}) copy-start(f32[31,256]{1,0:T(8,128)} %taps_ref.1) | copy-start | bytes 95236
  144.0 28.0 %collective-permute-start.9 = (bf16[4,16,16,512]{3,2,1,0:T(8,128)(2,1)S(1)}, bf16[4,16,16,512]{3,2,1,0:T(8,128)(2,1)}, u32[]{:S(2)}, u32[]{:S(2)}) collective-permute-start(bf16[4,16,16,512]{3,2,1,0:T(8,128)(2,1)S(1)} %pad_maximum_fusion.refs_10_.refs_7_), channel_id=1, source_target_pairs={{0,4},{4,0},{1,5},{5,1},{2,6},{6,2},{3,7},{7,3},{8,12},{12,8},{9,1... | collective-permute-start | bytes 3145736 | tf_op jit(solution)/shard_map/ppermute | solution.py:36
  146.7 25.3 %all-to-all-start.3 = ((f32[16,1,2176]{2,1,0:T(1,128)}), f32[16,1,2176]{2,1,0:T(1,128)S(1)}, u32[]{:S(2)}, u32[]{:S(2)}) async-start(f32[16,1,2176]{2,1,0:T(1,128)} %broadcast_in_dim.17), calls=%async_computation.3 | async-start | bytes 278528 | tf_op jit(solution)/shard_map/all_to_all | solution.py:25
  157.9 14.1 %copy-start.3 = (f32[256]{0:T(256)S(1)}, f32[256]{0:T(256)}, u32[]{:S(2)}) copy-start(f32[256]{0:T(256)} %param.31) | copy-start | bytes 3076
  176.4 12.9 %collective-permute-start.10 = (bf16[64,2048]{1,0:T(8,128)(2,1)S(1)}, bf16[64,2048]{1,0:T(8,128)(2,1)S(1)}, u32[]{:S(2)}, u32[]{:S(2)}) collective-permute-start(bf16[64,2048]{1,0:T(8,128)(2,1)S(1)} %get-tuple-element.59), channel_id=1, source_target_pairs={{0,3},{1,0},{2,1},{3,2},{4,7},{5,4},{6,5},{7,6},{8,11},{9,8},{10,9... | collective-permute-start | bytes 786440 | tf_op jit(solution)/shard_map/ppermute | solution.py:41
  180.4 9.5 %collective-permute-start.12 = (bf16[64,2048]{1,0:T(8,128)(2,1)S(1)}, bf16[64,2048]{1,0:T(8,128)(2,1)S(1)}, u32[]{:S(2)}, u32[]{:S(2)}) collective-permute-start(bf16[64,2048]{1,0:T(8,128)(2,1)S(1)} %get-tuple-element.60), channel_id=1, source_target_pairs={{0,1},{1,2},{2,3},{3,0},{4,5},{5,6},{6,7},{7,4},{8,9},{9,10},{10,1... | collective-permute-start | bytes 786440 | tf_op jit(solution)/shard_map/ppermute | solution.py:41
  190.0 15.0 %collective-permute-start.13 = (bf16[128,2048]{1,0:T(8,128)(2,1)S(1)}, bf16[128,2048]{1,0:T(8,128)(2,1)S(1)}, u32[]{:S(2)}, u32[]{:S(2)}) collective-permute-start(bf16[128,2048]{1,0:T(8,128)(2,1)S(1)} %get-tuple-element.58), channel_id=1, source_target_pairs={{0,1},{1,2},{2,3},{3,0},{4,5},{5,6},{6,7},{7,4},{8,9},{9,10},{10,1... | collective-permute-start | bytes 1572872 | tf_op jit(solution)/shard_map/ppermute | solution.py:41
  193.5 13.4 %collective-permute-start.11 = (bf16[128,2048]{1,0:T(8,128)(2,1)S(1)}, bf16[128,2048]{1,0:T(8,128)(2,1)S(1)}, u32[]{:S(2)}, u32[]{:S(2)}) collective-permute-start(bf16[128,2048]{1,0:T(8,128)(2,1)S(1)} %get-tuple-element.57), channel_id=1, source_target_pairs={{0,3},{1,0},{2,1},{3,2},{4,7},{5,4},{6,5},{7,6},{8,11},{9,8},{10,9... | collective-permute-start | bytes 1572872 | tf_op jit(solution)/shard_map/ppermute | solution.py:41

commit v10 on v8

--- a/solution.py
+++ b/solution.py
@@ -132,28 +132,35 @@
     )
 
 
-def state_in_kernel(place_ref, normed_ref, own_ref, other_ref, out_ref, weight_ref, done):
+def state_in_kernel(
+    place_ref, normed_all, own_ref, other_ref, out_ref, weight_ref, done, normed_ref, normed_done
+):
     rows = normed_ref.shape[1]
-    arrived(natural_order(place_ref, own_ref, other_ref, weight_ref, done))
+    whole = fetch(normed_all, normed_ref, normed_done.at[0])
+    arrived([*natural_order(place_ref, own_ref, other_ref, weight_ref, done), whole])
     out_ref[...] = projected(normed_ref, weight_ref, slice(HALO, rows)).astype(BF16)
 
 
 def conv_kernel(
     place_ref,
-    normed_ref,
     taps_ref,
+    normed_all,
     own_ref,
     other_ref,
     raw_ref,
     sums_ref,
     weight_ref,
     done,
+    normed_ref,
+    normed_done,
     glu_ref,
     shifted_ref,
 ):
     _, rows, _ = normed_ref.shape
     count, width = raw_ref.shape
-    arrived(natural_order(place_ref, own_ref, other_ref, weight_ref, done, first_lane=width))
+    whole = fetch(normed_all, normed_ref, normed_done.at[0])
+    weights_begun = natural_order(place_ref, own_ref, other_ref, weight_ref, done, first_lane=width)
+    arrived([*weights_begun, whole])
     both = projected(normed_ref, weight_ref, slice(0, rows))
     value = both[:, :width].astype(BF16).astype(F32)
     gate = both[:, width:].astype(BF16).astype(F32)
@@ -644,9 +651,13 @@
     )
     device = dict(shift=total, rates=rates)
     project_x = copies(planes[:, :, : 3 * width], "x")
+    normed_scratch = [
+        pltpu.VMEM((parts, rows, depth_part), BF16),
+        pltpu.SemaphoreType.DMA((1,)),
+    ]
     normed = call(
         norm_kernel,
-        jax.ShapeDtypeStruct((parts, rows, depth_part), BF16),
+        pltpu.HBM((parts, rows, depth_part), BF16),
         (*far_from_core(extended, ahead, top, bottom, behind), norm_gain.reshape(parts, 1, depth_part)),
         scalars=(place,),
         mib=12,
@@ -663,10 +674,10 @@
     u_in = call(
         state_in_kernel,
         jax.ShapeDtypeStruct((count, width), BF16),
-        (normed,),
-        apart=far_from_core(project_x, project_other),
+        (),
+        apart=far_from_core(normed, project_x, project_other),
         scalars=(place,),
-        scratch=weight_scratch(project_x, width),
+        scratch=(*weight_scratch(project_x, width), *normed_scratch),
         mib=12,
         flops=2 * count * depth * width,
         bytes_accessed=4 * depth * count,
@@ -717,11 +728,12 @@
             pltpu.HBM((count, width), F32),
             jax.ShapeDtypeStruct((2, count), F32),
         ),
-        (normed, conv_taps),
-        apart=far_from_core(project_x, project_other),
+        (conv_taps,),
+        apart=far_from_core(normed, project_x, project_other),
         scalars=(place,),
         scratch=(
             *weight_scratch(project_x, 2 * width),
+            *normed_scratch,
             pltpu.VMEM((rows + 8, width), F32),
             pltpu.VMEM((8, rows, width), F32),
         ),

time: 215 us -> 217 us (level)
  Pallas kernels: 36.4 us -> 39.1 us
    pallas_call x8, Pallas kernels: 36.4 us -> 39.1 us  [call(): pl.pallas_call(body, compiler_params=pltpu.CompilerParams(vmem_limit_byte...]
  transfers between devices with their start and end apart: 19 -> 19, of which waited for: 12 -> 11; matrix products, arithmetic and copies ran while one was open for 2% -> 2% of each run, Pallas kernels for 15% -> 16%
where the time goes in v10:
time: 217 us; the launch traced here: 214 us
  starting transfers between devices  76.8 us (35%)
  waiting for transfers between devices  61.6 us (28%)
  Pallas kernels  39.1 us (18%)
  blocking collectives  26.9 us (12%)
  local copies, waits for them, and re-layouts  4.58 us (2%)
  other arithmetic  4.17 us (2%)
    ppermute x14, starting transfers between devices, from_ahead(): lax.ppermute(block, axis, [(i, (i - distance) % count) for i in range(cou...  44 us
    pallas_call x8, Pallas kernels, call(): pl.pallas_call(body, compiler_params=pltpu.CompilerParams(vmem_limit_byte...  39.1 us
    ppermute x14, waiting for transfers between devices, from_ahead(): lax.ppermute(block, axis, [(i, (i - distance) % count) for i in range(cou...  34.2 us
    all_to_all x2, blocking collectives, copies(): lax.all_to_all(jnp.broadcast_to(value[None], (peers, *value.shape)), axis...  26.9 us
    all_to_all x2, starting transfers between devices, copies(): lax.all_to_all(jnp.broadcast_to(value[None], (peers, *value.shape)), axis...  26.4 us
    all_to_all x2, waiting for transfers between devices, copies(): lax.all_to_all(jnp.broadcast_to(value[None], (peers, *value.shape)), axis...  24.7 us
  transfers between devices with their start and end apart: 19, of which 11 were waited for; matrix products, arithmetic and copies ran while one was open for 2% of the time, Pallas kernels for 16%

profile of v10, /device:TPU:6, one launch (start us, length us, event | category | flops | bytes accessed | tf_op | source)
XLA Modules:
  0.0 213.9 jit_solution(3873466321467156304)
XLA Ops:
  0.0 0.8 maximum_bitcast_fusion
  0.8 0.7 pad_maximum_fusion.1
  1.5 0.9 broadcast_in_dim.12
  2.4 15.2 %all-to-all-start = ((bf16[16,16,1280]{2,1,0:T(8,128)(2,1)}), bf16[16,16,1280]{2,1,0:T(8,128)(2,1)S(1)}, u32[]{:S(2)}, u32[]{:S(2)}) async-start(bf16[16,16,1280]{2,1,0:T(8,128)(2,1)} %broadcast_in_dim.12), calls=%async_computation | async-start | bytes 1310720 | tf_op jit(solution)/shard_map/all_to_all | solution.py:25
  17.6 0.0 copy-start.4
  17.7 0.1 fusion.14
  17.8 0.1 reshape.133.refs_1_
  17.9 0.1 mul.192
  18.0 0.1 mul.164
  18.0 0.1 reshape.134.refs_8_
  18.2 0.3 multiply_sine_fusion.1
  18.6 0.6 fusion.11
  19.2 7.5 %shard_map.163 = (f32[512,256]{1,0:T(8,128)}, f32[512,256]{1,0:T(8,128)}, bf16[256,2048]{1,0:T(8,128)(2,1)}, bf16[256,2048]{1,0:T(8,128)(2,1)}, f32[5,16,1024]{2...) custom-call(f32[16,512]{1,0:T(8,128)S(1)} %copy-done.4, ...), custom_call_target="tpu_custom_call" | custom-call | flops 83886080 | bytes 4194304 | tf_op jit(solution)/shard_map/pallas_call | solution.py:53
  26.7 24.6 %all-to-all-done = bf16[16,16,1280]{2,1,0:T(8,128)(2,1)S(1)} async-done(((bf16[16,16,1280]{2,1,0:T(8,128)(2,1)}), bf16[16,16,1280]{2,1,0:T(8,128)(2,1)S(1)}, u32[]{:S(2)}, u32[]{:S(2)}) %all-to-all-start) | async-done | bytes 655392 | tf_op jit(solution)/shard_map/all_to_all | solution.py:25
  51.4 0.1 broadcast_in_dim.13
  51.5 0.0 copy-start.15
  51.5 18.4 %all_to_all.20.own_ref = bf16[4,16,16,768]{3,2,1,0:T(8,128)(2,1)} all-to-all(bf16[4,16,16,768]{3,2,1,0:T(8,128)(2,1)S(1)} %broadcast_in_dim.13), channel_id=1, replica_groups=mesh['z'=16,'x'=4,'c'=2,'tp'=4] {'x'}, dimensions={0} | all-to-all | bytes 3145728 | tf_op jit(solution)/shard_map/all_to_all | solution.py:25
  69.9 2.0 collective-permute-start.5
  71.9 2.4 %collective-permute-start = (bf16[32,512]{1,0:T(8,128)(2,1)S(1)}, bf16[32,512]{1,0:T(8,128)(2,1)S(1)}, u32[]{:S(2)}, u32[]{:S(2)}) collective-permute-start(bf16[32,512]{1,0:T(8,128)(2,1)S(1)} %slice.52), channel_id=1, source_target_pairs={{0,4},{4,8},{8,12},{12,16},{16,20},{20,24},{24,28},{28,32},{32,36}... | collective-permute-start | bytes 98312 | tf_op jit(solution)/shard_map/ppermute | solution.py:32
  74.4 2.8 %collective-permute-done = bf16[32,512]{1,0:T(8,128)(2,1)S(1)} collective-permute-done((bf16[32,512]{1,0:T(8,128)(2,1)S(1)}, bf16[32,512]{1,0:T(8,128)(2,1)S(1)}, u32[]{:S(2)}, u32[]{:S(2)}) %collective-permute-start) | collective-permute-done | bytes 32800 | tf_op jit(solution)/shard_map/ppermute | solution.py:32
  77.2 4.9 %collective-permute-start.1 = (bf16[544,512]{1,0:T(8,128)(2,1)S(1)}, bf16[544,512]{1,0:T(8,128)(2,1)S(1)}, u32[]{:S(2)}, u32[]{:S(2)}) collective-permute-start(bf16[544,512]{1,0:T(8,128)(2,1)S(1)} %constant_dynamic-update-slice_fusion.own_ref), channel_id=1, source_target_pairs={{0,3},{1,0},{2,1},{3,2},{4,7},{5,4},{6,5},{7,6},{8,11},{9,8},{10,9... | collective-permute-start | bytes 1671176 | tf_op jit(solution)/shard_map/ppermute | solution.py:41
  82.2 1.9 collective-permute-start.3
  84.1 10.5 %collective-permute-done.1.ahead_ref = bf16[544,512]{1,0:T(8,128)(2,1)S(1)} collective-permute-done((bf16[544,512]{1,0:T(8,128)(2,1)S(1)}, bf16[544,512]{1,0:T(8,128)(2,1)S(1)}, u32[]{:S(2)}, u32[]{:S(2)}) %collective-permute-start.1) | collective-permute-done | bytes 557088 | tf_op jit(solution)/shard_map/ppermute | solution.py:41
  94.6 0.7 slice.62
  95.4 5.6 %collective-permute-start.2 = (bf16[272,512]{1,0:T(8,128)(2,1)}, bf16[272,512]{1,0:T(8,128)(2,1)S(1)}, u32[]{:S(2)}, u32[]{:S(2)}) collective-permute-start(bf16[272,512]{1,0:T(8,128)(2,1)} %slice.62), channel_id=1, source_target_pairs={{0,3},{1,0},{2,1},{3,2},{4,7},{5,4},{6,5},{7,6},{8,11},{9,8},{10,9... | collective-permute-start | bytes 835592 | tf_op jit(solution)/shard_map/ppermute | solution.py:41
  101.0 0.8 slice.63
  101.8 1.9 collective-permute-start.4
  103.7 0.1 pad_add_fusion.place_ref
  103.8 3.9 %collective-permute-done.2.top_ref = bf16[272,512]{1,0:T(8,128)(2,1)S(1)} collective-permute-done((bf16[272,512]{1,0:T(8,128)(2,1)}, bf16[272,512]{1,0:T(8,128)(2,1)S(1)}, u32[]{:S(2)}, u32[]{:S(2)}) %collective-permute-start.2) | collective-permute-done | bytes 278560 | tf_op jit(solution)/shard_map/ppermute | solution.py:41
  107.7 6.0 %collective-permute-done.4.bottom_ref = bf16[272,512]{1,0:T(8,128)(2,1)S(1)} collective-permute-done((bf16[272,512]{1,0:T(8,128)(2,1)}, bf16[272,512]{1,0:T(8,128)(2,1)S(1)}, u32[]{:S(2)}, u32[]{:S(2)}) %collective-permute-start.4) | collective-permute-done | bytes 278560 | tf_op jit(solution)/shard_map/ppermute | solution.py:41
  113.7 0.7 copy-done.17
  114.4 3.8 %shard_map.164.normed_all = bf16[4,544,512]{2,1,0:T(8,128)(2,1)} custom-call(s32[4]{0:T(128)S(1)} %pad_add_fusion.place_ref, bf16[544,512]{1,0:T(8,128)(2,1)} %copy-done.14, bf16[544,512]{1,0:T(8,128)(2,1)} %copy-done.12, bf16[272,512]{1,0:T(8,128)(2,1)} %copy-done.16, bf16[272,512]{1,0:T(8,128)(2,1)} %copy-done.17, bf16[544,512]{1,0:T(8,128)(2,1)} %copy-done.13, ...), custom_call_target="tpu_custom_call" | custom-call | flops 8388608 | bytes 4194304 | tf_op jit(solution)/shard_map/pallas_call | solution.py:53
  118.3 1.9 collective-permute-start.9
  120.2 2.6 %collective-permute-start.10 = (bf16[16,16,512]{2,1,0:T(8,128)(2,1)S(1)}, bf16[16,16,512]{2,1,0:T(8,128)(2,1)S(1)}, u32[]{:S(2)}, u32[]{:S(2)}) collective-permute-start(bf16[16,16,512]{2,1,0:T(8,128)(2,1)S(1)} %slice.51), channel_id=1, source_target_pairs={{0,16},{8,24},{16,0},{24,8},{1,17},{9,25},{17,1},{25,9},{2,18},{10... | collective-permute-start | bytes 786440 | tf_op jit(solution)/shard_map/ppermute | solution.py:41
  122.8 4.4 %collective-permute-start.11 = (bf16[16,16,512]{2,1,0:T(8,128)(2,1)S(1)}, bf16[16,16,512]{2,1,0:T(8,128)(2,1)S(1)}, u32[]{:S(2)}, u32[]{:S(2)}) collective-permute-start(bf16[16,16,512]{2,1,0:T(8,128)(2,1)S(1)} %slice.51), channel_id=1, source_target_pairs={{0,8},{8,16},{16,24},{24,0},{1,9},{9,17},{17,25},{25,1},{2,10},{10... | collective-permute-start | bytes 786440 | tf_op jit(solution)/shard_map/ppermute | solution.py:41
  127.3 0.1 fusion.5.lower_ref
  127.4 0.0 copy-start.5
  127.4 0.0 copy-start.7
  127.5 3.5 %shard_map.166.u_ref = bf16[512,256]{1,0:T(8,128)(2,1)S(1)} custom-call(s32[4]{0:T(128)S(1)} %pad_add_fusion.place_ref, bf16[4,544,512]{2,1,0:T(8,128)(2,1)} %shard_map.164.normed_all, bf16[4,16,16,768]{3,2,1,0:T(8,128)(2,1)} %all_to_all.20.own_ref, bf16[4,16,16,768]{3,2,1,0:T(8,128)(2,1)} %collective-permute-done.5.other_ref), custom_call_target="tpu_custom_call" | custom-call | flops 536870912 | bytes 4194304 | tf_op jit(solution)/shard_map/pallas_call | solution.py:53
  131.1 4.9 %shard_map.167 = (f32[512,256]{1,0:T(8,128)}, f32[1,2176]{1,0:T(1,128)S(1)}) custom-call(bf16[512,256]{1,0:T(8,128)(2,1)S(1)} %shard_map.166.u_ref, f32[512,256]{1,0:T(8,128)S(1)} %copy-done.7, f32[512,256]{1,0:T(8,128)S(1)} %copy-done.8, bf16[256,2048]{1,0:T(8,128)(2,1)S(1)} %copy-done.6, bf16[256,2048]{1,0:T(8,128)(2,1)S(1)} %copy-done, ...), custom_call_target="tpu_custom_call" | custom-call | flops 1610612736 | bytes 4194304 | tf_op jit(solution)/shard_map/pallas_call | solution.py:53
  136.0 0.9 collective-permute-done.11
  137.0 0.1 pad_maximum_fusion.refs_13_.refs_10_
  137.1 1.9 collective-permute-start.12
  139.1 8.6 %all_to_all.21.near_ref = f32[8,1,2176]{2,1,0:T(1,128)S(1)} all-to-all(f32[8,1,2176]{2,1,0:T(1,128)S(1)} %broadcast_in_dim.15), channel_id=1, replica_groups=mesh['z'=16,'x'=4,'c'=2,'tp'=4] {'x','c'}, dimensions={0} | all-to-all | bytes 139264 | tf_op jit(solution)/shard_map/all_to_all | solution.py:25
  147.7 0.9 shard_map.168
  148.6 0.7 broadcast_in_dim.17
  149.4 11.2 %all-to-all-start.3 = ((f32[16,1,2176]{2,1,0:T(1,128)}), f32[16,1,2176]{2,1,0:T(1,128)S(1)}, u32[]{:S(2)}, u32[]{:S(2)}) async-start(f32[16,1,2176]{2,1,0:T(1,128)} %broadcast_in_dim.17), calls=%async_computation.3 | async-start | bytes 278528 | tf_op jit(solution)/shard_map/all_to_all | solution.py:25
  160.6 7.0 %shard_map.165 = (f32[512,256]{1,0:T(8,128)}, f32[2,512]{1,0:T(2,128)S(1)}) custom-call(s32[4]{0:T(128)S(1)} %pad_add_fusion.place_ref, f32[31,256]{1,0:T(8,128)S(1)} %copy-done.1, bf16[4,544,512]{2,1,0:T(8,128)(2,1)} %shard_map.164.normed_all, bf16[4,16,16,768]{3,2,1,0:T(8,128)(2,1)} %all_to_all.20.own_ref, ...), custom_call_target="tpu_custom_call" | custom-call | flops 1073741824 | bytes 4194304 | tf_op jit(solution)/shard_map/pallas_call | solution.py:53
  167.6 1.9 collective-permute-start.6
  169.5 3.3 %collective-permute-start.7 = (f32[2,512]{1,0:T(2,128)S(1)}, f32[2,512]{1,0:T(2,128)S(1)}, u32[]{:S(2)}, u32[]{:S(2)}) collective-permute-start(f32[2,512]{1,0:T(2,128)S(1)} %get-tuple-element.34.refs_1_), channel_id=1, source_target_pairs={{0,2},{1,3},{2,0},{3,1},{4,6},{5,7},{6,4},{7,5},{8,10},{9,11},{10,... | collective-permute-start | bytes 12296 | tf_op jit(solution)/shard_map/ppermute | solution.py:41
  172.8 2.5 %collective-permute-start.8 = (f32[2,512]{1,0:T(2,128)S(1)}, f32[2,512]{1,0:T(2,128)S(1)}, u32[]{:S(2)}, u32[]{:S(2)}) collective-permute-start(f32[2,512]{1,0:T(2,128)S(1)} %get-tuple-element.34.refs_1_), channel_id=1, source_target_pairs={{0,1},{1,2},{2,3},{3,0},{4,5},{5,6},{6,7},{7,4},{8,9},{9,10},{10,1... | collective-permute-start | bytes 12296 | tf_op jit(solution)/shard_map/ppermute | solution.py:41
  175.4 1.1 collective-permute-done.7.refs_3_
  176.5 3.1 %collective-permute-done.8.refs_4_ = f32[2,512]{1,0:T(2,128)S(1)} collective-permute-done((f32[2,512]{1,0:T(2,128)S(1)}, f32[2,512]{1,0:T(2,128)S(1)}, u32[]{:S(2)}, u32[]{:S(2)}) %collective-permute-start.8) | collective-permute-done | bytes 4128 | tf_op jit(solution)/shard_map/ppermute | solution.py:41
  179.6 4.3 %shard_map.169 = (bf16[1,128,2048]{2,1,0:T(8,128)(2,1)S(1)}, f32[2,1024]{1,0:T(2,128)S(1)}) custom-call(s32[4]{0:T(128)S(1)} %pad_add_fusion.place_ref, f32[1,256]{1,0:T(1,128)S(1)} %bitcast.57, f32[2,512]{1,0:T(2,128)S(1)} %get-tuple-element.34.refs_1_, f32[2,512]{1,0:T(2,128)S(1)} %collective-permute-done.6.refs_2_, ...), custom_call_target="tpu_custom_call" | custom-call | flops 268435456 | bytes 4194304 | tf_op jit(solution)/shard_map/pallas_call | solution.py:53
  184.0 4.0 %collective-permute-start.13 = (bf16[64,2048]{1,0:T(8,128)(2,1)S(1)}, bf16[64,2048]{1,0:T(8,128)(2,1)S(1)}, u32[]{:S(2)}, u32[]{:S(2)}) collective-permute-start(bf16[64,2048]{1,0:T(8,128)(2,1)S(1)} %get-tuple-element.59), channel_id=1, source_target_pairs={{0,3},{1,0},{2,1},{3,2},{4,7},{5,4},{6,5},{7,6},{8,11},{9,8},{10,9... | collective-permute-start | bytes 786440 | tf_op jit(solution)/shard_map/ppermute | solution.py:41
  188.0 1.9 collective-permute-start.15
  189.9 7.1 %shard_map.170 = bf16[3,128,2048]{2,1,0:T(8,128)(2,1)S(1)} custom-call(s32[4]{0:T(128)S(1)} %pad_add_fusion.place_ref, f32[1,256]{1,0:T(1,128)S(1)} %bitcast.58, f32[2,512]{1,0:T(2,128)S(1)} %get-tuple-element.34.refs_1_, f32[2,512]{1,0:T(2,128)S(1)} %collective-permute-done.6.refs_2_, f32[2,512]{1,0:T(2,128)S(1)} %collective-permute-done.7.refs_3_, ...), custom_call_target="tpu_custom_call" | custom-call | flops 805306368 | bytes 4194304 | tf_op jit(solution)/shard_map/pallas_call | solution.py:53
  197.1 0.4 collective-permute-done.15
  197.5 0.2 fusion.1
  197.6 1.9 collective-permute-start.16
  199.6 5.1 %collective-permute-start.14 = (bf16[128,2048]{1,0:T(8,128)(2,1)S(1)}, bf16[128,2048]{1,0:T(8,128)(2,1)S(1)}, u32[]{:S(2)}, u32[]{:S(2)}) collective-permute-start(bf16[128,2048]{1,0:T(8,128)(2,1)S(1)} %get-tuple-element.57), channel_id=1, source_target_pairs={{0,3},{1,0},{2,1},{3,2},{4,7},{5,4},{6,5},{7,6},{8,11},{9,8},{10,9... | collective-permute-start | bytes 1572872 | tf_op jit(solution)/shard_map/ppermute | solution.py:41
  204.7 7.0 %collective-permute-done.16 = bf16[128,2048]{1,0:T(8,128)(2,1)S(1)} collective-permute-done((bf16[128,2048]{1,0:T(8,128)(2,1)S(1)}, bf16[128,2048]{1,0:T(8,128)(2,1)S(1)}, u32[]{:S(2)}, u32[]{:S(2)}) %collective-permute-start.16) | collective-permute-done | bytes 524320 | tf_op jit(solution)/shard_map/ppermute | solution.py:41
  211.7 1.2 collective-permute-done.14
  212.8 1.0 fusion.3
  (69 shorter events, 0.5 us)
Async XLA Ops:
  0.0 17.6 %copy-start.23 = (f32[16]{0:T(128)S(1)}, f32[16]{0:T(128)}, u32[]{:S(2)}) copy-start(f32[16]{0:T(128)} %param.24) | copy-start | bytes 196
  0.0 17.7 %copy-start.21 = (f32[16,64]{1,0:T(8,128)S(1)}, f32[16,64]{1,0:T(8,128)}, u32[]{:S(2)}) copy-start(f32[16,64]{1,0:T(8,128)} %param.23) | copy-start | bytes 12292
  0.0 17.7 %copy-start.22 = (f32[16,64]{1,0:T(8,128)S(1)}, f32[16,64]{1,0:T(8,128)}, u32[]{:S(2)}) copy-start(f32[16,64]{1,0:T(8,128)} %param.22) | copy-start | bytes 12292
  0.0 18.0 %copy-start.20 = (f32[2,16,64]{2,1,0:T(8,128)S(1)}, f32[2,16,64]{2,1,0:T(8,128)}, u32[]{:S(2)}) copy-start(f32[2,16,64]{2,1,0:T(8,128)} %param.29) | copy-start | bytes 24580
  0.0 18.1 %copy-start.18 = (f32[2,16,16,64]{3,2,1,0:T(8,128)S(1)}, f32[2,16,16,64]{3,2,1,0:T(8,128)}, u32[]{:S(2)}) copy-start(f32[2,16,16,64]{3,2,1,0:T(8,128)} %param.26) | copy-start | bytes 393220
  1.5 17.0 %copy-start.19 = (f32[2,16,16,64]{3,2,1,0:T(8,128)S(1)}, f32[2,16,16,64]{3,2,1,0:T(8,128)}, u32[]{:S(2)}) copy-start(f32[2,16,16,64]{3,2,1,0:T(8,128)} %param.27) | copy-start | bytes 393220
  2.4 48.9 %all-to-all-start = ((bf16[16,16,1280]{2,1,0:T(8,128)(2,1)}), bf16[16,16,1280]{2,1,0:T(8,128)(2,1)S(1)}, u32[]{:S(2)}, u32[]{:S(2)}) async-start(bf16[16,16,1280]{2,1,0:T(8,128)(2,1)} %broadcast_in_dim.12), calls=%async_computation | async-start | bytes 1310720 | tf_op jit(solution)/shard_map/all_to_all | solution.py:25
  17.6 1.5 copy-start.4
  51.5 20.4 %copy-start.15 = (bf16[512,512]{1,0:T(8,128)(2,1)S(1)}, bf16[512,512]{1,0:T(8,128)(2,1)}, u32[]{:S(2)}) copy-start(bf16[512,512]{1,0:T(8,128)(2,1)} %param.17) | copy-start | bytes 1572868
  69.9 44.6 %copy-start.2 = (f32[2048]{0:T(1024)S(1)}, f32[2048]{0:T(1024)}, u32[]{:S(2)}) copy-start(f32[2048]{0:T(1024)} %param.18) | copy-start | bytes 24580
  69.9 57.6 %collective-permute-start.5 = (bf16[4,16,16,768]{3,2,1,0:T(8,128)(2,1)}, bf16[4,16,16,768]{3,2,1,0:T(8,128)(2,1)}, u32[]{:S(2)}, u32[]{:S(2)}) collective-permute-start(bf16[4,16,16,768]{3,2,1,0:T(8,128)(2,1)} %all_to_all.20.own_ref), channel_id=1, source_target_pairs={{0,4},{4,0},{1,5},{5,1},{2,6},{6,2},{3,7},{7,3},{8,12},{12,8},{9,1... | collective-permute-start | bytes 4718600 | tf_op jit(solution)/shard_map/ppermute | solution.py:36
  71.9 5.2 %collective-permute-start = (bf16[32,512]{1,0:T(8,128)(2,1)S(1)}, bf16[32,512]{1,0:T(8,128)(2,1)S(1)}, u32[]{:S(2)}, u32[]{:S(2)}) collective-permute-start(bf16[32,512]{1,0:T(8,128)(2,1)S(1)} %slice.52), channel_id=1, source_target_pairs={{0,4},{4,8},{8,12},{12,16},{16,20},{20,24},{24,28},{28,32},{32,36}... | collective-permute-start | bytes 98312 | tf_op jit(solution)/shard_map/ppermute | solution.py:32
  77.2 36.5 %copy-start.14 = (bf16[544,512]{1,0:T(8,128)(2,1)}, bf16[544,512]{1,0:T(8,128)(2,1)S(1)}, u32[]{:S(2)}) copy-start(bf16[544,512]{1,0:T(8,128)(2,1)S(1)} %constant_dynamic-update-slice_fusion.own_ref) | copy-start | bytes 1671172
  77.2 17.4 %collective-permute-start.1 = (bf16[544,512]{1,0:T(8,128)(2,1)S(1)}, bf16[544,512]{1,0:T(8,128)(2,1)S(1)}, u32[]{:S(2)}, u32[]{:S(2)}) collective-permute-start(bf16[544,512]{1,0:T(8,128)(2,1)S(1)} %constant_dynamic-update-slice_fusion.own_ref), channel_id=1, source_target_pairs={{0,3},{1,0},{2,1},{3,2},{4,7},{5,4},{6,5},{7,6},{8,11},{9,8},{10,9... | collective-permute-start | bytes 1671176 | tf_op jit(solution)/shard_map/ppermute | solution.py:41
  82.2 18.8 %collective-permute-start.3 = (bf16[544,512]{1,0:T(8,128)(2,1)S(1)}, bf16[544,512]{1,0:T(8,128)(2,1)S(1)}, u32[]{:S(2)}, u32[]{:S(2)}) collective-permute-start(bf16[544,512]{1,0:T(8,128)(2,1)S(1)} %constant_dynamic-update-slice_fusion.own_ref), channel_id=1, source_target_pairs={{0,1},{1,2},{2,3},{3,0},{4,5},{5,6},{6,7},{7,4},{8,9},{9,10},{10,1... | collective-permute-start | bytes 1671176 | tf_op jit(solution)/shard_map/ppermute | solution.py:41
  94.6 19.1 %copy-start.12 = (bf16[544,512]{1,0:T(8,128)(2,1)}, bf16[544,512]{1,0:T(8,128)(2,1)S(1)}, u32[]{:S(2)}) copy-start(bf16[544,512]{1,0:T(8,128)(2,1)S(1)} %collective-permute-done.1.ahead_ref) | copy-start | bytes 1671172
  95.4 12.3 %collective-permute-start.2 = (bf16[272,512]{1,0:T(8,128)(2,1)}, bf16[272,512]{1,0:T(8,128)(2,1)S(1)}, u32[]{:S(2)}, u32[]{:S(2)}) collective-permute-start(bf16[272,512]{1,0:T(8,128)(2,1)} %slice.62), channel_id=1, source_target_pairs={{0,3},{1,0},{2,1},{3,2},{4,7},{5,4},{6,5},{7,6},{8,11},{9,8},{10,9... | collective-permute-start | bytes 835592 | tf_op jit(solution)/shard_map/ppermute | solution.py:41
  101.0 12.7 %copy-start.13 = (bf16[544,512]{1,0:T(8,128)(2,1)}, bf16[544,512]{1,0:T(8,128)(2,1)S(1)}, u32[]{:S(2)}) copy-start(bf16[544,512]{1,0:T(8,128)(2,1)S(1)} %collective-permute-done.3.behind_ref) | copy-start | bytes 1671172
  101.8 11.9 %collective-permute-start.4 = (bf16[272,512]{1,0:T(8,128)(2,1)}, bf16[272,512]{1,0:T(8,128)(2,1)S(1)}, u32[]{:S(2)}, u32[]{:S(2)}) collective-permute-start(bf16[272,512]{1,0:T(8,128)(2,1)} %slice.63), channel_id=1, source_target_pairs={{0,1},{1,2},{2,3},{3,0},{4,5},{5,6},{6,7},{7,4},{8,9},{9,10},{10,1... | collective-permute-start | bytes 835592 | tf_op jit(solution)/shard_map/ppermute | solution.py:41
  107.7 6.0 %copy-start.16 = (bf16[272,512]{1,0:T(8,128)(2,1)}, bf16[272,512]{1,0:T(8,128)(2,1)S(1)}, u32[]{:S(2)}) copy-start(bf16[272,512]{1,0:T(8,128)(2,1)S(1)} %collective-permute-done.2.top_ref) | copy-start | bytes 835588
  113.7 0.7 copy-start.17
  118.3 17.7 %collective-permute-start.9 = (bf16[16,16,512]{2,1,0:T(8,128)(2,1)S(1)}, bf16[16,16,512]{2,1,0:T(8,128)(2,1)S(1)}, u32[]{:S(2)}, u32[]{:S(2)}) collective-permute-start(bf16[16,16,512]{2,1,0:T(8,128)(2,1)S(1)} %slice.51), channel_id=1, source_target_pairs={{0,24},{8,0},{16,8},{24,16},{1,25},{9,1},{17,9},{25,17},{2,26},{10... | collective-permute-start | bytes 786440 | tf_op jit(solution)/shard_map/ppermute | solution.py:41
  120.2 15.8 %collective-permute-start.10 = (bf16[16,16,512]{2,1,0:T(8,128)(2,1)S(1)}, bf16[16,16,512]{2,1,0:T(8,128)(2,1)S(1)}, u32[]{:S(2)}, u32[]{:S(2)}) collective-permute-start(bf16[16,16,512]{2,1,0:T(8,128)(2,1)S(1)} %slice.51), channel_id=1, source_target_pairs={{0,16},{8,24},{16,0},{24,8},{1,17},{9,25},{17,1},{25,9},{2,18},{10... | collective-permute-start | bytes 786440 | tf_op jit(solution)/shard_map/ppermute | solution.py:41
  122.8 14.1 %collective-permute-start.11 = (bf16[16,16,512]{2,1,0:T(8,128)(2,1)S(1)}, bf16[16,16,512]{2,1,0:T(8,128)(2,1)S(1)}, u32[]{:S(2)}, u32[]{:S(2)}) collective-permute-start(bf16[16,16,512]{2,1,0:T(8,128)(2,1)S(1)} %slice.51), channel_id=1, source_target_pairs={{0,8},{8,16},{16,24},{24,0},{1,9},{9,17},{17,25},{25,1},{2,10},{10... | collective-permute-start | bytes 786440 | tf_op jit(solution)/shard_map/ppermute | solution.py:41
  127.4 3.6 %copy-start = (bf16[256,2048]{1,0:T(8,128)(2,1)S(1)}, bf16[256,2048]{1,0:T(8,128)(2,1)}, u32[]{:S(2)}) copy-start(bf16[256,2048]{1,0:T(8,128)(2,1)} %get-tuple-element.38.out_mat_ref.refs_12_.refs_9_) | copy-start | bytes 3145732
  127.4 3.6 %copy-start.5 = (f32[256]{0:T(256)S(1)}, f32[256]{0:T(256)}, u32[]{:S(2)}) copy-start(f32[256]{0:T(256)} %param.28) | copy-start | bytes 3076
  127.4 3.6 %copy-start.6 = (bf16[256,2048]{1,0:T(8,128)(2,1)S(1)}, bf16[256,2048]{1,0:T(8,128)(2,1)}, u32[]{:S(2)}) copy-start(bf16[256,2048]{1,0:T(8,128)(2,1)} %get-tuple-element.37.in_ref) | copy-start | bytes 3145732
  127.4 3.6 %copy-start.7 = (f32[512,256]{1,0:T(8,128)S(1)}, f32[512,256]{1,0:T(8,128)}, u32[]{:S(2)}) copy-start(f32[512,256]{1,0:T(8,128)} %get-tuple-element.35.grow_ref) | copy-start | bytes 1572868
  127.4 3.6 %copy-start.8 = (f32[512,256]{1,0:T(8,128)S(1)}, f32[512,256]{1,0:T(8,128)}, u32[]{:S(2)}) copy-start(f32[512,256]{1,0:T(8,128)} %get-tuple-element.36.shrink_ref) | copy-start | bytes 1572868
  127.4 3.6 %copy-start.9 = (f32[5,16,1024]{2,1,0:T(8,128)S(1)}, f32[5,16,1024]{2,1,0:T(8,128)}, u32[]{:S(2)}) copy-start(f32[5,16,1024]{2,1,0:T(8,128)} %get-tuple-element.39.hop_re_ref) | copy-start | bytes 983044
  127.4 3.6 %copy-start.10 = (f32[5,16,1024]{2,1,0:T(8,128)S(1)}, f32[5,16,1024]{2,1,0:T(8,128)}, u32[]{:S(2)}) copy-start(f32[5,16,1024]{2,1,0:T(8,128)} %get-tuple-element.40.hop_im_ref) | copy-start | bytes 983044
  127.4 3.6 %copy-start.11 = (f32[1,128]{1,0:T(1,128)S(1)}, f32[1,128]{1,0:T(1,128)}, u32[]{:S(2)}) copy-start(f32[1,128]{1,0:T(1,128)} %get-tuple-element.41.shift_ref) | copy-start | bytes 1540
  136.0 24.5 %copy-start.1 = (f32[31,256]{1,0:T(8,128)S(1)}, f32[31,256]{1,0:T(8,128)}, u32[]{:S(2)}) copy-start(f32[31,256]{1,0:T(8,128)} %taps_ref.1) | copy-start | bytes 95236
  137.1 42.5 %collective-permute-start.12 = (bf16[4,16,16,512]{3,2,1,0:T(8,128)(2,1)S(1)}, bf16[4,16,16,512]{3,2,1,0:T(8,128)(2,1)S(1)}, u32[]{:S(2)}, u32[]{:S(2)}) collective-permute-start(bf16[4,16,16,512]{3,2,1,0:T(8,128)(2,1)S(1)} %pad_maximum_fusion.refs_13_.refs_10_), channel_id=1, source_target_pairs={{0,4},{4,0},{1,5},{5,1},{2,6},{6,2},{3,7},{7,3},{8,12},{12,8},{9,1... | collective-permute-start | bytes 3145736 | tf_op jit(solution)/shard_map/ppermute | solution.py:36
  149.4 30.2 %all-to-all-start.3 = ((f32[16,1,2176]{2,1,0:T(1,128)}), f32[16,1,2176]{2,1,0:T(1,128)S(1)}, u32[]{:S(2)}, u32[]{:S(2)}) async-start(f32[16,1,2176]{2,1,0:T(1,128)} %broadcast_in_dim.17), calls=%async_computation.3 | async-start | bytes 278528 | tf_op jit(solution)/shard_map/all_to_all | solution.py:25
  160.5 19.1 %copy-start.3 = (f32[256]{0:T(256)S(1)}, f32[256]{0:T(256)}, u32[]{:S(2)}) copy-start(f32[256]{0:T(256)} %param.31) | copy-start | bytes 3076
  167.6 7.8 %collective-permute-start.6 = (f32[2,512]{1,0:T(2,128)S(1)}, f32[2,512]{1,0:T(2,128)S(1)}, u32[]{:S(2)}, u32[]{:S(2)}) collective-permute-start(f32[2,512]{1,0:T(2,128)S(1)} %get-tuple-element.34.refs_1_), channel_id=1, source_target_pairs={{0,3},{1,0},{2,1},{3,2},{4,7},{5,4},{6,5},{7,6},{8,11},{9,8},{10,9... | collective-permute-start | bytes 12296 | tf_op jit(solution)/shard_map/ppermute | solution.py:41
  169.5 7.0 %collective-permute-start.7 = (f32[2,512]{1,0:T(2,128)S(1)}, f32[2,512]{1,0:T(2,128)S(1)}, u32[]{:S(2)}, u32[]{:S(2)}) collective-permute-start(f32[2,512]{1,0:T(2,128)S(1)} %get-tuple-element.34.refs_1_), channel_id=1, source_target_pairs={{0,2},{1,3},{2,0},{3,1},{4,6},{5,7},{6,4},{7,5},{8,10},{9,11},{10,... | collective-permute-start | bytes 12296 | tf_op jit(solution)/shard_map/ppermute | solution.py:41
  172.8 6.8 %collective-permute-start.8 = (f32[2,512]{1,0:T(2,128)S(1)}, f32[2,512]{1,0:T(2,128)S(1)}, u32[]{:S(2)}, u32[]{:S(2)}) collective-permute-start(f32[2,512]{1,0:T(2,128)S(1)} %get-tuple-element.34.refs_1_), channel_id=1, source_target_pairs={{0,1},{1,2},{2,3},{3,0},{4,5},{5,6},{6,7},{7,4},{8,9},{9,10},{10,1... | collective-permute-start | bytes 12296 | tf_op jit(solution)/shard_map/ppermute | solution.py:41
  184.0 13.1 %collective-permute-start.13 = (bf16[64,2048]{1,0:T(8,128)(2,1)S(1)}, bf16[64,2048]{1,0:T(8,128)(2,1)S(1)}, u32[]{:S(2)}, u32[]{:S(2)}) collective-permute-start(bf16[64,2048]{1,0:T(8,128)(2,1)S(1)} %get-tuple-element.59), channel_id=1, source_target_pairs={{0,3},{1,0},{2,1},{3,2},{4,7},{5,4},{6,5},{7,6},{8,11},{9,8},{10,9... | collective-permute-start | bytes 786440 | tf_op jit(solution)/shard_map/ppermute | solution.py:41
  188.0 9.5 %collective-permute-start.15 = (bf16[64,2048]{1,0:T(8,128)(2,1)S(1)}, bf16[64,2048]{1,0:T(8,128)(2,1)S(1)}, u32[]{:S(2)}, u32[]{:S(2)}) collective-permute-start(bf16[64,2048]{1,0:T(8,128)(2,1)S(1)} %get-tuple-element.60), channel_id=1, source_target_pairs={{0,1},{1,2},{2,3},{3,0},{4,5},{5,6},{6,7},{7,4},{8,9},{9,10},{10,1... | collective-permute-start | bytes 786440 | tf_op jit(solution)/shard_map/ppermute | solution.py:41
  197.6 14.0 %collective-permute-start.16 = (bf16[128,2048]{1,0:T(8,128)(2,1)S(1)}, bf16[128,2048]{1,0:T(8,128)(2,1)S(1)}, u32[]{:S(2)}, u32[]{:S(2)}) collective-permute-start(bf16[128,2048]{1,0:T(8,128)(2,1)S(1)} %get-tuple-element.58), channel_id=1, source_target_pairs={{0,1},{1,2},{2,3},{3,0},{4,5},{5,6},{6,7},{7,4},{8,9},{9,10},{10,1... | collective-permute-start | bytes 1572872 | tf_op jit(solution)/shard_map/ppermute | solution.py:41
  199.6 13.3 %collective-permute-start.14 = (bf16[128,2048]{1,0:T(8,128)(2,1)S(1)}, bf16[128,2048]{1,0:T(8,128)(2,1)S(1)}, u32[]{:S(2)}, u32[]{:S(2)}) collective-permute-start(bf16[128,2048]{1,0:T(8,128)(2,1)S(1)} %get-tuple-element.57), channel_id=1, source_target_pairs={{0,3},{1,0},{2,1},{3,2},{4,7},{5,4},{6,5},{7,6},{8,11},{9,8},{10,9... | collective-permute-start | bytes 1572872 | tf_op jit(solution)/shard_map/ppermute | solution.py:41
